TPU v7x, 32 devices: a whole 2x2x4 slice. The times are simulated.
32 devices in a mesh: sp: 16 (over z, y, x), tp: 2 (over core).
Axes of the slice: x: 2, y: 2, z: 4, core: 2. Of those that a mesh axis runs over, the one named last changes fastest.
Arguments:
- residual: bfloat16 [2048, 2048], P('sp'), may hold values from -6 to 6
- query_first: bfloat16 [2048, 8, 128], P('sp', 'tp'), may hold values from -6.5 to 6.5
- key_first: bfloat16 [2048, 8, 128], P('sp', 'tp'), may hold values from -6.5 to 6.5
- value_first: bfloat16 [2048, 8, 128], P('sp', 'tp'), may hold values from -6 to 6
- query_second: bfloat16 [2048, 8, 64], P('sp', 'tp'), may hold values from -6.5 to 6.5
- key_second: bfloat16 [2048, 8, 64], P('sp', 'tp'), may hold values from -6.5 to 6.5
- value_second: bfloat16 [2048, 8, 64], P('sp', 'tp'), may hold values from -6 to 6
- balance_first: float32 [8], P('tp'), may hold values from 0.3 to 0.8
- balance_second: float32 [8], P('tp'), may hold values from 0.3 to 0.8
- head_gain_first: float32 [128], replicated, may hold values from 0.1 to 1.9
- head_gain_second: float32 [64], replicated, may hold values from 0.1 to 1.9
- out_first: bfloat16 [1024, 2048], P('tp'), may hold values from -0.15625 to 0.15625
- out_second: bfloat16 [512, 2048], P('tp'), may hold values from -0.15625 to 0.15625
- mlp_gain: float32 [2048], replicated, may hold values from 0.1 to 1.9
- up_weight: bfloat16 [2048, 8192], P('sp', 'tp'), may hold values from -0.125 to 0.125
- down_weight: bfloat16 [2048, 8192], P('sp', 'tp'), may hold values from -0.0625 to 0.0625
Outputs:
- layer_out: bfloat16 [2048, 2048], P('sp')
All inputs are finite; a program needn't handle non-finite values.
Results may differ from a plain program's by a relative error of at most 0.018.
Values may be sent and summed in bfloat16 or wider, within the bound.
No kernel may reach another device: no remote copies, remote signals or barrier semaphores. Data moves between devices by JAX's collectives and lax.ppermute only.
A program may use at most 128 MiB of HBM per device.

v0:
```python
import math

import jax
import jax.numpy as jnp
from jax import lax
from jax.sharding import PartitionSpec as P

DK_A = 64
DK_B = 32


EPSILON = 1e-06
HEAD_SCALE = 0.8


def attend(queries, keys, values, balance, gain, device, head_size):
    tokens = queries.shape[0]
    heads = queries.shape[1]
    seq = keys.shape[0]
    depth = values.shape[2]
    block = math.gcd(512, seq)
    scale = head_size ** (-0.5)
    query_maps = queries.reshape(tokens, heads, 2, head_size)
    key_maps = keys.reshape(seq, heads, 2, head_size)
    first_row = device * tokens
    positions = first_row + jnp.arange(tokens, dtype=jnp.int32)
    needed = (first_row + tokens + block - 1) // block

    def block_scores(number):
        start = number * block
        key_block = lax.dynamic_slice_in_dim(key_maps, start, block, 0)
        scores = (
            jnp.einsum("qhmd,khmd->hmqk", query_maps, key_block, preferred_element_type=jnp.float32)
            * scale
        )
        columns = start + jnp.arange(block, dtype=jnp.int32)
        visible = columns[None, :] <= positions[:, None]
        return (jnp.where(visible, scores, -jnp.inf), start)

    def statistics(number, carry):
        highest, total = carry
        scores, start = block_scores(number)
        fresh = jnp.maximum(highest, jnp.max(scores, axis=-1, keepdims=True))
        total = total * jnp.exp(highest - fresh) + jnp.sum(
            jnp.exp(scores - fresh), axis=-1, keepdims=True
        )
        return (fresh, total)

    start_high = jnp.full((heads, 2, tokens, 1), -jnp.inf, jnp.float32)
    start_total = jnp.zeros((heads, 2, tokens, 1), jnp.float32)
    highest, total = lax.fori_loop(0, needed, statistics, (start_high, start_total))

    def accumulate(number, result):
        scores, start = block_scores(number)
        probs = jnp.exp(scores - highest) / total
        mixed = (probs[:, 0] - balance[:, None, None] * probs[:, 1]).astype(jnp.bfloat16)
        value_block = lax.dynamic_slice_in_dim(values, start, block, 0)
        return result + jnp.einsum(
            "hqk,khe->qhe", mixed, value_block, preferred_element_type=jnp.float32
        )

    summed = lax.fori_loop(0, needed, accumulate, jnp.zeros((tokens, heads, depth), jnp.float32))
    power = jnp.mean(summed * summed, axis=-1, keepdims=True)
    normed = summed * lax.rsqrt(power + EPSILON) * gain * HEAD_SCALE
    return normed.astype(jnp.bfloat16).reshape(tokens, heads * depth)


def body(
    residual,
    query_first,
    key_first,
    value_first,
    query_second,
    key_second,
    value_second,
    balance_first,
    balance_second,
    head_gain_first,
    head_gain_second,
    out_first,
    out_second,
    mlp_gain,
    up_weight,
    down_weight,
):
    device = lax.axis_index("sp")
    keys_first, values_first, keys_second, values_second = (
        lax.all_gather(key_first, "sp", axis=0, tiled=True),
        lax.all_gather(value_first, "sp", axis=0, tiled=True),
        lax.all_gather(key_second, "sp", axis=0, tiled=True),
        lax.all_gather(value_second, "sp", axis=0, tiled=True),
    )
    heads_first = attend(
        query_first, keys_first, values_first, balance_first, head_gain_first, device, DK_A
    )
    heads_second = attend(
        query_second, keys_second, values_second, balance_second, head_gain_second, device, DK_B
    )
    head_term = jnp.dot(heads_first, out_first, preferred_element_type=jnp.float32) + jnp.dot(
        heads_second, out_second, preferred_element_type=jnp.float32
    )
    head_total = lax.psum(head_term.astype(jnp.bfloat16), "tp").astype(jnp.float32)
    mixed = (residual.astype(jnp.float32) + head_total).astype(jnp.bfloat16)
    mixed_float = mixed.astype(jnp.float32)
    power = jnp.mean(mixed_float * mixed_float, axis=-1, keepdims=True)
    normed = (mixed_float * lax.rsqrt(power + EPSILON) * mlp_gain).astype(jnp.bfloat16)
    up_whole, down_whole = (
        lax.all_gather(up_weight, "sp", axis=0, tiled=True),
        lax.all_gather(down_weight, "sp", axis=0, tiled=True),
    )
    lifted = jnp.dot(normed, up_whole, preferred_element_type=jnp.float32)
    active = jax.nn.relu(lifted)
    hidden = (active * active).astype(jnp.bfloat16)
    down_term = lax.dot_general(
        hidden, down_whole, (((1,), (1,)), ((), ())), preferred_element_type=jnp.float32
    )
    added = lax.psum(down_term.astype(jnp.bfloat16), "tp").astype(jnp.float32)
    return (mixed_float + added).astype(jnp.bfloat16)


def solution(mesh):
    in_specs = (
        P("sp", None),
        P("sp", "tp", None),
        P("sp", "tp", None),
        P("sp", "tp", None),
        P("sp", "tp", None),
        P("sp", "tp", None),
        P("sp", "tp", None),
        P("tp"),
        P("tp"),
        P(),
        P(),
        P("tp", None),
        P("tp", None),
        P(),
        P("sp", "tp"),
        P("sp", "tp"),
    )
    out_specs = P("sp", None)
    return jax.shard_map(body, mesh=mesh, in_specs=in_specs, out_specs=out_specs, check_vma=False)
```

profile of v0, /device:TPU:0, one launch (start us, length us, event | category | flops | bytes accessed | tf_op | source)
XLA Modules:
  0.0 704.4 jit_solution(6318953147037284549)
XLA Ops:
  6.5 0.0 copy-start
  6.5 0.0 all-gather.13.cloned.1.call-start
  6.5 0.7 all-gather.13.cloned.1.call-update
  7.3 0.0 all-gather.11.cloned.1.call-start
  7.3 0.7 all-gather.11.cloned.1.call-update
  8.0 0.0 all-gather.9.cloned.1.call-start
  8.1 0.7 all-gather.9.cloned.1.call-update
  8.7 0.0 all-gather.7.cloned.1.call-start
  8.8 1.7 copy.36
  10.5 0.0 all-gather.7.cloned.1.call-update
  10.5 0.0 all-reduce.3.cloned.1.call-start
  10.5 1.0 copy.38
  11.6 52.6 %all-gather.13.cloned.1.call-done = bf16[2048,4,64]{0,2,1:T(8,128)(2,1)} async-done(((bf16[128,4,64]{0,2,1:T(8,128)(2,1)}), bf16[2048,4,64]{0,2,1:T(8,128)(2,1)}) %all-gather.13.cloned.1.call-update) | async-done | bytes 1048592 | tf_op jit(solution)/shard_map/all_gather | solution.py:90
  64.2 0.0 copy-start.3
  64.2 2.2 while.50
  64.2 0.1 broadcast_compare_fusion.10
  64.3 1.5 fusion.92
  65.9 0.4 exponential_reduce_fusion.5
  66.4 50.9 %all-gather.11.cloned.1.call-done = bf16[2048,4,64]{0,2,1:T(8,128)(2,1)} async-done(((bf16[128,4,64]{0,2,1:T(8,128)(2,1)}), bf16[2048,4,64]{0,2,1:T(8,128)(2,1)}) %all-gather.11.cloned.1.call-update) | async-done | bytes 1048592 | tf_op jit(solution)/shard_map/all_gather | solution.py:91
  117.3 0.0 copy-done.3
  117.3 0.0 copy-start.6
  117.3 3.2 while.51
  117.4 0.1 broadcast_compare_fusion.11
  117.5 1.7 fusion.97
  119.2 1.3 fusion.98
  120.6 0.0 copy-done.6
  120.6 0.1 multiply_convert_fusion.1
  120.7 1.6 fusion.56
  122.2 57.3 %all-gather.9.cloned.1.call-done = bf16[2048,4,128]{2,1,0:T(4,128)(2,1)} async-done(((bf16[128,4,128]{2,1,0:T(4,128)(2,1)}), bf16[2048,4,128]{2,1,0:T(4,128)(2,1)}) %all-gather.9.cloned.1.call-update) | async-done | bytes 2097168 | tf_op jit(solution)/shard_map/all_gather | solution.py:88
  179.5 4.3 copy.37
  183.9 0.0 copy-start.4
  183.9 2.3 while.48
  183.9 0.1 broadcast_compare_fusion.8
  184.1 1.6 fusion.84
  185.7 0.4 exponential_reduce_fusion.4
  186.2 57.7 %all-gather.7.cloned.1.call-done = bf16[2048,4,128]{0,2,1:T(8,128)(2,1)} async-done(((bf16[128,4,128]{0,2,1:T(8,128)(2,1)}), bf16[2048,4,128]{0,2,1:T(8,128)(2,1)}) %all-gather.7.cloned.1.call-update) | async-done | bytes 2097168 | tf_op jit(solution)/shard_map/all_gather | solution.py:89
  243.9 0.0 copy-done.4
  243.9 0.0 copy-start.7
  243.9 3.4 while.49
  243.9 0.1 broadcast_compare_fusion.9
  244.1 1.8 fusion.89
  245.9 1.4 fusion.90
  247.4 0.0 copy-done.7
  247.4 0.1 multiply_convert_fusion
  247.5 0.0 copy-done
  247.5 1.3 fusion.44
  248.8 0.0 copy-start.1
  248.8 0.0 all-reduce.3.cloned.1.call-update
  248.8 0.0 all-gather.15.cloned.1.call-start
  248.8 0.5 all-gather.15.cloned.1.call-update
  249.4 0.0 all-gather.17.cloned.1.call-start
  249.4 0.7 all-gather.17.cloned.1.call-update
  250.1 0.0 all-reduce.5.cloned.1.call-start
  250.2 25.8 %all-reduce.3.cloned.1.call-done = bf16[128,2048]{1,0:T(8,128)(2,1)} async-done(((bf16[128,2048]{1,0:T(8,128)(2,1)}), bf16[128,2048]{1,0:T(8,128)(2,1)}) %all-reduce.3.cloned.1.call-update) | async-done | bytes 524304 | tf_op jit(solution)/shard_map/psum | solution.py:102
  275.9 0.0 copy-done.1
  275.9 1.3 fusion.45
  277.2 193.6 %all-gather.15.cloned.1.call-done = bf16[2048,4096]{1,0:T(8,128)(2,1)} async-done(((bf16[128,4096]{1,0:T(8,128)(2,1)}), bf16[2048,4096]{1,0:T(8,128)(2,1)}) %all-gather.15.cloned.1.call-update) | async-done | bytes 16777232 | tf_op jit(solution)/shard_map/all_gather | solution.py:108
  470.8 192.0 %all-gather.17.cloned.1.call-done = bf16[2048,4096]{1,0:T(8,128)(2,1)} async-done(((bf16[128,4096]{1,0:T(8,128)(2,1)}), bf16[2048,4096]{1,0:T(8,128)(2,1)}) %all-gather.17.cloned.1.call-update) | async-done | bytes 16777232 | tf_op jit(solution)/shard_map/all_gather | solution.py:109
  662.8 0.0 copy-done.5
  662.8 15.7 %convolution_convert_fusion = bf16[128,2048]{1,0:T(8,128)(2,1)} fusion(bf16[2048,4096]{1,0:T(8,128)(2,1)} %all-gather.17.cloned.1.call-done, bf16[2048,4096]{1,0:T(8,128)(2,1)} %all-gather.15.cloned.1.call-done, f32[2048]{0:T(1024)S(1)} %copy-done.5, f32[128]{0:T(128)S(1)} %add_rsqrt_fusion.2, bf16[128,2048]{1,0:T(8,128)(2,1)} %all-reduce.3.cloned.1.call-done, ...), kind=kOutput, calls=%fused_computation.69 | convolution fusion | flops 4298899456 | bytes 35136000 | tf_op jit(solution)/shard_map/dot_general | solution.py:114
  678.5 0.0 all-reduce.5.cloned.1.call-update
  678.5 16.9 %all-reduce.5.cloned.1.call-done = bf16[128,2048]{1,0:T(8,128)(2,1)} async-done(((bf16[128,2048]{1,0:T(8,128)(2,1)}), bf16[128,2048]{1,0:T(8,128)(2,1)}) %all-reduce.5.cloned.1.call-update) | async-done | bytes 524304 | tf_op jit(solution)/shard_map/psum | solution.py:117
  695.5 0.0 copy-done.2
  695.5 2.1 fusion.48
  (27 shorter events, 0.2 us)
Async XLA Ops:
  6.5 241.0 %copy-start = (bf16[512,2048]{1,0:T(8,128)(2,1)S(1)}, bf16[512,2048]{1,0:T(8,128)(2,1)}, u32[]{:S(2)}) copy-start(bf16[512,2048]{1,0:T(8,128)(2,1)} %param.35) | copy-start | bytes 6291460
  6.5 57.6 %all-gather.13.cloned.1.call-start = ((), (), s32[]{:S(2)}) async-start(), calls=%async_computation.3 | async-start | bytes 1114112 | tf_op jit(solution)/shard_map/all_gather | solution.py:90
  7.3 110.1 %all-gather.11.cloned.1.call-start = ((), (), s32[]{:S(2)}) async-start(), calls=%async_computation.2 | async-start | bytes 1114112 | tf_op jit(solution)/shard_map/all_gather | solution.py:91
  8.0 171.5 %all-gather.9.cloned.1.call-start = ((), (), s32[]{:S(2)}) async-start(), calls=%async_computation.1 | async-start | bytes 2228224 | tf_op jit(solution)/shard_map/all_gather | solution.py:88
  8.7 235.1 %all-gather.7.cloned.1.call-start = ((), (), s32[]{:S(2)}) async-start(), calls=%async_computation | async-start | bytes 2228224 | tf_op jit(solution)/shard_map/all_gather | solution.py:89
  10.5 265.4 %all-reduce.3.cloned.1.call-start = ((), (), s32[]{:S(2)}) async-start(), calls=%async_computation.4 | async-start | bytes 1048576 | tf_op jit(solution)/shard_map/psum | solution.py:102
  64.2 53.1 %copy-start.3 = (f32[4]{0:T(128)S(1)}, f32[4]{0:T(128)}, u32[]{:S(2)}) copy-start(f32[4]{0:T(128)} %param.32) | copy-start | bytes 52
  117.3 3.2 copy-start.6
  183.9 60.0 %copy-start.4 = (f32[4]{0:T(128)S(1)}, f32[4]{0:T(128)}, u32[]{:S(2)}) copy-start(f32[4]{0:T(128)} %param.31) | copy-start | bytes 52
  243.9 3.5 copy-start.7
  248.8 27.2 %copy-start.1 = (bf16[128,2048]{1,0:T(8,128)(2,1)S(1)}, bf16[128,2048]{1,0:T(8,128)(2,1)}, u32[]{:S(2)}) copy-start(bf16[128,2048]{1,0:T(8,128)(2,1)} %param.24) | copy-start | bytes 1572868
  248.8 414.0 %copy-start.5 = (f32[2048]{0:T(1024)S(1)}, f32[2048]{0:T(1024)}, u32[]{:S(2)}) copy-start(f32[2048]{0:T(1024)} %param.37) | copy-start | bytes 24580
  248.8 222.0 %all-gather.15.cloned.1.call-start = ((), (), s32[]{:S(2)}) async-start(), calls=%async_computation.5 | async-start | bytes 17825792 | tf_op jit(solution)/shard_map/all_gather | solution.py:108
  249.4 413.4 %all-gather.17.cloned.1.call-start = ((), (), s32[]{:S(2)}) async-start(), calls=%async_computation.6 | async-start | bytes 17825792 | tf_op jit(solution)/shard_map/all_gather | solution.py:109
  250.1 445.3 %all-reduce.5.cloned.1.call-start = ((), (), s32[]{:S(2)}) async-start(), calls=%async_computation.7 | async-start | bytes 1048576 | tf_op jit(solution)/shard_map/psum | solution.py:117
  277.2 418.2 %copy-start.2 = (bf16[128,2048]{1,0:T(8,128)(2,1)S(1)}, bf16[128,2048]{1,0:T(8,128)(2,1)}, u32[]{:S(2)}) copy-start(bf16[128,2048]{1,0:T(8,128)(2,1)} %all-reduce.3.cloned.1.call-done) | copy-start | bytes 1572868
Sparse Core Ops, SparseCore 0:
  10.0 54.0 all-gather.12
  66.9 50.3 all-gather.10
  120.1 59.3 all-gather.8
  182.1 61.7 all-gather.6
  248.9 26.9 all-reduce.2
  278.5 192.1 all-gather.14
  473.6 189.1 all-gather.16
  678.6 16.7 all-reduce.4
where the time goes:
time: 705 us; the launch traced here: 704 us
  waiting for transfers between devices  650 us (92%)
  matrix products  27.9 us (4%)
  between operations  13.7 us (2%)
  local copies, waits for them, and re-layouts  7.12 us (1%)
    all_gather x1, waiting for transfers between devices, body(): lax.all_gather(up_weight, 'sp', axis=0, tiled=True)  194 us
    all_gather x1, waiting for transfers between devices, body(): lax.all_gather(down_weight, 'sp', axis=0, tiled=True)  192 us
    all_gather x1, waiting for transfers between devices, body(): lax.all_gather(value_first, 'sp', axis=0, tiled=True)  57.7 us
    all_gather x1, waiting for transfers between devices, body(): lax.all_gather(key_first, 'sp', axis=0, tiled=True)  57.3 us
    all_gather x1, waiting for transfers between devices, body(): lax.all_gather(key_second, 'sp', axis=0, tiled=True)  52.6 us
    all_gather x1, waiting for transfers between devices, body(): lax.all_gather(value_second, 'sp', axis=0, tiled=True)  50.9 us
    psum x1, waiting for transfers between devices, body(): lax.psum(head_term.astype(jnp.bfloat16), 'tp').astype(jnp.float32)  25.8 us
    psum x1, waiting for transfers between devices, body(): added = lax.psum(down_term.astype(jnp.bfloat16), 'tp').astype(jnp.float32)  16.9 us
  transfers between devices with their start and end apart: 8, of which 8 were waited for; matrix products, arithmetic and copies ran while one was open for 2% of the time, Pallas kernels for 0%

commit v1 on v0

--- a/solution.py
+++ b/solution.py
@@ -1,8 +1,11 @@
+import functools
 import math
 
 import jax
 import jax.numpy as jnp
 from jax import lax
+from jax.experimental import pallas as pl
+from jax.experimental.pallas import tpu as pltpu
 from jax.sharding import PartitionSpec as P
 
 DK_A = 64
@@ -118,6 +121,328 @@
     return (mixed_float + added).astype(jnp.bfloat16)
 
 
+VMEM = pltpu.VMEM
+SMEM = pltpu.SMEM
+ROWS = 128
+
+
+def vmem_specs(count):
+    return [pl.BlockSpec(memory_space=VMEM)] * count
+
+
+def attend_kernel(slots, plane, tokens, index, balance_a, balance_b, gain_a, gain_b, *refs):
+    queries, kv_pieces, out = refs[:slots], refs[slots : slots + plane], refs[slots + plane]
+    query, keyval, scores = refs[slots + plane + 1 :]
+    z, g = index[0], index[1]
+    wide = plane * tokens
+    for k in range(slots):
+        query[z ^ k] = queries[k][...]
+        for p in range(plane):
+            start = pl.multiple_of(((z ^ k) * plane + (g ^ p)) * tokens, tokens)
+            keyval[pl.ds(start, tokens), :] = kv_pieces[p][k]
+    lane = lax.broadcasted_iota(jnp.int32, (tokens, 128), 1)
+    row = lax.broadcasted_iota(jnp.int32, (2 * tokens, wide), 0) % tokens
+    column = lax.broadcasted_iota(jnp.int32, (2 * tokens, wide), 1)
+    visible = column <= row + g * tokens
+
+    def group(number, place, size, key_lo, value_lo, balance):
+        packed = query[number][:, place : place + 2 * size]
+        if 2 * size < 128:
+            packed = jnp.concatenate(
+                [packed, jnp.zeros((tokens, 128 - 2 * size), packed.dtype)], axis=1
+            )
+        zero = jnp.zeros_like(packed)
+        both = jnp.concatenate(
+            [jnp.where(lane < size, packed, zero), jnp.where(lane >= size, packed, zero)], axis=0
+        )
+        factor = size ** (-0.5) * math.log2(math.e)
+        highest = None
+        for c in range(number + 1):
+            part = lax.dot_general(
+                both,
+                keyval[c * wide : (c + 1) * wide, key_lo : key_lo + 128],
+                (((1,), (1,)), ((), ())),
+                preferred_element_type=jnp.float32,
+            )
+            if c == number:
+                part = jnp.where(visible, part, -jnp.inf)
+            scores[:, c * wide : (c + 1) * wide] = part
+            top = jnp.max(part, axis=1, keepdims=True)
+            highest = top if highest is None else jnp.maximum(highest, top)
+        total = jnp.zeros((2 * tokens, 1), jnp.float32)
+        for c in range(number + 1):
+            part = jnp.exp2((scores[:, c * wide : (c + 1) * wide] - highest) * factor)
+            scores[:, c * wide : (c + 1) * wide] = part
+            total = total + jnp.sum(part, axis=1, keepdims=True)
+        share = 1.0 / total
+        first, second = share[:tokens], share[tokens:] * balance
+        summed = jnp.zeros((tokens, 128), jnp.float32)
+        for c in range(number + 1):
+            span = slice(c * wide, (c + 1) * wide)
+            weights = (scores[:tokens, span] * first - scores[tokens:, span] * second).astype(
+                jnp.bfloat16
+            )
+            summed = summed + jnp.dot(
+                weights, keyval[span, value_lo : value_lo + 128], preferred_element_type=jnp.float32
+            )
+        return summed
+
+    def normed(summed, gain):
+        power = jnp.mean(summed * summed, axis=-1, keepdims=True)
+        return (summed * lax.rsqrt(power + EPSILON) * gain[...] * HEAD_SCALE).astype(jnp.bfloat16)
+
+    for number in range(slots):
+        summed = group(number, 0, DK_A, 0, 256, balance_a[z])
+        out[z ^ number, :, 0:128] = normed(summed, gain_a)
+        summed = group(number, 128, DK_B, 128, 128, balance_b[z])[:, 64:128]
+        out[z ^ number, :, 128:192] = normed(summed, gain_b)
+
+
+def project_kernel(slots, half, index, *refs):
+    pieces, out_a, out_b, own, other, left = (
+        refs[:slots],
+        refs[slots],
+        refs[slots + 1],
+        refs[slots + 2],
+        refs[slots + 3],
+        refs[slots + 4],
+    )
+    z, core = index[0], index[2]
+    mine = pl.multiple_of(core * half, half)
+    theirs = pl.multiple_of((1 - core) * half, half)
+    for k in range(slots):
+        left[k, :half] = pieces[k][pl.ds(mine, half), :]
+        left[k, half:] = pieces[k][pl.ds(theirs, half), :]
+    tile = 512
+    for n in range(out_a.shape[1] // tile):
+        span = slice(n * tile, (n + 1) * tile)
+        total = jnp.zeros((2 * half, tile), jnp.float32)
+        for k in range(slots):
+            head = z ^ k
+            total += jnp.dot(
+                left[k, :, 0:128],
+                out_a[pl.ds(pl.multiple_of(head * 128, 128), 128), span],
+                preferred_element_type=jnp.float32,
+            )
+            total += jnp.dot(
+                left[k, :, 128:192],
+                out_b[pl.ds(pl.multiple_of(head * 64, 64), 64), span],
+                preferred_element_type=jnp.float32,
+            )
+        total = total.astype(jnp.bfloat16)
+        own[:, span] = total[:half]
+        other[:, span] = total[half:]
+
+
+def norm_kernel(half, index, residual, own, other, gain, mixed, normed):
+    mine = pl.multiple_of(index[2] * half, half)
+    total = own[...].astype(jnp.float32) + other[...].astype(jnp.float32)
+    rounded = (residual[pl.ds(mine, half), :].astype(jnp.float32) + total).astype(jnp.bfloat16)
+    mixed[...] = rounded
+    value = rounded.astype(jnp.float32)
+    power = jnp.mean(value * value, axis=-1, keepdims=True)
+    normed[...] = (value * lax.rsqrt(power + EPSILON) * gain[...]).astype(jnp.bfloat16)
+
+
+def mixer_kernel(slots, plane, index, *refs):
+    rows, refs = refs[: 2 * slots], refs[2 * slots :]
+    ups, downs = refs[:plane], refs[plane : 2 * plane]
+    own, other, left, hidden = refs[2 * plane :]
+    z, g = index[0], index[1]
+    half = rows[0].shape[0]
+    block = ups[0].shape[0] // slots
+    width = ups[0].shape[1]
+    every = 2 * slots * half
+
+    def place(k, p):
+        return pl.ds(pl.multiple_of(((z ^ k) * plane + (g ^ p)) * block, block), block)
+
+    for r, piece in enumerate(rows):
+        for p in range(plane):
+            for k in range(slots):
+                at = (p * slots + k) * block
+                left[r * half : (r + 1) * half, at : at + block] = piece[:, place(k, p)]
+    tile = 256
+    for n in range(width // tile):
+        span = slice(n * tile, (n + 1) * tile)
+        total = jnp.zeros((every, tile), jnp.float32)
+        for p in range(plane):
+            part = slots * block
+            total += jnp.dot(
+                left[:, p * part : (p + 1) * part],
+                ups[p][:, span],
+                preferred_element_type=jnp.float32,
+            )
+        active = jnp.maximum(total, 0.0)
+        hidden[:, span] = (active * active).astype(jnp.bfloat16)
+    for p in range(plane):
+        for pair in range(0, slots, 2):
+            part = lax.dot_general(
+                hidden[...],
+                downs[p][pair * block : (pair + 2) * block, :],
+                (((1,), (1,)), ((), ())),
+                preferred_element_type=jnp.float32,
+            ).astype(jnp.bfloat16)
+            for k in (pair, pair + 1):
+                at = (k - pair) * block
+                for r in range(slots):
+                    rest = (r + slots) * half
+                    own[r, :, place(k, p)] = part[r * half : (r + 1) * half, at : at + block]
+                    other[r, :, place(k, p)] = part[rest : rest + half, at : at + block]
+
+
+def fast_body(slots, plane, *arguments):
+    (
+        residual,
+        query_first,
+        key_first,
+        value_first,
+        query_second,
+        key_second,
+        value_second,
+        balance_first,
+        balance_second,
+        head_gain_first,
+        head_gain_second,
+        out_first,
+        out_second,
+        mlp_gain,
+        up_weight,
+        down_weight,
+    ) = arguments
+    count = slots * plane
+    tokens, width = residual.shape
+    half = tokens // 2
+    device, core = lax.axis_index("sp"), lax.axis_index("tp")
+    z, g = device // plane, device % plane
+    index = jnp.stack([z, g, core]).astype(jnp.int32)
+
+    def along(value, k):
+        if k == 0:
+            return value
+        return lax.ppermute(
+            value, "sp", [(i, (i // plane ^ k) * plane + i % plane) for i in range(count)]
+        )
+
+    def across(value, k):
+        if k == 0:
+            return value
+        return lax.ppermute(value, "sp", [(i, i ^ k) for i in range(count)])
+
+    def swap(value):
+        return lax.ppermute(value, "tp", [(0, 1), (1, 0)])
+
+    packed = jnp.concatenate(
+        [key_first, key_second, value_second, value_first, query_first, query_second], axis=2
+    ).transpose(1, 0, 2)
+    got = [along(lax.dynamic_index_in_dim(packed, z ^ k, 0, False), k) for k in range(slots)]
+    keyval = jnp.stack([piece[:, :384] for piece in got])
+    queries = [piece[:, 384:] for piece in got]
+    kv_pieces = [across(keyval, p) for p in range(plane)]
+
+    up_weight, down_weight, keyval = lax.optimization_barrier((up_weight, down_weight, keyval))
+    hidden = up_weight.shape[1] // slots
+
+    def spread(weight):
+        parts = [
+            along(lax.dynamic_slice_in_dim(weight, (z ^ k) * hidden, hidden, 1), k)
+            for k in range(slots)
+        ]
+        mine = jnp.concatenate(parts, axis=0)
+        return [across(mine, p) for p in range(plane)]
+
+    ups = spread(up_weight)
+    downs = spread(down_weight)
+
+    smem = pl.BlockSpec(memory_space=SMEM)
+    sequence = count * tokens
+    heads = pl.pallas_call(
+        functools.partial(attend_kernel, slots, plane, tokens),
+        out_shape=jax.ShapeDtypeStruct((slots, tokens, 192), jnp.bfloat16),
+        in_specs=[smem] * 3 + vmem_specs(2 + slots + plane),
+        out_specs=pl.BlockSpec(memory_space=VMEM),
+        scratch_shapes=[
+            VMEM((slots, tokens, 192), jnp.bfloat16),
+            VMEM((sequence, 384), jnp.bfloat16),
+            VMEM((2 * tokens, sequence), jnp.float32),
+        ],
+        cost_estimate=pl.CostEstimate(flops=8 * 10**9, bytes_accessed=2 * 10**6, transcendentals=0),
+        name="attend",
+    )(
+        index,
+        balance_first,
+        balance_second,
+        head_gain_first[None],
+        head_gain_second[None],
+        *queries,
+        *kv_pieces,
+    )
+    pieces = [along(heads[k], k) for k in range(slots)]
+    row_shape = jax.ShapeDtypeStruct((half, width), jnp.bfloat16)
+    own, other = pl.pallas_call(
+        functools.partial(project_kernel, slots, half),
+        out_shape=(row_shape, row_shape),
+        in_specs=[smem] + vmem_specs(slots + 2),
+        out_specs=tuple(vmem_specs(2)),
+        scratch_shapes=[VMEM((slots, tokens, 192), jnp.bfloat16)],
+        cost_estimate=pl.CostEstimate(flops=2 * 10**9, bytes_accessed=4 * 10**6, transcendentals=0),
+        name="project",
+    )(index, *pieces, out_first, out_second)
+    mixed, normed = pl.pallas_call(
+        functools.partial(norm_kernel, half),
+        out_shape=(row_shape, row_shape),
+        in_specs=[smem] + vmem_specs(4),
+        out_specs=tuple(vmem_specs(2)),
+        cost_estimate=pl.CostEstimate(flops=10**9, bytes_accessed=10**6, transcendentals=0),
+        name="norm",
+    )(index, residual, own, swap(other), mlp_gain[None])
+    own_rows = [along(normed, k) for k in range(slots)]
+    other_rows = [swap(piece) for piece in own_rows]
+    part_shape = jax.ShapeDtypeStruct((slots, half, width), jnp.bfloat16)
+    own, other = pl.pallas_call(
+        functools.partial(mixer_kernel, slots, plane),
+        out_shape=(part_shape, part_shape),
+        in_specs=[smem] + vmem_specs(2 * slots + 2 * plane),
+        out_specs=tuple(vmem_specs(2)),
+        scratch_shapes=[
+            VMEM((2 * slots * half, width), jnp.bfloat16),
+            VMEM((2 * slots * half, hidden), jnp.bfloat16),
+        ],
+        cost_estimate=pl.CostEstimate(flops=6 * 10**9, bytes_accessed=10**7, transcendentals=0),
+        name="mixer",
+    )(index, *own_rows, *other_rows, *ups, *downs)
+    summed = own.astype(jnp.float32) + swap(other).astype(jnp.float32)
+    sent = summed.astype(jnp.bfloat16)
+    total = summed[0]
+    for k in range(1, slots):
+        total = total + along(sent[k], k).astype(jnp.float32)
+    mine = (mixed.astype(jnp.float32) + total).astype(jnp.bfloat16)
+    theirs = swap(mine)
+    return jnp.where(
+        core == 0, jnp.concatenate([mine, theirs]), jnp.concatenate([theirs, mine])
+    )
+
+
+def dispatch(count, cores, *arguments):
+    heads, other_heads = arguments[1].shape[1], arguments[4].shape[1]
+    plane = count // heads
+    fits = (
+        cores == 2
+        and heads == other_heads
+        and plane == 4
+        and plane * heads == count
+        and arguments[3].shape[2] == 128
+        and arguments[6].shape[2] == 64
+    )
+    if fits:
+        return fast_body(heads, plane, *arguments)
+    return body(*arguments)
+
+
+def plan(mesh):
+    return functools.partial(dispatch, mesh.shape["sp"], mesh.shape["tp"])
+
+
 def solution(mesh):
     in_specs = (
         P("sp", None),
@@ -138,4 +463,5 @@
         P("sp", "tp"),
     )
     out_specs = P("sp", None)
-    return jax.shard_map(body, mesh=mesh, in_specs=in_specs, out_specs=out_specs, check_vma=False)
+    chosen = plan(mesh)
+    return jax.shard_map(chosen, mesh=mesh, in_specs=in_specs, out_specs=out_specs, check_vma=False)

time: 705 us -> 235 us (0.33)
  waiting for transfers between devices: 650 us -> 140 us
  starting transfers between devices: 0.28 us -> 52.5 us
  matrix products: 27.9 us -> 0 us
  Pallas kernels: 0 us -> 24.7 us
  between operations: 13.7 us -> 0.38 us
    all_gather x6 -> x0, waiting for transfers between devices: 604 us -> none  [the longest x1 194 us: body(): lax.all_gather(up_weight, 'sp', axis=0, tiled=True)]
    ppermute x0 -> x34, waiting for transfers between devices: none -> 140 us  [the longest x9 69.2 us: across(): return lax.ppermute(value, 'sp', [(i, i ^ k) for i in range(count)])]
    ppermute x0 -> x34, starting transfers between devices: none -> 52.5 us  [the longest x18 40.9 us: along(): lax.ppermute(value, 'sp', [(i, (i // plane ^ k) * plane + i % plane) for...]
    psum x2 -> x0, waiting for transfers between devices: 42.7 us -> none  [the longest x1 25.8 us: body(): lax.psum(head_term.astype(jnp.bfloat16), 'tp').astype(jnp.float32)]
    dot_general x9 -> x0, matrix products: 27.9 us -> none  [the longest x1 15.7 us: body(): lax.dot_general(hidden, down_whole, (((1,), (1,)), ((), ())), preferred_e...]
    pallas_call x0 -> x4, Pallas kernels: none -> 24.7 us  [the longest x1 10.4 us: fast_body(): pl.pallas_call(functools.partial(mixer_kernel, slots, plane), out_shape=(...]
  transfers between devices with their start and end apart: 8 -> 34, of which waited for: 8 -> 21; matrix products, arithmetic and copies ran while one was open for 2% -> 2% of each run, Pallas kernels for 0% -> 6%
where the time goes in v1:
time: 235 us; the launch traced here: 234 us
  waiting for transfers between devices  140 us (60%)
  starting transfers between devices  52.5 us (22%)
  Pallas kernels  24.7 us (11%)
  local copies, waits for them, and re-layouts  13.2 us (6%)
  other arithmetic  3.52 us (1%)
    ppermute x9, waiting for transfers between devices, across(): return lax.ppermute(value, 'sp', [(i, i ^ k) for i in range(count)])  69.2 us
    ppermute x18, waiting for transfers between devices, along(): lax.ppermute(value, 'sp', [(i, (i // plane ^ k) * plane + i % plane) for...  66.4 us
    ppermute x18, starting transfers between devices, along(): lax.ppermute(value, 'sp', [(i, (i // plane ^ k) * plane + i % plane) for...  40.9 us
    ppermute x9, starting transfers between devices, across(): return lax.ppermute(value, 'sp', [(i, i ^ k) for i in range(count)])  11 us
    pallas_call x1, Pallas kernels, fast_body(): pl.pallas_call(functools.partial(mixer_kernel, slots, plane), out_shape=(...  10.4 us
    unnamed x52, local copies, waits for them, and re-layouts  8.12 us
    pallas_call x1, Pallas kernels, fast_body(): pl.pallas_call(functools.partial(attend_kernel, slots, plane, tokens), ou...  8 us
  transfers between devices with their start and end apart: 34, of which 21 were waited for; matrix products, arithmetic and copies ran while one was open for 2% of the time, Pallas kernels for 6%

profile of v1, /device:TPU:0, one launch (start us, length us, event | category | flops | bytes accessed | tf_op | source)
XLA Modules:
  0.0 234.3 jit_solution(1466015422380264973)
XLA Ops:
  0.0 1.0 copy.22
  1.0 1.0 copy.20
  2.1 1.0 copy.21
  3.2 0.9 constant_dynamic-update-slice_fusion.4
  4.0 0.9 constant_dynamic-update-slice_fusion.3
  4.9 0.9 constant_dynamic-update-slice_fusion
  6.0 3.1 %collective-permute-start = (bf16[128,576]{1,0:T(8,128)(2,1)S(1)}, bf16[128,576]{1,0:T(8,128)(2,1)S(1)}, u32[]{:S(2)}, u32[]{:S(2)}) collective-permute-start(bf16[128,576]{1,0:T(8,128)(2,1)S(1)} %copy.24), channel_id=1, source_target_pairs={{0,8},{2,10},{4,12},{6,14},{8,0},{10,2},{12,4},{14,6},{16,24},{18,... | collective-permute-start | bytes 442376 | tf_op jit(solution)/shard_map/ppermute | solution.py:323
  9.3 2.7 %collective-permute-start.1 = (bf16[128,576]{1,0:T(8,128)(2,1)S(1)}, bf16[128,576]{1,0:T(8,128)(2,1)S(1)}, u32[]{:S(2)}, u32[]{:S(2)}) collective-permute-start(bf16[128,576]{1,0:T(8,128)(2,1)S(1)} %copy.25), channel_id=1, source_target_pairs={{0,16},{2,18},{4,20},{6,22},{8,24},{10,26},{12,28},{14,30},{16,0},... | collective-permute-start | bytes 442376 | tf_op jit(solution)/shard_map/ppermute | solution.py:323
  12.3 3.4 %collective-permute-done = bf16[128,576]{1,0:T(8,128)(2,1)S(1)} collective-permute-done((bf16[128,576]{1,0:T(8,128)(2,1)S(1)}, bf16[128,576]{1,0:T(8,128)(2,1)S(1)}, u32[]{:S(2)}, u32[]{:S(2)}) %collective-permute-start) | collective-permute-done | bytes 147488 | tf_op jit(solution)/shard_map/ppermute | solution.py:323
  15.7 8.6 %collective-permute-done.1 = bf16[128,576]{1,0:T(8,128)(2,1)S(1)} collective-permute-done((bf16[128,576]{1,0:T(8,128)(2,1)S(1)}, bf16[128,576]{1,0:T(8,128)(2,1)S(1)}, u32[]{:S(2)}, u32[]{:S(2)}) %collective-permute-start.1) | collective-permute-done | bytes 147488 | tf_op jit(solution)/shard_map/ppermute | solution.py:323
  24.5 2.5 %collective-permute-start.5 = (bf16[4,128,384]{2,1,0:T(8,128)(2,1)S(1)}, bf16[4,128,384]{2,1,0:T(8,128)(2,1)}, u32[]{:S(2)}, u32[]{:S(2)}) collective-permute-start(bf16[4,128,384]{2,1,0:T(8,128)(2,1)S(1)} %pad_maximum_fusion.2.refs_4_), channel_id=1, source_target_pairs={{0,6},{2,4},{4,2},{6,0},{8,14},{10,12},{12,10},{14,8},{16,22},{18,... | collective-permute-start | bytes 1179656 | tf_op jit(solution)/shard_map/ppermute | solution.py:330
  27.0 0.5 collective-permute-start.4
  27.5 0.5 collective-permute-start.3
  28.0 0.7 copy.28.refs_0_
  28.8 0.6 pad_add_fusion.index
  29.4 2.3 collective-permute-start.25
  31.8 1.9 collective-permute-start.24
  33.6 0.6 slice.65.refs_1_
  34.2 0.6 slice.66.refs_2_
  34.9 0.6 slice.67.refs_3_
  35.5 2.1 collective-permute-done.5.refs_7_
  37.5 2.7 %collective-permute-start.23 = (bf16[128,1024]{1,0:T(8,128)(2,1)S(1)}, bf16[128,1024]{1,0:T(8,128)(2,1)S(1)}, u32[]{:S(2)}, u32[]{:S(2)}) collective-permute-start(bf16[128,1024]{1,0:T(8,128)(2,1)S(1)} %get-tuple-element.29), channel_id=1, source_target_pairs={{0,8},{2,10},{4,12},{6,14},{8,0},{10,2},{12,4},{14,6},{16,24},{18,... | collective-permute-start | bytes 786440 | tf_op jit(solution)/shard_map/ppermute | solution.py:323
  40.3 1.9 collective-permute-done.4.refs_6_
  42.3 8.0 %attend.1 = bf16[4,128,192]{2,1,0:T(8,128)(2,1)} custom-call(s32[3]{0:T(128)} %pad_add_fusion.index, f32[4]{0:T(128)} %balance_a.1, f32[4]{0:T(128)} %balance_b.1, f32[1,128]{1,0:T(1,128)} %bitcast.49, f32[1,64]{1,0:T(1,128)} %bitcast.50, bf16[128,192]{1,0:T(8,128)(2,1)} %copy.28.refs_0_, bf16[128,192]{1,0:T(8,128)(2,1)} %slice.65.refs_1_, ...), custom_call_target="tpu_custom_call" | custom-call | flops 8000000000 | bytes 2000000 | tf_op jit(solution)/shard_map/attend/pallas_call | solution.py:359
  50.3 1.6 slice_bitcast_fusion.7
  51.9 2.9 %collective-permute-start.8 = (bf16[128,192]{1,0:T(8,128)(2,1)S(1)}, bf16[128,192]{1,0:T(8,128)(2,1)S(1)}, u32[]{:S(2)}, u32[]{:S(2)}) collective-permute-start(bf16[128,192]{1,0:T(8,128)(2,1)S(1)} %get-tuple-element.38), channel_id=1, source_target_pairs={{0,24},{2,26},{4,28},{6,30},{8,16},{10,18},{12,20},{14,22},{16,8},... | collective-permute-start | bytes 147464 | tf_op jit(solution)/shard_map/ppermute | solution.py:323
  54.7 2.8 %collective-permute-start.7 = (bf16[128,192]{1,0:T(8,128)(2,1)S(1)}, bf16[128,192]{1,0:T(8,128)(2,1)S(1)}, u32[]{:S(2)}, u32[]{:S(2)}) collective-permute-start(bf16[128,192]{1,0:T(8,128)(2,1)S(1)} %get-tuple-element.39), channel_id=1, source_target_pairs={{0,16},{2,18},{4,20},{6,22},{8,24},{10,26},{12,28},{14,30},{16,0},... | collective-permute-start | bytes 147464 | tf_op jit(solution)/shard_map/ppermute | solution.py:323
  58.0 1.7 collective-permute-start.28
  59.7 2.0 collective-permute-done.7.refs_2_
  61.7 0.5 collective-permute-done.6.refs_1_
  62.3 0.5 copy-done.20
  62.8 4.1 %project.1 = (bf16[64,2048]{1,0:T(8,128)(2,1)}, bf16[64,2048]{1,0:T(8,128)(2,1)}) custom-call(s32[3]{0:T(128)} %pad_add_fusion.index, bf16[128,192]{1,0:T(8,128)(2,1)} %get-tuple-element.41.refs_0_, bf16[128,192]{1,0:T(8,128)(2,1)} %copy-done.20, bf16[128,192]{1,0:T(8,128)(2,1)} %copy-done.19, bf16[128,192]{1,0:T(8,128)(2,1)} %copy-done.18, ...), custom_call_target="tpu_custom_call" | custom-call | flops 2000000000 | bytes 4000000 | tf_op jit(solution)/shard_map/project/pallas_call | solution.py:382
  67.0 3.2 %collective-permute-start.19 = (bf16[128,1024]{1,0:T(8,128)(2,1)S(1)}, bf16[128,1024]{1,0:T(8,128)(2,1)S(1)}, u32[]{:S(2)}, u32[]{:S(2)}) collective-permute-start(bf16[128,1024]{1,0:T(8,128)(2,1)S(1)} %get-tuple-element.31), channel_id=1, source_target_pairs={{0,24},{2,26},{4,28},{6,30},{8,16},{10,18},{12,20},{14,22},{16,8},... | collective-permute-start | bytes 786440 | tf_op jit(solution)/shard_map/ppermute | solution.py:323
  70.2 1.2 collective-permute-start.17
  71.5 0.7 copy-done.17
  72.2 2.1 norm.1
  74.3 3.2 %collective-permute-start.12 = (bf16[64,2048]{1,0:T(8,128)(2,1)}, bf16[64,2048]{1,0:T(8,128)(2,1)S(1)}, u32[]{:S(2)}, u32[]{:S(2)}) collective-permute-start(bf16[64,2048]{1,0:T(8,128)(2,1)} %get-tuple-element.16.refs_0_), channel_id=1, source_target_pairs={{0,24},{2,26},{4,28},{6,30},{8,16},{10,18},{12,20},{14,22},{16,8},... | collective-permute-start | bytes 786440 | tf_op jit(solution)/shard_map/ppermute | solution.py:323
  77.5 0.7 collective-permute-done.19
  78.2 10.9 %collective-permute-start.11 = (bf16[64,2048]{1,0:T(8,128)(2,1)}, bf16[64,2048]{1,0:T(8,128)(2,1)S(1)}, u32[]{:S(2)}, u32[]{:S(2)}) collective-permute-start(bf16[64,2048]{1,0:T(8,128)(2,1)} %get-tuple-element.16.refs_0_), channel_id=1, source_target_pairs={{0,16},{2,18},{4,20},{6,22},{8,24},{10,26},{12,28},{14,30},{16,0},... | collective-permute-start | bytes 786440 | tf_op jit(solution)/shard_map/ppermute | solution.py:323
  89.1 15.6 %collective-permute-done.18 = bf16[128,1024]{1,0:T(8,128)(2,1)S(1)} collective-permute-done((bf16[128,1024]{1,0:T(8,128)(2,1)S(1)}, bf16[128,1024]{1,0:T(8,128)(2,1)S(1)}, u32[]{:S(2)}, u32[]{:S(2)}) %collective-permute-start.18) | collective-permute-done | bytes 262176 | tf_op jit(solution)/shard_map/ppermute | solution.py:323
  104.8 0.5 collective-permute-start.16
  105.3 10.3 %collective-permute-done.11.refs_2_ = bf16[64,2048]{1,0:T(8,128)(2,1)S(1)} collective-permute-done((bf16[64,2048]{1,0:T(8,128)(2,1)}, bf16[64,2048]{1,0:T(8,128)(2,1)S(1)}, u32[]{:S(2)}, u32[]{:S(2)}) %collective-permute-start.11) | collective-permute-done | bytes 262176 | tf_op jit(solution)/shard_map/ppermute | solution.py:323
  115.6 2.3 collective-permute-done.10.refs_1_
  118.0 1.6 collective-permute-start.27
  119.6 0.7 collective-permute-start.26
  120.3 1.4 collective-permute-start.22
  121.7 1.5 collective-permute-start.21
  123.2 0.6 collective-permute-start.20
  123.8 20.3 %collective-permute-done.27.refs_14_ = bf16[512,1024]{1,0:T(8,128)(2,1)S(1)} collective-permute-done((bf16[512,1024]{1,0:T(8,128)(2,1)S(1)}, bf16[512,1024]{1,0:T(8,128)(2,1)S(1)}, u32[]{:S(2)}, u32[]{:S(2)}) %collective-permute-start.27) | collective-permute-done | bytes 1048608 | tf_op jit(solution)/shard_map/ppermute | solution.py:330
  144.1 1.6 collective-permute-done.26.refs_13_
  145.7 22.5 %collective-permute-done.22.refs_11_ = bf16[512,1024]{1,0:T(8,128)(2,1)S(1)} collective-permute-done((bf16[512,1024]{1,0:T(8,128)(2,1)S(1)}, bf16[512,1024]{1,0:T(8,128)(2,1)S(1)}, u32[]{:S(2)}, u32[]{:S(2)}) %collective-permute-start.22) | collective-permute-done | bytes 1048608 | tf_op jit(solution)/shard_map/ppermute | solution.py:330
  168.2 20.4 %collective-permute-done.21.refs_10_ = bf16[512,1024]{1,0:T(8,128)(2,1)S(1)} collective-permute-done((bf16[512,1024]{1,0:T(8,128)(2,1)S(1)}, bf16[512,1024]{1,0:T(8,128)(2,1)S(1)}, u32[]{:S(2)}, u32[]{:S(2)}) %collective-permute-start.21) | collective-permute-done | bytes 1048608 | tf_op jit(solution)/shard_map/ppermute | solution.py:330
  188.7 1.0 copy-done.9
  189.7 0.4 collective-permute-done.20.refs_9_
  190.1 10.4 %mixer.1 = (bf16[4,64,2048]{2,1,0:T(8,128)(2,1)}, bf16[4,64,2048]{2,1,0:T(8,128)(2,1)}) custom-call(s32[3]{0:T(128)} %pad_add_fusion.index, bf16[64,2048]{1,0:T(8,128)(2,1)} %get-tuple-element.16.refs_0_, bf16[64,2048]{1,0:T(8,128)(2,1)} %copy-done.12, bf16[64,2048]{1,0:T(8,128)(2,1)} %copy-done.11, bf16[64,2048]{1,0:T(8,128)(2,1)} %copy-done.10, ...), custom_call_target="tpu_custom_call" | custom-call | flops 6000000000 | bytes 10000000 | tf_op jit(solution)/shard_map/mixer/pallas_call | solution.py:402
  200.5 2.9 %collective-permute-done.29 = bf16[4,64,2048]{2,1,0:T(8,128)(2,1)S(1)} collective-permute-done((bf16[4,64,2048]{2,1,0:T(8,128)(2,1)}, bf16[4,64,2048]{2,1,0:T(8,128)(2,1)S(1)}, u32[]{:S(2)}, u32[]{:S(2)}) %collective-permute-start.29) | collective-permute-done | bytes 1048608 | tf_op jit(solution)/shard_map/ppermute | solution.py:333
  203.4 1.7 fusion.5
  205.2 2.2 collective-permute-start.32
  207.4 1.3 collective-permute-start.31
  208.7 5.0 %collective-permute-done.30 = bf16[64,2048]{1,0:T(8,128)(2,1)S(1)} collective-permute-done((bf16[64,2048]{1,0:T(8,128)(2,1)S(1)}, bf16[64,2048]{1,0:T(8,128)(2,1)S(1)}, u32[]{:S(2)}, u32[]{:S(2)}) %collective-permute-start.30) | collective-permute-done | bytes 262176 | tf_op jit(solution)/shard_map/ppermute | solution.py:323
  213.7 6.5 %collective-permute-done.32 = bf16[64,2048]{1,0:T(8,128)(2,1)S(1)} collective-permute-done((bf16[64,2048]{1,0:T(8,128)(2,1)S(1)}, bf16[64,2048]{1,0:T(8,128)(2,1)S(1)}, u32[]{:S(2)}, u32[]{:S(2)}) %collective-permute-start.32) | collective-permute-done | bytes 262176 | tf_op jit(solution)/shard_map/ppermute | solution.py:323
  220.2 11.4 %collective-permute-done.31 = bf16[64,2048]{1,0:T(8,128)(2,1)S(1)} collective-permute-done((bf16[64,2048]{1,0:T(8,128)(2,1)S(1)}, bf16[64,2048]{1,0:T(8,128)(2,1)S(1)}, u32[]{:S(2)}, u32[]{:S(2)}) %collective-permute-start.31) | collective-permute-done | bytes 262176 | tf_op jit(solution)/shard_map/ppermute | solution.py:323
  231.9 1.5 collective-permute-done.33
  233.4 0.9 maximum_select_fusion
  (84 shorter events, 2.3 us)
Async XLA Ops:
  5.8 23.6 %copy-start = (bf16[128,4096]{1,0:T(8,128)(2,1)S(1)}, bf16[128,4096]{1,0:T(8,128)(2,1)}, u32[]{:S(2)}) copy-start(bf16[128,4096]{1,0:T(8,128)(2,1)} %param.31) | copy-start | bytes 3145732
  6.0 9.7 %collective-permute-start = (bf16[128,576]{1,0:T(8,128)(2,1)S(1)}, bf16[128,576]{1,0:T(8,128)(2,1)S(1)}, u32[]{:S(2)}, u32[]{:S(2)}) collective-permute-start(bf16[128,576]{1,0:T(8,128)(2,1)S(1)} %copy.24), channel_id=1, source_target_pairs={{0,8},{2,10},{4,12},{6,14},{8,0},{10,2},{12,4},{14,6},{16,24},{18,... | collective-permute-start | bytes 442376 | tf_op jit(solution)/shard_map/ppermute | solution.py:323
  9.3 15.1 %collective-permute-start.1 = (bf16[128,576]{1,0:T(8,128)(2,1)S(1)}, bf16[128,576]{1,0:T(8,128)(2,1)S(1)}, u32[]{:S(2)}, u32[]{:S(2)}) collective-permute-start(bf16[128,576]{1,0:T(8,128)(2,1)S(1)} %copy.25), channel_id=1, source_target_pairs={{0,16},{2,18},{4,20},{6,22},{8,24},{10,26},{12,28},{14,30},{16,0},... | collective-permute-start | bytes 442376 | tf_op jit(solution)/shard_map/ppermute | solution.py:323
  12.1 12.3 %collective-permute-start.2 = (bf16[128,576]{1,0:T(8,128)(2,1)S(1)}, bf16[128,576]{1,0:T(8,128)(2,1)S(1)}, u32[]{:S(2)}, u32[]{:S(2)}) collective-permute-start(bf16[128,576]{1,0:T(8,128)(2,1)S(1)} %copy.26), channel_id=1, source_target_pairs={{0,24},{2,26},{4,28},{6,30},{8,16},{10,18},{12,20},{14,22},{16,8},... | collective-permute-start | bytes 442376 | tf_op jit(solution)/shard_map/ppermute | solution.py:323
  24.5 17.8 %copy-start.4 = (bf16[4,128,384]{2,1,0:T(8,128)(2,1)}, bf16[4,128,384]{2,1,0:T(8,128)(2,1)S(1)}, u32[]{:S(2)}) copy-start(bf16[4,128,384]{2,1,0:T(8,128)(2,1)S(1)} %pad_maximum_fusion.2.refs_4_) | copy-start | bytes 1179652
  24.5 13.1 %collective-permute-start.5 = (bf16[4,128,384]{2,1,0:T(8,128)(2,1)S(1)}, bf16[4,128,384]{2,1,0:T(8,128)(2,1)}, u32[]{:S(2)}, u32[]{:S(2)}) collective-permute-start(bf16[4,128,384]{2,1,0:T(8,128)(2,1)S(1)} %pad_maximum_fusion.2.refs_4_), channel_id=1, source_target_pairs={{0,6},{2,4},{4,2},{6,0},{8,14},{10,12},{12,10},{14,8},{16,22},{18,... | collective-permute-start | bytes 1179656 | tf_op jit(solution)/shard_map/ppermute | solution.py:330
  27.0 15.2 %collective-permute-start.4 = (bf16[4,128,384]{2,1,0:T(8,128)(2,1)S(1)}, bf16[4,128,384]{2,1,0:T(8,128)(2,1)}, u32[]{:S(2)}, u32[]{:S(2)}) collective-permute-start(bf16[4,128,384]{2,1,0:T(8,128)(2,1)S(1)} %pad_maximum_fusion.2.refs_4_), channel_id=1, source_target_pairs={{0,4},{2,6},{4,0},{6,2},{8,12},{10,14},{12,8},{14,10},{16,20},{18,... | collective-permute-start | bytes 1179656 | tf_op jit(solution)/shard_map/ppermute | solution.py:330
  27.5 14.8 %collective-permute-start.3 = (bf16[4,128,384]{2,1,0:T(8,128)(2,1)S(1)}, bf16[4,128,384]{2,1,0:T(8,128)(2,1)}, u32[]{:S(2)}, u32[]{:S(2)}) collective-permute-start(bf16[4,128,384]{2,1,0:T(8,128)(2,1)S(1)} %pad_maximum_fusion.2.refs_4_), channel_id=1, source_target_pairs={{0,2},{2,0},{4,6},{6,4},{8,10},{10,8},{12,14},{14,12},{16,18},{18,... | collective-permute-start | bytes 1179656 | tf_op jit(solution)/shard_map/ppermute | solution.py:330
  29.4 28.1 %collective-permute-start.25 = (bf16[128,1024]{1,0:T(8,128)(2,1)S(1)}, bf16[128,1024]{1,0:T(8,128)(2,1)S(1)}, u32[]{:S(2)}, u32[]{:S(2)}) collective-permute-start(bf16[128,1024]{1,0:T(8,128)(2,1)S(1)} %get-tuple-element.27), channel_id=1, source_target_pairs={{0,24},{2,26},{4,28},{6,30},{8,16},{10,18},{12,20},{14,22},{16,8},... | collective-permute-start | bytes 786440 | tf_op jit(solution)/shard_map/ppermute | solution.py:323
  31.8 26.1 %collective-permute-start.24 = (bf16[128,1024]{1,0:T(8,128)(2,1)S(1)}, bf16[128,1024]{1,0:T(8,128)(2,1)S(1)}, u32[]{:S(2)}, u32[]{:S(2)}) collective-permute-start(bf16[128,1024]{1,0:T(8,128)(2,1)S(1)} %get-tuple-element.28), channel_id=1, source_target_pairs={{0,16},{2,18},{4,20},{6,22},{8,24},{10,26},{12,28},{14,30},{16,0},... | collective-permute-start | bytes 786440 | tf_op jit(solution)/shard_map/ppermute | solution.py:323
  37.5 20.3 %collective-permute-start.23 = (bf16[128,1024]{1,0:T(8,128)(2,1)S(1)}, bf16[128,1024]{1,0:T(8,128)(2,1)S(1)}, u32[]{:S(2)}, u32[]{:S(2)}) collective-permute-start(bf16[128,1024]{1,0:T(8,128)(2,1)S(1)} %get-tuple-element.29), channel_id=1, source_target_pairs={{0,8},{2,10},{4,12},{6,14},{8,0},{10,2},{12,4},{14,6},{16,24},{18,... | collective-permute-start | bytes 786440 | tf_op jit(solution)/shard_map/ppermute | solution.py:323
  51.9 7.8 %collective-permute-start.8 = (bf16[128,192]{1,0:T(8,128)(2,1)S(1)}, bf16[128,192]{1,0:T(8,128)(2,1)S(1)}, u32[]{:S(2)}, u32[]{:S(2)}) collective-permute-start(bf16[128,192]{1,0:T(8,128)(2,1)S(1)} %get-tuple-element.38), channel_id=1, source_target_pairs={{0,24},{2,26},{4,28},{6,30},{8,16},{10,18},{12,20},{14,22},{16,8},... | collective-permute-start | bytes 147464 | tf_op jit(solution)/shard_map/ppermute | solution.py:323
  54.7 7.0 %collective-permute-start.7 = (bf16[128,192]{1,0:T(8,128)(2,1)S(1)}, bf16[128,192]{1,0:T(8,128)(2,1)S(1)}, u32[]{:S(2)}, u32[]{:S(2)}) collective-permute-start(bf16[128,192]{1,0:T(8,128)(2,1)S(1)} %get-tuple-element.39), channel_id=1, source_target_pairs={{0,16},{2,18},{4,20},{6,22},{8,24},{10,26},{12,28},{14,30},{16,0},... | collective-permute-start | bytes 147464 | tf_op jit(solution)/shard_map/ppermute | solution.py:323
  57.6 4.6 %collective-permute-start.6 = (bf16[128,192]{1,0:T(8,128)(2,1)S(1)}, bf16[128,192]{1,0:T(8,128)(2,1)S(1)}, u32[]{:S(2)}, u32[]{:S(2)}) collective-permute-start(bf16[128,192]{1,0:T(8,128)(2,1)S(1)} %get-tuple-element.40), channel_id=1, source_target_pairs={{0,8},{2,10},{4,12},{6,14},{8,0},{10,2},{12,4},{14,6},{16,24},{18,... | collective-permute-start | bytes 147464 | tf_op jit(solution)/shard_map/ppermute | solution.py:323
  58.0 61.7 %copy-start.2 = (bf16[512,1024]{1,0:T(8,128)(2,1)}, bf16[512,1024]{1,0:T(8,128)(2,1)S(1)}, u32[]{:S(2)}) copy-start(bf16[512,1024]{1,0:T(8,128)(2,1)S(1)} %pad_maximum_fusion.1.refs_12_) | copy-start | bytes 3145732
  58.0 65.2 %collective-permute-start.28 = (bf16[512,1024]{1,0:T(8,128)(2,1)S(1)}, bf16[512,1024]{1,0:T(8,128)(2,1)}, u32[]{:S(2)}, u32[]{:S(2)}) collective-permute-start(bf16[512,1024]{1,0:T(8,128)(2,1)S(1)} %pad_maximum_fusion.1.refs_12_), channel_id=1, source_target_pairs={{0,6},{2,4},{4,2},{6,0},{8,14},{10,12},{12,10},{14,8},{16,22},{18,... | collective-permute-start | bytes 3145736 | tf_op jit(solution)/shard_map/ppermute | solution.py:330
  59.7 2.5 %copy-start.18 = (bf16[128,192]{1,0:T(8,128)(2,1)}, bf16[128,192]{1,0:T(8,128)(2,1)S(1)}, u32[]{:S(2)}) copy-start(bf16[128,192]{1,0:T(8,128)(2,1)S(1)} %collective-permute-done.8.refs_3_) | copy-start | bytes 147460
  61.7 0.6 copy-start.19
  62.2 0.6 copy-start.20
  62.8 4.1 %copy-start.1 = (bf16[128,4096]{1,0:T(8,128)(2,1)S(1)}, bf16[128,4096]{1,0:T(8,128)(2,1)}, u32[]{:S(2)}) copy-start(bf16[128,4096]{1,0:T(8,128)(2,1)} %param.30) | copy-start | bytes 3145732
  66.9 4.6 %collective-permute-start.9 = (bf16[64,2048]{1,0:T(8,128)(2,1)}, bf16[64,2048]{1,0:T(8,128)(2,1)S(1)}, u32[]{:S(2)}, u32[]{:S(2)}) collective-permute-start(bf16[64,2048]{1,0:T(8,128)(2,1)} %get-tuple-element.14), channel_id=1, source_target_pairs={{0,1},{1,0},{2,3},{3,2},{4,5},{5,4},{6,7},{7,6},{8,9},{9,8},{10,11... | collective-permute-start | bytes 786440 | tf_op jit(solution)/shard_map/ppermute | solution.py:333
  67.0 11.2 %collective-permute-start.19 = (bf16[128,1024]{1,0:T(8,128)(2,1)S(1)}, bf16[128,1024]{1,0:T(8,128)(2,1)S(1)}, u32[]{:S(2)}, u32[]{:S(2)}) collective-permute-start(bf16[128,1024]{1,0:T(8,128)(2,1)S(1)} %get-tuple-element.31), channel_id=1, source_target_pairs={{0,24},{2,26},{4,28},{6,30},{8,16},{10,18},{12,20},{14,22},{16,8},... | collective-permute-start | bytes 786440 | tf_op jit(solution)/shard_map/ppermute | solution.py:323
  70.2 34.5 %collective-permute-start.18 = (bf16[128,1024]{1,0:T(8,128)(2,1)S(1)}, bf16[128,1024]{1,0:T(8,128)(2,1)S(1)}, u32[]{:S(2)}, u32[]{:S(2)}) collective-permute-start(bf16[128,1024]{1,0:T(8,128)(2,1)S(1)} %get-tuple-element.32), channel_id=1, source_target_pairs={{0,16},{2,18},{4,20},{6,22},{8,24},{10,26},{12,28},{14,30},{16,0},... | collective-permute-start | bytes 786440 | tf_op jit(solution)/shard_map/ppermute | solution.py:323
  70.2 34.5 %collective-permute-start.17 = (bf16[128,1024]{1,0:T(8,128)(2,1)S(1)}, bf16[128,1024]{1,0:T(8,128)(2,1)S(1)}, u32[]{:S(2)}, u32[]{:S(2)}) collective-permute-start(bf16[128,1024]{1,0:T(8,128)(2,1)S(1)} %get-tuple-element.33), channel_id=1, source_target_pairs={{0,8},{2,10},{4,12},{6,14},{8,0},{10,2},{12,4},{14,6},{16,24},{18,... | collective-permute-start | bytes 786440 | tf_op jit(solution)/shard_map/ppermute | solution.py:323
  71.5 0.7 copy-start.17
  74.3 30.4 %collective-permute-start.12 = (bf16[64,2048]{1,0:T(8,128)(2,1)}, bf16[64,2048]{1,0:T(8,128)(2,1)S(1)}, u32[]{:S(2)}, u32[]{:S(2)}) collective-permute-start(bf16[64,2048]{1,0:T(8,128)(2,1)} %get-tuple-element.16.refs_0_), channel_id=1, source_target_pairs={{0,24},{2,26},{4,28},{6,30},{8,16},{10,18},{12,20},{14,22},{16,8},... | collective-permute-start | bytes 786440 | tf_op jit(solution)/shard_map/ppermute | solution.py:323
  78.2 37.4 %collective-permute-start.11 = (bf16[64,2048]{1,0:T(8,128)(2,1)}, bf16[64,2048]{1,0:T(8,128)(2,1)S(1)}, u32[]{:S(2)}, u32[]{:S(2)}) collective-permute-start(bf16[64,2048]{1,0:T(8,128)(2,1)} %get-tuple-element.16.refs_0_), channel_id=1, source_target_pairs={{0,16},{2,18},{4,20},{6,22},{8,24},{10,26},{12,28},{14,30},{16,0},... | collective-permute-start | bytes 786440 | tf_op jit(solution)/shard_map/ppermute | solution.py:323
  104.7 13.2 %collective-permute-start.10 = (bf16[64,2048]{1,0:T(8,128)(2,1)}, bf16[64,2048]{1,0:T(8,128)(2,1)S(1)}, u32[]{:S(2)}, u32[]{:S(2)}) collective-permute-start(bf16[64,2048]{1,0:T(8,128)(2,1)} %get-tuple-element.16.refs_0_), channel_id=1, source_target_pairs={{0,8},{2,10},{4,12},{6,14},{8,0},{10,2},{12,4},{14,6},{16,24},{18,... | collective-permute-start | bytes 786440 | tf_op jit(solution)/shard_map/ppermute | solution.py:323
  104.8 13.3 %collective-permute-start.13 = (bf16[64,2048]{1,0:T(8,128)(2,1)}, bf16[64,2048]{1,0:T(8,128)(2,1)S(1)}, u32[]{:S(2)}, u32[]{:S(2)}) collective-permute-start(bf16[64,2048]{1,0:T(8,128)(2,1)} %get-tuple-element.16.refs_0_), channel_id=1, source_target_pairs={{0,1},{1,0},{2,3},{3,2},{4,5},{5,4},{6,7},{7,6},{8,9},{9,8},{10,11... | collective-permute-start | bytes 786440 | tf_op jit(solution)/shard_map/ppermute | solution.py:333
  104.8 83.9 %copy-start.10 = (bf16[64,2048]{1,0:T(8,128)(2,1)}, bf16[64,2048]{1,0:T(8,128)(2,1)S(1)}, u32[]{:S(2)}) copy-start(bf16[64,2048]{1,0:T(8,128)(2,1)S(1)} %collective-permute-done.12.refs_3_) | copy-start | bytes 786436
  104.8 14.9 %collective-permute-start.16 = (bf16[64,2048]{1,0:T(8,128)(2,1)S(1)}, bf16[64,2048]{1,0:T(8,128)(2,1)S(1)}, u32[]{:S(2)}, u32[]{:S(2)}) collective-permute-start(bf16[64,2048]{1,0:T(8,128)(2,1)S(1)} %collective-permute-done.12.refs_3_), channel_id=1, source_target_pairs={{0,1},{1,0},{2,3},{3,2},{4,5},{5,4},{6,7},{7,6},{8,9},{9,8},{10,11... | collective-permute-start | bytes 786440 | tf_op jit(solution)/shard_map/ppermute | solution.py:333
  115.6 73.0 %copy-start.11 = (bf16[64,2048]{1,0:T(8,128)(2,1)}, bf16[64,2048]{1,0:T(8,128)(2,1)S(1)}, u32[]{:S(2)}) copy-start(bf16[64,2048]{1,0:T(8,128)(2,1)S(1)} %collective-permute-done.11.refs_2_) | copy-start | bytes 786436
  115.6 4.7 %collective-permute-start.15 = (bf16[64,2048]{1,0:T(8,128)(2,1)S(1)}, bf16[64,2048]{1,0:T(8,128)(2,1)S(1)}, u32[]{:S(2)}, u32[]{:S(2)}) collective-permute-start(bf16[64,2048]{1,0:T(8,128)(2,1)S(1)} %collective-permute-done.11.refs_2_), channel_id=1, source_target_pairs={{0,1},{1,0},{2,3},{3,2},{4,5},{5,4},{6,7},{7,6},{8,9},{9,8},{10,11... | collective-permute-start | bytes 786440 | tf_op jit(solution)/shard_map/ppermute | solution.py:333
  117.9 70.7 %copy-start.12 = (bf16[64,2048]{1,0:T(8,128)(2,1)}, bf16[64,2048]{1,0:T(8,128)(2,1)S(1)}, u32[]{:S(2)}) copy-start(bf16[64,2048]{1,0:T(8,128)(2,1)S(1)} %collective-permute-done.10.refs_1_) | copy-start | bytes 786436
  117.9 3.7 %collective-permute-start.14 = (bf16[64,2048]{1,0:T(8,128)(2,1)S(1)}, bf16[64,2048]{1,0:T(8,128)(2,1)S(1)}, u32[]{:S(2)}, u32[]{:S(2)}) collective-permute-start(bf16[64,2048]{1,0:T(8,128)(2,1)S(1)} %collective-permute-done.10.refs_1_), channel_id=1, source_target_pairs={{0,1},{1,0},{2,3},{3,2},{4,5},{5,4},{6,7},{7,6},{8,9},{9,8},{10,11... | collective-permute-start | bytes 786440 | tf_op jit(solution)/shard_map/ppermute | solution.py:333
  118.0 72.1 %copy-start.3 = (bf16[512,1024]{1,0:T(8,128)(2,1)}, bf16[512,1024]{1,0:T(8,128)(2,1)S(1)}, u32[]{:S(2)}) copy-start(bf16[512,1024]{1,0:T(8,128)(2,1)S(1)} %pad_maximum_fusion.refs_8_) | copy-start | bytes 3145732
  118.0 70.6 %copy-start.13 = (bf16[64,2048]{1,0:T(8,128)(2,1)}, bf16[64,2048]{1,0:T(8,128)(2,1)S(1)}, u32[]{:S(2)}) copy-start(bf16[64,2048]{1,0:T(8,128)(2,1)S(1)} %collective-permute-done.13.refs_4_) | copy-start | bytes 786436
  118.0 26.1 %collective-permute-start.27 = (bf16[512,1024]{1,0:T(8,128)(2,1)S(1)}, bf16[512,1024]{1,0:T(8,128)(2,1)S(1)}, u32[]{:S(2)}, u32[]{:S(2)}) collective-permute-start(bf16[512,1024]{1,0:T(8,128)(2,1)S(1)} %pad_maximum_fusion.1.refs_12_), channel_id=1, source_target_pairs={{0,4},{2,6},{4,0},{6,2},{8,12},{10,14},{12,8},{14,10},{16,20},{18,... | collective-permute-start | bytes 3145736 | tf_op jit(solution)/shard_map/ppermute | solution.py:330
  119.6 69.0 %copy-start.14 = (bf16[64,2048]{1,0:T(8,128)(2,1)}, bf16[64,2048]{1,0:T(8,128)(2,1)S(1)}, u32[]{:S(2)}) copy-start(bf16[64,2048]{1,0:T(8,128)(2,1)S(1)} %collective-permute-done.16.refs_7_) | copy-start | bytes 786436
  119.6 26.1 %collective-permute-start.26 = (bf16[512,1024]{1,0:T(8,128)(2,1)S(1)}, bf16[512,1024]{1,0:T(8,128)(2,1)S(1)}, u32[]{:S(2)}, u32[]{:S(2)}) collective-permute-start(bf16[512,1024]{1,0:T(8,128)(2,1)S(1)} %pad_maximum_fusion.1.refs_12_), channel_id=1, source_target_pairs={{0,2},{2,0},{4,6},{6,4},{8,10},{10,8},{12,14},{14,12},{16,18},{18,... | collective-permute-start | bytes 3145736 | tf_op jit(solution)/shard_map/ppermute | solution.py:330
  120.3 68.3 %copy-start.15 = (bf16[64,2048]{1,0:T(8,128)(2,1)}, bf16[64,2048]{1,0:T(8,128)(2,1)S(1)}, u32[]{:S(2)}) copy-start(bf16[64,2048]{1,0:T(8,128)(2,1)S(1)} %collective-permute-done.15.refs_6_) | copy-start | bytes 786436
  120.3 47.9 %collective-permute-start.22 = (bf16[512,1024]{1,0:T(8,128)(2,1)S(1)}, bf16[512,1024]{1,0:T(8,128)(2,1)S(1)}, u32[]{:S(2)}, u32[]{:S(2)}) collective-permute-start(bf16[512,1024]{1,0:T(8,128)(2,1)S(1)} %pad_maximum_fusion.refs_8_), channel_id=1, source_target_pairs={{0,6},{2,4},{4,2},{6,0},{8,14},{10,12},{12,10},{14,8},{16,22},{18,... | collective-permute-start | bytes 3145736 | tf_op jit(solution)/shard_map/ppermute | solution.py:330
  121.7 67.0 %copy-start.16 = (bf16[64,2048]{1,0:T(8,128)(2,1)}, bf16[64,2048]{1,0:T(8,128)(2,1)S(1)}, u32[]{:S(2)}) copy-start(bf16[64,2048]{1,0:T(8,128)(2,1)S(1)} %collective-permute-done.14.refs_5_) | copy-start | bytes 786436
  121.7 66.9 %collective-permute-start.21 = (bf16[512,1024]{1,0:T(8,128)(2,1)S(1)}, bf16[512,1024]{1,0:T(8,128)(2,1)S(1)}, u32[]{:S(2)}, u32[]{:S(2)}) collective-permute-start(bf16[512,1024]{1,0:T(8,128)(2,1)S(1)} %pad_maximum_fusion.refs_8_), channel_id=1, source_target_pairs={{0,4},{2,6},{4,0},{6,2},{8,12},{10,14},{12,8},{14,10},{16,20},{18,... | collective-permute-start | bytes 3145736 | tf_op jit(solution)/shard_map/ppermute | solution.py:330
  123.2 66.9 %collective-permute-start.20 = (bf16[512,1024]{1,0:T(8,128)(2,1)S(1)}, bf16[512,1024]{1,0:T(8,128)(2,1)}, u32[]{:S(2)}, u32[]{:S(2)}) collective-permute-start(bf16[512,1024]{1,0:T(8,128)(2,1)S(1)} %pad_maximum_fusion.refs_8_), channel_id=1, source_target_pairs={{0,2},{2,0},{4,6},{6,4},{8,10},{10,8},{12,14},{14,12},{16,18},{18,... | collective-permute-start | bytes 3145736 | tf_op jit(solution)/shard_map/ppermute | solution.py:330
  144.1 45.9 %copy-start.6 = (bf16[512,1024]{1,0:T(8,128)(2,1)}, bf16[512,1024]{1,0:T(8,128)(2,1)S(1)}, u32[]{:S(2)}) copy-start(bf16[512,1024]{1,0:T(8,128)(2,1)S(1)} %collective-permute-done.27.refs_14_) | copy-start | bytes 3145732
  145.7 42.9 %copy-start.7 = (bf16[512,1024]{1,0:T(8,128)(2,1)}, bf16[512,1024]{1,0:T(8,128)(2,1)S(1)}, u32[]{:S(2)}) copy-start(bf16[512,1024]{1,0:T(8,128)(2,1)S(1)} %collective-permute-done.26.refs_13_) | copy-start | bytes 3145732
  168.2 20.5 %copy-start.8 = (bf16[512,1024]{1,0:T(8,128)(2,1)}, bf16[512,1024]{1,0:T(8,128)(2,1)S(1)}, u32[]{:S(2)}) copy-start(bf16[512,1024]{1,0:T(8,128)(2,1)S(1)} %collective-permute-done.22.refs_11_) | copy-start | bytes 3145732
  188.7 1.0 copy-start.9
  200.5 2.9 %collective-permute-start.29 = (bf16[4,64,2048]{2,1,0:T(8,128)(2,1)}, bf16[4,64,2048]{2,1,0:T(8,128)(2,1)S(1)}, u32[]{:S(2)}, u32[]{:S(2)}) collective-permute-start(bf16[4,64,2048]{2,1,0:T(8,128)(2,1)} %get-tuple-element.20), channel_id=1, source_target_pairs={{0,1},{1,0},{2,3},{3,2},{4,5},{5,4},{6,7},{7,6},{8,9},{9,8},{10,11... | collective-permute-start | bytes 3145736 | tf_op jit(solution)/shard_map/ppermute | solution.py:333
  203.4 28.2 %copy-start.5 = (bf16[64,2048]{1,0:T(8,128)(2,1)S(1)}, bf16[64,2048]{1,0:T(8,128)(2,1)}, u32[]{:S(2)}) copy-start(bf16[64,2048]{1,0:T(8,128)(2,1)} %get-tuple-element.15) | copy-start | bytes 786436
  205.2 8.6 %collective-permute-start.30 = (bf16[64,2048]{1,0:T(8,128)(2,1)S(1)}, bf16[64,2048]{1,0:T(8,128)(2,1)S(1)}, u32[]{:S(2)}, u32[]{:S(2)}) collective-permute-start(bf16[64,2048]{1,0:T(8,128)(2,1)S(1)} %get-tuple-element.23), channel_id=1, source_target_pairs={{0,8},{2,10},{4,12},{6,14},{8,0},{10,2},{12,4},{14,6},{16,24},{18,... | collective-permute-start | bytes 786440 | tf_op jit(solution)/shard_map/ppermute | solution.py:323
  205.2 15.0 %collective-permute-start.32 = (bf16[64,2048]{1,0:T(8,128)(2,1)S(1)}, bf16[64,2048]{1,0:T(8,128)(2,1)S(1)}, u32[]{:S(2)}, u32[]{:S(2)}) collective-permute-start(bf16[64,2048]{1,0:T(8,128)(2,1)S(1)} %get-tuple-element.24), channel_id=1, source_target_pairs={{0,24},{2,26},{4,28},{6,30},{8,16},{10,18},{12,20},{14,22},{16,8},... | collective-permute-start | bytes 786440 | tf_op jit(solution)/shard_map/ppermute | solution.py:323
  207.4 24.2 %collective-permute-start.31 = (bf16[64,2048]{1,0:T(8,128)(2,1)S(1)}, bf16[64,2048]{1,0:T(8,128)(2,1)S(1)}, u32[]{:S(2)}, u32[]{:S(2)}) collective-permute-start(bf16[64,2048]{1,0:T(8,128)(2,1)S(1)} %get-tuple-element.25), channel_id=1, source_target_pairs={{0,16},{2,18},{4,20},{6,22},{8,24},{10,26},{12,28},{14,30},{16,0},... | collective-permute-start | bytes 786440 | tf_op jit(solution)/shard_map/ppermute | solution.py:323
  231.8 1.6 collective-permute-start.33

commit v2 on v1

--- a/solution.py
+++ b/solution.py
@@ -42,7 +42,7 @@
 
     def statistics(number, carry):
         highest, total = carry
-        scores, start = block_scores(number)
+        scores, _ = block_scores(number)
         fresh = jnp.maximum(highest, jnp.max(scores, axis=-1, keepdims=True))
         total = total * jnp.exp(highest - fresh) + jnp.sum(
             jnp.exp(scores - fresh), axis=-1, keepdims=True
@@ -123,20 +123,33 @@
 
 VMEM = pltpu.VMEM
 SMEM = pltpu.SMEM
-ROWS = 128
 
 
 def vmem_specs(count):
     return [pl.BlockSpec(memory_space=VMEM)] * count
 
 
+def pack_kernel(slots, index, key_a, key_b, value_b, value_a, query_a, query_b, *refs):
+    outs, packed = refs[:slots], refs[slots]
+    for head in range(slots):
+        packed[head, :, 0:128] = key_a[:, head, :]
+        packed[head, :, 128:192] = key_b[head].T
+        packed[head, :, 192:256] = value_b[head].T
+        packed[head, :, 256:384] = value_a[:, head, :]
+        packed[head, :, 384:512] = query_a[:, head, :]
+        packed[head, :, 512:576] = query_b[head].T
+    for k in range(slots):
+        outs[k][...] = packed[index[0] ^ k]
+
+
 def attend_kernel(slots, plane, tokens, index, balance_a, balance_b, gain_a, gain_b, *refs):
-    queries, kv_pieces, out = refs[:slots], refs[slots : slots + plane], refs[slots + plane]
-    query, keyval, scores = refs[slots + plane + 1 :]
+    queries, kv_pieces = refs[:slots], refs[slots : slots + plane]
+    outs = refs[slots + plane : 2 * slots + plane]
+    query, keyval, scores, out = refs[2 * slots + plane :]
     z, g = index[0], index[1]
     wide = plane * tokens
     for k in range(slots):
-        query[z ^ k] = queries[k][...]
+        query[z ^ k] = queries[k][:, 384:576]
         for p in range(plane):
             start = pl.multiple_of(((z ^ k) * plane + (g ^ p)) * tokens, tokens)
             keyval[pl.ds(start, tokens), :] = kv_pieces[p][k]
@@ -193,9 +206,11 @@
 
     for number in range(slots):
         summed = group(number, 0, DK_A, 0, 256, balance_a[z])
-        out[z ^ number, :, 0:128] = normed(summed, gain_a)
+        out[number, :, 0:128] = normed(summed, gain_a)
         summed = group(number, 128, DK_B, 128, 128, balance_b[z])[:, 64:128]
-        out[z ^ number, :, 128:192] = normed(summed, gain_b)
+        out[number, :, 128:192] = normed(summed, gain_b)
+    for k in range(slots):
+        outs[k][...] = out[z ^ k]
 
 
 def project_kernel(slots, half, index, *refs):
@@ -244,51 +259,55 @@
     normed[...] = (value * lax.rsqrt(power + EPSILON) * gain[...]).astype(jnp.bfloat16)
 
 
-def mixer_kernel(slots, plane, index, *refs):
-    rows, refs = refs[: 2 * slots], refs[2 * slots :]
-    ups, downs = refs[:plane], refs[plane : 2 * plane]
-    own, other, left, hidden = refs[2 * plane :]
+def arrange_kernel(slots, plane, first, split, index, *refs):
+    firsts, rests, far, out = refs[:plane], refs[plane : 2 * plane - 1], refs[-3:-1], refs[-1]
     z, g = index[0], index[1]
+    block = out.shape[0] // (slots * plane)
+
+    def put(k, p, value):
+        place = pl.multiple_of(((z ^ k) * plane + (g ^ p)) * block, block)
+        out[pl.ds(place, block), :] = value
+
+    for p in range(plane):
+        put(0, p, firsts[p][first * block : (first + 1) * block, :])
+        for k in range(1, slots):
+            if p < plane - 1:
+                put(k, p, rests[p][(k - 1) * block : k * block, :])
+            elif k <= split:
+                put(k, p, far[0][(k - 1) * block : k * block, :])
+            else:
+                put(k, p, far[1][(k - 1 - split) * block : (k - split) * block, :])
+
+
+def lift_kernel(up, *refs):
+    rows, hidden, left = refs[:-2], refs[-2], refs[-1]
     half = rows[0].shape[0]
-    block = ups[0].shape[0] // slots
-    width = ups[0].shape[1]
-    every = 2 * slots * half
-
-    def place(k, p):
-        return pl.ds(pl.multiple_of(((z ^ k) * plane + (g ^ p)) * block, block), block)
-
     for r, piece in enumerate(rows):
-        for p in range(plane):
-            for k in range(slots):
-                at = (p * slots + k) * block
-                left[r * half : (r + 1) * half, at : at + block] = piece[:, place(k, p)]
+        left[r * half : (r + 1) * half, :] = piece[...]
     tile = 256
+    for n in range(up.shape[1] // tile):
+        span = slice(n * tile, (n + 1) * tile)
+        active = jnp.maximum(
+            jnp.dot(left[...], up[:, span], preferred_element_type=jnp.float32), 0.0
+        )
+        hidden[:, span] = (active * active).astype(jnp.bfloat16)
+
+
+def lower_kernel(hidden, down, own, other):
+    count, half, width = own.shape
+    tile = 512
     for n in range(width // tile):
         span = slice(n * tile, (n + 1) * tile)
-        total = jnp.zeros((every, tile), jnp.float32)
-        for p in range(plane):
-            part = slots * block
-            total += jnp.dot(
-                left[:, p * part : (p + 1) * part],
-                ups[p][:, span],
-                preferred_element_type=jnp.float32,
-            )
-        active = jnp.maximum(total, 0.0)
-        hidden[:, span] = (active * active).astype(jnp.bfloat16)
-    for p in range(plane):
-        for pair in range(0, slots, 2):
-            part = lax.dot_general(
-                hidden[...],
-                downs[p][pair * block : (pair + 2) * block, :],
-                (((1,), (1,)), ((), ())),
-                preferred_element_type=jnp.float32,
-            ).astype(jnp.bfloat16)
-            for k in (pair, pair + 1):
-                at = (k - pair) * block
-                for r in range(slots):
-                    rest = (r + slots) * half
-                    own[r, :, place(k, p)] = part[r * half : (r + 1) * half, at : at + block]
-                    other[r, :, place(k, p)] = part[rest : rest + half, at : at + block]
+        part = lax.dot_general(
+            hidden[...],
+            down[span, :],
+            (((1,), (1,)), ((), ())),
+            preferred_element_type=jnp.float32,
+        ).astype(jnp.bfloat16)
+        for r in range(count):
+            rest = (r + count) * half
+            own[r, :, span] = part[r * half : (r + 1) * half]
+            other[r, :, span] = part[rest : rest + half]
 
 
 def fast_body(slots, plane, *arguments):
@@ -332,39 +351,71 @@
     def swap(value):
         return lax.ppermute(value, "tp", [(0, 1), (1, 0)])
 
-    packed = jnp.concatenate(
-        [key_first, key_second, value_second, value_first, query_first, query_second], axis=2
-    ).transpose(1, 0, 2)
-    got = [along(lax.dynamic_index_in_dim(packed, z ^ k, 0, False), k) for k in range(slots)]
+    smem = pl.BlockSpec(memory_space=SMEM)
+    packed = pl.pallas_call(
+        functools.partial(pack_kernel, slots),
+        out_shape=(jax.ShapeDtypeStruct((tokens, 576), jnp.bfloat16),) * slots,
+        in_specs=[smem] + vmem_specs(6),
+        out_specs=tuple(vmem_specs(slots)),
+        scratch_shapes=[VMEM((slots, tokens, 576), jnp.bfloat16)],
+        compiler_params=pltpu.CompilerParams(vmem_limit_bytes=8 * 2**20),
+                cost_estimate=pl.CostEstimate(flops=10**8, bytes_accessed=10**6, transcendentals=0),
+        name="pack",
+    )(
+        index,
+        key_first,
+        key_second.transpose(1, 2, 0),
+        value_second.transpose(1, 2, 0),
+        value_first,
+        query_first,
+        query_second.transpose(1, 2, 0),
+    )
+    got = [along(packed[k], k) for k in range(slots)]
     keyval = jnp.stack([piece[:, :384] for piece in got])
-    queries = [piece[:, 384:] for piece in got]
     kv_pieces = [across(keyval, p) for p in range(plane)]
 
-    up_weight, down_weight, keyval = lax.optimization_barrier((up_weight, down_weight, keyval))
     hidden = up_weight.shape[1] // slots
 
-    def spread(weight):
-        parts = [
-            along(lax.dynamic_slice_in_dim(weight, (z ^ k) * hidden, hidden, 1), k)
-            for k in range(slots)
+    def column(weight, k):
+        return lax.dynamic_slice_in_dim(weight, (z ^ k) * hidden, hidden, 1)
+
+    early = jnp.concatenate([column(up_weight, 0), column(down_weight, 0)], axis=0)
+    firsts = [across(early, p) for p in range(plane)]
+    block = up_weight.shape[0]
+
+    def spread(weight, first, split):
+        parts = [along(column(weight, k), k) for k in range(1, slots)]
+        mine = jnp.concatenate(parts, axis=0)
+        near = [across(mine, p) for p in (1, 2)]
+        way = 1 if first == 0 else 2
+        far = [
+            across(near[2 - way][: split * block], way),
+            across(near[way - 1][split * block :], 3 - way),
         ]
-        mine = jnp.concatenate(parts, axis=0)
-        return [across(mine, p) for p in range(plane)]
-
-    ups = spread(up_weight)
-    downs = spread(down_weight)
-
-    smem = pl.BlockSpec(memory_space=SMEM)
+        return pl.pallas_call(
+            functools.partial(arrange_kernel, slots, plane, first, split),
+            out_shape=jax.ShapeDtypeStruct((count * block, hidden), jnp.bfloat16),
+            in_specs=[smem] + vmem_specs(2 * plane + 1),
+            out_specs=pl.BlockSpec(memory_space=VMEM),
+            compiler_params=pltpu.CompilerParams(vmem_limit_bytes=16 * 2**20),
+            cost_estimate=pl.CostEstimate(flops=10**8, bytes_accessed=10**6, transcendentals=0),
+        )(index, *firsts, mine, *near, *far)
+
+    up = spread(up_weight, 0, 2)
+    down = spread(down_weight, 1, 2)
+
     sequence = count * tokens
     heads = pl.pallas_call(
         functools.partial(attend_kernel, slots, plane, tokens),
-        out_shape=jax.ShapeDtypeStruct((slots, tokens, 192), jnp.bfloat16),
+        out_shape=(jax.ShapeDtypeStruct((tokens, 192), jnp.bfloat16),) * slots,
         in_specs=[smem] * 3 + vmem_specs(2 + slots + plane),
-        out_specs=pl.BlockSpec(memory_space=VMEM),
-        scratch_shapes=[
+        out_specs=tuple(vmem_specs(slots)),
+        compiler_params=pltpu.CompilerParams(vmem_limit_bytes=24 * 2**20),
+                scratch_shapes=[
             VMEM((slots, tokens, 192), jnp.bfloat16),
             VMEM((sequence, 384), jnp.bfloat16),
             VMEM((2 * tokens, sequence), jnp.float32),
+            VMEM((slots, tokens, 192), jnp.bfloat16),
         ],
         cost_estimate=pl.CostEstimate(flops=8 * 10**9, bytes_accessed=2 * 10**6, transcendentals=0),
         name="attend",
@@ -374,7 +425,7 @@
         balance_second,
         head_gain_first[None],
         head_gain_second[None],
-        *queries,
+        *got,
         *kv_pieces,
     )
     pieces = [along(heads[k], k) for k in range(slots)]
@@ -385,7 +436,8 @@
         in_specs=[smem] + vmem_specs(slots + 2),
         out_specs=tuple(vmem_specs(2)),
         scratch_shapes=[VMEM((slots, tokens, 192), jnp.bfloat16)],
-        cost_estimate=pl.CostEstimate(flops=2 * 10**9, bytes_accessed=4 * 10**6, transcendentals=0),
+        compiler_params=pltpu.CompilerParams(vmem_limit_bytes=16 * 2**20),
+                cost_estimate=pl.CostEstimate(flops=2 * 10**9, bytes_accessed=4 * 10**6, transcendentals=0),
         name="project",
     )(index, *pieces, out_first, out_second)
     mixed, normed = pl.pallas_call(
@@ -393,29 +445,49 @@
         out_shape=(row_shape, row_shape),
         in_specs=[smem] + vmem_specs(4),
         out_specs=tuple(vmem_specs(2)),
-        cost_estimate=pl.CostEstimate(flops=10**9, bytes_accessed=10**6, transcendentals=0),
+        compiler_params=pltpu.CompilerParams(vmem_limit_bytes=8 * 2**20),
+                cost_estimate=pl.CostEstimate(flops=10**9, bytes_accessed=10**6, transcendentals=0),
         name="norm",
     )(index, residual, own, swap(other), mlp_gain[None])
     own_rows = [along(normed, k) for k in range(slots)]
     other_rows = [swap(piece) for piece in own_rows]
-    part_shape = jax.ShapeDtypeStruct((slots, half, width), jnp.bfloat16)
-    own, other = pl.pallas_call(
-        functools.partial(mixer_kernel, slots, plane),
-        out_shape=(part_shape, part_shape),
-        in_specs=[smem] + vmem_specs(2 * slots + 2 * plane),
-        out_specs=tuple(vmem_specs(2)),
-        scratch_shapes=[
-            VMEM((2 * slots * half, width), jnp.bfloat16),
-            VMEM((2 * slots * half, hidden), jnp.bfloat16),
-        ],
-        cost_estimate=pl.CostEstimate(flops=6 * 10**9, bytes_accessed=10**7, transcendentals=0),
-        name="mixer",
-    )(index, *own_rows, *other_rows, *ups, *downs)
-    summed = own.astype(jnp.float32) + swap(other).astype(jnp.float32)
-    sent = summed.astype(jnp.bfloat16)
-    total = summed[0]
+    group = slots // 2
+    part_shape = jax.ShapeDtypeStruct((group, half, width), jnp.bfloat16)
+    total = None
+
+    def lift(lo):
+        chosen = own_rows[lo : lo + group] + other_rows[lo : lo + group]
+        return pl.pallas_call(
+            lift_kernel,
+            out_shape=jax.ShapeDtypeStruct((2 * group * half, hidden), jnp.bfloat16),
+            in_specs=vmem_specs(1 + 2 * group),
+            out_specs=pl.BlockSpec(memory_space=VMEM),
+            scratch_shapes=[VMEM((2 * group * half, width), jnp.bfloat16)],
+            compiler_params=pltpu.CompilerParams(vmem_limit_bytes=16 * 2**20),
+            cost_estimate=pl.CostEstimate(flops=3 * 10**9, bytes_accessed=10**6, transcendentals=0),
+        )(up, *chosen)
+
+    def lower(active):
+        return pl.pallas_call(
+            lower_kernel,
+            out_shape=(part_shape, part_shape),
+            in_specs=vmem_specs(2),
+            out_specs=tuple(vmem_specs(2)),
+            compiler_params=pltpu.CompilerParams(vmem_limit_bytes=16 * 2**20),
+            cost_estimate=pl.CostEstimate(flops=3 * 10**9, bytes_accessed=10**6, transcendentals=0),
+        )(active, down)
+
+    actives = {lo: lift(lo) for lo in (0, group)}
+    terms = {}
+    for lo in (group, 0):
+        own, other = lower(actives[lo])
+        summed = own.astype(jnp.float32) + swap(other).astype(jnp.float32)
+        for k in range(lo, lo + group):
+            piece = summed[k - lo]
+            terms[k] = piece if k == 0 else along(piece.astype(jnp.bfloat16), k)
+    total = terms[0]
     for k in range(1, slots):
-        total = total + along(sent[k], k).astype(jnp.float32)
+        total = total + terms[k].astype(jnp.float32)
     mine = (mixed.astype(jnp.float32) + total).astype(jnp.bfloat16)
     theirs = swap(mine)
     return jnp.where(
@@ -463,5 +535,6 @@
         P("sp", "tp"),
     )
     out_specs = P("sp", None)
-    chosen = plan(mesh)
-    return jax.shard_map(chosen, mesh=mesh, in_specs=in_specs, out_specs=out_specs, check_vma=False)
+    return jax.shard_map(
+        plan(mesh), mesh=mesh, in_specs=in_specs, out_specs=out_specs, check_vma=False
+    )

time: 235 us -> 182 us (0.77)
  waiting for transfers between devices: 140 us -> 99.3 us
  Pallas kernels: 24.7 us -> 17.9 us
  local copies, waits for them, and re-layouts: 13.2 us -> 8.15 us
    ppermute x9 -> x14, waiting for transfers between devices: 69.2 us -> 31.8 us  [across(): return lax.ppermute(value, 'sp', [(i, i ^ k) for i in range(count)])]
    ppermute x18, starting transfers between devices: 40.9 us -> 32.6 us  [along(): lax.ppermute(value, 'sp', [(i, (i // plane ^ k) * plane + i % plane) for...]
    ppermute x9 -> x14, starting transfers between devices: 11 us -> 18.3 us  [across(): return lax.ppermute(value, 'sp', [(i, i ^ k) for i in range(count)])]
    unnamed x52 -> x32, local copies, waits for them, and re-layouts: 8.12 us -> 5.35 us
    dynamic_slice x2, local copies, waits for them, and re-layouts: 0.17 us -> 2.55 us  [column(): return lax.dynamic_slice_in_dim(weight, (z ^ k) * hidden, hidden, 1)]
    pallas_call x1 -> x7, Pallas kernels: 10.4 us -> 8.97 us  [the longest x2 2.74 us: lift(): pl.pallas_call(lift_kernel, out_shape=jax.ShapeDtypeStruct((2 * group * h...]
  transfers between devices with their start and end apart: 34 -> 40, of which waited for: 21 -> 14; matrix products, arithmetic and copies ran while one was open for 2% -> 2% of each run, Pallas kernels for 6% -> 9%
where the time goes in v2:
time: 182 us; the launch traced here: 180 us
  waiting for transfers between devices  99.3 us (55%)
  starting transfers between devices  52.7 us (29%)
  Pallas kernels  17.9 us (10%)
  local copies, waits for them, and re-layouts  8.15 us (4%)
    ppermute x18, waiting for transfers between devices, along(): lax.ppermute(value, 'sp', [(i, (i // plane ^ k) * plane + i % plane) for...  64.4 us
    ppermute x18, starting transfers between devices, along(): lax.ppermute(value, 'sp', [(i, (i // plane ^ k) * plane + i % plane) for...  32.6 us
    ppermute x14, waiting for transfers between devices, across(): return lax.ppermute(value, 'sp', [(i, i ^ k) for i in range(count)])  31.8 us
    ppermute x14, starting transfers between devices, across(): return lax.ppermute(value, 'sp', [(i, i ^ k) for i in range(count)])  18.3 us
    pallas_call x1, Pallas kernels, fast_body(): pl.pallas_call(functools.partial(attend_kernel, slots, plane, tokens), ou...  6.39 us
    unnamed x32, local copies, waits for them, and re-layouts  5.35 us
  transfers between devices with their start and end apart: 40, of which 14 were waited for; matrix products, arithmetic and copies ran while one was open for 2% of the time, Pallas kernels for 9%

profile of v2, /device:TPU:0, one launch (start us, length us, event | category | flops | bytes accessed | tf_op | source)
XLA Modules:
  0.0 180.0 jit_solution(7213189026177000646)
XLA Ops:
  0.1 0.9 copy-done
  1.0 0.9 copy-done.1
  1.9 0.9 copy-done.2
  2.8 0.8 copy-done.3
  3.6 0.8 copy-done.4
  4.5 0.8 copy-done.5
  5.3 2.0 %pack.1 = (bf16[128,576]{1,0:T(8,128)(2,1)S(1)}, bf16[128,576]{1,0:T(8,128)(2,1)S(1)}, bf16[128,576]{1,0:T(8,128)(2,1)S(1)}, bf16[128,576]{1,0:T(8,128)(2,1)S(1)}) custom-call(s32[3]{0:T(128)S(1)} %pad_add_fusion.index, bf16[128,4,128]{2,1,0:T(4,128)(2,1)S(1)} %copy-done, bf16[4,64,128]{2,1,0:T(8,128)(2,1)S(1)} %bitcast.35, ...), custom_call_target="tpu_custom_call" | custom-call | flops 100000000 | bytes 1000000 | tf_op jit(solution)/shard_map/pack/pallas_call | solution.py:355
  7.4 5.1 %collective-permute-start.2 = (bf16[128,576]{1,0:T(8,128)(2,1)S(1)}, bf16[128,576]{1,0:T(8,128)(2,1)S(1)}, u32[]{:S(2)}, u32[]{:S(2)}) collective-permute-start(bf16[128,576]{1,0:T(8,128)(2,1)S(1)} %get-tuple-element.24), channel_id=1, source_target_pairs={{0,24},{2,26},{4,28},{6,30},{8,16},{10,18},{12,20},{14,22},{16,8},... | collective-permute-start | bytes 442376 | tf_op jit(solution)/shard_map/ppermute | solution.py:342
  12.5 0.6 collective-permute-start
  13.1 1.3 constant_dynamic-slice_fusion.3
  14.5 1.5 collective-permute-start.13
  15.9 2.9 %collective-permute-start.14 = (bf16[128,1024]{1,0:T(8,128)(2,1)S(1)}, bf16[128,1024]{1,0:T(8,128)(2,1)S(1)}, u32[]{:S(2)}, u32[]{:S(2)}) collective-permute-start(bf16[128,1024]{1,0:T(8,128)(2,1)S(1)} %get-tuple-element.44), channel_id=1, source_target_pairs={{0,16},{2,18},{4,20},{6,22},{8,24},{10,26},{12,28},{14,30},{16,0},... | collective-permute-start | bytes 786440 | tf_op jit(solution)/shard_map/ppermute | solution.py:342
  18.9 1.3 constant_dynamic-slice_fusion
  20.2 1.3 collective-permute-start.15
  21.5 5.9 %collective-permute-done.1.refs_2_ = bf16[128,576]{1,0:T(8,128)(2,1)S(1)} collective-permute-done((bf16[128,576]{1,0:T(8,128)(2,1)S(1)}, bf16[128,576]{1,0:T(8,128)(2,1)S(1)}, u32[]{:S(2)}, u32[]{:S(2)}) %collective-permute-start.1) | collective-permute-done | bytes 147488 | tf_op jit(solution)/shard_map/ppermute | solution.py:342
  27.5 3.3 %collective-permute-start.24 = (bf16[128,1024]{1,0:T(8,128)(2,1)S(1)}, bf16[128,1024]{1,0:T(8,128)(2,1)S(1)}, u32[]{:S(2)}, u32[]{:S(2)}) collective-permute-start(bf16[128,1024]{1,0:T(8,128)(2,1)S(1)} %get-tuple-element.40), channel_id=1, source_target_pairs={{0,16},{2,18},{4,20},{6,22},{8,24},{10,26},{12,28},{14,30},{16,0},... | collective-permute-start | bytes 786440 | tf_op jit(solution)/shard_map/ppermute | solution.py:342
  30.8 1.8 collective-permute-done.13
  32.6 1.5 collective-permute-start.3
  34.2 10.1 %collective-permute-done.14 = bf16[128,1024]{1,0:T(8,128)(2,1)S(1)} collective-permute-done((bf16[128,1024]{1,0:T(8,128)(2,1)S(1)}, bf16[128,1024]{1,0:T(8,128)(2,1)S(1)}, u32[]{:S(2)}, u32[]{:S(2)}) %collective-permute-start.14) | collective-permute-done | bytes 262176 | tf_op jit(solution)/shard_map/ppermute | solution.py:342
  44.3 1.5 collective-permute-start.4
  45.8 0.9 collective-permute-done.23
  46.7 2.4 %collective-permute-start.5 = (bf16[4,128,384]{2,1,0:T(8,128)(2,1)S(1)}, bf16[4,128,384]{2,1,0:T(8,128)(2,1)S(1)}, u32[]{:S(2)}, u32[]{:S(2)}) collective-permute-start(bf16[4,128,384]{2,1,0:T(8,128)(2,1)S(1)} %pad_maximum_fusion.1.refs_4_), channel_id=1, source_target_pairs={{0,6},{2,4},{4,2},{6,0},{8,14},{10,12},{12,10},{14,8},{16,22},{18,... | collective-permute-start | bytes 1179656 | tf_op jit(solution)/shard_map/ppermute | solution.py:349
  49.2 0.6 collective-permute-start.10
  49.8 10.3 %collective-permute-done.24 = bf16[128,1024]{1,0:T(8,128)(2,1)S(1)} collective-permute-done((bf16[128,1024]{1,0:T(8,128)(2,1)S(1)}, bf16[128,1024]{1,0:T(8,128)(2,1)S(1)}, u32[]{:S(2)}, u32[]{:S(2)}) %collective-permute-start.24) | collective-permute-done | bytes 262176 | tf_op jit(solution)/shard_map/ppermute | solution.py:342
  60.2 1.5 collective-permute-start.11
  61.7 2.5 %collective-permute-start.25 = (bf16[128,1024]{1,0:T(8,128)(2,1)S(1)}, bf16[128,1024]{1,0:T(8,128)(2,1)S(1)}, u32[]{:S(2)}, u32[]{:S(2)}) collective-permute-start(bf16[128,1024]{1,0:T(8,128)(2,1)S(1)} %get-tuple-element.37), channel_id=1, source_target_pairs={{0,24},{2,26},{4,28},{6,30},{8,16},{10,18},{12,20},{14,22},{16,8},... | collective-permute-start | bytes 786440 | tf_op jit(solution)/shard_map/ppermute | solution.py:342
  64.3 0.5 collective-permute-start.17
  64.8 6.4 %attend.1 = (bf16[128,192]{1,0:T(8,128)(2,1)S(1)}, bf16[128,192]{1,0:T(8,128)(2,1)S(1)}, bf16[128,192]{1,0:T(8,128)(2,1)S(1)}, bf16[128,192]{1,0:T(8,128)(2,1)S(1)}) custom-call(s32[3]{0:T(128)S(1)} %pad_add_fusion.index, f32[4]{0:T(128)S(1)} %copy-done.10, f32[4]{0:T(128)S(1)} %copy-done.11, f32[1,128]{1,0:T(1,128)S(1)} %bitcast.39, f32[1,64]{1,0:T(1,128)S(1)} %bitcast.40, ...), custom_call_target="tpu_custom_call" | custom-call | flops 8000000000 | bytes 2000000 | tf_op jit(solution)/shard_map/attend/pallas_call | solution.py:408
  71.3 2.7 %collective-permute-start.7 = (bf16[128,192]{1,0:T(8,128)(2,1)S(1)}, bf16[128,192]{1,0:T(8,128)(2,1)S(1)}, u32[]{:S(2)}, u32[]{:S(2)}) collective-permute-start(bf16[128,192]{1,0:T(8,128)(2,1)S(1)} %get-tuple-element.27), channel_id=1, source_target_pairs={{0,16},{2,18},{4,20},{6,22},{8,24},{10,26},{12,28},{14,30},{16,0},... | collective-permute-start | bytes 147464 | tf_op jit(solution)/shard_map/ppermute | solution.py:342
  74.1 1.6 collective-permute-start.26
  75.7 0.8 collective-permute-start.16
  76.5 1.5 collective-permute-start.27
  78.0 2.5 %collective-permute-start.8 = (bf16[128,192]{1,0:T(8,128)(2,1)S(1)}, bf16[128,192]{1,0:T(8,128)(2,1)S(1)}, u32[]{:S(2)}, u32[]{:S(2)}) collective-permute-start(bf16[128,192]{1,0:T(8,128)(2,1)S(1)} %get-tuple-element.28), channel_id=1, source_target_pairs={{0,24},{2,26},{4,28},{6,30},{8,16},{10,18},{12,20},{14,22},{16,8},... | collective-permute-start | bytes 147464 | tf_op jit(solution)/shard_map/ppermute | solution.py:342
  80.5 3.7 %collective-permute-done.8.refs_3_ = bf16[128,192]{1,0:T(8,128)(2,1)S(1)} collective-permute-done((bf16[128,192]{1,0:T(8,128)(2,1)S(1)}, bf16[128,192]{1,0:T(8,128)(2,1)S(1)}, u32[]{:S(2)}, u32[]{:S(2)}) %collective-permute-start.8) | collective-permute-done | bytes 49184 | tf_op jit(solution)/shard_map/ppermute | solution.py:342
  84.2 1.2 collective-permute-start.12
  85.3 1.8 project.1
  87.1 4.7 %collective-permute-done.17.refs_6_ = bf16[384,1024]{1,0:T(8,128)(2,1)S(1)} collective-permute-done((bf16[384,1024]{1,0:T(8,128)(2,1)S(1)}, bf16[384,1024]{1,0:T(8,128)(2,1)S(1)}, u32[]{:S(2)}, u32[]{:S(2)}) %collective-permute-start.17) | collective-permute-done | bytes 786464 | tf_op jit(solution)/shard_map/ppermute | solution.py:349
  91.9 1.5 collective-permute-done.9.other
  93.4 1.5 collective-permute-start.18
  94.9 0.8 norm.1
  95.7 27.1 %collective-permute-done.12.refs_3_ = bf16[256,1024]{1,0:T(8,128)(2,1)S(1)} collective-permute-done((bf16[256,1024]{1,0:T(8,128)(2,1)S(1)}, bf16[256,1024]{1,0:T(8,128)(2,1)S(1)}, u32[]{:S(2)}, u32[]{:S(2)}) %collective-permute-start.12) | collective-permute-done | bytes 524320 | tf_op jit(solution)/shard_map/ppermute | solution.py:349
  122.8 1.1 collective-permute-start.32
  123.9 1.4 collective-permute-start.33
  125.3 1.6 collective-permute-start.28
  126.9 0.6 collective-permute-start.19
  127.5 10.6 %collective-permute-done.32.refs_0_ = bf16[64,2048]{1,0:T(8,128)(2,1)S(1)} collective-permute-done((bf16[64,2048]{1,0:T(8,128)(2,1)S(1)}, bf16[64,2048]{1,0:T(8,128)(2,1)S(1)}, u32[]{:S(2)}, u32[]{:S(2)}) %collective-permute-start.32) | collective-permute-done | bytes 262176 | tf_op jit(solution)/shard_map/ppermute | solution.py:342
  138.1 1.5 collective-permute-start.29
  139.6 0.5 collective-permute-start.35
  140.1 0.8 shard_map.154.up
  141.0 3.5 %collective-permute-done.20.refs_1_ = bf16[64,2048]{1,0:T(8,128)(2,1)S(1)} collective-permute-done((bf16[64,2048]{1,0:T(8,128)(2,1)S(1)}, bf16[64,2048]{1,0:T(8,128)(2,1)S(1)}, u32[]{:S(2)}, u32[]{:S(2)}) %collective-permute-start.20) | collective-permute-done | bytes 262176 | tf_op jit(solution)/shard_map/ppermute | solution.py:342
  144.5 0.5 collective-permute-start.22
  145.0 0.8 shard_map.156.down
  145.9 1.5 shard_map.158.hidden
  147.3 1.3 shard_map.159
  148.7 1.3 shard_map.155.hidden
  150.0 1.3 shard_map.157
  151.3 0.5 collective-permute-start.30
  152.0 5.5 %collective-permute-start.37 = (bf16[64,2048]{1,0:T(8,128)(2,1)S(1)}, bf16[64,2048]{1,0:T(8,128)(2,1)S(1)}, u32[]{:S(2)}, u32[]{:S(2)}) collective-permute-start(bf16[64,2048]{1,0:T(8,128)(2,1)S(1)} %get-tuple-element.45), channel_id=1, source_target_pairs={{0,16},{2,18},{4,20},{6,22},{8,24},{10,26},{12,28},{14,30},{16,0},... | collective-permute-start | bytes 786440 | tf_op jit(solution)/shard_map/ppermute | solution.py:342
  157.5 2.1 %collective-permute-start.38 = (bf16[64,2048]{1,0:T(8,128)(2,1)S(1)}, bf16[64,2048]{1,0:T(8,128)(2,1)S(1)}, u32[]{:S(2)}, u32[]{:S(2)}) collective-permute-start(bf16[64,2048]{1,0:T(8,128)(2,1)S(1)} %get-tuple-element.46), channel_id=1, source_target_pairs={{0,24},{2,26},{4,28},{6,30},{8,16},{10,18},{12,20},{14,22},{16,8},... | collective-permute-start | bytes 786440 | tf_op jit(solution)/shard_map/ppermute | solution.py:342
  159.8 16.1 %collective-permute-done.37 = bf16[64,2048]{1,0:T(8,128)(2,1)S(1)} collective-permute-done((bf16[64,2048]{1,0:T(8,128)(2,1)S(1)}, bf16[64,2048]{1,0:T(8,128)(2,1)S(1)}, u32[]{:S(2)}, u32[]{:S(2)}) %collective-permute-start.37) | collective-permute-done | bytes 262176 | tf_op jit(solution)/shard_map/ppermute | solution.py:342
  175.9 1.3 collective-permute-done.31
  177.3 0.2 fusion.4
  177.5 1.5 collective-permute-done.39
  179.1 0.9 maximum_select_fusion
  (79 shorter events, 1.2 us)
Async XLA Ops:
  0.1 0.9 copy-start
  1.0 0.9 copy-start.1
  1.9 0.9 copy-start.2
  2.8 0.8 copy-start.3
  3.6 0.8 copy-start.4
  4.5 0.8 copy-start.5
  7.4 12.8 %collective-permute-start.2 = (bf16[128,576]{1,0:T(8,128)(2,1)S(1)}, bf16[128,576]{1,0:T(8,128)(2,1)S(1)}, u32[]{:S(2)}, u32[]{:S(2)}) collective-permute-start(bf16[128,576]{1,0:T(8,128)(2,1)S(1)} %get-tuple-element.24), channel_id=1, source_target_pairs={{0,24},{2,26},{4,28},{6,30},{8,16},{10,18},{12,20},{14,22},{16,8},... | collective-permute-start | bytes 442376 | tf_op jit(solution)/shard_map/ppermute | solution.py:342
  12.5 14.9 %collective-permute-start.1 = (bf16[128,576]{1,0:T(8,128)(2,1)S(1)}, bf16[128,576]{1,0:T(8,128)(2,1)S(1)}, u32[]{:S(2)}, u32[]{:S(2)}) collective-permute-start(bf16[128,576]{1,0:T(8,128)(2,1)S(1)} %get-tuple-element.23), channel_id=1, source_target_pairs={{0,16},{2,18},{4,20},{6,22},{8,24},{10,26},{12,28},{14,30},{16,0},... | collective-permute-start | bytes 442376 | tf_op jit(solution)/shard_map/ppermute | solution.py:342
  12.5 14.9 %collective-permute-start = (bf16[128,576]{1,0:T(8,128)(2,1)S(1)}, bf16[128,576]{1,0:T(8,128)(2,1)S(1)}, u32[]{:S(2)}, u32[]{:S(2)}) collective-permute-start(bf16[128,576]{1,0:T(8,128)(2,1)S(1)} %get-tuple-element.22), channel_id=1, source_target_pairs={{0,8},{2,10},{4,12},{6,14},{8,0},{10,2},{12,4},{14,6},{16,24},{18,... | collective-permute-start | bytes 442376 | tf_op jit(solution)/shard_map/ppermute | solution.py:342
  14.4 50.4 %copy-start.10 = (f32[4]{0:T(128)S(1)}, f32[4]{0:T(128)}, u32[]{:S(2)}) copy-start(f32[4]{0:T(128)} %balance_a.1) | copy-start | bytes 52
  14.4 50.4 %copy-start.11 = (f32[4]{0:T(128)S(1)}, f32[4]{0:T(128)}, u32[]{:S(2)}) copy-start(f32[4]{0:T(128)} %balance_b.1) | copy-start | bytes 52
  14.4 50.4 %copy-start.12 = (f32[128]{0:T(128)S(1)}, f32[128]{0:T(128)}, u32[]{:S(2)}) copy-start(f32[128]{0:T(128)} %param.25) | copy-start | bytes 1540
  14.5 50.3 %copy-start.13 = (f32[64]{0:T(128)S(1)}, f32[64]{0:T(128)}, u32[]{:S(2)}) copy-start(f32[64]{0:T(128)} %param.26) | copy-start | bytes 772
  14.5 18.1 %collective-permute-start.13 = (bf16[128,1024]{1,0:T(8,128)(2,1)S(1)}, bf16[128,1024]{1,0:T(8,128)(2,1)S(1)}, u32[]{:S(2)}, u32[]{:S(2)}) collective-permute-start(bf16[128,1024]{1,0:T(8,128)(2,1)S(1)} %get-tuple-element.42), channel_id=1, source_target_pairs={{0,8},{2,10},{4,12},{6,14},{8,0},{10,2},{12,4},{14,6},{16,24},{18,... | collective-permute-start | bytes 786440 | tf_op jit(solution)/shard_map/ppermute | solution.py:342
  15.9 28.3 %collective-permute-start.14 = (bf16[128,1024]{1,0:T(8,128)(2,1)S(1)}, bf16[128,1024]{1,0:T(8,128)(2,1)S(1)}, u32[]{:S(2)}, u32[]{:S(2)}) collective-permute-start(bf16[128,1024]{1,0:T(8,128)(2,1)S(1)} %get-tuple-element.44), channel_id=1, source_target_pairs={{0,16},{2,18},{4,20},{6,22},{8,24},{10,26},{12,28},{14,30},{16,0},... | collective-permute-start | bytes 786440 | tf_op jit(solution)/shard_map/ppermute | solution.py:342
  20.2 29.0 %collective-permute-start.15 = (bf16[128,1024]{1,0:T(8,128)(2,1)S(1)}, bf16[128,1024]{1,0:T(8,128)(2,1)S(1)}, u32[]{:S(2)}, u32[]{:S(2)}) collective-permute-start(bf16[128,1024]{1,0:T(8,128)(2,1)S(1)} %get-tuple-element.41), channel_id=1, source_target_pairs={{0,24},{2,26},{4,28},{6,30},{8,16},{10,18},{12,20},{14,22},{16,8},... | collective-permute-start | bytes 786440 | tf_op jit(solution)/shard_map/ppermute | solution.py:342
  27.4 19.3 %collective-permute-start.23 = (bf16[128,1024]{1,0:T(8,128)(2,1)S(1)}, bf16[128,1024]{1,0:T(8,128)(2,1)S(1)}, u32[]{:S(2)}, u32[]{:S(2)}) collective-permute-start(bf16[128,1024]{1,0:T(8,128)(2,1)S(1)} %get-tuple-element.38), channel_id=1, source_target_pairs={{0,8},{2,10},{4,12},{6,14},{8,0},{10,2},{12,4},{14,6},{16,24},{18,... | collective-permute-start | bytes 786440 | tf_op jit(solution)/shard_map/ppermute | solution.py:342
  27.5 32.7 %collective-permute-start.24 = (bf16[128,1024]{1,0:T(8,128)(2,1)S(1)}, bf16[128,1024]{1,0:T(8,128)(2,1)S(1)}, u32[]{:S(2)}, u32[]{:S(2)}) collective-permute-start(bf16[128,1024]{1,0:T(8,128)(2,1)S(1)} %get-tuple-element.40), channel_id=1, source_target_pairs={{0,16},{2,18},{4,20},{6,22},{8,24},{10,26},{12,28},{14,30},{16,0},... | collective-permute-start | bytes 786440 | tf_op jit(solution)/shard_map/ppermute | solution.py:342
  32.6 29.1 %collective-permute-start.3 = (bf16[4,128,384]{2,1,0:T(8,128)(2,1)S(1)}, bf16[4,128,384]{2,1,0:T(8,128)(2,1)S(1)}, u32[]{:S(2)}, u32[]{:S(2)}) collective-permute-start(bf16[4,128,384]{2,1,0:T(8,128)(2,1)S(1)} %pad_maximum_fusion.1.refs_4_), channel_id=1, source_target_pairs={{0,2},{2,0},{4,6},{6,4},{8,10},{10,8},{12,14},{14,12},{16,18},{18,... | collective-permute-start | bytes 1179656 | tf_op jit(solution)/shard_map/ppermute | solution.py:349
  44.3 20.0 %collective-permute-start.4 = (bf16[4,128,384]{2,1,0:T(8,128)(2,1)S(1)}, bf16[4,128,384]{2,1,0:T(8,128)(2,1)S(1)}, u32[]{:S(2)}, u32[]{:S(2)}) collective-permute-start(bf16[4,128,384]{2,1,0:T(8,128)(2,1)S(1)} %pad_maximum_fusion.1.refs_4_), channel_id=1, source_target_pairs={{0,4},{2,6},{4,0},{6,2},{8,12},{10,14},{12,8},{14,10},{16,20},{18,... | collective-permute-start | bytes 1179656 | tf_op jit(solution)/shard_map/ppermute | solution.py:349
  46.7 18.1 %collective-permute-start.5 = (bf16[4,128,384]{2,1,0:T(8,128)(2,1)S(1)}, bf16[4,128,384]{2,1,0:T(8,128)(2,1)S(1)}, u32[]{:S(2)}, u32[]{:S(2)}) collective-permute-start(bf16[4,128,384]{2,1,0:T(8,128)(2,1)S(1)} %pad_maximum_fusion.1.refs_4_), channel_id=1, source_target_pairs={{0,6},{2,4},{4,2},{6,0},{8,14},{10,12},{12,10},{14,8},{16,22},{18,... | collective-permute-start | bytes 1179656 | tf_op jit(solution)/shard_map/ppermute | solution.py:349
  49.2 24.9 %collective-permute-start.10 = (bf16[256,1024]{1,0:T(8,128)(2,1)S(1)}, bf16[256,1024]{1,0:T(8,128)(2,1)S(1)}, u32[]{:S(2)}, u32[]{:S(2)}) collective-permute-start(bf16[256,1024]{1,0:T(8,128)(2,1)S(1)} %pad_maximum_fusion.refs_0_), channel_id=1, source_target_pairs={{0,2},{2,0},{4,6},{6,4},{8,10},{10,8},{12,14},{14,12},{16,18},{18,... | collective-permute-start | bytes 1572872 | tf_op jit(solution)/shard_map/ppermute | solution.py:349
  60.2 15.5 %collective-permute-start.11 = (bf16[256,1024]{1,0:T(8,128)(2,1)S(1)}, bf16[256,1024]{1,0:T(8,128)(2,1)S(1)}, u32[]{:S(2)}, u32[]{:S(2)}) collective-permute-start(bf16[256,1024]{1,0:T(8,128)(2,1)S(1)} %pad_maximum_fusion.refs_0_), channel_id=1, source_target_pairs={{0,4},{2,6},{4,0},{6,2},{8,12},{10,14},{12,8},{14,10},{16,20},{18,... | collective-permute-start | bytes 1572872 | tf_op jit(solution)/shard_map/ppermute | solution.py:349
  61.7 9.6 %collective-permute-start.25 = (bf16[128,1024]{1,0:T(8,128)(2,1)S(1)}, bf16[128,1024]{1,0:T(8,128)(2,1)S(1)}, u32[]{:S(2)}, u32[]{:S(2)}) collective-permute-start(bf16[128,1024]{1,0:T(8,128)(2,1)S(1)} %get-tuple-element.37), channel_id=1, source_target_pairs={{0,24},{2,26},{4,28},{6,30},{8,16},{10,18},{12,20},{14,22},{16,8},... | collective-permute-start | bytes 786440 | tf_op jit(solution)/shard_map/ppermute | solution.py:342
  64.3 27.6 %collective-permute-start.17 = (bf16[384,1024]{1,0:T(8,128)(2,1)S(1)}, bf16[384,1024]{1,0:T(8,128)(2,1)S(1)}, u32[]{:S(2)}, u32[]{:S(2)}) collective-permute-start(bf16[384,1024]{1,0:T(8,128)(2,1)S(1)} %constant_dynamic-update-slice_fusion.refs_4_), channel_id=1, source_target_pairs={{0,4},{2,6},{4,0},{6,2},{8,12},{10,14},{12,8},{14,10},{16,20},{18,... | collective-permute-start | bytes 2359304 | tf_op jit(solution)/shard_map/ppermute | solution.py:349
  64.8 20.5 %copy-start.6 = (bf16[512,2048]{1,0:T(8,128)(2,1)S(1)}, bf16[512,2048]{1,0:T(8,128)(2,1)}, u32[]{:S(2)}) copy-start(bf16[512,2048]{1,0:T(8,128)(2,1)} %refs_4_.1) | copy-start | bytes 6291460
  64.8 20.5 %copy-start.7 = (bf16[256,2048]{1,0:T(8,128)(2,1)S(1)}, bf16[256,2048]{1,0:T(8,128)(2,1)}, u32[]{:S(2)}) copy-start(bf16[256,2048]{1,0:T(8,128)(2,1)} %refs_5_.1) | copy-start | bytes 3145732
  71.2 5.2 %collective-permute-start.6 = (bf16[128,192]{1,0:T(8,128)(2,1)S(1)}, bf16[128,192]{1,0:T(8,128)(2,1)S(1)}, u32[]{:S(2)}, u32[]{:S(2)}) collective-permute-start(bf16[128,192]{1,0:T(8,128)(2,1)S(1)} %get-tuple-element.26), channel_id=1, source_target_pairs={{0,8},{2,10},{4,12},{6,14},{8,0},{10,2},{12,4},{14,6},{16,24},{18,... | collective-permute-start | bytes 147464 | tf_op jit(solution)/shard_map/ppermute | solution.py:342
  71.3 6.7 %collective-permute-start.7 = (bf16[128,192]{1,0:T(8,128)(2,1)S(1)}, bf16[128,192]{1,0:T(8,128)(2,1)S(1)}, u32[]{:S(2)}, u32[]{:S(2)}) collective-permute-start(bf16[128,192]{1,0:T(8,128)(2,1)S(1)} %get-tuple-element.27), channel_id=1, source_target_pairs={{0,16},{2,18},{4,20},{6,22},{8,24},{10,26},{12,28},{14,30},{16,0},... | collective-permute-start | bytes 147464 | tf_op jit(solution)/shard_map/ppermute | solution.py:342
  74.1 49.8 %collective-permute-start.26 = (bf16[384,1024]{1,0:T(8,128)(2,1)S(1)}, bf16[384,1024]{1,0:T(8,128)(2,1)S(1)}, u32[]{:S(2)}, u32[]{:S(2)}) collective-permute-start(bf16[384,1024]{1,0:T(8,128)(2,1)S(1)} %constant_dynamic-update-slice_fusion.3.refs_4_), channel_id=1, source_target_pairs={{0,2},{2,0},{4,6},{6,4},{8,10},{10,8},{12,14},{14,12},{16,18},{18,... | collective-permute-start | bytes 2359304 | tf_op jit(solution)/shard_map/ppermute | solution.py:349
  75.7 49.6 %collective-permute-start.16 = (bf16[384,1024]{1,0:T(8,128)(2,1)S(1)}, bf16[384,1024]{1,0:T(8,128)(2,1)S(1)}, u32[]{:S(2)}, u32[]{:S(2)}) collective-permute-start(bf16[384,1024]{1,0:T(8,128)(2,1)S(1)} %constant_dynamic-update-slice_fusion.refs_4_), channel_id=1, source_target_pairs={{0,2},{2,0},{4,6},{6,4},{8,10},{10,8},{12,14},{14,12},{16,18},{18,... | collective-permute-start | bytes 2359304 | tf_op jit(solution)/shard_map/ppermute | solution.py:349
  76.5 50.5 %collective-permute-start.27 = (bf16[384,1024]{1,0:T(8,128)(2,1)S(1)}, bf16[384,1024]{1,0:T(8,128)(2,1)S(1)}, u32[]{:S(2)}, u32[]{:S(2)}) collective-permute-start(bf16[384,1024]{1,0:T(8,128)(2,1)S(1)} %constant_dynamic-update-slice_fusion.3.refs_4_), channel_id=1, source_target_pairs={{0,4},{2,6},{4,0},{6,2},{8,12},{10,14},{12,8},{14,10},{16,20},{18,... | collective-permute-start | bytes 2359304 | tf_op jit(solution)/shard_map/ppermute | solution.py:349
  78.0 6.2 %collective-permute-start.8 = (bf16[128,192]{1,0:T(8,128)(2,1)S(1)}, bf16[128,192]{1,0:T(8,128)(2,1)S(1)}, u32[]{:S(2)}, u32[]{:S(2)}) collective-permute-start(bf16[128,192]{1,0:T(8,128)(2,1)S(1)} %get-tuple-element.28), channel_id=1, source_target_pairs={{0,24},{2,26},{4,28},{6,30},{8,16},{10,18},{12,20},{14,22},{16,8},... | collective-permute-start | bytes 147464 | tf_op jit(solution)/shard_map/ppermute | solution.py:342
  84.2 38.6 %collective-permute-start.12 = (bf16[256,1024]{1,0:T(8,128)(2,1)S(1)}, bf16[256,1024]{1,0:T(8,128)(2,1)S(1)}, u32[]{:S(2)}, u32[]{:S(2)}) collective-permute-start(bf16[256,1024]{1,0:T(8,128)(2,1)S(1)} %pad_maximum_fusion.refs_0_), channel_id=1, source_target_pairs={{0,6},{2,4},{4,2},{6,0},{8,14},{10,12},{12,10},{14,8},{16,22},{18,... | collective-permute-start | bytes 1572872 | tf_op jit(solution)/shard_map/ppermute | solution.py:349
  85.3 9.5 %copy-start.8 = (bf16[128,2048]{1,0:T(8,128)(2,1)S(1)}, bf16[128,2048]{1,0:T(8,128)(2,1)}, u32[]{:S(2)}) copy-start(bf16[128,2048]{1,0:T(8,128)(2,1)} %residual.1) | copy-start | bytes 1572868
  85.3 9.5 %copy-start.9 = (f32[2048]{0:T(1024)S(1)}, f32[2048]{0:T(1024)}, u32[]{:S(2)}) copy-start(f32[2048]{0:T(1024)} %param.29) | copy-start | bytes 24580
  91.8 1.5 collective-permute-start.9
  93.4 46.3 %collective-permute-start.18 = (bf16[256,1024]{1,0:T(8,128)(2,1)S(1)}, bf16[256,1024]{1,0:T(8,128)(2,1)S(1)}, u32[]{:S(2)}, u32[]{:S(2)}) collective-permute-start(bf16[256,1024]{1,0:T(8,128)(2,1)S(1)} %slice.54), channel_id=1, source_target_pairs={{0,2},{2,0},{4,6},{6,4},{8,10},{10,8},{12,14},{14,12},{16,18},{18,... | collective-permute-start | bytes 1572872 | tf_op jit(solution)/shard_map/ppermute | solution.py:349
  122.8 15.3 %collective-permute-start.32 = (bf16[64,2048]{1,0:T(8,128)(2,1)S(1)}, bf16[64,2048]{1,0:T(8,128)(2,1)S(1)}, u32[]{:S(2)}, u32[]{:S(2)}) collective-permute-start(bf16[64,2048]{1,0:T(8,128)(2,1)S(1)} %get-tuple-element.32.refs_0_), channel_id=1, source_target_pairs={{0,16},{2,18},{4,20},{6,22},{8,24},{10,26},{12,28},{14,30},{16,0},... | collective-permute-start | bytes 786440 | tf_op jit(solution)/shard_map/ppermute | solution.py:342
  123.9 14.3 %collective-permute-start.33 = (bf16[64,2048]{1,0:T(8,128)(2,1)S(1)}, bf16[64,2048]{1,0:T(8,128)(2,1)S(1)}, u32[]{:S(2)}, u32[]{:S(2)}) collective-permute-start(bf16[64,2048]{1,0:T(8,128)(2,1)S(1)} %get-tuple-element.32.refs_0_), channel_id=1, source_target_pairs={{0,24},{2,26},{4,28},{6,30},{8,16},{10,18},{12,20},{14,22},{16,8},... | collective-permute-start | bytes 786440 | tf_op jit(solution)/shard_map/ppermute | solution.py:342
  125.3 19.7 %collective-permute-start.28 = (bf16[256,1024]{1,0:T(8,128)(2,1)S(1)}, bf16[256,1024]{1,0:T(8,128)(2,1)S(1)}, u32[]{:S(2)}, u32[]{:S(2)}) collective-permute-start(bf16[256,1024]{1,0:T(8,128)(2,1)S(1)} %slice.56), channel_id=1, source_target_pairs={{0,4},{2,6},{4,0},{6,2},{8,12},{10,14},{12,8},{14,10},{16,20},{18,... | collective-permute-start | bytes 1572872 | tf_op jit(solution)/shard_map/ppermute | solution.py:349
  126.9 12.7 %collective-permute-start.19 = (bf16[128,1024]{1,0:T(8,128)(2,1)S(1)}, bf16[128,1024]{1,0:T(8,128)(2,1)S(1)}, u32[]{:S(2)}, u32[]{:S(2)}) collective-permute-start(bf16[128,1024]{1,0:T(8,128)(2,1)S(1)} %slice.55), channel_id=1, source_target_pairs={{0,4},{2,6},{4,0},{6,2},{8,12},{10,14},{12,8},{14,10},{16,20},{18,... | collective-permute-start | bytes 786440 | tf_op jit(solution)/shard_map/ppermute | solution.py:349
  138.1 6.4 %collective-permute-start.20 = (bf16[64,2048]{1,0:T(8,128)(2,1)S(1)}, bf16[64,2048]{1,0:T(8,128)(2,1)S(1)}, u32[]{:S(2)}, u32[]{:S(2)}) collective-permute-start(bf16[64,2048]{1,0:T(8,128)(2,1)S(1)} %get-tuple-element.32.refs_0_), channel_id=1, source_target_pairs={{0,8},{2,10},{4,12},{6,14},{8,0},{10,2},{12,4},{14,6},{16,24},{18,... | collective-permute-start | bytes 786440 | tf_op jit(solution)/shard_map/ppermute | solution.py:342
  138.1 6.4 %collective-permute-start.29 = (bf16[128,1024]{1,0:T(8,128)(2,1)S(1)}, bf16[128,1024]{1,0:T(8,128)(2,1)S(1)}, u32[]{:S(2)}, u32[]{:S(2)}) collective-permute-start(bf16[128,1024]{1,0:T(8,128)(2,1)S(1)} %slice.57), channel_id=1, source_target_pairs={{0,2},{2,0},{4,6},{6,4},{8,10},{10,8},{12,14},{14,12},{16,18},{18,... | collective-permute-start | bytes 786440 | tf_op jit(solution)/shard_map/ppermute | solution.py:349
  139.6 6.2 %collective-permute-start.34 = (bf16[64,2048]{1,0:T(8,128)(2,1)S(1)}, bf16[64,2048]{1,0:T(8,128)(2,1)S(1)}, u32[]{:S(2)}, u32[]{:S(2)}) collective-permute-start(bf16[64,2048]{1,0:T(8,128)(2,1)S(1)} %collective-permute-done.32.refs_0_), channel_id=1, source_target_pairs={{0,1},{1,0},{2,3},{3,2},{4,5},{5,4},{6,7},{7,6},{8,9},{9,8},{10,11... | collective-permute-start | bytes 786440 | tf_op jit(solution)/shard_map/ppermute | solution.py:352
  139.6 6.2 %collective-permute-start.35 = (bf16[64,2048]{1,0:T(8,128)(2,1)S(1)}, bf16[64,2048]{1,0:T(8,128)(2,1)S(1)}, u32[]{:S(2)}, u32[]{:S(2)}) collective-permute-start(bf16[64,2048]{1,0:T(8,128)(2,1)S(1)} %collective-permute-done.33.refs_1_), channel_id=1, source_target_pairs={{0,1},{1,0},{2,3},{3,2},{4,5},{5,4},{6,7},{7,6},{8,9},{9,8},{10,11... | collective-permute-start | bytes 786440 | tf_op jit(solution)/shard_map/ppermute | solution.py:352
  144.5 4.2 %collective-permute-start.21 = (bf16[64,2048]{1,0:T(8,128)(2,1)S(1)}, bf16[64,2048]{1,0:T(8,128)(2,1)S(1)}, u32[]{:S(2)}, u32[]{:S(2)}) collective-permute-start(bf16[64,2048]{1,0:T(8,128)(2,1)S(1)} %get-tuple-element.32.refs_0_), channel_id=1, source_target_pairs={{0,1},{1,0},{2,3},{3,2},{4,5},{5,4},{6,7},{7,6},{8,9},{9,8},{10,11... | collective-permute-start | bytes 786440 | tf_op jit(solution)/shard_map/ppermute | solution.py:352
  144.5 4.2 %collective-permute-start.22 = (bf16[64,2048]{1,0:T(8,128)(2,1)S(1)}, bf16[64,2048]{1,0:T(8,128)(2,1)S(1)}, u32[]{:S(2)}, u32[]{:S(2)}) collective-permute-start(bf16[64,2048]{1,0:T(8,128)(2,1)S(1)} %collective-permute-done.20.refs_1_), channel_id=1, source_target_pairs={{0,1},{1,0},{2,3},{3,2},{4,5},{5,4},{6,7},{7,6},{8,9},{9,8},{10,11... | collective-permute-start | bytes 786440 | tf_op jit(solution)/shard_map/ppermute | solution.py:352
  148.6 3.2 %collective-permute-start.36 = (bf16[2,64,2048]{2,1,0:T(8,128)(2,1)S(1)}, bf16[2,64,2048]{2,1,0:T(8,128)(2,1)S(1)}, u32[]{:S(2)}, u32[]{:S(2)}) collective-permute-start(bf16[2,64,2048]{2,1,0:T(8,128)(2,1)S(1)} %get-tuple-element.36), channel_id=1, source_target_pairs={{0,1},{1,0},{2,3},{3,2},{4,5},{5,4},{6,7},{7,6},{8,9},{9,8},{10,11... | collective-permute-start | bytes 1572872 | tf_op jit(solution)/shard_map/ppermute | solution.py:352
  151.3 8.3 %collective-permute-start.30 = (bf16[2,64,2048]{2,1,0:T(8,128)(2,1)S(1)}, bf16[2,64,2048]{2,1,0:T(8,128)(2,1)S(1)}, u32[]{:S(2)}, u32[]{:S(2)}) collective-permute-start(bf16[2,64,2048]{2,1,0:T(8,128)(2,1)S(1)} %get-tuple-element.34), channel_id=1, source_target_pairs={{0,1},{1,0},{2,3},{3,2},{4,5},{5,4},{6,7},{7,6},{8,9},{9,8},{10,11... | collective-permute-start | bytes 1572872 | tf_op jit(solution)/shard_map/ppermute | solution.py:352
  152.0 23.9 %collective-permute-start.37 = (bf16[64,2048]{1,0:T(8,128)(2,1)S(1)}, bf16[64,2048]{1,0:T(8,128)(2,1)S(1)}, u32[]{:S(2)}, u32[]{:S(2)}) collective-permute-start(bf16[64,2048]{1,0:T(8,128)(2,1)S(1)} %get-tuple-element.45), channel_id=1, source_target_pairs={{0,16},{2,18},{4,20},{6,22},{8,24},{10,26},{12,28},{14,30},{16,0},... | collective-permute-start | bytes 786440 | tf_op jit(solution)/shard_map/ppermute | solution.py:342
  157.5 18.4 %collective-permute-start.38 = (bf16[64,2048]{1,0:T(8,128)(2,1)S(1)}, bf16[64,2048]{1,0:T(8,128)(2,1)S(1)}, u32[]{:S(2)}, u32[]{:S(2)}) collective-permute-start(bf16[64,2048]{1,0:T(8,128)(2,1)S(1)} %get-tuple-element.46), channel_id=1, source_target_pairs={{0,24},{2,26},{4,28},{6,30},{8,16},{10,18},{12,20},{14,22},{16,8},... | collective-permute-start | bytes 786440 | tf_op jit(solution)/shard_map/ppermute | solution.py:342
  159.8 17.5 %collective-permute-start.31 = (bf16[64,2048]{1,0:T(8,128)(2,1)S(1)}, bf16[64,2048]{1,0:T(8,128)(2,1)S(1)}, u32[]{:S(2)}, u32[]{:S(2)}) collective-permute-start(bf16[64,2048]{1,0:T(8,128)(2,1)S(1)} %fusion.5), channel_id=1, source_target_pairs={{0,8},{2,10},{4,12},{6,14},{8,0},{10,2},{12,4},{14,6},{16,24},{18,... | collective-permute-start | bytes 786440 | tf_op jit(solution)/shard_map/ppermute | solution.py:342
  177.4 1.6 collective-permute-start.39

commit v3 on v2

--- a/solution.py
+++ b/solution.py
@@ -129,8 +129,18 @@
     return [pl.BlockSpec(memory_space=VMEM)] * count
 
 
-def pack_kernel(slots, index, key_a, key_b, value_b, value_a, query_a, query_b, *refs):
-    outs, packed = refs[:slots], refs[slots]
+def pack_kernel(slots, index, *refs):
+    sources, outs, held = refs[:6], refs[6 : 6 + slots], refs[6 + slots : -2]
+    packed, arrived = refs[-2:]
+    copies = [
+        pltpu.make_async_copy(source, target, arrived.at[i])
+        for i, (source, target) in enumerate(zip(sources, held))
+    ]
+    for copy in copies:
+        copy.start()
+    for copy in copies:
+        copy.wait()
+    key_a, key_b, value_b, value_a, query_a, query_b = held
     for head in range(slots):
         packed[head, :, 0:128] = key_a[:, head, :]
         packed[head, :, 128:192] = key_b[head].T
@@ -142,17 +152,39 @@
         outs[k][...] = packed[index[0] ^ k]
 
 
+def cut_kernel(slots, width, index, *refs):
+    weights, pairs, ups, downs = refs[:2], refs[2:4], refs[4 : 2 + slots], refs[2 + slots : -1]
+    arrived = refs[-1]
+    block = weights[0].shape[0]
+    copies = []
+    for i, (weight, pieces) in enumerate(zip(weights, (ups, downs))):
+        for k in range(slots):
+            place = pl.ds(pl.multiple_of((index[0] ^ k) * width, width), width)
+            target = pairs[k].at[pl.ds(i * block, block), :] if k < 2 else pieces[k - 2]
+            copies.append(
+                pltpu.make_async_copy(weight.at[:, place], target, arrived.at[i * slots + k])
+            )
+    for copy in copies:
+        copy.start()
+    for copy in copies:
+        copy.wait()
+
+
 def attend_kernel(slots, plane, tokens, index, balance_a, balance_b, gain_a, gain_b, *refs):
-    queries, kv_pieces = refs[:slots], refs[slots : slots + plane]
-    outs = refs[slots + plane : 2 * slots + plane]
-    query, keyval, scores, out = refs[2 * slots + plane :]
+    queries, kv_pieces = refs[:slots], refs[slots : slots + plane + 1]
+    outs = refs[slots + plane + 1 : 2 * slots + plane + 1]
+    query, keyval, scores, out = refs[2 * slots + plane + 1 :]
     z, g = index[0], index[1]
     wide = plane * tokens
     for k in range(slots):
         query[z ^ k] = queries[k][:, 384:576]
         for p in range(plane):
             start = pl.multiple_of(((z ^ k) * plane + (g ^ p)) * tokens, tokens)
-            keyval[pl.ds(start, tokens), :] = kv_pieces[p][k]
+            if p < plane - 1:
+                keyval[pl.ds(start, tokens), :] = kv_pieces[p][k]
+            else:
+                part = slots // 2
+                keyval[pl.ds(start, tokens), :] = kv_pieces[p + k // part][k % part]
     lane = lax.broadcasted_iota(jnp.int32, (tokens, 128), 1)
     row = lax.broadcasted_iota(jnp.int32, (2 * tokens, wide), 0) % tokens
     column = lax.broadcasted_iota(jnp.int32, (2 * tokens, wide), 1)
@@ -259,24 +291,12 @@
     normed[...] = (value * lax.rsqrt(power + EPSILON) * gain[...]).astype(jnp.bfloat16)
 
 
-def arrange_kernel(slots, plane, first, split, index, *refs):
-    firsts, rests, far, out = refs[:plane], refs[plane : 2 * plane - 1], refs[-3:-1], refs[-1]
+def arrange_kernel(moves, plane, block, index, *refs):
+    out = refs[-1]
     z, g = index[0], index[1]
-    block = out.shape[0] // (slots * plane)
-
-    def put(k, p, value):
+    for p, k, number, at in moves:
         place = pl.multiple_of(((z ^ k) * plane + (g ^ p)) * block, block)
-        out[pl.ds(place, block), :] = value
-
-    for p in range(plane):
-        put(0, p, firsts[p][first * block : (first + 1) * block, :])
-        for k in range(1, slots):
-            if p < plane - 1:
-                put(k, p, rests[p][(k - 1) * block : k * block, :])
-            elif k <= split:
-                put(k, p, far[0][(k - 1) * block : k * block, :])
-            else:
-                put(k, p, far[1][(k - 1 - split) * block : (k - split) * block, :])
+        out[pl.ds(place, block), :] = refs[number][at * block : (at + 1) * block, :]
 
 
 def lift_kernel(up, *refs):
@@ -352,17 +372,9 @@
         return lax.ppermute(value, "tp", [(0, 1), (1, 0)])
 
     smem = pl.BlockSpec(memory_space=SMEM)
-    packed = pl.pallas_call(
-        functools.partial(pack_kernel, slots),
-        out_shape=(jax.ShapeDtypeStruct((tokens, 576), jnp.bfloat16),) * slots,
-        in_specs=[smem] + vmem_specs(6),
-        out_specs=tuple(vmem_specs(slots)),
-        scratch_shapes=[VMEM((slots, tokens, 576), jnp.bfloat16)],
-        compiler_params=pltpu.CompilerParams(vmem_limit_bytes=8 * 2**20),
-                cost_estimate=pl.CostEstimate(flops=10**8, bytes_accessed=10**6, transcendentals=0),
-        name="pack",
-    )(
-        index,
+    hidden = up_weight.shape[1] // slots
+    block = up_weight.shape[0]
+    sources = (
         key_first,
         key_second.transpose(1, 2, 0),
         value_second.transpose(1, 2, 0),
@@ -370,45 +382,93 @@
         query_first,
         query_second.transpose(1, 2, 0),
     )
+    packed = pl.pallas_call(
+        functools.partial(pack_kernel, slots),
+        out_shape=(jax.ShapeDtypeStruct((tokens, 576), jnp.bfloat16),) * slots,
+        in_specs=[smem] + [pl.BlockSpec(memory_space=pltpu.HBM)] * 6,
+        out_specs=tuple(vmem_specs(slots)),
+        scratch_shapes=[VMEM(source.shape, jnp.bfloat16) for source in sources]
+        + [VMEM((slots, tokens, 576), jnp.bfloat16), pltpu.SemaphoreType.DMA((6,))],
+        cost_estimate=pl.CostEstimate(flops=10**8, bytes_accessed=10**6, transcendentals=0),
+        name="pack",
+    )(index, *sources)
+    piece_shape = jax.ShapeDtypeStruct((block, hidden), jnp.bfloat16)
+    cuts = pl.pallas_call(
+        functools.partial(cut_kernel, slots, hidden),
+        out_shape=(jax.ShapeDtypeStruct((2 * block, hidden), jnp.bfloat16),) * 2
+        + (piece_shape,) * (2 * slots - 4),
+        in_specs=[smem] + [pl.BlockSpec(memory_space=pltpu.HBM)] * 2,
+        out_specs=tuple(vmem_specs(2 * slots - 2)),
+        scratch_shapes=[pltpu.SemaphoreType.DMA((2 * slots,))],
+        cost_estimate=pl.CostEstimate(flops=10**8, bytes_accessed=10**6, transcendentals=0),
+        name="cut",
+    )(index, up_weight, down_weight)
+    early, both, cut_up, cut_down = cuts[0], cuts[1], cuts[2:slots], cuts[slots:]
     got = [along(packed[k], k) for k in range(slots)]
     keyval = jnp.stack([piece[:, :384] for piece in got])
-    kv_pieces = [across(keyval, p) for p in range(plane)]
-
-    hidden = up_weight.shape[1] // slots
-
-    def column(weight, k):
-        return lax.dynamic_slice_in_dim(weight, (z ^ k) * hidden, hidden, 1)
-
-    early = jnp.concatenate([column(up_weight, 0), column(down_weight, 0)], axis=0)
-    firsts = [across(early, p) for p in range(plane)]
-    block = up_weight.shape[0]
-
-    def spread(weight, first, split):
-        parts = [along(column(weight, k), k) for k in range(1, slots)]
-        mine = jnp.concatenate(parts, axis=0)
-        near = [across(mine, p) for p in (1, 2)]
-        way = 1 if first == 0 else 2
-        far = [
-            across(near[2 - way][: split * block], way),
-            across(near[way - 1][split * block :], 3 - way),
-        ]
+    kv_pieces = [across(keyval, p) for p in range(plane - 1)]
+    halves = (kv_pieces[2][: slots // 2], kv_pieces[1][slots // 2 :])
+    kv_pieces.append(across(halves[0], 1))
+    kv_pieces.append(across(halves[1], 2))
+
+    firsts = [across(early, p) for p in range(3)]
+    last_up = across(firsts[2][:block], 1)
+    last_down = across(firsts[1][block:], 2)
+
+    def gather(arrays, turn):
+        mine = jnp.concatenate(arrays, axis=0) if len(arrays) > 1 else arrays[0]
+        near = [mine, across(mine, 1), across(mine, 2)]
+        blocks = mine.shape[0] // block
+        split = (blocks + 1) // 2
+        ways = (1, 2) if turn == 0 else (2, 1)
+        pieces = [[(p, near[p], i) for p in range(3)] for i in range(blocks)]
+        for way, lo, hi in ((ways[0], 0, split), (ways[1], split, blocks)):
+            if hi > lo:
+                far = across(near[3 - way][lo * block : hi * block], way)
+                for i in range(lo, hi):
+                    pieces[i].append((3, far, i - lo))
+        return pieces
+
+    def arrange(pieces):
+        arrays = []
+        moves = []
+        for p, k, array, at in pieces:
+            numbers = [i for i, other in enumerate(arrays) if other is array]
+            if not numbers:
+                numbers = [len(arrays)]
+                arrays.append(array)
+            moves.append((p, k, numbers[0], at))
         return pl.pallas_call(
-            functools.partial(arrange_kernel, slots, plane, first, split),
+            functools.partial(arrange_kernel, tuple(moves), plane, block),
             out_shape=jax.ShapeDtypeStruct((count * block, hidden), jnp.bfloat16),
-            in_specs=[smem] + vmem_specs(2 * plane + 1),
+            in_specs=[smem] + vmem_specs(len(arrays)),
             out_specs=pl.BlockSpec(memory_space=VMEM),
             compiler_params=pltpu.CompilerParams(vmem_limit_bytes=16 * 2**20),
             cost_estimate=pl.CostEstimate(flops=10**8, bytes_accessed=10**6, transcendentals=0),
-        )(index, *firsts, mine, *near, *far)
-
-    up = spread(up_weight, 0, 2)
-    down = spread(down_weight, 1, 2)
+        )(index, *arrays)
+
+    own_up = [(p, 0, firsts[p], 0) for p in range(3)] + [(3, 0, last_up, 0)]
+    own_down = [(p, 0, firsts[p], 1) for p in range(3)] + [(3, 0, last_down, 0)]
+
+    def label(k, pieces):
+        return [(p, k, array, at) for p, array, at in pieces]
+
+    moved = [along(both, 1)] + [along(cut, k) for k, cut in zip(range(2, slots), cut_up)]
+    group = gather(moved, 0)
+    own_up += label(1, group[0])
+    own_down += label(1, group[1])
+    for k in range(2, slots):
+        own_up += label(k, group[k])
+    for k, cut in zip(range(2, slots), cut_down):
+        own_down += label(k, gather([along(cut, k)], k % 2)[0])
+    up = arrange(own_up)
+    down = arrange(own_down)
 
     sequence = count * tokens
     heads = pl.pallas_call(
         functools.partial(attend_kernel, slots, plane, tokens),
         out_shape=(jax.ShapeDtypeStruct((tokens, 192), jnp.bfloat16),) * slots,
-        in_specs=[smem] * 3 + vmem_specs(2 + slots + plane),
+        in_specs=[smem] * 3 + vmem_specs(3 + slots + plane),
         out_specs=tuple(vmem_specs(slots)),
         compiler_params=pltpu.CompilerParams(vmem_limit_bytes=24 * 2**20),
                 scratch_shapes=[
@@ -455,8 +515,8 @@
     part_shape = jax.ShapeDtypeStruct((group, half, width), jnp.bfloat16)
     total = None
 
-    def lift(lo):
-        chosen = own_rows[lo : lo + group] + other_rows[lo : lo + group]
+    def lift(chosen_slots):
+        chosen = [own_rows[k] for k in chosen_slots] + [other_rows[k] for k in chosen_slots]
         return pl.pallas_call(
             lift_kernel,
             out_shape=jax.ShapeDtypeStruct((2 * group * half, hidden), jnp.bfloat16),
@@ -477,13 +537,13 @@
             cost_estimate=pl.CostEstimate(flops=3 * 10**9, bytes_accessed=10**6, transcendentals=0),
         )(active, down)
 
-    actives = {lo: lift(lo) for lo in (0, group)}
     terms = {}
-    for lo in (group, 0):
-        own, other = lower(actives[lo])
-        summed = own.astype(jnp.float32) + swap(other).astype(jnp.float32)
-        for k in range(lo, lo + group):
-            piece = summed[k - lo]
+    for chosen in (list(range(1, slots, 2)), list(range(slots - 2, -1, -2))):
+        own, other = lower(lift(chosen))
+        other = swap(other)
+        summed = own.astype(jnp.float32) + other.astype(jnp.float32)
+        for at, k in enumerate(chosen):
+            piece = summed[at]
             terms[k] = piece if k == 0 else along(piece.astype(jnp.bfloat16), k)
     total = terms[0]
     for k in range(1, slots):

time: 182 us -> 164 us (0.901)
  the two profiles are of different devices: /device:TPU:0 before, /device:TPU:9 now
where the time goes in v3:
time: 164 us
  waiting for transfers between devices  82.1 us (50%)
  starting transfers between devices  54.5 us (33%)
  Pallas kernels  23.3 us (14%)
  other arithmetic  2.02 us (1%)
    ppermute x17, waiting for transfers between devices, along(): lax.ppermute(value, 'sp', [(i, (i // plane ^ k) * plane + i % plane) for...  59.7 us
    ppermute x8, starting transfers between devices, swap(): return lax.ppermute(value, 'tp', [(0, 1), (1, 0)])  29.2 us
    ppermute x18, waiting for transfers between devices, across(): return lax.ppermute(value, 'sp', [(i, i ^ k) for i in range(count)])  20.6 us
    ppermute x18, starting transfers between devices, across(): return lax.ppermute(value, 'sp', [(i, i ^ k) for i in range(count)])  13.8 us
    ppermute x17, starting transfers between devices, along(): lax.ppermute(value, 'sp', [(i, (i // plane ^ k) * plane + i % plane) for...  11.6 us
    pallas_call x1, Pallas kernels, fast_body(): pl.pallas_call(functools.partial(attend_kernel, slots, plane, tokens), ou...  6.39 us
    pallas_call x1, Pallas kernels, fast_body(): pl.pallas_call(functools.partial(pack_kernel, slots), out_shape=(jax.Shap...  3.85 us
    pallas_call x1, Pallas kernels, fast_body(): pl.pallas_call(functools.partial(cut_kernel, slots, hidden), out_shape=(j...  3.56 us
  transfers between devices with their start and end apart: 43, of which 19 were waited for; matrix products, arithmetic and copies ran while one was open for 1% of the time, Pallas kernels for 12%

profile of v3, /device:TPU:9, one launch (start us, length us, event | category | flops | bytes accessed | tf_op | source)
XLA Modules:
  0.0 163.7 jit_solution(5428493353063825001)
XLA Ops:
  0.0 0.6 pad_add_fusion.index
  0.7 3.8 %pack.1 = (bf16[128,576]{1,0:T(8,128)(2,1)}, bf16[128,576]{1,0:T(8,128)(2,1)}, bf16[128,576]{1,0:T(8,128)(2,1)}, bf16[128,576]{1,0:T(8,128)(2,1)}) custom-call(s32[3]{0:T(128)} %pad_add_fusion.index, bf16[128,4,128]{2,1,0:T(4,128)(2,1)} %refs_0_.2, bf16[4,64,128]{2,1,0:T(8,128)(2,1)} %bitcast.38, bf16[4,64,128]{2,1,0:T(8,128)(2,1)} %bitcast.39, ...), custom_call_target="tpu_custom_call" | custom-call | flops 100000000 | bytes 1000000 | tf_op jit(solution)/shard_map/pack/pallas_call | solution.py:385
  4.6 2.5 %collective-permute-start.1 = (bf16[128,576]{1,0:T(8,128)(2,1)}, bf16[128,576]{1,0:T(8,128)(2,1)S(1)}, u32[]{:S(2)}, u32[]{:S(2)}) collective-permute-start(bf16[128,576]{1,0:T(8,128)(2,1)} %get-tuple-element.29), channel_id=1, source_target_pairs={{0,16},{2,18},{4,20},{6,22},{8,24},{10,26},{12,28},{14,30},{16,0},... | collective-permute-start | bytes 442376 | tf_op jit(solution)/shard_map/ppermute | solution.py:362
  7.1 0.2 collective-permute-start.2
  7.2 3.6 %cut.1 = (bf16[256,1024]{1,0:T(8,128)(2,1)}, bf16[256,1024]{1,0:T(8,128)(2,1)}, bf16[128,1024]{1,0:T(8,128)(2,1)}, bf16[128,1024]{1,0:T(8,128)(2,1)}, bf16[128,1...) custom-call(s32[3]{0:T(128)} %pad_add_fusion.index, bf16[128,4096]{1,0:T(8,128)(2,1)} %refs_0_.3, bf16[128,4096]{1,0:T(8,128)(2,1)} %refs_1_.1), custom_call_target="tpu_custom_call" | custom-call | flops 100000000 | bytes 1000000 | tf_op jit(solution)/shard_map/cut/pallas_call | solution.py:396
  10.8 1.2 collective-permute-start.14
  12.0 0.9 slice_bitcast_fusion.6
  12.9 1.5 collective-permute-done.1.refs_2_
  14.5 7.0 %collective-permute-done.2.refs_3_ = bf16[128,576]{1,0:T(8,128)(2,1)S(1)} collective-permute-done((bf16[128,576]{1,0:T(8,128)(2,1)}, bf16[128,576]{1,0:T(8,128)(2,1)S(1)}, u32[]{:S(2)}, u32[]{:S(2)}) %collective-permute-start.2) | collective-permute-done | bytes 147488 | tf_op jit(solution)/shard_map/ppermute | solution.py:362
  21.5 1.3 collective-permute-start.4
  22.8 1.2 collective-permute-start.3
  24.1 1.5 collective-permute-start.16
  25.5 4.2 %collective-permute-done.14 = bf16[256,1024]{1,0:T(8,128)(2,1)S(1)} collective-permute-done((bf16[256,1024]{1,0:T(8,128)(2,1)}, bf16[256,1024]{1,0:T(8,128)(2,1)S(1)}, u32[]{:S(2)}, u32[]{:S(2)}) %collective-permute-start.14) | collective-permute-done | bytes 524320 | tf_op jit(solution)/shard_map/ppermute | solution.py:362
  29.8 0.7 collective-permute-done.4.refs_6_
  30.5 1.4 collective-permute-start.5
  32.0 1.9 %collective-permute-start.6 = (bf16[2,128,384]{2,1,0:T(8,128)(2,1)S(1)}, bf16[2,128,384]{2,1,0:T(8,128)(2,1)S(1)}, u32[]{:S(2)}, u32[]{:S(2)}) collective-permute-start(bf16[2,128,384]{2,1,0:T(8,128)(2,1)S(1)} %slice.63), channel_id=1, source_target_pairs={{0,4},{2,6},{4,0},{6,2},{8,12},{10,14},{12,8},{14,10},{16,20},{18,... | collective-permute-start | bytes 589832 | tf_op jit(solution)/shard_map/ppermute | solution.py:369
  33.9 1.0 collective-permute-done.15
  34.9 12.4 %collective-permute-done.16 = bf16[128,1024]{1,0:T(8,128)(2,1)S(1)} collective-permute-done((bf16[128,1024]{1,0:T(8,128)(2,1)}, bf16[128,1024]{1,0:T(8,128)(2,1)S(1)}, u32[]{:S(2)}, u32[]{:S(2)}) %collective-permute-start.16) | collective-permute-done | bytes 262176 | tf_op jit(solution)/shard_map/ppermute | solution.py:362
  47.3 0.2 collective-permute-start.18
  47.5 0.3 collective-permute-start.17
  47.9 6.4 %attend.1 = (bf16[128,192]{1,0:T(8,128)(2,1)S(1)}, bf16[128,192]{1,0:T(8,128)(2,1)S(1)}, bf16[128,192]{1,0:T(8,128)(2,1)S(1)}, bf16[128,192]{1,0:T(8,128)(2,1)S(1)}) custom-call(s32[3]{0:T(128)S(1)} %copy-done.2, f32[4]{0:T(128)S(1)} %copy-done.7, f32[4]{0:T(128)S(1)} %copy-done.8, f32[1,128]{1,0:T(1,128)S(1)} %bitcast.36, f32[1,64]{1,0:T(1,128)S(1)} %bitcast.37, ...), custom_call_target="tpu_custom_call" | custom-call | flops 8000000000 | bytes 2000000 | tf_op jit(solution)/shard_map/attend/pallas_call | solution.py:468
  54.4 1.3 collective-permute-start.12
  55.7 0.7 collective-permute-start.8
  56.4 1.3 collective-permute-done.7.refs_1_
  57.8 0.5 collective-permute-start.9
  58.2 1.5 collective-permute-done.8.refs_2_
  59.7 1.4 collective-permute-start.25
  61.1 1.0 collective-permute-done.9.refs_3_
  62.1 1.8 %project.1 = (bf16[64,2048]{1,0:T(8,128)(2,1)S(1)}, bf16[64,2048]{1,0:T(8,128)(2,1)S(1)}) custom-call(s32[3]{0:T(128)S(1)} %copy-done.2, bf16[128,192]{1,0:T(8,128)(2,1)S(1)} %get-tuple-element.31.refs_0_, bf16[128,192]{1,0:T(8,128)(2,1)S(1)} %collective-permute-done.7.refs_1_, bf16[128,192]{1,0:T(8,128)(2,1)S(1)} %collective-permute-done.8.refs_2_, ...), custom_call_target="tpu_custom_call" | custom-call | flops 2000000000 | bytes 4000000 | tf_op jit(solution)/shard_map/project/pallas_call | solution.py:493
  63.9 8.7 %collective-permute-start.10 = (bf16[64,2048]{1,0:T(8,128)(2,1)S(1)}, bf16[64,2048]{1,0:T(8,128)(2,1)S(1)}, u32[]{:S(2)}, u32[]{:S(2)}) collective-permute-start(bf16[64,2048]{1,0:T(8,128)(2,1)S(1)} %get-tuple-element.36), channel_id=1, source_target_pairs={{0,1},{1,0},{2,3},{3,2},{4,5},{5,4},{6,7},{7,6},{8,9},{9,8},{10,11... | collective-permute-start | bytes 786440 | tf_op jit(solution)/shard_map/ppermute | solution.py:372
  72.6 1.2 collective-permute-start.11
  73.8 1.3 collective-permute-start.29
  75.0 0.2 collective-permute-start.27
  75.3 5.3 %collective-permute-done.12.refs_2_ = bf16[256,1024]{1,0:T(8,128)(2,1)S(1)} collective-permute-done((bf16[256,1024]{1,0:T(8,128)(2,1)S(1)}, bf16[256,1024]{1,0:T(8,128)(2,1)S(1)}, u32[]{:S(2)}, u32[]{:S(2)}) %collective-permute-start.12) | collective-permute-done | bytes 524320 | tf_op jit(solution)/shard_map/ppermute | solution.py:369
  80.8 0.2 collective-permute-start.20
  81.1 0.8 norm.1
  81.9 1.2 collective-permute-done.29.refs_12_
  83.0 1.2 collective-permute-start.13
  84.2 2.0 %collective-permute-done.27.refs_10_ = bf16[128,1024]{1,0:T(8,128)(2,1)S(1)} collective-permute-done((bf16[128,1024]{1,0:T(8,128)(2,1)S(1)}, bf16[128,1024]{1,0:T(8,128)(2,1)S(1)}, u32[]{:S(2)}, u32[]{:S(2)}) %collective-permute-start.27) | collective-permute-done | bytes 262176 | tf_op jit(solution)/shard_map/ppermute | solution.py:369
  86.4 12.5 %collective-permute-done.13.refs_3_ = bf16[128,1024]{1,0:T(8,128)(2,1)S(1)} collective-permute-done((bf16[128,1024]{1,0:T(8,128)(2,1)S(1)}, bf16[128,1024]{1,0:T(8,128)(2,1)S(1)}, u32[]{:S(2)}, u32[]{:S(2)}) %collective-permute-start.13) | collective-permute-done | bytes 262176 | tf_op jit(solution)/shard_map/ppermute | solution.py:369
  98.9 0.2 collective-permute-start.31
  99.2 13.6 %collective-permute-start.23 = (bf16[64,2048]{1,0:T(8,128)(2,1)S(1)}, bf16[64,2048]{1,0:T(8,128)(2,1)S(1)}, u32[]{:S(2)}, u32[]{:S(2)}) collective-permute-start(bf16[64,2048]{1,0:T(8,128)(2,1)S(1)} %get-tuple-element.42.refs_1_), channel_id=1, source_target_pairs={{0,1},{1,0},{2,3},{3,2},{4,5},{5,4},{6,7},{7,6},{8,9},{9,8},{10,11... | collective-permute-start | bytes 786440 | tf_op jit(solution)/shard_map/ppermute | solution.py:372
  112.9 0.8 shard_map.154.up
  113.7 1.3 collective-permute-start.24
  115.0 1.3 collective-permute-start.28
  116.5 1.3 shard_map.155.hidden
  117.8 6.0 %collective-permute-done.35.refs_1_ = bf16[64,2048]{1,0:T(8,128)(2,1)S(1)} collective-permute-done((bf16[64,2048]{1,0:T(8,128)(2,1)S(1)}, bf16[64,2048]{1,0:T(8,128)(2,1)S(1)}, u32[]{:S(2)}, u32[]{:S(2)}) %collective-permute-start.35) | collective-permute-done | bytes 262176 | tf_op jit(solution)/shard_map/ppermute | solution.py:362
  123.8 5.4 %collective-permute-start.37 = (bf16[64,2048]{1,0:T(8,128)(2,1)S(1)}, bf16[64,2048]{1,0:T(8,128)(2,1)S(1)}, u32[]{:S(2)}, u32[]{:S(2)}) collective-permute-start(bf16[64,2048]{1,0:T(8,128)(2,1)S(1)} %collective-permute-done.35.refs_1_), channel_id=1, source_target_pairs={{0,1},{1,0},{2,3},{3,2},{4,5},{5,4},{6,7},{7,6},{8,9},{9,8},{10,11... | collective-permute-start | bytes 786440 | tf_op jit(solution)/shard_map/ppermute | solution.py:372
  129.3 1.0 shard_map.156.down
  130.3 1.3 shard_map.157
  131.6 0.6 collective-permute-start.33
  132.1 1.3 shard_map.158.hidden
  133.4 1.3 shard_map.159
  135.0 1.1 collective-permute-start.40
  136.1 0.6 collective-permute-done.38
  136.9 0.7 collective-permute-start.39
  137.6 0.4 collective-permute-start.41
  138.0 9.4 %collective-permute-done.40 = bf16[64,2048]{1,0:T(8,128)(2,1)S(1)} collective-permute-done((bf16[64,2048]{1,0:T(8,128)(2,1)S(1)}, bf16[64,2048]{1,0:T(8,128)(2,1)S(1)}, u32[]{:S(2)}, u32[]{:S(2)}) %collective-permute-start.40) | collective-permute-done | bytes 262176 | tf_op jit(solution)/shard_map/ppermute | solution.py:362
  147.4 1.6 collective-permute-done.39
  149.0 11.7 %collective-permute-done.41 = bf16[64,2048]{1,0:T(8,128)(2,1)S(1)} collective-permute-done((bf16[64,2048]{1,0:T(8,128)(2,1)S(1)}, bf16[64,2048]{1,0:T(8,128)(2,1)S(1)}, u32[]{:S(2)}, u32[]{:S(2)}) %collective-permute-start.41) | collective-permute-done | bytes 262176 | tf_op jit(solution)/shard_map/ppermute | solution.py:362
  160.7 0.2 fusion.4
  160.9 0.7 collective-permute-start.42
  161.6 1.2 collective-permute-done.42
  162.8 0.9 maximum_select_fusion
  (80 shorter events, 1.6 us)
Async XLA Ops:
  0.0 47.8 %copy-start.10 = (f32[64]{0:T(128)S(1)}, f32[64]{0:T(128)}, u32[]{:S(2)}) copy-start(f32[64]{0:T(128)} %param.26) | copy-start | bytes 772
  0.0 47.8 %copy-start.9 = (f32[128]{0:T(128)S(1)}, f32[128]{0:T(128)}, u32[]{:S(2)}) copy-start(f32[128]{0:T(128)} %param.25) | copy-start | bytes 1540
  0.0 47.8 %copy-start.8 = (f32[4]{0:T(128)S(1)}, f32[4]{0:T(128)}, u32[]{:S(2)}) copy-start(f32[4]{0:T(128)} %balance_b.1) | copy-start | bytes 52
  0.0 47.8 %copy-start.7 = (f32[4]{0:T(128)S(1)}, f32[4]{0:T(128)}, u32[]{:S(2)}) copy-start(f32[4]{0:T(128)} %balance_a.1) | copy-start | bytes 52
  0.7 47.1 %copy-start.2 = (s32[3]{0:T(128)S(1)}, s32[3]{0:T(128)}, u32[]{:S(2)}) copy-start(s32[3]{0:T(128)} %pad_add_fusion.index) | copy-start | bytes 40
  4.5 43.3 %copy-start.1 = (bf16[128,576]{1,0:T(8,128)(2,1)S(1)}, bf16[128,576]{1,0:T(8,128)(2,1)}, u32[]{:S(2)}) copy-start(bf16[128,576]{1,0:T(8,128)(2,1)} %get-tuple-element.27.refs_0_) | copy-start | bytes 442372
  4.5 8.4 %collective-permute-start = (bf16[128,576]{1,0:T(8,128)(2,1)}, bf16[128,576]{1,0:T(8,128)(2,1)S(1)}, u32[]{:S(2)}, u32[]{:S(2)}) collective-permute-start(bf16[128,576]{1,0:T(8,128)(2,1)} %get-tuple-element.28), channel_id=1, source_target_pairs={{0,8},{2,10},{4,12},{6,14},{8,0},{10,2},{12,4},{14,6},{16,24},{18,... | collective-permute-start | bytes 442376 | tf_op jit(solution)/shard_map/ppermute | solution.py:362
  4.6 9.9 %collective-permute-start.1 = (bf16[128,576]{1,0:T(8,128)(2,1)}, bf16[128,576]{1,0:T(8,128)(2,1)S(1)}, u32[]{:S(2)}, u32[]{:S(2)}) collective-permute-start(bf16[128,576]{1,0:T(8,128)(2,1)} %get-tuple-element.29), channel_id=1, source_target_pairs={{0,16},{2,18},{4,20},{6,22},{8,24},{10,26},{12,28},{14,30},{16,0},... | collective-permute-start | bytes 442376 | tf_op jit(solution)/shard_map/ppermute | solution.py:362
  7.1 14.4 %collective-permute-start.2 = (bf16[128,576]{1,0:T(8,128)(2,1)}, bf16[128,576]{1,0:T(8,128)(2,1)S(1)}, u32[]{:S(2)}, u32[]{:S(2)}) collective-permute-start(bf16[128,576]{1,0:T(8,128)(2,1)} %get-tuple-element.30), channel_id=1, source_target_pairs={{0,24},{2,26},{4,28},{6,30},{8,16},{10,18},{12,20},{14,22},{16,8},... | collective-permute-start | bytes 442376 | tf_op jit(solution)/shard_map/ppermute | solution.py:362
  10.8 18.9 %collective-permute-start.14 = (bf16[256,1024]{1,0:T(8,128)(2,1)}, bf16[256,1024]{1,0:T(8,128)(2,1)S(1)}, u32[]{:S(2)}, u32[]{:S(2)}) collective-permute-start(bf16[256,1024]{1,0:T(8,128)(2,1)} %get-tuple-element.39), channel_id=1, source_target_pairs={{0,8},{2,10},{4,12},{6,14},{8,0},{10,2},{12,4},{14,6},{16,24},{18,... | collective-permute-start | bytes 1572872 | tf_op jit(solution)/shard_map/ppermute | solution.py:362
  21.5 9.0 %collective-permute-start.4 = (bf16[4,128,384]{2,1,0:T(8,128)(2,1)S(1)}, bf16[4,128,384]{2,1,0:T(8,128)(2,1)S(1)}, u32[]{:S(2)}, u32[]{:S(2)}) collective-permute-start(bf16[4,128,384]{2,1,0:T(8,128)(2,1)S(1)} %pad_maximum_fusion.refs_4_), channel_id=1, source_target_pairs={{0,4},{2,6},{4,0},{6,2},{8,12},{10,14},{12,8},{14,10},{16,20},{18,... | collective-permute-start | bytes 1179656 | tf_op jit(solution)/shard_map/ppermute | solution.py:369
  22.8 9.1 %collective-permute-start.3 = (bf16[4,128,384]{2,1,0:T(8,128)(2,1)S(1)}, bf16[4,128,384]{2,1,0:T(8,128)(2,1)S(1)}, u32[]{:S(2)}, u32[]{:S(2)}) collective-permute-start(bf16[4,128,384]{2,1,0:T(8,128)(2,1)S(1)} %pad_maximum_fusion.refs_4_), channel_id=1, source_target_pairs={{0,2},{2,0},{4,6},{6,4},{8,10},{10,8},{12,14},{14,12},{16,18},{18,... | collective-permute-start | bytes 1179656 | tf_op jit(solution)/shard_map/ppermute | solution.py:369
  24.0 10.8 %collective-permute-start.15 = (bf16[128,1024]{1,0:T(8,128)(2,1)}, bf16[128,1024]{1,0:T(8,128)(2,1)S(1)}, u32[]{:S(2)}, u32[]{:S(2)}) collective-permute-start(bf16[128,1024]{1,0:T(8,128)(2,1)} %get-tuple-element.40), channel_id=1, source_target_pairs={{0,16},{2,18},{4,20},{6,22},{8,24},{10,26},{12,28},{14,30},{16,0},... | collective-permute-start | bytes 786440 | tf_op jit(solution)/shard_map/ppermute | solution.py:362
  24.1 23.2 %collective-permute-start.16 = (bf16[128,1024]{1,0:T(8,128)(2,1)}, bf16[128,1024]{1,0:T(8,128)(2,1)S(1)}, u32[]{:S(2)}, u32[]{:S(2)}) collective-permute-start(bf16[128,1024]{1,0:T(8,128)(2,1)} %get-tuple-element.41), channel_id=1, source_target_pairs={{0,24},{2,26},{4,28},{6,30},{8,16},{10,18},{12,20},{14,22},{16,8},... | collective-permute-start | bytes 786440 | tf_op jit(solution)/shard_map/ppermute | solution.py:362
  30.5 17.2 %collective-permute-start.5 = (bf16[2,128,384]{2,1,0:T(8,128)(2,1)S(1)}, bf16[2,128,384]{2,1,0:T(8,128)(2,1)S(1)}, u32[]{:S(2)}, u32[]{:S(2)}) collective-permute-start(bf16[2,128,384]{2,1,0:T(8,128)(2,1)S(1)} %slice.62), channel_id=1, source_target_pairs={{0,2},{2,0},{4,6},{6,4},{8,10},{10,8},{12,14},{14,12},{16,18},{18,... | collective-permute-start | bytes 589832 | tf_op jit(solution)/shard_map/ppermute | solution.py:369
  32.0 15.8 %collective-permute-start.6 = (bf16[2,128,384]{2,1,0:T(8,128)(2,1)S(1)}, bf16[2,128,384]{2,1,0:T(8,128)(2,1)S(1)}, u32[]{:S(2)}, u32[]{:S(2)}) collective-permute-start(bf16[2,128,384]{2,1,0:T(8,128)(2,1)S(1)} %slice.63), channel_id=1, source_target_pairs={{0,4},{2,6},{4,0},{6,2},{8,12},{10,14},{12,8},{14,10},{16,20},{18,... | collective-permute-start | bytes 589832 | tf_op jit(solution)/shard_map/ppermute | solution.py:369
  47.3 26.5 %collective-permute-start.18 = (bf16[512,1024]{1,0:T(8,128)(2,1)S(1)}, bf16[512,1024]{1,0:T(8,128)(2,1)S(1)}, u32[]{:S(2)}, u32[]{:S(2)}) collective-permute-start(bf16[512,1024]{1,0:T(8,128)(2,1)S(1)} %constant_dynamic-update-slice_fusion.refs_4_), channel_id=1, source_target_pairs={{0,4},{2,6},{4,0},{6,2},{8,12},{10,14},{12,8},{14,10},{16,20},{18,... | collective-permute-start | bytes 3145736 | tf_op jit(solution)/shard_map/ppermute | solution.py:369
  47.5 27.5 %collective-permute-start.17 = (bf16[512,1024]{1,0:T(8,128)(2,1)S(1)}, bf16[512,1024]{1,0:T(8,128)(2,1)S(1)}, u32[]{:S(2)}, u32[]{:S(2)}) collective-permute-start(bf16[512,1024]{1,0:T(8,128)(2,1)S(1)} %constant_dynamic-update-slice_fusion.refs_4_), channel_id=1, source_target_pairs={{0,2},{2,0},{4,6},{6,4},{8,10},{10,8},{12,14},{14,12},{16,18},{18,... | collective-permute-start | bytes 3145736 | tf_op jit(solution)/shard_map/ppermute | solution.py:369
  47.8 6.5 %copy-start = (bf16[256,1024]{1,0:T(8,128)(2,1)S(1)}, bf16[256,1024]{1,0:T(8,128)(2,1)}, u32[]{:S(2)}) copy-start(bf16[256,1024]{1,0:T(8,128)(2,1)} %get-tuple-element.38.refs_0_) | copy-start | bytes 1572868
  47.8 11.9 %copy-start.12 = (bf16[128,1024]{1,0:T(8,128)(2,1)S(1)}, bf16[128,1024]{1,0:T(8,128)(2,1)}, u32[]{:S(2)}) copy-start(bf16[128,1024]{1,0:T(8,128)(2,1)} %get-tuple-element.43) | copy-start | bytes 786436
  47.8 14.3 %copy-start.3 = (bf16[512,2048]{1,0:T(8,128)(2,1)S(1)}, bf16[512,2048]{1,0:T(8,128)(2,1)}, u32[]{:S(2)}) copy-start(bf16[512,2048]{1,0:T(8,128)(2,1)} %refs_4_.3) | copy-start | bytes 6291460
  47.9 14.2 %copy-start.4 = (bf16[256,2048]{1,0:T(8,128)(2,1)S(1)}, bf16[256,2048]{1,0:T(8,128)(2,1)}, u32[]{:S(2)}) copy-start(bf16[256,2048]{1,0:T(8,128)(2,1)} %refs_5_.1) | copy-start | bytes 3145732
  54.3 19.5 %copy-start.11 = (bf16[128,1024]{1,0:T(8,128)(2,1)S(1)}, bf16[128,1024]{1,0:T(8,128)(2,1)}, u32[]{:S(2)}) copy-start(bf16[128,1024]{1,0:T(8,128)(2,1)} %get-tuple-element.44) | copy-start | bytes 786436
  54.3 3.5 %collective-permute-start.7 = (bf16[128,192]{1,0:T(8,128)(2,1)S(1)}, bf16[128,192]{1,0:T(8,128)(2,1)S(1)}, u32[]{:S(2)}, u32[]{:S(2)}) collective-permute-start(bf16[128,192]{1,0:T(8,128)(2,1)S(1)} %get-tuple-element.32), channel_id=1, source_target_pairs={{0,8},{2,10},{4,12},{6,14},{8,0},{10,2},{12,4},{14,6},{16,24},{18,... | collective-permute-start | bytes 147464 | tf_op jit(solution)/shard_map/ppermute | solution.py:362
  54.4 26.3 %collective-permute-start.12 = (bf16[256,1024]{1,0:T(8,128)(2,1)S(1)}, bf16[256,1024]{1,0:T(8,128)(2,1)S(1)}, u32[]{:S(2)}, u32[]{:S(2)}) collective-permute-start(bf16[256,1024]{1,0:T(8,128)(2,1)S(1)} %copy-done), channel_id=1, source_target_pairs={{0,4},{2,6},{4,0},{6,2},{8,12},{10,14},{12,8},{14,10},{16,20},{18,... | collective-permute-start | bytes 1572872 | tf_op jit(solution)/shard_map/ppermute | solution.py:369
  55.7 4.1 %collective-permute-start.8 = (bf16[128,192]{1,0:T(8,128)(2,1)S(1)}, bf16[128,192]{1,0:T(8,128)(2,1)S(1)}, u32[]{:S(2)}, u32[]{:S(2)}) collective-permute-start(bf16[128,192]{1,0:T(8,128)(2,1)S(1)} %get-tuple-element.33), channel_id=1, source_target_pairs={{0,16},{2,18},{4,20},{6,22},{8,24},{10,26},{12,28},{14,30},{16,0},... | collective-permute-start | bytes 147464 | tf_op jit(solution)/shard_map/ppermute | solution.py:362
  57.8 4.3 %collective-permute-start.9 = (bf16[128,192]{1,0:T(8,128)(2,1)S(1)}, bf16[128,192]{1,0:T(8,128)(2,1)S(1)}, u32[]{:S(2)}, u32[]{:S(2)}) collective-permute-start(bf16[128,192]{1,0:T(8,128)(2,1)S(1)} %get-tuple-element.34), channel_id=1, source_target_pairs={{0,24},{2,26},{4,28},{6,30},{8,16},{10,18},{12,20},{14,22},{16,8},... | collective-permute-start | bytes 147464 | tf_op jit(solution)/shard_map/ppermute | solution.py:362
  59.7 12.8 %collective-permute-start.25 = (bf16[128,1024]{1,0:T(8,128)(2,1)S(1)}, bf16[128,1024]{1,0:T(8,128)(2,1)S(1)}, u32[]{:S(2)}, u32[]{:S(2)}) collective-permute-start(bf16[128,1024]{1,0:T(8,128)(2,1)S(1)} %copy-done.12), channel_id=1, source_target_pairs={{0,16},{2,18},{4,20},{6,22},{8,24},{10,26},{12,28},{14,30},{16,0},... | collective-permute-start | bytes 786440 | tf_op jit(solution)/shard_map/ppermute | solution.py:362
  62.1 18.9 %copy-start.5 = (bf16[128,2048]{1,0:T(8,128)(2,1)S(1)}, bf16[128,2048]{1,0:T(8,128)(2,1)}, u32[]{:S(2)}) copy-start(bf16[128,2048]{1,0:T(8,128)(2,1)} %residual.1) | copy-start | bytes 1572868
  62.1 19.0 %copy-start.6 = (f32[2048]{0:T(1024)S(1)}, f32[2048]{0:T(1024)}, u32[]{:S(2)}) copy-start(f32[2048]{0:T(1024)} %param.29) | copy-start | bytes 24580
  63.9 16.9 %collective-permute-start.10 = (bf16[64,2048]{1,0:T(8,128)(2,1)S(1)}, bf16[64,2048]{1,0:T(8,128)(2,1)S(1)}, u32[]{:S(2)}, u32[]{:S(2)}) collective-permute-start(bf16[64,2048]{1,0:T(8,128)(2,1)S(1)} %get-tuple-element.36), channel_id=1, source_target_pairs={{0,1},{1,0},{2,3},{3,2},{4,5},{5,4},{6,7},{7,6},{8,9},{9,8},{10,11... | collective-permute-start | bytes 786440 | tf_op jit(solution)/shard_map/ppermute | solution.py:372
  72.6 13.7 %collective-permute-start.11 = (bf16[256,1024]{1,0:T(8,128)(2,1)S(1)}, bf16[256,1024]{1,0:T(8,128)(2,1)S(1)}, u32[]{:S(2)}, u32[]{:S(2)}) collective-permute-start(bf16[256,1024]{1,0:T(8,128)(2,1)S(1)} %copy-done), channel_id=1, source_target_pairs={{0,2},{2,0},{4,6},{6,4},{8,10},{10,8},{12,14},{14,12},{16,18},{18,... | collective-permute-start | bytes 1572872 | tf_op jit(solution)/shard_map/ppermute | solution.py:369
  73.8 9.3 %collective-permute-start.29 = (bf16[128,1024]{1,0:T(8,128)(2,1)S(1)}, bf16[128,1024]{1,0:T(8,128)(2,1)S(1)}, u32[]{:S(2)}, u32[]{:S(2)}) collective-permute-start(bf16[128,1024]{1,0:T(8,128)(2,1)S(1)} %copy-done.11), channel_id=1, source_target_pairs={{0,24},{2,26},{4,28},{6,30},{8,16},{10,18},{12,20},{14,22},{16,8},... | collective-permute-start | bytes 786440 | tf_op jit(solution)/shard_map/ppermute | solution.py:362
  75.0 11.2 %collective-permute-start.27 = (bf16[128,1024]{1,0:T(8,128)(2,1)S(1)}, bf16[128,1024]{1,0:T(8,128)(2,1)S(1)}, u32[]{:S(2)}, u32[]{:S(2)}) collective-permute-start(bf16[128,1024]{1,0:T(8,128)(2,1)S(1)} %collective-permute-done.25.refs_8_), channel_id=1, source_target_pairs={{0,4},{2,6},{4,0},{6,2},{8,12},{10,14},{12,8},{14,10},{16,20},{18,... | collective-permute-start | bytes 786440 | tf_op jit(solution)/shard_map/ppermute | solution.py:369
  80.6 18.5 %collective-permute-start.19 = (bf16[256,1024]{1,0:T(8,128)(2,1)S(1)}, bf16[256,1024]{1,0:T(8,128)(2,1)S(1)}, u32[]{:S(2)}, u32[]{:S(2)}) collective-permute-start(bf16[256,1024]{1,0:T(8,128)(2,1)S(1)} %slice.65), channel_id=1, source_target_pairs={{0,2},{2,0},{4,6},{6,4},{8,10},{10,8},{12,14},{14,12},{16,18},{18,... | collective-permute-start | bytes 1572872 | tf_op jit(solution)/shard_map/ppermute | solution.py:369
  80.8 32.0 %collective-permute-start.20 = (bf16[256,1024]{1,0:T(8,128)(2,1)S(1)}, bf16[256,1024]{1,0:T(8,128)(2,1)S(1)}, u32[]{:S(2)}, u32[]{:S(2)}) collective-permute-start(bf16[256,1024]{1,0:T(8,128)(2,1)S(1)} %slice.66), channel_id=1, source_target_pairs={{0,4},{2,6},{4,0},{6,2},{8,12},{10,14},{12,8},{14,10},{16,20},{18,... | collective-permute-start | bytes 1572872 | tf_op jit(solution)/shard_map/ppermute | solution.py:369
  83.0 15.9 %collective-permute-start.13 = (bf16[128,1024]{1,0:T(8,128)(2,1)S(1)}, bf16[128,1024]{1,0:T(8,128)(2,1)S(1)}, u32[]{:S(2)}, u32[]{:S(2)}) collective-permute-start(bf16[128,1024]{1,0:T(8,128)(2,1)S(1)} %slice.64), channel_id=1, source_target_pairs={{0,2},{2,0},{4,6},{6,4},{8,10},{10,8},{12,14},{14,12},{16,18},{18,... | collective-permute-start | bytes 786440 | tf_op jit(solution)/shard_map/ppermute | solution.py:369
  86.3 12.9 %collective-permute-start.21 = (bf16[64,2048]{1,0:T(8,128)(2,1)S(1)}, bf16[64,2048]{1,0:T(8,128)(2,1)S(1)}, u32[]{:S(2)}, u32[]{:S(2)}) collective-permute-start(bf16[64,2048]{1,0:T(8,128)(2,1)S(1)} %get-tuple-element.42.refs_1_), channel_id=1, source_target_pairs={{0,16},{2,18},{4,20},{6,22},{8,24},{10,26},{12,28},{14,30},{16,0},... | collective-permute-start | bytes 786440 | tf_op jit(solution)/shard_map/ppermute | solution.py:362
  86.3 27.4 %collective-permute-start.26 = (bf16[128,1024]{1,0:T(8,128)(2,1)S(1)}, bf16[128,1024]{1,0:T(8,128)(2,1)S(1)}, u32[]{:S(2)}, u32[]{:S(2)}) collective-permute-start(bf16[128,1024]{1,0:T(8,128)(2,1)S(1)} %collective-permute-done.25.refs_8_), channel_id=1, source_target_pairs={{0,2},{2,0},{4,6},{6,4},{8,10},{10,8},{12,14},{14,12},{16,18},{18,... | collective-permute-start | bytes 786440 | tf_op jit(solution)/shard_map/ppermute | solution.py:369
  98.9 16.1 %collective-permute-start.31 = (bf16[128,1024]{1,0:T(8,128)(2,1)S(1)}, bf16[128,1024]{1,0:T(8,128)(2,1)S(1)}, u32[]{:S(2)}, u32[]{:S(2)}) collective-permute-start(bf16[128,1024]{1,0:T(8,128)(2,1)S(1)} %collective-permute-done.29.refs_12_), channel_id=1, source_target_pairs={{0,4},{2,6},{4,0},{6,2},{8,12},{10,14},{12,8},{14,10},{16,20},{18,... | collective-permute-start | bytes 786440 | tf_op jit(solution)/shard_map/ppermute | solution.py:369
  99.2 17.2 %collective-permute-start.30 = (bf16[128,1024]{1,0:T(8,128)(2,1)S(1)}, bf16[128,1024]{1,0:T(8,128)(2,1)S(1)}, u32[]{:S(2)}, u32[]{:S(2)}) collective-permute-start(bf16[128,1024]{1,0:T(8,128)(2,1)S(1)} %collective-permute-done.29.refs_12_), channel_id=1, source_target_pairs={{0,2},{2,0},{4,6},{6,4},{8,10},{10,8},{12,14},{14,12},{16,18},{18,... | collective-permute-start | bytes 786440 | tf_op jit(solution)/shard_map/ppermute | solution.py:369
  99.2 17.3 %collective-permute-start.23 = (bf16[64,2048]{1,0:T(8,128)(2,1)S(1)}, bf16[64,2048]{1,0:T(8,128)(2,1)S(1)}, u32[]{:S(2)}, u32[]{:S(2)}) collective-permute-start(bf16[64,2048]{1,0:T(8,128)(2,1)S(1)} %get-tuple-element.42.refs_1_), channel_id=1, source_target_pairs={{0,1},{1,0},{2,3},{3,2},{4,5},{5,4},{6,7},{7,6},{8,9},{9,8},{10,11... | collective-permute-start | bytes 786440 | tf_op jit(solution)/shard_map/ppermute | solution.py:372
  112.8 3.7 %collective-permute-start.22 = (bf16[64,2048]{1,0:T(8,128)(2,1)S(1)}, bf16[64,2048]{1,0:T(8,128)(2,1)S(1)}, u32[]{:S(2)}, u32[]{:S(2)}) collective-permute-start(bf16[64,2048]{1,0:T(8,128)(2,1)S(1)} %collective-permute-done.21.refs_0_), channel_id=1, source_target_pairs={{0,1},{1,0},{2,3},{3,2},{4,5},{5,4},{6,7},{7,6},{8,9},{9,8},{10,11... | collective-permute-start | bytes 786440 | tf_op jit(solution)/shard_map/ppermute | solution.py:372
  113.7 15.5 %collective-permute-start.24 = (bf16[128,1024]{1,0:T(8,128)(2,1)S(1)}, bf16[128,1024]{1,0:T(8,128)(2,1)S(1)}, u32[]{:S(2)}, u32[]{:S(2)}) collective-permute-start(bf16[128,1024]{1,0:T(8,128)(2,1)S(1)} %slice.67), channel_id=1, source_target_pairs={{0,4},{2,6},{4,0},{6,2},{8,12},{10,14},{12,8},{14,10},{16,20},{18,... | collective-permute-start | bytes 786440 | tf_op jit(solution)/shard_map/ppermute | solution.py:369
  115.0 14.2 %collective-permute-start.28 = (bf16[128,1024]{1,0:T(8,128)(2,1)S(1)}, bf16[128,1024]{1,0:T(8,128)(2,1)S(1)}, u32[]{:S(2)}, u32[]{:S(2)}) collective-permute-start(bf16[128,1024]{1,0:T(8,128)(2,1)S(1)} %collective-permute-done.27.refs_10_), channel_id=1, source_target_pairs={{0,2},{2,0},{4,6},{6,4},{8,10},{10,8},{12,14},{14,12},{16,18},{18,... | collective-permute-start | bytes 786440 | tf_op jit(solution)/shard_map/ppermute | solution.py:369
  116.3 12.9 %collective-permute-start.32 = (bf16[128,1024]{1,0:T(8,128)(2,1)S(1)}, bf16[128,1024]{1,0:T(8,128)(2,1)S(1)}, u32[]{:S(2)}, u32[]{:S(2)}) collective-permute-start(bf16[128,1024]{1,0:T(8,128)(2,1)S(1)} %collective-permute-done.30.refs_13_), channel_id=1, source_target_pairs={{0,4},{2,6},{4,0},{6,2},{8,12},{10,14},{12,8},{14,10},{16,20},{18,... | collective-permute-start | bytes 786440 | tf_op jit(solution)/shard_map/ppermute | solution.py:369
  116.5 7.3 %collective-permute-start.35 = (bf16[64,2048]{1,0:T(8,128)(2,1)S(1)}, bf16[64,2048]{1,0:T(8,128)(2,1)S(1)}, u32[]{:S(2)}, u32[]{:S(2)}) collective-permute-start(bf16[64,2048]{1,0:T(8,128)(2,1)S(1)} %get-tuple-element.42.refs_1_), channel_id=1, source_target_pairs={{0,24},{2,26},{4,28},{6,30},{8,16},{10,18},{12,20},{14,22},{16,8},... | collective-permute-start | bytes 786440 | tf_op jit(solution)/shard_map/ppermute | solution.py:362
  116.5 12.8 %collective-permute-start.34 = (bf16[64,2048]{1,0:T(8,128)(2,1)S(1)}, bf16[64,2048]{1,0:T(8,128)(2,1)S(1)}, u32[]{:S(2)}, u32[]{:S(2)}) collective-permute-start(bf16[64,2048]{1,0:T(8,128)(2,1)S(1)} %get-tuple-element.42.refs_1_), channel_id=1, source_target_pairs={{0,8},{2,10},{4,12},{6,14},{8,0},{10,2},{12,4},{14,6},{16,24},{18,... | collective-permute-start | bytes 786440 | tf_op jit(solution)/shard_map/ppermute | solution.py:362
  123.8 8.4 %collective-permute-start.37 = (bf16[64,2048]{1,0:T(8,128)(2,1)S(1)}, bf16[64,2048]{1,0:T(8,128)(2,1)S(1)}, u32[]{:S(2)}, u32[]{:S(2)}) collective-permute-start(bf16[64,2048]{1,0:T(8,128)(2,1)S(1)} %collective-permute-done.35.refs_1_), channel_id=1, source_target_pairs={{0,1},{1,0},{2,3},{3,2},{4,5},{5,4},{6,7},{7,6},{8,9},{9,8},{10,11... | collective-permute-start | bytes 786440 | tf_op jit(solution)/shard_map/ppermute | solution.py:372
  129.2 2.9 %collective-permute-start.36 = (bf16[64,2048]{1,0:T(8,128)(2,1)S(1)}, bf16[64,2048]{1,0:T(8,128)(2,1)S(1)}, u32[]{:S(2)}, u32[]{:S(2)}) collective-permute-start(bf16[64,2048]{1,0:T(8,128)(2,1)S(1)} %collective-permute-done.34.refs_0_), channel_id=1, source_target_pairs={{0,1},{1,0},{2,3},{3,2},{4,5},{5,4},{6,7},{7,6},{8,9},{9,8},{10,11... | collective-permute-start | bytes 786440 | tf_op jit(solution)/shard_map/ppermute | solution.py:372
  131.6 3.2 %collective-permute-start.33 = (bf16[2,64,2048]{2,1,0:T(8,128)(2,1)S(1)}, bf16[2,64,2048]{2,1,0:T(8,128)(2,1)S(1)}, u32[]{:S(2)}, u32[]{:S(2)}) collective-permute-start(bf16[2,64,2048]{2,1,0:T(8,128)(2,1)S(1)} %get-tuple-element.46), channel_id=1, source_target_pairs={{0,1},{1,0},{2,3},{3,2},{4,5},{5,4},{6,7},{7,6},{8,9},{9,8},{10,11... | collective-permute-start | bytes 1572872 | tf_op jit(solution)/shard_map/ppermute | solution.py:372
  134.7 2.0 %collective-permute-start.38 = (bf16[2,64,2048]{2,1,0:T(8,128)(2,1)S(1)}, bf16[2,64,2048]{2,1,0:T(8,128)(2,1)S(1)}, u32[]{:S(2)}, u32[]{:S(2)}) collective-permute-start(bf16[2,64,2048]{2,1,0:T(8,128)(2,1)S(1)} %get-tuple-element.48), channel_id=1, source_target_pairs={{0,1},{1,0},{2,3},{3,2},{4,5},{5,4},{6,7},{7,6},{8,9},{9,8},{10,11... | collective-permute-start | bytes 1572872 | tf_op jit(solution)/shard_map/ppermute | solution.py:372
  135.0 12.4 %collective-permute-start.40 = (bf16[64,2048]{1,0:T(8,128)(2,1)S(1)}, bf16[64,2048]{1,0:T(8,128)(2,1)S(1)}, u32[]{:S(2)}, u32[]{:S(2)}) collective-permute-start(bf16[64,2048]{1,0:T(8,128)(2,1)S(1)} %fusion.5), channel_id=1, source_target_pairs={{0,16},{2,18},{4,20},{6,22},{8,24},{10,26},{12,28},{14,30},{16,0},... | collective-permute-start | bytes 786440 | tf_op jit(solution)/shard_map/ppermute | solution.py:362
  136.9 12.1 %collective-permute-start.39 = (bf16[64,2048]{1,0:T(8,128)(2,1)S(1)}, bf16[64,2048]{1,0:T(8,128)(2,1)S(1)}, u32[]{:S(2)}, u32[]{:S(2)}) collective-permute-start(bf16[64,2048]{1,0:T(8,128)(2,1)S(1)} %get-tuple-element.49), channel_id=1, source_target_pairs={{0,8},{2,10},{4,12},{6,14},{8,0},{10,2},{12,4},{14,6},{16,24},{18,... | collective-permute-start | bytes 786440 | tf_op jit(solution)/shard_map/ppermute | solution.py:362
  137.6 23.1 %collective-permute-start.41 = (bf16[64,2048]{1,0:T(8,128)(2,1)S(1)}, bf16[64,2048]{1,0:T(8,128)(2,1)S(1)}, u32[]{:S(2)}, u32[]{:S(2)}) collective-permute-start(bf16[64,2048]{1,0:T(8,128)(2,1)S(1)} %get-tuple-element.50), channel_id=1, source_target_pairs={{0,24},{2,26},{4,28},{6,30},{8,16},{10,18},{12,20},{14,22},{16,8},... | collective-permute-start | bytes 786440 | tf_op jit(solution)/shard_map/ppermute | solution.py:362
  160.9 1.9 %collective-permute-start.42 = (bf16[64,2048]{1,0:T(8,128)(2,1)S(1)}, bf16[64,2048]{1,0:T(8,128)(2,1)S(1)}, u32[]{:S(2)}, u32[]{:S(2)}) collective-permute-start(bf16[64,2048]{1,0:T(8,128)(2,1)S(1)} %fusion.4), channel_id=1, source_target_pairs={{0,1},{1,0},{2,3},{3,2},{4,5},{5,4},{6,7},{7,6},{8,9},{9,8},{10,11... | collective-permute-start | bytes 786440 | tf_op jit(solution)/shard_map/ppermute | solution.py:372

commit v4 on v3

--- a/solution.py
+++ b/solution.py
@@ -123,6 +123,7 @@
 
 VMEM = pltpu.VMEM
 SMEM = pltpu.SMEM
+DIRECT = 0.375
 
 
 def vmem_specs(count):
@@ -509,7 +510,8 @@
                 cost_estimate=pl.CostEstimate(flops=10**9, bytes_accessed=10**6, transcendentals=0),
         name="norm",
     )(index, residual, own, swap(other), mlp_gain[None])
-    own_rows = [along(normed, k) for k in range(slots)]
+    own_rows = [along(normed, k) for k in range(3)]
+    own_rows.append(along(own_rows[2], 1))
     other_rows = [swap(piece) for piece in own_rows]
     group = slots // 2
     part_shape = jax.ShapeDtypeStruct((group, half, width), jnp.bfloat16)
@@ -537,17 +539,22 @@
             cost_estimate=pl.CostEstimate(flops=3 * 10**9, bytes_accessed=10**6, transcendentals=0),
         )(active, down)
 
-    terms = {}
-    for chosen in (list(range(1, slots, 2)), list(range(slots - 2, -1, -2))):
+    def finish(chosen):
         own, other = lower(lift(chosen))
         other = swap(other)
         summed = own.astype(jnp.float32) + other.astype(jnp.float32)
-        for at, k in enumerate(chosen):
-            piece = summed[at]
-            terms[k] = piece if k == 0 else along(piece.astype(jnp.bfloat16), k)
-    total = terms[0]
-    for k in range(1, slots):
-        total = total + terms[k].astype(jnp.float32)
+        return summed[0], summed[1]
+
+    farthest, far = finish((3, 2))
+    direct = 128 * round(width * DIRECT / 128)
+    sent, far_sent = farthest.astype(jnp.bfloat16), far.astype(jnp.bfloat16)
+    passed = along(sent[:, direct:], 1).astype(jnp.float32)
+    straight = along(sent[:, :direct], 3).astype(jnp.float32)
+    straight = straight + along(far_sent[:, :direct], 2).astype(jnp.float32)
+    relayed = along((far[:, direct:] + passed).astype(jnp.bfloat16), 2).astype(jnp.float32)
+    near, total = finish((1, 0))
+    total = total + along(near.astype(jnp.bfloat16), 1).astype(jnp.float32)
+    total = total + jnp.concatenate([straight, relayed], axis=1)
     mine = (mixed.astype(jnp.float32) + total).astype(jnp.bfloat16)
     theirs = swap(mine)
     return jnp.where(
@@ -562,6 +569,7 @@
         cores == 2
         and heads == other_heads
         and plane == 4
+        and heads == 4
         and plane * heads == count
         and arguments[3].shape[2] == 128
         and arguments[6].shape[2] == 64

time: 164 us -> 166 us (1.012)
  the two profiles are of different devices: /device:TPU:9 before, /device:TPU:0 now
where the time goes in v4:
time: 166 us
  waiting for transfers between devices  81.6 us (49%)
  starting transfers between devices  57.5 us (35%)
  Pallas kernels  23.3 us (14%)
  other arithmetic  2.05 us (1%)
    ppermute x19, waiting for transfers between devices, along(): lax.ppermute(value, 'sp', [(i, (i // plane ^ k) * plane + i % plane) for...  64.1 us
    ppermute x19, starting transfers between devices, along(): lax.ppermute(value, 'sp', [(i, (i // plane ^ k) * plane + i % plane) for...  31.5 us
    ppermute x18, starting transfers between devices, across(): return lax.ppermute(value, 'sp', [(i, i ^ k) for i in range(count)])  24.6 us
    ppermute x18, waiting for transfers between devices, across(): return lax.ppermute(value, 'sp', [(i, i ^ k) for i in range(count)])  14.8 us
    pallas_call x1, Pallas kernels, fast_body(): pl.pallas_call(functools.partial(attend_kernel, slots, plane, tokens), ou...  6.39 us
    pallas_call x1, Pallas kernels, fast_body(): pl.pallas_call(functools.partial(pack_kernel, slots), out_shape=(jax.Shap...  3.84 us
    pallas_call x1, Pallas kernels, fast_body(): pl.pallas_call(functools.partial(cut_kernel, slots, hidden), out_shape=(j...  3.56 us
  transfers between devices with their start and end apart: 45, of which 19 were waited for; matrix products, arithmetic and copies ran while one was open for 1% of the time, Pallas kernels for 12%

profile of v4, /device:TPU:0, one launch (start us, length us, event | category | flops | bytes accessed | tf_op | source)
XLA Modules:
  0.0 166.3 jit_solution(3088988198252099616)
XLA Ops:
  0.0 0.6 pad_add_fusion.index
  0.7 3.8 %pack.1 = (bf16[128,576]{1,0:T(8,128)(2,1)}, bf16[128,576]{1,0:T(8,128)(2,1)}, bf16[128,576]{1,0:T(8,128)(2,1)}, bf16[128,576]{1,0:T(8,128)(2,1)}) custom-call(s32[3]{0:T(128)} %pad_add_fusion.index, bf16[128,4,128]{2,1,0:T(4,128)(2,1)} %refs_0_.2, bf16[4,64,128]{2,1,0:T(8,128)(2,1)} %bitcast.36, bf16[4,64,128]{2,1,0:T(8,128)(2,1)} %bitcast.37, ...), custom_call_target="tpu_custom_call" | custom-call | flops 100000000 | bytes 1000000 | tf_op jit(solution)/shard_map/pack/pallas_call | solution.py:386
  4.5 3.2 %collective-permute-start = (bf16[128,576]{1,0:T(8,128)(2,1)}, bf16[128,576]{1,0:T(8,128)(2,1)S(1)}, u32[]{:S(2)}, u32[]{:S(2)}) collective-permute-start(bf16[128,576]{1,0:T(8,128)(2,1)} %get-tuple-element.28), channel_id=1, source_target_pairs={{0,8},{2,10},{4,12},{6,14},{8,0},{10,2},{12,4},{14,6},{16,24},{18,... | collective-permute-start | bytes 442376 | tf_op jit(solution)/shard_map/ppermute | solution.py:363
  7.7 2.6 %collective-permute-start.1 = (bf16[128,576]{1,0:T(8,128)(2,1)}, bf16[128,576]{1,0:T(8,128)(2,1)S(1)}, u32[]{:S(2)}, u32[]{:S(2)}) collective-permute-start(bf16[128,576]{1,0:T(8,128)(2,1)} %get-tuple-element.29), channel_id=1, source_target_pairs={{0,16},{2,18},{4,20},{6,22},{8,24},{10,26},{12,28},{14,30},{16,0},... | collective-permute-start | bytes 442376 | tf_op jit(solution)/shard_map/ppermute | solution.py:363
  10.3 3.6 %cut.1 = (bf16[256,1024]{1,0:T(8,128)(2,1)}, bf16[256,1024]{1,0:T(8,128)(2,1)}, bf16[128,1024]{1,0:T(8,128)(2,1)}, bf16[128,1024]{1,0:T(8,128)(2,1)}, bf16[128,1...) custom-call(s32[3]{0:T(128)} %pad_add_fusion.index, bf16[128,4096]{1,0:T(8,128)(2,1)} %refs_0_.3, bf16[128,4096]{1,0:T(8,128)(2,1)} %refs_1_.1), custom_call_target="tpu_custom_call" | custom-call | flops 100000000 | bytes 1000000 | tf_op jit(solution)/shard_map/cut/pallas_call | solution.py:397
  13.8 1.0 collective-permute-start.14
  14.8 0.9 slice_bitcast_fusion.5
  15.7 7.2 %collective-permute-done.1.refs_2_ = bf16[128,576]{1,0:T(8,128)(2,1)S(1)} collective-permute-done((bf16[128,576]{1,0:T(8,128)(2,1)}, bf16[128,576]{1,0:T(8,128)(2,1)S(1)}, u32[]{:S(2)}, u32[]{:S(2)}) %collective-permute-start.1) | collective-permute-done | bytes 147488 | tf_op jit(solution)/shard_map/ppermute | solution.py:363
  23.0 1.6 collective-permute-start.4
  24.6 1.5 collective-permute-start.3
  26.1 3.7 %collective-permute-start.15 = (bf16[128,1024]{1,0:T(8,128)(2,1)}, bf16[128,1024]{1,0:T(8,128)(2,1)S(1)}, u32[]{:S(2)}, u32[]{:S(2)}) collective-permute-start(bf16[128,1024]{1,0:T(8,128)(2,1)} %get-tuple-element.40), channel_id=1, source_target_pairs={{0,16},{2,18},{4,20},{6,22},{8,24},{10,26},{12,28},{14,30},{16,0},... | collective-permute-start | bytes 786440 | tf_op jit(solution)/shard_map/ppermute | solution.py:363
  29.8 1.3 collective-permute-start.16
  31.1 3.7 %collective-permute-done.14 = bf16[256,1024]{1,0:T(8,128)(2,1)S(1)} collective-permute-done((bf16[256,1024]{1,0:T(8,128)(2,1)}, bf16[256,1024]{1,0:T(8,128)(2,1)S(1)}, u32[]{:S(2)}, u32[]{:S(2)}) %collective-permute-start.14) | collective-permute-done | bytes 524320 | tf_op jit(solution)/shard_map/ppermute | solution.py:363
  34.9 2.0 %collective-permute-start.5 = (bf16[2,128,384]{2,1,0:T(8,128)(2,1)S(1)}, bf16[2,128,384]{2,1,0:T(8,128)(2,1)S(1)}, u32[]{:S(2)}, u32[]{:S(2)}) collective-permute-start(bf16[2,128,384]{2,1,0:T(8,128)(2,1)S(1)} %slice.77), channel_id=1, source_target_pairs={{0,2},{2,0},{4,6},{6,4},{8,10},{10,8},{12,14},{14,12},{16,18},{18,... | collective-permute-start | bytes 589832 | tf_op jit(solution)/shard_map/ppermute | solution.py:370
  37.0 2.1 %collective-permute-start.6 = (bf16[2,128,384]{2,1,0:T(8,128)(2,1)S(1)}, bf16[2,128,384]{2,1,0:T(8,128)(2,1)S(1)}, u32[]{:S(2)}, u32[]{:S(2)}) collective-permute-start(bf16[2,128,384]{2,1,0:T(8,128)(2,1)S(1)} %slice.78), channel_id=1, source_target_pairs={{0,4},{2,6},{4,0},{6,2},{8,12},{10,14},{12,8},{14,10},{16,20},{18,... | collective-permute-start | bytes 589832 | tf_op jit(solution)/shard_map/ppermute | solution.py:370
  39.1 9.3 %collective-permute-done.15 = bf16[128,1024]{1,0:T(8,128)(2,1)S(1)} collective-permute-done((bf16[128,1024]{1,0:T(8,128)(2,1)}, bf16[128,1024]{1,0:T(8,128)(2,1)S(1)}, u32[]{:S(2)}, u32[]{:S(2)}) %collective-permute-start.15) | collective-permute-done | bytes 262176 | tf_op jit(solution)/shard_map/ppermute | solution.py:363
  48.4 0.6 collective-permute-start.18
  49.7 6.4 %attend.1 = (bf16[128,192]{1,0:T(8,128)(2,1)S(1)}, bf16[128,192]{1,0:T(8,128)(2,1)S(1)}, bf16[128,192]{1,0:T(8,128)(2,1)S(1)}, bf16[128,192]{1,0:T(8,128)(2,1)S(1)}) custom-call(s32[3]{0:T(128)S(1)} %copy-done.2, f32[4]{0:T(128)S(1)} %copy-done.7, f32[4]{0:T(128)S(1)} %copy-done.8, f32[1,128]{1,0:T(1,128)S(1)} %bitcast.34, f32[1,64]{1,0:T(1,128)S(1)} %bitcast.35, ...), custom_call_target="tpu_custom_call" | custom-call | flops 8000000000 | bytes 2000000 | tf_op jit(solution)/shard_map/attend/pallas_call | solution.py:469
  56.1 3.9 %collective-permute-start.7 = (bf16[128,192]{1,0:T(8,128)(2,1)S(1)}, bf16[128,192]{1,0:T(8,128)(2,1)S(1)}, u32[]{:S(2)}, u32[]{:S(2)}) collective-permute-start(bf16[128,192]{1,0:T(8,128)(2,1)S(1)} %get-tuple-element.32), channel_id=1, source_target_pairs={{0,8},{2,10},{4,12},{6,14},{8,0},{10,2},{12,4},{14,6},{16,24},{18,... | collective-permute-start | bytes 147464 | tf_op jit(solution)/shard_map/ppermute | solution.py:363
  60.0 2.4 %collective-permute-start.9 = (bf16[128,192]{1,0:T(8,128)(2,1)S(1)}, bf16[128,192]{1,0:T(8,128)(2,1)S(1)}, u32[]{:S(2)}, u32[]{:S(2)}) collective-permute-start(bf16[128,192]{1,0:T(8,128)(2,1)S(1)} %get-tuple-element.34), channel_id=1, source_target_pairs={{0,24},{2,26},{4,28},{6,30},{8,16},{10,18},{12,20},{14,22},{16,8},... | collective-permute-start | bytes 147464 | tf_op jit(solution)/shard_map/ppermute | solution.py:363
  62.4 0.6 collective-permute-done.7.refs_1_
  63.1 1.5 collective-permute-start.12
  64.6 0.8 collective-permute-done.8.refs_2_
  65.4 0.8 collective-permute-done.9.refs_3_
  66.2 1.8 %project.1 = (bf16[64,2048]{1,0:T(8,128)(2,1)S(1)}, bf16[64,2048]{1,0:T(8,128)(2,1)S(1)}) custom-call(s32[3]{0:T(128)S(1)} %copy-done.2, bf16[128,192]{1,0:T(8,128)(2,1)S(1)} %get-tuple-element.31.refs_0_, bf16[128,192]{1,0:T(8,128)(2,1)S(1)} %collective-permute-done.7.refs_1_, bf16[128,192]{1,0:T(8,128)(2,1)S(1)} %collective-permute-done.8.refs_2_, ...), custom_call_target="tpu_custom_call" | custom-call | flops 2000000000 | bytes 4000000 | tf_op jit(solution)/shard_map/project/pallas_call | solution.py:494
  68.1 1.8 %collective-permute-start.25 = (bf16[128,1024]{1,0:T(8,128)(2,1)S(1)}, bf16[128,1024]{1,0:T(8,128)(2,1)S(1)}, u32[]{:S(2)}, u32[]{:S(2)}) collective-permute-start(bf16[128,1024]{1,0:T(8,128)(2,1)S(1)} %copy-done.12), channel_id=1, source_target_pairs={{0,16},{2,18},{4,20},{6,22},{8,24},{10,26},{12,28},{14,30},{16,0},... | collective-permute-start | bytes 786440 | tf_op jit(solution)/shard_map/ppermute | solution.py:363
  69.9 1.5 collective-permute-start.11
  71.4 0.8 norm.1
  72.2 1.4 collective-permute-done.18.refs_6_
  73.6 1.2 collective-permute-start.29
  74.8 5.1 %collective-permute-start.35 = (bf16[64,2048]{1,0:T(8,128)(2,1)S(1)}, bf16[64,2048]{1,0:T(8,128)(2,1)S(1)}, u32[]{:S(2)}, u32[]{:S(2)}) collective-permute-start(bf16[64,2048]{1,0:T(8,128)(2,1)S(1)} %get-tuple-element.42.refs_1_), channel_id=1, source_target_pairs={{0,16},{2,18},{4,20},{6,22},{8,24},{10,26},{12,28},{14,30},{16,0},... | collective-permute-start | bytes 786440 | tf_op jit(solution)/shard_map/ppermute | solution.py:363
  80.0 15.1 %collective-permute-done.25.refs_8_ = bf16[128,1024]{1,0:T(8,128)(2,1)S(1)} collective-permute-done((bf16[128,1024]{1,0:T(8,128)(2,1)S(1)}, bf16[128,1024]{1,0:T(8,128)(2,1)S(1)}, u32[]{:S(2)}, u32[]{:S(2)}) %collective-permute-start.25) | collective-permute-done | bytes 262176 | tf_op jit(solution)/shard_map/ppermute | solution.py:363
  95.1 1.5 collective-permute-start.19
  96.6 1.5 collective-permute-start.20
  98.1 0.6 collective-permute-start.13
  98.7 7.0 %collective-permute-done.35.refs_1_ = bf16[64,2048]{1,0:T(8,128)(2,1)S(1)} collective-permute-done((bf16[64,2048]{1,0:T(8,128)(2,1)S(1)}, bf16[64,2048]{1,0:T(8,128)(2,1)S(1)}, u32[]{:S(2)}, u32[]{:S(2)}) %collective-permute-start.35) | collective-permute-done | bytes 262176 | tf_op jit(solution)/shard_map/ppermute | solution.py:363
  105.8 1.5 collective-permute-start.27
  107.3 6.3 %collective-permute-done.13.refs_3_ = bf16[128,1024]{1,0:T(8,128)(2,1)S(1)} collective-permute-done((bf16[128,1024]{1,0:T(8,128)(2,1)S(1)}, bf16[128,1024]{1,0:T(8,128)(2,1)S(1)}, u32[]{:S(2)}, u32[]{:S(2)}) %collective-permute-start.13) | collective-permute-done | bytes 262176 | tf_op jit(solution)/shard_map/ppermute | solution.py:370
  113.5 1.5 collective-permute-start.26
  115.0 0.5 collective-permute-start.30
  116.1 0.8 shard_map.154.up
  116.9 1.6 collective-permute-start.31
  118.5 4.2 %collective-permute-done.26.refs_9_ = bf16[128,1024]{1,0:T(8,128)(2,1)S(1)} collective-permute-done((bf16[128,1024]{1,0:T(8,128)(2,1)S(1)}, bf16[128,1024]{1,0:T(8,128)(2,1)S(1)}, u32[]{:S(2)}, u32[]{:S(2)}) %collective-permute-start.26) | collective-permute-done | bytes 262176 | tf_op jit(solution)/shard_map/ppermute | solution.py:370
  122.7 1.5 collective-permute-start.24
  124.2 1.4 collective-permute-done.30.refs_13_
  125.6 1.5 collective-permute-start.28
  127.1 1.5 collective-permute-start.32
  129.0 1.3 shard_map.158.hidden
  130.3 4.7 %collective-permute-done.21.refs_0_ = bf16[64,2048]{1,0:T(8,128)(2,1)S(1)} collective-permute-done((bf16[64,2048]{1,0:T(8,128)(2,1)S(1)}, bf16[64,2048]{1,0:T(8,128)(2,1)S(1)}, u32[]{:S(2)}, u32[]{:S(2)}) %collective-permute-start.21) | collective-permute-done | bytes 262176 | tf_op jit(solution)/shard_map/ppermute | solution.py:363
  135.0 1.5 collective-permute-done.32.refs_15_
  136.5 1.0 shard_map.156.down
  137.5 1.3 shard_map.159
  138.9 1.3 shard_map.155.hidden
  140.2 1.3 shard_map.157
  141.5 0.5 collective-permute-start.33
  142.4 1.2 collective-permute-done.33
  143.8 0.9 collective-permute-start.34
  144.6 2.8 %collective-permute-start.40 = (bf16[64,768]{1,0:T(8,128)(2,1)S(1)}, bf16[64,768]{1,0:T(8,128)(2,1)S(1)}, u32[]{:S(2)}, u32[]{:S(2)}) collective-permute-start(bf16[64,768]{1,0:T(8,128)(2,1)S(1)} %slice.86), channel_id=1, source_target_pairs={{0,24},{2,26},{4,28},{6,30},{8,16},{10,18},{12,20},{14,22},{16,8},... | collective-permute-start | bytes 294920 | tf_op jit(solution)/shard_map/ppermute | solution.py:363
  147.4 2.0 %collective-permute-done.42 = bf16[64,1280]{1,0:T(8,128)(2,1)S(1)} collective-permute-done((bf16[64,1280]{1,0:T(8,128)(2,1)S(1)}, bf16[64,1280]{1,0:T(8,128)(2,1)S(1)}, u32[]{:S(2)}, u32[]{:S(2)}) %collective-permute-start.42) | collective-permute-done | bytes 163872 | tf_op jit(solution)/shard_map/ppermute | solution.py:363
  149.4 1.3 collective-permute-start.43
  150.7 7.2 %collective-permute-done.40 = bf16[64,768]{1,0:T(8,128)(2,1)S(1)} collective-permute-done((bf16[64,768]{1,0:T(8,128)(2,1)S(1)}, bf16[64,768]{1,0:T(8,128)(2,1)S(1)}, u32[]{:S(2)}, u32[]{:S(2)}) %collective-permute-start.40) | collective-permute-done | bytes 98336 | tf_op jit(solution)/shard_map/ppermute | solution.py:363
  157.9 5.7 %collective-permute-done.43 = bf16[64,1280]{1,0:T(8,128)(2,1)S(1)} collective-permute-done((bf16[64,1280]{1,0:T(8,128)(2,1)S(1)}, bf16[64,1280]{1,0:T(8,128)(2,1)S(1)}, u32[]{:S(2)}, u32[]{:S(2)}) %collective-permute-start.43) | collective-permute-done | bytes 163872 | tf_op jit(solution)/shard_map/ppermute | solution.py:363
  163.9 1.5 collective-permute-done.44
  165.4 0.9 maximum_select_fusion
  (91 shorter events, 2.7 us)
Async XLA Ops:
  0.0 49.6 %copy-start.10 = (f32[64]{0:T(128)S(1)}, f32[64]{0:T(128)}, u32[]{:S(2)}) copy-start(f32[64]{0:T(128)} %param.26) | copy-start | bytes 772
  0.0 49.6 %copy-start.9 = (f32[128]{0:T(128)S(1)}, f32[128]{0:T(128)}, u32[]{:S(2)}) copy-start(f32[128]{0:T(128)} %param.25) | copy-start | bytes 1540
  0.0 49.6 %copy-start.8 = (f32[4]{0:T(128)S(1)}, f32[4]{0:T(128)}, u32[]{:S(2)}) copy-start(f32[4]{0:T(128)} %balance_b.1) | copy-start | bytes 52
  0.0 49.6 %copy-start.7 = (f32[4]{0:T(128)S(1)}, f32[4]{0:T(128)}, u32[]{:S(2)}) copy-start(f32[4]{0:T(128)} %balance_a.1) | copy-start | bytes 52
  0.6 49.0 %copy-start.2 = (s32[3]{0:T(128)S(1)}, s32[3]{0:T(128)}, u32[]{:S(2)}) copy-start(s32[3]{0:T(128)} %pad_add_fusion.index) | copy-start | bytes 40
  4.5 45.1 %copy-start.1 = (bf16[128,576]{1,0:T(8,128)(2,1)S(1)}, bf16[128,576]{1,0:T(8,128)(2,1)}, u32[]{:S(2)}) copy-start(bf16[128,576]{1,0:T(8,128)(2,1)} %get-tuple-element.27.refs_0_) | copy-start | bytes 442372
  4.5 11.2 %collective-permute-start = (bf16[128,576]{1,0:T(8,128)(2,1)}, bf16[128,576]{1,0:T(8,128)(2,1)S(1)}, u32[]{:S(2)}, u32[]{:S(2)}) collective-permute-start(bf16[128,576]{1,0:T(8,128)(2,1)} %get-tuple-element.28), channel_id=1, source_target_pairs={{0,8},{2,10},{4,12},{6,14},{8,0},{10,2},{12,4},{14,6},{16,24},{18,... | collective-permute-start | bytes 442376 | tf_op jit(solution)/shard_map/ppermute | solution.py:363
  7.7 15.2 %collective-permute-start.1 = (bf16[128,576]{1,0:T(8,128)(2,1)}, bf16[128,576]{1,0:T(8,128)(2,1)S(1)}, u32[]{:S(2)}, u32[]{:S(2)}) collective-permute-start(bf16[128,576]{1,0:T(8,128)(2,1)} %get-tuple-element.29), channel_id=1, source_target_pairs={{0,16},{2,18},{4,20},{6,22},{8,24},{10,26},{12,28},{14,30},{16,0},... | collective-permute-start | bytes 442376 | tf_op jit(solution)/shard_map/ppermute | solution.py:363
  10.3 12.7 %collective-permute-start.2 = (bf16[128,576]{1,0:T(8,128)(2,1)}, bf16[128,576]{1,0:T(8,128)(2,1)S(1)}, u32[]{:S(2)}, u32[]{:S(2)}) collective-permute-start(bf16[128,576]{1,0:T(8,128)(2,1)} %get-tuple-element.30), channel_id=1, source_target_pairs={{0,24},{2,26},{4,28},{6,30},{8,16},{10,18},{12,20},{14,22},{16,8},... | collective-permute-start | bytes 442376 | tf_op jit(solution)/shard_map/ppermute | solution.py:363
  13.8 21.0 %collective-permute-start.14 = (bf16[256,1024]{1,0:T(8,128)(2,1)}, bf16[256,1024]{1,0:T(8,128)(2,1)S(1)}, u32[]{:S(2)}, u32[]{:S(2)}) collective-permute-start(bf16[256,1024]{1,0:T(8,128)(2,1)} %get-tuple-element.39), channel_id=1, source_target_pairs={{0,8},{2,10},{4,12},{6,14},{8,0},{10,2},{12,4},{14,6},{16,24},{18,... | collective-permute-start | bytes 1572872 | tf_op jit(solution)/shard_map/ppermute | solution.py:363
  23.0 11.9 %collective-permute-start.4 = (bf16[4,128,384]{2,1,0:T(8,128)(2,1)S(1)}, bf16[4,128,384]{2,1,0:T(8,128)(2,1)S(1)}, u32[]{:S(2)}, u32[]{:S(2)}) collective-permute-start(bf16[4,128,384]{2,1,0:T(8,128)(2,1)S(1)} %pad_maximum_fusion.refs_4_), channel_id=1, source_target_pairs={{0,4},{2,6},{4,0},{6,2},{8,12},{10,14},{12,8},{14,10},{16,20},{18,... | collective-permute-start | bytes 1179656 | tf_op jit(solution)/shard_map/ppermute | solution.py:370
  24.6 12.3 %collective-permute-start.3 = (bf16[4,128,384]{2,1,0:T(8,128)(2,1)S(1)}, bf16[4,128,384]{2,1,0:T(8,128)(2,1)S(1)}, u32[]{:S(2)}, u32[]{:S(2)}) collective-permute-start(bf16[4,128,384]{2,1,0:T(8,128)(2,1)S(1)} %pad_maximum_fusion.refs_4_), channel_id=1, source_target_pairs={{0,2},{2,0},{4,6},{6,4},{8,10},{10,8},{12,14},{14,12},{16,18},{18,... | collective-permute-start | bytes 1179656 | tf_op jit(solution)/shard_map/ppermute | solution.py:370
  26.1 22.2 %collective-permute-start.15 = (bf16[128,1024]{1,0:T(8,128)(2,1)}, bf16[128,1024]{1,0:T(8,128)(2,1)S(1)}, u32[]{:S(2)}, u32[]{:S(2)}) collective-permute-start(bf16[128,1024]{1,0:T(8,128)(2,1)} %get-tuple-element.40), channel_id=1, source_target_pairs={{0,16},{2,18},{4,20},{6,22},{8,24},{10,26},{12,28},{14,30},{16,0},... | collective-permute-start | bytes 786440 | tf_op jit(solution)/shard_map/ppermute | solution.py:363
  29.8 18.6 %collective-permute-start.16 = (bf16[128,1024]{1,0:T(8,128)(2,1)}, bf16[128,1024]{1,0:T(8,128)(2,1)S(1)}, u32[]{:S(2)}, u32[]{:S(2)}) collective-permute-start(bf16[128,1024]{1,0:T(8,128)(2,1)} %get-tuple-element.41), channel_id=1, source_target_pairs={{0,24},{2,26},{4,28},{6,30},{8,16},{10,18},{12,20},{14,22},{16,8},... | collective-permute-start | bytes 786440 | tf_op jit(solution)/shard_map/ppermute | solution.py:363
  34.9 14.6 %collective-permute-start.5 = (bf16[2,128,384]{2,1,0:T(8,128)(2,1)S(1)}, bf16[2,128,384]{2,1,0:T(8,128)(2,1)S(1)}, u32[]{:S(2)}, u32[]{:S(2)}) collective-permute-start(bf16[2,128,384]{2,1,0:T(8,128)(2,1)S(1)} %slice.77), channel_id=1, source_target_pairs={{0,2},{2,0},{4,6},{6,4},{8,10},{10,8},{12,14},{14,12},{16,18},{18,... | collective-permute-start | bytes 589832 | tf_op jit(solution)/shard_map/ppermute | solution.py:370
  37.0 12.6 %collective-permute-start.6 = (bf16[2,128,384]{2,1,0:T(8,128)(2,1)S(1)}, bf16[2,128,384]{2,1,0:T(8,128)(2,1)S(1)}, u32[]{:S(2)}, u32[]{:S(2)}) collective-permute-start(bf16[2,128,384]{2,1,0:T(8,128)(2,1)S(1)} %slice.78), channel_id=1, source_target_pairs={{0,4},{2,6},{4,0},{6,2},{8,12},{10,14},{12,8},{14,10},{16,20},{18,... | collective-permute-start | bytes 589832 | tf_op jit(solution)/shard_map/ppermute | solution.py:370
  48.4 25.2 %collective-permute-start.18 = (bf16[512,1024]{1,0:T(8,128)(2,1)S(1)}, bf16[512,1024]{1,0:T(8,128)(2,1)S(1)}, u32[]{:S(2)}, u32[]{:S(2)}) collective-permute-start(bf16[512,1024]{1,0:T(8,128)(2,1)S(1)} %constant_dynamic-update-slice_fusion.refs_4_), channel_id=1, source_target_pairs={{0,4},{2,6},{4,0},{6,2},{8,12},{10,14},{12,8},{14,10},{16,20},{18,... | collective-permute-start | bytes 3145736 | tf_op jit(solution)/shard_map/ppermute | solution.py:370
  49.0 25.7 %collective-permute-start.17 = (bf16[512,1024]{1,0:T(8,128)(2,1)S(1)}, bf16[512,1024]{1,0:T(8,128)(2,1)S(1)}, u32[]{:S(2)}, u32[]{:S(2)}) collective-permute-start(bf16[512,1024]{1,0:T(8,128)(2,1)S(1)} %constant_dynamic-update-slice_fusion.refs_4_), channel_id=1, source_target_pairs={{0,2},{2,0},{4,6},{6,4},{8,10},{10,8},{12,14},{14,12},{16,18},{18,... | collective-permute-start | bytes 3145736 | tf_op jit(solution)/shard_map/ppermute | solution.py:370
  49.6 13.5 %copy-start = (bf16[256,1024]{1,0:T(8,128)(2,1)S(1)}, bf16[256,1024]{1,0:T(8,128)(2,1)}, u32[]{:S(2)}) copy-start(bf16[256,1024]{1,0:T(8,128)(2,1)} %get-tuple-element.38.refs_0_) | copy-start | bytes 1572868
  49.6 16.5 %copy-start.3 = (bf16[512,2048]{1,0:T(8,128)(2,1)S(1)}, bf16[512,2048]{1,0:T(8,128)(2,1)}, u32[]{:S(2)}) copy-start(bf16[512,2048]{1,0:T(8,128)(2,1)} %refs_4_.3) | copy-start | bytes 6291460
  49.6 16.5 %copy-start.4 = (bf16[256,2048]{1,0:T(8,128)(2,1)S(1)}, bf16[256,2048]{1,0:T(8,128)(2,1)}, u32[]{:S(2)}) copy-start(bf16[256,2048]{1,0:T(8,128)(2,1)} %refs_5_.1) | copy-start | bytes 3145732
  56.1 12.0 %copy-start.12 = (bf16[128,1024]{1,0:T(8,128)(2,1)S(1)}, bf16[128,1024]{1,0:T(8,128)(2,1)}, u32[]{:S(2)}) copy-start(bf16[128,1024]{1,0:T(8,128)(2,1)} %get-tuple-element.43) | copy-start | bytes 786436
  56.1 15.3 %copy-start.5 = (bf16[128,2048]{1,0:T(8,128)(2,1)S(1)}, bf16[128,2048]{1,0:T(8,128)(2,1)}, u32[]{:S(2)}) copy-start(bf16[128,2048]{1,0:T(8,128)(2,1)} %residual.1) | copy-start | bytes 1572868
  56.1 15.3 %copy-start.6 = (f32[2048]{0:T(1024)S(1)}, f32[2048]{0:T(1024)}, u32[]{:S(2)}) copy-start(f32[2048]{0:T(1024)} %param.29) | copy-start | bytes 24580
  56.1 7.0 %collective-permute-start.7 = (bf16[128,192]{1,0:T(8,128)(2,1)S(1)}, bf16[128,192]{1,0:T(8,128)(2,1)S(1)}, u32[]{:S(2)}, u32[]{:S(2)}) collective-permute-start(bf16[128,192]{1,0:T(8,128)(2,1)S(1)} %get-tuple-element.32), channel_id=1, source_target_pairs={{0,8},{2,10},{4,12},{6,14},{8,0},{10,2},{12,4},{14,6},{16,24},{18,... | collective-permute-start | bytes 147464 | tf_op jit(solution)/shard_map/ppermute | solution.py:363
  60.0 5.4 %collective-permute-start.8 = (bf16[128,192]{1,0:T(8,128)(2,1)S(1)}, bf16[128,192]{1,0:T(8,128)(2,1)S(1)}, u32[]{:S(2)}, u32[]{:S(2)}) collective-permute-start(bf16[128,192]{1,0:T(8,128)(2,1)S(1)} %get-tuple-element.33), channel_id=1, source_target_pairs={{0,16},{2,18},{4,20},{6,22},{8,24},{10,26},{12,28},{14,30},{16,0},... | collective-permute-start | bytes 147464 | tf_op jit(solution)/shard_map/ppermute | solution.py:363
  60.0 6.2 %collective-permute-start.9 = (bf16[128,192]{1,0:T(8,128)(2,1)S(1)}, bf16[128,192]{1,0:T(8,128)(2,1)S(1)}, u32[]{:S(2)}, u32[]{:S(2)}) collective-permute-start(bf16[128,192]{1,0:T(8,128)(2,1)S(1)} %get-tuple-element.34), channel_id=1, source_target_pairs={{0,24},{2,26},{4,28},{6,30},{8,16},{10,18},{12,20},{14,22},{16,8},... | collective-permute-start | bytes 147464 | tf_op jit(solution)/shard_map/ppermute | solution.py:363
  63.1 33.5 %collective-permute-start.12 = (bf16[256,1024]{1,0:T(8,128)(2,1)S(1)}, bf16[256,1024]{1,0:T(8,128)(2,1)S(1)}, u32[]{:S(2)}, u32[]{:S(2)}) collective-permute-start(bf16[256,1024]{1,0:T(8,128)(2,1)S(1)} %copy-done), channel_id=1, source_target_pairs={{0,4},{2,6},{4,0},{6,2},{8,12},{10,14},{12,8},{14,10},{16,20},{18,... | collective-permute-start | bytes 1572872 | tf_op jit(solution)/shard_map/ppermute | solution.py:370
  66.2 7.4 %copy-start.11 = (bf16[128,1024]{1,0:T(8,128)(2,1)S(1)}, bf16[128,1024]{1,0:T(8,128)(2,1)}, u32[]{:S(2)}) copy-start(bf16[128,1024]{1,0:T(8,128)(2,1)} %get-tuple-element.44) | copy-start | bytes 786436
  68.0 1.9 %collective-permute-start.10 = (bf16[64,2048]{1,0:T(8,128)(2,1)S(1)}, bf16[64,2048]{1,0:T(8,128)(2,1)S(1)}, u32[]{:S(2)}, u32[]{:S(2)}) collective-permute-start(bf16[64,2048]{1,0:T(8,128)(2,1)S(1)} %get-tuple-element.36), channel_id=1, source_target_pairs={{0,1},{1,0},{2,3},{3,2},{4,5},{5,4},{6,7},{7,6},{8,9},{9,8},{10,11... | collective-permute-start | bytes 786440 | tf_op jit(solution)/shard_map/ppermute | solution.py:373
  68.1 27.0 %collective-permute-start.25 = (bf16[128,1024]{1,0:T(8,128)(2,1)S(1)}, bf16[128,1024]{1,0:T(8,128)(2,1)S(1)}, u32[]{:S(2)}, u32[]{:S(2)}) collective-permute-start(bf16[128,1024]{1,0:T(8,128)(2,1)S(1)} %copy-done.12), channel_id=1, source_target_pairs={{0,16},{2,18},{4,20},{6,22},{8,24},{10,26},{12,28},{14,30},{16,0},... | collective-permute-start | bytes 786440 | tf_op jit(solution)/shard_map/ppermute | solution.py:363
  69.9 35.9 %collective-permute-start.11 = (bf16[256,1024]{1,0:T(8,128)(2,1)S(1)}, bf16[256,1024]{1,0:T(8,128)(2,1)S(1)}, u32[]{:S(2)}, u32[]{:S(2)}) collective-permute-start(bf16[256,1024]{1,0:T(8,128)(2,1)S(1)} %copy-done), channel_id=1, source_target_pairs={{0,2},{2,0},{4,6},{6,4},{8,10},{10,8},{12,14},{14,12},{16,18},{18,... | collective-permute-start | bytes 1572872 | tf_op jit(solution)/shard_map/ppermute | solution.py:370
  73.6 24.5 %collective-permute-start.29 = (bf16[128,1024]{1,0:T(8,128)(2,1)S(1)}, bf16[128,1024]{1,0:T(8,128)(2,1)S(1)}, u32[]{:S(2)}, u32[]{:S(2)}) collective-permute-start(bf16[128,1024]{1,0:T(8,128)(2,1)S(1)} %copy-done.11), channel_id=1, source_target_pairs={{0,24},{2,26},{4,28},{6,30},{8,16},{10,18},{12,20},{14,22},{16,8},... | collective-permute-start | bytes 786440 | tf_op jit(solution)/shard_map/ppermute | solution.py:363
  74.8 31.0 %collective-permute-start.35 = (bf16[64,2048]{1,0:T(8,128)(2,1)S(1)}, bf16[64,2048]{1,0:T(8,128)(2,1)S(1)}, u32[]{:S(2)}, u32[]{:S(2)}) collective-permute-start(bf16[64,2048]{1,0:T(8,128)(2,1)S(1)} %get-tuple-element.42.refs_1_), channel_id=1, source_target_pairs={{0,16},{2,18},{4,20},{6,22},{8,24},{10,26},{12,28},{14,30},{16,0},... | collective-permute-start | bytes 786440 | tf_op jit(solution)/shard_map/ppermute | solution.py:363
  95.1 20.5 %collective-permute-start.19 = (bf16[256,1024]{1,0:T(8,128)(2,1)S(1)}, bf16[256,1024]{1,0:T(8,128)(2,1)S(1)}, u32[]{:S(2)}, u32[]{:S(2)}) collective-permute-start(bf16[256,1024]{1,0:T(8,128)(2,1)S(1)} %slice.80), channel_id=1, source_target_pairs={{0,2},{2,0},{4,6},{6,4},{8,10},{10,8},{12,14},{14,12},{16,18},{18,... | collective-permute-start | bytes 1572872 | tf_op jit(solution)/shard_map/ppermute | solution.py:370
  96.6 19.0 %collective-permute-start.20 = (bf16[256,1024]{1,0:T(8,128)(2,1)S(1)}, bf16[256,1024]{1,0:T(8,128)(2,1)S(1)}, u32[]{:S(2)}, u32[]{:S(2)}) collective-permute-start(bf16[256,1024]{1,0:T(8,128)(2,1)S(1)} %slice.81), channel_id=1, source_target_pairs={{0,4},{2,6},{4,0},{6,2},{8,12},{10,14},{12,8},{14,10},{16,20},{18,... | collective-permute-start | bytes 1572872 | tf_op jit(solution)/shard_map/ppermute | solution.py:370
  98.1 15.4 %collective-permute-start.13 = (bf16[128,1024]{1,0:T(8,128)(2,1)S(1)}, bf16[128,1024]{1,0:T(8,128)(2,1)S(1)}, u32[]{:S(2)}, u32[]{:S(2)}) collective-permute-start(bf16[128,1024]{1,0:T(8,128)(2,1)S(1)} %slice.79), channel_id=1, source_target_pairs={{0,2},{2,0},{4,6},{6,4},{8,10},{10,8},{12,14},{14,12},{16,18},{18,... | collective-permute-start | bytes 786440 | tf_op jit(solution)/shard_map/ppermute | solution.py:370
  105.8 9.3 %collective-permute-start.36 = (bf16[64,2048]{1,0:T(8,128)(2,1)S(1)}, bf16[64,2048]{1,0:T(8,128)(2,1)S(1)}, u32[]{:S(2)}, u32[]{:S(2)}) collective-permute-start(bf16[64,2048]{1,0:T(8,128)(2,1)S(1)} %collective-permute-done.35.refs_1_), channel_id=1, source_target_pairs={{0,8},{2,10},{4,12},{6,14},{8,0},{10,2},{12,4},{14,6},{16,24},{18,... | collective-permute-start | bytes 786440 | tf_op jit(solution)/shard_map/ppermute | solution.py:363
  105.8 11.2 %collective-permute-start.27 = (bf16[128,1024]{1,0:T(8,128)(2,1)S(1)}, bf16[128,1024]{1,0:T(8,128)(2,1)S(1)}, u32[]{:S(2)}, u32[]{:S(2)}) collective-permute-start(bf16[128,1024]{1,0:T(8,128)(2,1)S(1)} %collective-permute-done.25.refs_8_), channel_id=1, source_target_pairs={{0,4},{2,6},{4,0},{6,2},{8,12},{10,14},{12,8},{14,10},{16,20},{18,... | collective-permute-start | bytes 786440 | tf_op jit(solution)/shard_map/ppermute | solution.py:370
  113.5 9.2 %collective-permute-start.26 = (bf16[128,1024]{1,0:T(8,128)(2,1)S(1)}, bf16[128,1024]{1,0:T(8,128)(2,1)S(1)}, u32[]{:S(2)}, u32[]{:S(2)}) collective-permute-start(bf16[128,1024]{1,0:T(8,128)(2,1)S(1)} %collective-permute-done.25.refs_8_), channel_id=1, source_target_pairs={{0,2},{2,0},{4,6},{6,4},{8,10},{10,8},{12,14},{14,12},{16,18},{18,... | collective-permute-start | bytes 786440 | tf_op jit(solution)/shard_map/ppermute | solution.py:370
  115.0 10.6 %collective-permute-start.30 = (bf16[128,1024]{1,0:T(8,128)(2,1)S(1)}, bf16[128,1024]{1,0:T(8,128)(2,1)S(1)}, u32[]{:S(2)}, u32[]{:S(2)}) collective-permute-start(bf16[128,1024]{1,0:T(8,128)(2,1)S(1)} %collective-permute-done.29.refs_12_), channel_id=1, source_target_pairs={{0,2},{2,0},{4,6},{6,4},{8,10},{10,8},{12,14},{14,12},{16,18},{18,... | collective-permute-start | bytes 786440 | tf_op jit(solution)/shard_map/ppermute | solution.py:370
  115.6 11.5 %collective-permute-start.38 = (bf16[64,2048]{1,0:T(8,128)(2,1)S(1)}, bf16[64,2048]{1,0:T(8,128)(2,1)S(1)}, u32[]{:S(2)}, u32[]{:S(2)}) collective-permute-start(bf16[64,2048]{1,0:T(8,128)(2,1)S(1)} %collective-permute-done.35.refs_1_), channel_id=1, source_target_pairs={{0,1},{1,0},{2,3},{3,2},{4,5},{5,4},{6,7},{7,6},{8,9},{9,8},{10,11... | collective-permute-start | bytes 786440 | tf_op jit(solution)/shard_map/ppermute | solution.py:373
  115.6 13.1 %collective-permute-start.37 = (bf16[64,2048]{1,0:T(8,128)(2,1)S(1)}, bf16[64,2048]{1,0:T(8,128)(2,1)S(1)}, u32[]{:S(2)}, u32[]{:S(2)}) collective-permute-start(bf16[64,2048]{1,0:T(8,128)(2,1)S(1)} %collective-permute-done.36.refs_0_), channel_id=1, source_target_pairs={{0,1},{1,0},{2,3},{3,2},{4,5},{5,4},{6,7},{7,6},{8,9},{9,8},{10,11... | collective-permute-start | bytes 786440 | tf_op jit(solution)/shard_map/ppermute | solution.py:373
  116.9 13.3 %collective-permute-start.31 = (bf16[128,1024]{1,0:T(8,128)(2,1)S(1)}, bf16[128,1024]{1,0:T(8,128)(2,1)S(1)}, u32[]{:S(2)}, u32[]{:S(2)}) collective-permute-start(bf16[128,1024]{1,0:T(8,128)(2,1)S(1)} %collective-permute-done.29.refs_12_), channel_id=1, source_target_pairs={{0,4},{2,6},{4,0},{6,2},{8,12},{10,14},{12,8},{14,10},{16,20},{18,... | collective-permute-start | bytes 786440 | tf_op jit(solution)/shard_map/ppermute | solution.py:370
  122.7 13.8 %collective-permute-start.24 = (bf16[128,1024]{1,0:T(8,128)(2,1)S(1)}, bf16[128,1024]{1,0:T(8,128)(2,1)S(1)}, u32[]{:S(2)}, u32[]{:S(2)}) collective-permute-start(bf16[128,1024]{1,0:T(8,128)(2,1)S(1)} %slice.82), channel_id=1, source_target_pairs={{0,4},{2,6},{4,0},{6,2},{8,12},{10,14},{12,8},{14,10},{16,20},{18,... | collective-permute-start | bytes 786440 | tf_op jit(solution)/shard_map/ppermute | solution.py:370
  125.6 9.4 %collective-permute-start.28 = (bf16[128,1024]{1,0:T(8,128)(2,1)S(1)}, bf16[128,1024]{1,0:T(8,128)(2,1)S(1)}, u32[]{:S(2)}, u32[]{:S(2)}) collective-permute-start(bf16[128,1024]{1,0:T(8,128)(2,1)S(1)} %collective-permute-done.27.refs_10_), channel_id=1, source_target_pairs={{0,2},{2,0},{4,6},{6,4},{8,10},{10,8},{12,14},{14,12},{16,18},{18,... | collective-permute-start | bytes 786440 | tf_op jit(solution)/shard_map/ppermute | solution.py:370
  127.1 9.4 %collective-permute-start.32 = (bf16[128,1024]{1,0:T(8,128)(2,1)S(1)}, bf16[128,1024]{1,0:T(8,128)(2,1)S(1)}, u32[]{:S(2)}, u32[]{:S(2)}) collective-permute-start(bf16[128,1024]{1,0:T(8,128)(2,1)S(1)} %collective-permute-done.30.refs_13_), channel_id=1, source_target_pairs={{0,4},{2,6},{4,0},{6,2},{8,12},{10,14},{12,8},{14,10},{16,20},{18,... | collective-permute-start | bytes 786440 | tf_op jit(solution)/shard_map/ppermute | solution.py:370
  128.7 6.4 %collective-permute-start.21 = (bf16[64,2048]{1,0:T(8,128)(2,1)S(1)}, bf16[64,2048]{1,0:T(8,128)(2,1)S(1)}, u32[]{:S(2)}, u32[]{:S(2)}) collective-permute-start(bf16[64,2048]{1,0:T(8,128)(2,1)S(1)} %get-tuple-element.42.refs_1_), channel_id=1, source_target_pairs={{0,8},{2,10},{4,12},{6,14},{8,0},{10,2},{12,4},{14,6},{16,24},{18,... | collective-permute-start | bytes 786440 | tf_op jit(solution)/shard_map/ppermute | solution.py:363
  130.3 8.7 %collective-permute-start.23 = (bf16[64,2048]{1,0:T(8,128)(2,1)S(1)}, bf16[64,2048]{1,0:T(8,128)(2,1)S(1)}, u32[]{:S(2)}, u32[]{:S(2)}) collective-permute-start(bf16[64,2048]{1,0:T(8,128)(2,1)S(1)} %get-tuple-element.42.refs_1_), channel_id=1, source_target_pairs={{0,1},{1,0},{2,3},{3,2},{4,5},{5,4},{6,7},{7,6},{8,9},{9,8},{10,11... | collective-permute-start | bytes 786440 | tf_op jit(solution)/shard_map/ppermute | solution.py:373
  135.0 3.9 %collective-permute-start.22 = (bf16[64,2048]{1,0:T(8,128)(2,1)S(1)}, bf16[64,2048]{1,0:T(8,128)(2,1)S(1)}, u32[]{:S(2)}, u32[]{:S(2)}) collective-permute-start(bf16[64,2048]{1,0:T(8,128)(2,1)S(1)} %collective-permute-done.21.refs_0_), channel_id=1, source_target_pairs={{0,1},{1,0},{2,3},{3,2},{4,5},{5,4},{6,7},{7,6},{8,9},{9,8},{10,11... | collective-permute-start | bytes 786440 | tf_op jit(solution)/shard_map/ppermute | solution.py:373
  138.8 3.2 %collective-permute-start.39 = (bf16[2,64,2048]{2,1,0:T(8,128)(2,1)S(1)}, bf16[2,64,2048]{2,1,0:T(8,128)(2,1)S(1)}, u32[]{:S(2)}, u32[]{:S(2)}) collective-permute-start(bf16[2,64,2048]{2,1,0:T(8,128)(2,1)S(1)} %get-tuple-element.48), channel_id=1, source_target_pairs={{0,1},{1,0},{2,3},{3,2},{4,5},{5,4},{6,7},{7,6},{8,9},{9,8},{10,11... | collective-permute-start | bytes 1572872 | tf_op jit(solution)/shard_map/ppermute | solution.py:373
  141.5 2.1 %collective-permute-start.33 = (bf16[2,64,2048]{2,1,0:T(8,128)(2,1)S(1)}, bf16[2,64,2048]{2,1,0:T(8,128)(2,1)S(1)}, u32[]{:S(2)}, u32[]{:S(2)}) collective-permute-start(bf16[2,64,2048]{2,1,0:T(8,128)(2,1)S(1)} %get-tuple-element.46), channel_id=1, source_target_pairs={{0,1},{1,0},{2,3},{3,2},{4,5},{5,4},{6,7},{7,6},{8,9},{9,8},{10,11... | collective-permute-start | bytes 1572872 | tf_op jit(solution)/shard_map/ppermute | solution.py:373
  142.2 7.1 %collective-permute-start.42 = (bf16[64,1280]{1,0:T(8,128)(2,1)S(1)}, bf16[64,1280]{1,0:T(8,128)(2,1)S(1)}, u32[]{:S(2)}, u32[]{:S(2)}) collective-permute-start(bf16[64,1280]{1,0:T(8,128)(2,1)S(1)} %slice.90), channel_id=1, source_target_pairs={{0,8},{2,10},{4,12},{6,14},{8,0},{10,2},{12,4},{14,6},{16,24},{18,... | collective-permute-start | bytes 491528 | tf_op jit(solution)/shard_map/ppermute | solution.py:363
  143.8 19.9 %collective-permute-start.34 = (bf16[64,2048]{1,0:T(8,128)(2,1)S(1)}, bf16[64,2048]{1,0:T(8,128)(2,1)S(1)}, u32[]{:S(2)}, u32[]{:S(2)}) collective-permute-start(bf16[64,2048]{1,0:T(8,128)(2,1)S(1)} %fusion.5), channel_id=1, source_target_pairs={{0,8},{2,10},{4,12},{6,14},{8,0},{10,2},{12,4},{14,6},{16,24},{18,... | collective-permute-start | bytes 786440 | tf_op jit(solution)/shard_map/ppermute | solution.py:363
  144.6 13.2 %collective-permute-start.40 = (bf16[64,768]{1,0:T(8,128)(2,1)S(1)}, bf16[64,768]{1,0:T(8,128)(2,1)S(1)}, u32[]{:S(2)}, u32[]{:S(2)}) collective-permute-start(bf16[64,768]{1,0:T(8,128)(2,1)S(1)} %slice.86), channel_id=1, source_target_pairs={{0,24},{2,26},{4,28},{6,30},{8,16},{10,18},{12,20},{14,22},{16,8},... | collective-permute-start | bytes 294920 | tf_op jit(solution)/shard_map/ppermute | solution.py:363
  147.4 10.5 %collective-permute-start.41 = (bf16[64,768]{1,0:T(8,128)(2,1)S(1)}, bf16[64,768]{1,0:T(8,128)(2,1)S(1)}, u32[]{:S(2)}, u32[]{:S(2)}) collective-permute-start(bf16[64,768]{1,0:T(8,128)(2,1)S(1)} %slice.115), channel_id=1, source_target_pairs={{0,16},{2,18},{4,20},{6,22},{8,24},{10,26},{12,28},{14,30},{16,0},... | collective-permute-start | bytes 294920 | tf_op jit(solution)/shard_map/ppermute | solution.py:363
  149.4 14.2 %collective-permute-start.43 = (bf16[64,1280]{1,0:T(8,128)(2,1)S(1)}, bf16[64,1280]{1,0:T(8,128)(2,1)S(1)}, u32[]{:S(2)}, u32[]{:S(2)}) collective-permute-start(bf16[64,1280]{1,0:T(8,128)(2,1)S(1)} %fusion.4), channel_id=1, source_target_pairs={{0,16},{2,18},{4,20},{6,22},{8,24},{10,26},{12,28},{14,30},{16,0},... | collective-permute-start | bytes 491528 | tf_op jit(solution)/shard_map/ppermute | solution.py:363
  163.8 1.6 collective-permute-start.44

commit v5 on v4

--- a/solution.py
+++ b/solution.py
@@ -123,7 +123,7 @@
 
 VMEM = pltpu.VMEM
 SMEM = pltpu.SMEM
-DIRECT = 0.375
+DIRECT = 0.25
 
 
 def vmem_specs(count):
@@ -154,14 +154,14 @@
 
 
 def cut_kernel(slots, width, index, *refs):
-    weights, pairs, ups, downs = refs[:2], refs[2:4], refs[4 : 2 + slots], refs[2 + slots : -1]
+    weights, pairs, lasts = refs[:2], refs[2 : 1 + slots], refs[1 + slots : -1]
     arrived = refs[-1]
     block = weights[0].shape[0]
     copies = []
-    for i, (weight, pieces) in enumerate(zip(weights, (ups, downs))):
+    for i, (weight, last) in enumerate(zip(weights, lasts)):
         for k in range(slots):
             place = pl.ds(pl.multiple_of((index[0] ^ k) * width, width), width)
-            target = pairs[k].at[pl.ds(i * block, block), :] if k < 2 else pieces[k - 2]
+            target = last if k == slots - 1 else pairs[k].at[pl.ds(i * block, block), :]
             copies.append(
                 pltpu.make_async_copy(weight.at[:, place], target, arrived.at[i * slots + k])
             )
@@ -295,9 +295,9 @@
 def arrange_kernel(moves, plane, block, index, *refs):
     out = refs[-1]
     z, g = index[0], index[1]
-    for p, k, number, at in moves:
-        place = pl.multiple_of(((z ^ k) * plane + (g ^ p)) * block, block)
-        out[pl.ds(place, block), :] = refs[number][at * block : (at + 1) * block, :]
+    for p, k, number, source, target, rows in moves:
+        place = ((z ^ k) * plane + (g ^ p)) * block + target
+        out[pl.ds(pl.multiple_of(place, rows), rows), :] = refs[number][source : source + rows, :]
 
 
 def lift_kernel(up, *refs):
@@ -396,15 +396,15 @@
     piece_shape = jax.ShapeDtypeStruct((block, hidden), jnp.bfloat16)
     cuts = pl.pallas_call(
         functools.partial(cut_kernel, slots, hidden),
-        out_shape=(jax.ShapeDtypeStruct((2 * block, hidden), jnp.bfloat16),) * 2
-        + (piece_shape,) * (2 * slots - 4),
+        out_shape=(jax.ShapeDtypeStruct((2 * block, hidden), jnp.bfloat16),) * (slots - 1)
+        + (piece_shape,) * 2,
         in_specs=[smem] + [pl.BlockSpec(memory_space=pltpu.HBM)] * 2,
-        out_specs=tuple(vmem_specs(2 * slots - 2)),
+        out_specs=tuple(vmem_specs(slots + 1)),
         scratch_shapes=[pltpu.SemaphoreType.DMA((2 * slots,))],
         cost_estimate=pl.CostEstimate(flops=10**8, bytes_accessed=10**6, transcendentals=0),
         name="cut",
     )(index, up_weight, down_weight)
-    early, both, cut_up, cut_down = cuts[0], cuts[1], cuts[2:slots], cuts[slots:]
+    early, middle, distant, last_ups, last_downs = cuts
     got = [along(packed[k], k) for k in range(slots)]
     keyval = jnp.stack([piece[:, :384] for piece in got])
     kv_pieces = [across(keyval, p) for p in range(plane - 1)]
@@ -416,29 +416,31 @@
     last_up = across(firsts[2][:block], 1)
     last_down = across(firsts[1][block:], 2)
 
-    def gather(arrays, turn):
+    def gather(arrays):
         mine = jnp.concatenate(arrays, axis=0) if len(arrays) > 1 else arrays[0]
         near = [mine, across(mine, 1), across(mine, 2)]
         blocks = mine.shape[0] // block
-        split = (blocks + 1) // 2
-        ways = (1, 2) if turn == 0 else (2, 1)
-        pieces = [[(p, near[p], i) for p in range(3)] for i in range(blocks)]
-        for way, lo, hi in ((ways[0], 0, split), (ways[1], split, blocks)):
-            if hi > lo:
-                far = across(near[3 - way][lo * block : hi * block], way)
-                for i in range(lo, hi):
-                    pieces[i].append((3, far, i - lo))
+        pieces = [
+            [(p, near[p], i * block, 0, block) for p in range(3)] for i in range(blocks)
+        ]
+        split = mine.shape[0] // 2
+        rows = math.gcd(block, split)
+        for way, low in ((1, 0), (2, split)):
+            sent = near[3 - way][low : low + split]
+            far = across(sent, way)
+            for row in range(low, low + split, rows):
+                pieces[row // block].append((3, far, row - low, row % block, rows))
         return pieces
 
     def arrange(pieces):
         arrays = []
         moves = []
-        for p, k, array, at in pieces:
+        for p, k, array, *rest in pieces:
             numbers = [i for i, other in enumerate(arrays) if other is array]
             if not numbers:
                 numbers = [len(arrays)]
                 arrays.append(array)
-            moves.append((p, k, numbers[0], at))
+            moves.append((p, k, numbers[0], *rest))
         return pl.pallas_call(
             functools.partial(arrange_kernel, tuple(moves), plane, block),
             out_shape=jax.ShapeDtypeStruct((count * block, hidden), jnp.bfloat16),
@@ -448,20 +450,22 @@
             cost_estimate=pl.CostEstimate(flops=10**8, bytes_accessed=10**6, transcendentals=0),
         )(index, *arrays)
 
-    own_up = [(p, 0, firsts[p], 0) for p in range(3)] + [(3, 0, last_up, 0)]
-    own_down = [(p, 0, firsts[p], 1) for p in range(3)] + [(3, 0, last_down, 0)]
+    own_up = [(p, 0, firsts[p], 0, 0, block) for p in range(3)]
+    own_up.append((3, 0, last_up, 0, 0, block))
+    own_down = [(p, 0, firsts[p], block, 0, block) for p in range(3)]
+    own_down.append((3, 0, last_down, 0, 0, block))
 
     def label(k, pieces):
-        return [(p, k, array, at) for p, array, at in pieces]
-
-    moved = [along(both, 1)] + [along(cut, k) for k, cut in zip(range(2, slots), cut_up)]
-    group = gather(moved, 0)
-    own_up += label(1, group[0])
+        return [(p, k, *rest) for p, *rest in pieces]
+
+    first_moved = [along(middle, 1), along(last_ups, 3)]
+    group = gather(first_moved)
+    own_up += label(1, group[0]) + label(3, group[2])
     own_down += label(1, group[1])
-    for k in range(2, slots):
-        own_up += label(k, group[k])
-    for k, cut in zip(range(2, slots), cut_down):
-        own_down += label(k, gather([along(cut, k)], k % 2)[0])
+    group = gather([along(distant, 2)])
+    own_up += label(2, group[0])
+    own_down += label(2, group[1])
+    own_down += label(3, gather([along(last_downs, 3)])[0])
     up = arrange(own_up)
     down = arrange(own_down)
 

time: 166 us -> 176 us (1.060)
  waiting for transfers between devices: 81.6 us -> 95.4 us
  starting transfers between devices: 57.5 us -> 53.7 us
    ppermute x18 -> x20, waiting for transfers between devices: 14.8 us -> 42.7 us  [across(): return lax.ppermute(value, 'sp', [(i, i ^ k) for i in range(count)])]
    ppermute x19 -> x18, waiting for transfers between devices: 64.1 us -> 50.5 us  [along(): lax.ppermute(value, 'sp', [(i, (i // plane ^ k) * plane + i % plane) for...]
    ppermute x19 -> x18, starting transfers between devices: 31.5 us -> 27.7 us  [along(): lax.ppermute(value, 'sp', [(i, (i // plane ^ k) * plane + i % plane) for...]
    ppermute x18 -> x20, starting transfers between devices: 24.6 us -> 24.6 us  [across(): return lax.ppermute(value, 'sp', [(i, i ^ k) for i in range(count)])]
  transfers between devices with their start and end apart: 45 -> 46, of which waited for: 19 -> 19; matrix products, arithmetic and copies ran while one was open for 1% -> 1% of each run, Pallas kernels for 12% -> 11%
where the time goes in v5:
time: 176 us
  waiting for transfers between devices  95.4 us (54%)
  starting transfers between devices  53.7 us (31%)
  Pallas kernels  23.1 us (13%)
  other arithmetic  2.03 us (1%)
    ppermute x18, waiting for transfers between devices, along(): lax.ppermute(value, 'sp', [(i, (i // plane ^ k) * plane + i % plane) for...  50.5 us
    ppermute x20, waiting for transfers between devices, across(): return lax.ppermute(value, 'sp', [(i, i ^ k) for i in range(count)])  42.7 us
    ppermute x18, starting transfers between devices, along(): lax.ppermute(value, 'sp', [(i, (i // plane ^ k) * plane + i % plane) for...  27.7 us
    ppermute x20, starting transfers between devices, across(): return lax.ppermute(value, 'sp', [(i, i ^ k) for i in range(count)])  24.6 us
    pallas_call x1, Pallas kernels, fast_body(): pl.pallas_call(functools.partial(attend_kernel, slots, plane, tokens), ou...  6.4 us
    pallas_call x1, Pallas kernels, fast_body(): pl.pallas_call(functools.partial(pack_kernel, slots), out_shape=(jax.Shap...  3.85 us
    pallas_call x1, Pallas kernels, fast_body(): pl.pallas_call(functools.partial(cut_kernel, slots, hidden), out_shape=(j...  3.55 us
  transfers between devices with their start and end apart: 46, of which 19 were waited for; matrix products, arithmetic and copies ran while one was open for 1% of the time, Pallas kernels for 11%

profile of v5, /device:TPU:0, one launch (start us, length us, event | category | flops | bytes accessed | tf_op | source)
XLA Modules:
  0.0 176.1 jit_solution(7310117313399302689)
XLA Ops:
  0.0 0.6 pad_add_fusion.index
  0.6 3.8 %pack.1 = (bf16[128,576]{1,0:T(8,128)(2,1)}, bf16[128,576]{1,0:T(8,128)(2,1)}, bf16[128,576]{1,0:T(8,128)(2,1)}, bf16[128,576]{1,0:T(8,128)(2,1)}) custom-call(s32[3]{0:T(128)} %pad_add_fusion.index, bf16[128,4,128]{2,1,0:T(4,128)(2,1)} %refs_0_.2, bf16[4,64,128]{2,1,0:T(8,128)(2,1)} %bitcast.36, bf16[4,64,128]{2,1,0:T(8,128)(2,1)} %bitcast.37, ...), custom_call_target="tpu_custom_call" | custom-call | flops 100000000 | bytes 1000000 | tf_op jit(solution)/shard_map/pack/pallas_call | solution.py:386
  4.5 5.2 %collective-permute-start.2 = (bf16[128,576]{1,0:T(8,128)(2,1)}, bf16[128,576]{1,0:T(8,128)(2,1)S(1)}, u32[]{:S(2)}, u32[]{:S(2)}) collective-permute-start(bf16[128,576]{1,0:T(8,128)(2,1)} %get-tuple-element.29), channel_id=1, source_target_pairs={{0,24},{2,26},{4,28},{6,30},{8,16},{10,18},{12,20},{14,22},{16,8},... | collective-permute-start | bytes 442376 | tf_op jit(solution)/shard_map/ppermute | solution.py:363
  9.7 0.6 collective-permute-start
  10.3 3.5 %cut.1 = (bf16[256,1024]{1,0:T(8,128)(2,1)}, bf16[256,1024]{1,0:T(8,128)(2,1)}, bf16[256,1024]{1,0:T(8,128)(2,1)}, bf16[128,1024]{1,0:T(8,128)(2,1)}, bf16[128,1024]{1,0:T(8,128)(2,1)}) custom-call(s32[3]{0:T(128)} %pad_add_fusion.index, bf16[128,4096]{1,0:T(8,128)(2,1)} %refs_0_.3, bf16[128,4096]{1,0:T(8,128)(2,1)} %refs_1_.1), custom_call_target="tpu_custom_call" | custom-call | flops 100000000 | bytes 1000000 | tf_op jit(solution)/shard_map/cut/pallas_call | solution.py:397
  13.9 1.5 collective-permute-start.14
  15.3 0.9 slice_bitcast_fusion.5
  16.3 7.6 %collective-permute-done.1.refs_2_ = bf16[128,576]{1,0:T(8,128)(2,1)S(1)} collective-permute-done((bf16[128,576]{1,0:T(8,128)(2,1)}, bf16[128,576]{1,0:T(8,128)(2,1)S(1)}, u32[]{:S(2)}, u32[]{:S(2)}) %collective-permute-start.1) | collective-permute-done | bytes 147488 | tf_op jit(solution)/shard_map/ppermute | solution.py:363
  24.0 1.6 collective-permute-start.4
  25.6 1.5 collective-permute-start.3
  27.0 2.5 %collective-permute-start.15 = (bf16[128,1024]{1,0:T(8,128)(2,1)}, bf16[128,1024]{1,0:T(8,128)(2,1)S(1)}, u32[]{:S(2)}, u32[]{:S(2)}) collective-permute-start(bf16[128,1024]{1,0:T(8,128)(2,1)} %get-tuple-element.39), channel_id=1, source_target_pairs={{0,24},{2,26},{4,28},{6,30},{8,16},{10,18},{12,20},{14,22},{16,8},... | collective-permute-start | bytes 786440 | tf_op jit(solution)/shard_map/ppermute | solution.py:363
  29.5 1.3 collective-permute-start.29
  30.9 3.3 %collective-permute-done.4.refs_6_ = bf16[4,128,384]{2,1,0:T(8,128)(2,1)S(1)} collective-permute-done((bf16[4,128,384]{2,1,0:T(8,128)(2,1)S(1)}, bf16[4,128,384]{2,1,0:T(8,128)(2,1)S(1)}, u32[]{:S(2)}, u32[]{:S(2)}) %collective-permute-start.4) | collective-permute-done | bytes 393248 | tf_op jit(solution)/shard_map/ppermute | solution.py:370
  34.2 1.5 collective-permute-start.12
  35.7 1.6 collective-permute-start.5
  37.3 0.6 collective-permute-start.6
  37.9 1.0 collective-permute-done.15
  38.9 1.7 collective-permute-start.11
  40.6 3.1 %collective-permute-done.29.refs_13_ = bf16[128,1024]{1,0:T(8,128)(2,1)S(1)} collective-permute-done((bf16[128,1024]{1,0:T(8,128)(2,1)}, bf16[128,1024]{1,0:T(8,128)(2,1)S(1)}, u32[]{:S(2)}, u32[]{:S(2)}) %collective-permute-start.29) | collective-permute-done | bytes 262176 | tf_op jit(solution)/shard_map/ppermute | solution.py:363
  43.7 7.2 %collective-permute-start.20 = (bf16[256,1024]{1,0:T(8,128)(2,1)}, bf16[256,1024]{1,0:T(8,128)(2,1)S(1)}, u32[]{:S(2)}, u32[]{:S(2)}) collective-permute-start(bf16[256,1024]{1,0:T(8,128)(2,1)} %get-tuple-element.40), channel_id=1, source_target_pairs={{0,16},{2,18},{4,20},{6,22},{8,24},{10,26},{12,28},{14,30},{16,0},... | collective-permute-start | bytes 1572872 | tf_op jit(solution)/shard_map/ppermute | solution.py:363
  50.9 0.5 collective-permute-start.17
  51.4 6.1 %collective-permute-start.16 = (bf16[384,1024]{1,0:T(8,128)(2,1)S(1)}, bf16[384,1024]{1,0:T(8,128)(2,1)S(1)}, u32[]{:S(2)}, u32[]{:S(2)}) collective-permute-start(bf16[384,1024]{1,0:T(8,128)(2,1)S(1)} %constant_dynamic-update-slice_fusion.refs_4_), channel_id=1, source_target_pairs={{0,2},{2,0},{4,6},{6,4},{8,10},{10,8},{12,14},{14,12},{16,18},{18,... | collective-permute-start | bytes 2359304 | tf_op jit(solution)/shard_map/ppermute | solution.py:370
  57.6 6.4 %attend.1 = (bf16[128,192]{1,0:T(8,128)(2,1)S(1)}, bf16[128,192]{1,0:T(8,128)(2,1)S(1)}, bf16[128,192]{1,0:T(8,128)(2,1)S(1)}, bf16[128,192]{1,0:T(8,128)(2,1)S(1)}) custom-call(s32[3]{0:T(128)S(1)} %copy-done.2, f32[4]{0:T(128)S(1)} %copy-done.7, f32[4]{0:T(128)S(1)} %copy-done.8, f32[1,128]{1,0:T(1,128)S(1)} %bitcast.34, f32[1,64]{1,0:T(1,128)S(1)} %bitcast.35, ...), custom_call_target="tpu_custom_call" | custom-call | flops 8000000000 | bytes 2000000 | tf_op jit(solution)/shard_map/attend/pallas_call | solution.py:473
  64.0 8.4 %collective-permute-done.20.refs_9_ = bf16[256,1024]{1,0:T(8,128)(2,1)S(1)} collective-permute-done((bf16[256,1024]{1,0:T(8,128)(2,1)}, bf16[256,1024]{1,0:T(8,128)(2,1)S(1)}, u32[]{:S(2)}, u32[]{:S(2)}) %collective-permute-start.20) | collective-permute-done | bytes 524320 | tf_op jit(solution)/shard_map/ppermute | solution.py:363
  72.4 2.1 %collective-permute-start.8 = (bf16[128,192]{1,0:T(8,128)(2,1)S(1)}, bf16[128,192]{1,0:T(8,128)(2,1)S(1)}, u32[]{:S(2)}, u32[]{:S(2)}) collective-permute-start(bf16[128,192]{1,0:T(8,128)(2,1)S(1)} %get-tuple-element.32), channel_id=1, source_target_pairs={{0,16},{2,18},{4,20},{6,22},{8,24},{10,26},{12,28},{14,30},{16,0},... | collective-permute-start | bytes 147464 | tf_op jit(solution)/shard_map/ppermute | solution.py:363
  74.5 2.2 %collective-permute-done.7.refs_1_ = bf16[128,192]{1,0:T(8,128)(2,1)S(1)} collective-permute-done((bf16[128,192]{1,0:T(8,128)(2,1)S(1)}, bf16[128,192]{1,0:T(8,128)(2,1)S(1)}, u32[]{:S(2)}, u32[]{:S(2)}) %collective-permute-start.7) | collective-permute-done | bytes 49184 | tf_op jit(solution)/shard_map/ppermute | solution.py:363
  76.6 0.5 collective-permute-start.22
  77.1 0.5 collective-permute-done.8.refs_2_
  77.6 1.5 collective-permute-start.9
  79.1 4.7 %collective-permute-done.9.refs_3_ = bf16[128,192]{1,0:T(8,128)(2,1)S(1)} collective-permute-done((bf16[128,192]{1,0:T(8,128)(2,1)S(1)}, bf16[128,192]{1,0:T(8,128)(2,1)S(1)}, u32[]{:S(2)}, u32[]{:S(2)}) %collective-permute-start.9) | collective-permute-done | bytes 49184 | tf_op jit(solution)/shard_map/ppermute | solution.py:363
  83.8 1.0 collective-permute-start.31
  84.7 1.8 %project.1 = (bf16[64,2048]{1,0:T(8,128)(2,1)S(1)}, bf16[64,2048]{1,0:T(8,128)(2,1)S(1)}) custom-call(s32[3]{0:T(128)S(1)} %copy-done.2, bf16[128,192]{1,0:T(8,128)(2,1)S(1)} %get-tuple-element.30.refs_0_, bf16[128,192]{1,0:T(8,128)(2,1)S(1)} %collective-permute-done.7.refs_1_, bf16[128,192]{1,0:T(8,128)(2,1)S(1)} %collective-permute-done.8.refs_2_, ...), custom_call_target="tpu_custom_call" | custom-call | flops 2000000000 | bytes 4000000 | tf_op jit(solution)/shard_map/project/pallas_call | solution.py:498
  86.6 7.4 %collective-permute-done.31.refs_15_ = bf16[128,1024]{1,0:T(8,128)(2,1)S(1)} collective-permute-done((bf16[128,1024]{1,0:T(8,128)(2,1)S(1)}, bf16[128,1024]{1,0:T(8,128)(2,1)S(1)}, u32[]{:S(2)}, u32[]{:S(2)}) %collective-permute-start.31) | collective-permute-done | bytes 262176 | tf_op jit(solution)/shard_map/ppermute | solution.py:370
  94.1 0.5 collective-permute-start.21
  94.6 1.6 collective-permute-start.30
  96.2 0.5 collective-permute-start.13
  96.8 0.8 norm.1
  97.6 1.6 collective-permute-start.23
  99.5 15.0 %collective-permute-done.30.refs_14_ = bf16[128,1024]{1,0:T(8,128)(2,1)S(1)} collective-permute-done((bf16[128,1024]{1,0:T(8,128)(2,1)S(1)}, bf16[128,1024]{1,0:T(8,128)(2,1)S(1)}, u32[]{:S(2)}, u32[]{:S(2)}) %collective-permute-start.30) | collective-permute-done | bytes 262176 | tf_op jit(solution)/shard_map/ppermute | solution.py:370
  114.5 0.5 collective-permute-start.18
  115.0 5.1 %collective-permute-done.13.refs_3_ = bf16[128,1024]{1,0:T(8,128)(2,1)S(1)} collective-permute-done((bf16[128,1024]{1,0:T(8,128)(2,1)S(1)}, bf16[128,1024]{1,0:T(8,128)(2,1)S(1)}, u32[]{:S(2)}, u32[]{:S(2)}) %collective-permute-start.13) | collective-permute-done | bytes 262176 | tf_op jit(solution)/shard_map/ppermute | solution.py:370
  120.1 0.5 collective-permute-start.19
  120.6 5.1 %collective-permute-done.23.refs_12_ = bf16[128,1024]{1,0:T(8,128)(2,1)S(1)} collective-permute-done((bf16[128,1024]{1,0:T(8,128)(2,1)S(1)}, bf16[128,1024]{1,0:T(8,128)(2,1)S(1)}, u32[]{:S(2)}, u32[]{:S(2)}) %collective-permute-start.23) | collective-permute-done | bytes 262176 | tf_op jit(solution)/shard_map/ppermute | solution.py:370
  125.7 0.5 collective-permute-start.25
  126.3 4.9 %collective-permute-done.18.refs_7_ = bf16[192,1024]{1,0:T(8,128)(2,1)S(1)} collective-permute-done((bf16[192,1024]{1,0:T(8,128)(2,1)S(1)}, bf16[192,1024]{1,0:T(8,128)(2,1)S(1)}, u32[]{:S(2)}, u32[]{:S(2)}) %collective-permute-start.18) | collective-permute-done | bytes 393248 | tf_op jit(solution)/shard_map/ppermute | solution.py:370
  131.2 0.8 collective-permute-start.32
  132.0 0.8 shard_map.154.up
  132.8 2.1 %collective-permute-start.33 = (bf16[64,1024]{1,0:T(8,128)(2,1)S(1)}, bf16[64,1024]{1,0:T(8,128)(2,1)S(1)}, u32[]{:S(2)}, u32[]{:S(2)}) collective-permute-start(bf16[64,1024]{1,0:T(8,128)(2,1)S(1)} %slice.102), channel_id=1, source_target_pairs={{0,4},{2,6},{4,0},{6,2},{8,12},{10,14},{12,8},{14,10},{16,20},{18,... | collective-permute-start | bytes 393224 | tf_op jit(solution)/shard_map/ppermute | solution.py:370
  135.3 1.3 shard_map.155.hidden
  136.7 4.7 %collective-permute-done.37.refs_0_ = bf16[64,2048]{1,0:T(8,128)(2,1)S(1)} collective-permute-done((bf16[64,2048]{1,0:T(8,128)(2,1)S(1)}, bf16[64,2048]{1,0:T(8,128)(2,1)S(1)}, u32[]{:S(2)}, u32[]{:S(2)}) %collective-permute-start.37) | collective-permute-done | bytes 262176 | tf_op jit(solution)/shard_map/ppermute | solution.py:363
  141.4 1.9 %collective-permute-done.28.refs_12_ = bf16[128,1024]{1,0:T(8,128)(2,1)S(1)} collective-permute-done((bf16[128,1024]{1,0:T(8,128)(2,1)S(1)}, bf16[128,1024]{1,0:T(8,128)(2,1)S(1)}, u32[]{:S(2)}, u32[]{:S(2)}) %collective-permute-start.28) | collective-permute-done | bytes 262176 | tf_op jit(solution)/shard_map/ppermute | solution.py:370
  143.3 0.8 shard_map.156.down
  144.1 1.3 shard_map.157
  145.5 1.3 shard_map.158.hidden
  146.8 1.3 shard_map.159
  148.1 0.5 collective-permute-start.40
  148.8 0.7 collective-permute-start.35
  149.5 0.7 collective-permute-done.40
  150.3 0.8 collective-permute-start.43
  151.6 3.3 %collective-permute-start.41 = (bf16[64,512]{1,0:T(8,128)(2,1)S(1)}, bf16[64,512]{1,0:T(8,128)(2,1)S(1)}, u32[]{:S(2)}, u32[]{:S(2)}) collective-permute-start(bf16[64,512]{1,0:T(8,128)(2,1)S(1)} %slice.106), channel_id=1, source_target_pairs={{0,24},{2,26},{4,28},{6,30},{8,16},{10,18},{12,20},{14,22},{16,8},... | collective-permute-start | bytes 196616 | tf_op jit(solution)/shard_map/ppermute | solution.py:363
  154.9 9.2 %collective-permute-done.43 = bf16[64,1536]{1,0:T(8,128)(2,1)S(1)} collective-permute-done((bf16[64,1536]{1,0:T(8,128)(2,1)S(1)}, bf16[64,1536]{1,0:T(8,128)(2,1)S(1)}, u32[]{:S(2)}, u32[]{:S(2)}) %collective-permute-start.43) | collective-permute-done | bytes 196640 | tf_op jit(solution)/shard_map/ppermute | solution.py:363
  164.3 9.2 %collective-permute-done.44 = bf16[64,1536]{1,0:T(8,128)(2,1)S(1)} collective-permute-done((bf16[64,1536]{1,0:T(8,128)(2,1)S(1)}, bf16[64,1536]{1,0:T(8,128)(2,1)S(1)}, u32[]{:S(2)}, u32[]{:S(2)}) %collective-permute-start.44) | collective-permute-done | bytes 196640 | tf_op jit(solution)/shard_map/ppermute | solution.py:363
  173.7 1.5 collective-permute-done.45
  175.2 0.9 maximum_select_fusion
  (92 shorter events, 2.5 us)
Async XLA Ops:
  0.0 57.5 %copy-start.9 = (f32[128]{0:T(128)S(1)}, f32[128]{0:T(128)}, u32[]{:S(2)}) copy-start(f32[128]{0:T(128)} %param.25) | copy-start | bytes 1540
  0.0 57.5 %copy-start.10 = (f32[64]{0:T(128)S(1)}, f32[64]{0:T(128)}, u32[]{:S(2)}) copy-start(f32[64]{0:T(128)} %param.26) | copy-start | bytes 772
  0.0 57.5 %copy-start.7 = (f32[4]{0:T(128)S(1)}, f32[4]{0:T(128)}, u32[]{:S(2)}) copy-start(f32[4]{0:T(128)} %balance_a.1) | copy-start | bytes 52
  0.0 57.5 %copy-start.8 = (f32[4]{0:T(128)S(1)}, f32[4]{0:T(128)}, u32[]{:S(2)}) copy-start(f32[4]{0:T(128)} %balance_b.1) | copy-start | bytes 52
  0.6 56.9 %copy-start.2 = (s32[3]{0:T(128)S(1)}, s32[3]{0:T(128)}, u32[]{:S(2)}) copy-start(s32[3]{0:T(128)} %pad_add_fusion.index) | copy-start | bytes 40
  4.5 53.1 %copy-start.1 = (bf16[128,576]{1,0:T(8,128)(2,1)S(1)}, bf16[128,576]{1,0:T(8,128)(2,1)}, u32[]{:S(2)}) copy-start(bf16[128,576]{1,0:T(8,128)(2,1)} %get-tuple-element.26.refs_0_) | copy-start | bytes 442372
  4.5 11.7 %collective-permute-start.2 = (bf16[128,576]{1,0:T(8,128)(2,1)}, bf16[128,576]{1,0:T(8,128)(2,1)S(1)}, u32[]{:S(2)}, u32[]{:S(2)}) collective-permute-start(bf16[128,576]{1,0:T(8,128)(2,1)} %get-tuple-element.29), channel_id=1, source_target_pairs={{0,24},{2,26},{4,28},{6,30},{8,16},{10,18},{12,20},{14,22},{16,8},... | collective-permute-start | bytes 442376 | tf_op jit(solution)/shard_map/ppermute | solution.py:363
  9.7 14.2 %collective-permute-start.1 = (bf16[128,576]{1,0:T(8,128)(2,1)}, bf16[128,576]{1,0:T(8,128)(2,1)S(1)}, u32[]{:S(2)}, u32[]{:S(2)}) collective-permute-start(bf16[128,576]{1,0:T(8,128)(2,1)} %get-tuple-element.28), channel_id=1, source_target_pairs={{0,16},{2,18},{4,20},{6,22},{8,24},{10,26},{12,28},{14,30},{16,0},... | collective-permute-start | bytes 442376 | tf_op jit(solution)/shard_map/ppermute | solution.py:363
  9.7 14.2 %collective-permute-start = (bf16[128,576]{1,0:T(8,128)(2,1)}, bf16[128,576]{1,0:T(8,128)(2,1)S(1)}, u32[]{:S(2)}, u32[]{:S(2)}) collective-permute-start(bf16[128,576]{1,0:T(8,128)(2,1)} %get-tuple-element.27), channel_id=1, source_target_pairs={{0,8},{2,10},{4,12},{6,14},{8,0},{10,2},{12,4},{14,6},{16,24},{18,... | collective-permute-start | bytes 442376 | tf_op jit(solution)/shard_map/ppermute | solution.py:363
  13.9 23.4 %collective-permute-start.14 = (bf16[256,1024]{1,0:T(8,128)(2,1)}, bf16[256,1024]{1,0:T(8,128)(2,1)S(1)}, u32[]{:S(2)}, u32[]{:S(2)}) collective-permute-start(bf16[256,1024]{1,0:T(8,128)(2,1)} %get-tuple-element.38), channel_id=1, source_target_pairs={{0,8},{2,10},{4,12},{6,14},{8,0},{10,2},{12,4},{14,6},{16,24},{18,... | collective-permute-start | bytes 1572872 | tf_op jit(solution)/shard_map/ppermute | solution.py:363
  24.0 10.2 %collective-permute-start.4 = (bf16[4,128,384]{2,1,0:T(8,128)(2,1)S(1)}, bf16[4,128,384]{2,1,0:T(8,128)(2,1)S(1)}, u32[]{:S(2)}, u32[]{:S(2)}) collective-permute-start(bf16[4,128,384]{2,1,0:T(8,128)(2,1)S(1)} %pad_maximum_fusion.refs_4_), channel_id=1, source_target_pairs={{0,4},{2,6},{4,0},{6,2},{8,12},{10,14},{12,8},{14,10},{16,20},{18,... | collective-permute-start | bytes 1179656 | tf_op jit(solution)/shard_map/ppermute | solution.py:370
  25.6 10.2 %collective-permute-start.3 = (bf16[4,128,384]{2,1,0:T(8,128)(2,1)S(1)}, bf16[4,128,384]{2,1,0:T(8,128)(2,1)S(1)}, u32[]{:S(2)}, u32[]{:S(2)}) collective-permute-start(bf16[4,128,384]{2,1,0:T(8,128)(2,1)S(1)} %pad_maximum_fusion.refs_4_), channel_id=1, source_target_pairs={{0,2},{2,0},{4,6},{6,4},{8,10},{10,8},{12,14},{14,12},{16,18},{18,... | collective-permute-start | bytes 1179656 | tf_op jit(solution)/shard_map/ppermute | solution.py:370
  27.0 11.9 %collective-permute-start.15 = (bf16[128,1024]{1,0:T(8,128)(2,1)}, bf16[128,1024]{1,0:T(8,128)(2,1)S(1)}, u32[]{:S(2)}, u32[]{:S(2)}) collective-permute-start(bf16[128,1024]{1,0:T(8,128)(2,1)} %get-tuple-element.39), channel_id=1, source_target_pairs={{0,24},{2,26},{4,28},{6,30},{8,16},{10,18},{12,20},{14,22},{16,8},... | collective-permute-start | bytes 786440 | tf_op jit(solution)/shard_map/ppermute | solution.py:363
  29.5 14.2 %collective-permute-start.29 = (bf16[128,1024]{1,0:T(8,128)(2,1)}, bf16[128,1024]{1,0:T(8,128)(2,1)S(1)}, u32[]{:S(2)}, u32[]{:S(2)}) collective-permute-start(bf16[128,1024]{1,0:T(8,128)(2,1)} %get-tuple-element.42), channel_id=1, source_target_pairs={{0,24},{2,26},{4,28},{6,30},{8,16},{10,18},{12,20},{14,22},{16,8},... | collective-permute-start | bytes 786440 | tf_op jit(solution)/shard_map/ppermute | solution.py:363
  34.2 38.2 %collective-permute-start.12 = (bf16[256,1024]{1,0:T(8,128)(2,1)}, bf16[256,1024]{1,0:T(8,128)(2,1)S(1)}, u32[]{:S(2)}, u32[]{:S(2)}) collective-permute-start(bf16[256,1024]{1,0:T(8,128)(2,1)} %get-tuple-element.37.refs_0_), channel_id=1, source_target_pairs={{0,4},{2,6},{4,0},{6,2},{8,12},{10,14},{12,8},{14,10},{16,20},{18,... | collective-permute-start | bytes 1572872 | tf_op jit(solution)/shard_map/ppermute | solution.py:370
  35.7 15.2 %collective-permute-start.5 = (bf16[2,128,384]{2,1,0:T(8,128)(2,1)S(1)}, bf16[2,128,384]{2,1,0:T(8,128)(2,1)S(1)}, u32[]{:S(2)}, u32[]{:S(2)}) collective-permute-start(bf16[2,128,384]{2,1,0:T(8,128)(2,1)S(1)} %slice.93), channel_id=1, source_target_pairs={{0,2},{2,0},{4,6},{6,4},{8,10},{10,8},{12,14},{14,12},{16,18},{18,... | collective-permute-start | bytes 589832 | tf_op jit(solution)/shard_map/ppermute | solution.py:370
  37.3 14.1 %collective-permute-start.6 = (bf16[2,128,384]{2,1,0:T(8,128)(2,1)S(1)}, bf16[2,128,384]{2,1,0:T(8,128)(2,1)S(1)}, u32[]{:S(2)}, u32[]{:S(2)}) collective-permute-start(bf16[2,128,384]{2,1,0:T(8,128)(2,1)S(1)} %slice.94), channel_id=1, source_target_pairs={{0,4},{2,6},{4,0},{6,2},{8,12},{10,14},{12,8},{14,10},{16,20},{18,... | collective-permute-start | bytes 589832 | tf_op jit(solution)/shard_map/ppermute | solution.py:370
  38.9 47.6 %collective-permute-start.11 = (bf16[256,1024]{1,0:T(8,128)(2,1)}, bf16[256,1024]{1,0:T(8,128)(2,1)S(1)}, u32[]{:S(2)}, u32[]{:S(2)}) collective-permute-start(bf16[256,1024]{1,0:T(8,128)(2,1)} %get-tuple-element.37.refs_0_), channel_id=1, source_target_pairs={{0,2},{2,0},{4,6},{6,4},{8,10},{10,8},{12,14},{14,12},{16,18},{18,... | collective-permute-start | bytes 1572872 | tf_op jit(solution)/shard_map/ppermute | solution.py:370
  43.7 28.6 %collective-permute-start.20 = (bf16[256,1024]{1,0:T(8,128)(2,1)}, bf16[256,1024]{1,0:T(8,128)(2,1)S(1)}, u32[]{:S(2)}, u32[]{:S(2)}) collective-permute-start(bf16[256,1024]{1,0:T(8,128)(2,1)} %get-tuple-element.40), channel_id=1, source_target_pairs={{0,16},{2,18},{4,20},{6,22},{8,24},{10,26},{12,28},{14,30},{16,0},... | collective-permute-start | bytes 1572872 | tf_op jit(solution)/shard_map/ppermute | solution.py:363
  50.9 46.7 %collective-permute-start.17 = (bf16[384,1024]{1,0:T(8,128)(2,1)S(1)}, bf16[384,1024]{1,0:T(8,128)(2,1)S(1)}, u32[]{:S(2)}, u32[]{:S(2)}) collective-permute-start(bf16[384,1024]{1,0:T(8,128)(2,1)S(1)} %constant_dynamic-update-slice_fusion.refs_4_), channel_id=1, source_target_pairs={{0,4},{2,6},{4,0},{6,2},{8,12},{10,14},{12,8},{14,10},{16,20},{18,... | collective-permute-start | bytes 2359304 | tf_op jit(solution)/shard_map/ppermute | solution.py:370
  51.4 47.7 %collective-permute-start.16 = (bf16[384,1024]{1,0:T(8,128)(2,1)S(1)}, bf16[384,1024]{1,0:T(8,128)(2,1)S(1)}, u32[]{:S(2)}, u32[]{:S(2)}) collective-permute-start(bf16[384,1024]{1,0:T(8,128)(2,1)S(1)} %constant_dynamic-update-slice_fusion.refs_4_), channel_id=1, source_target_pairs={{0,2},{2,0},{4,6},{6,4},{8,10},{10,8},{12,14},{14,12},{16,18},{18,... | collective-permute-start | bytes 2359304 | tf_op jit(solution)/shard_map/ppermute | solution.py:370
  57.6 27.1 %copy-start.3 = (bf16[512,2048]{1,0:T(8,128)(2,1)S(1)}, bf16[512,2048]{1,0:T(8,128)(2,1)}, u32[]{:S(2)}) copy-start(bf16[512,2048]{1,0:T(8,128)(2,1)} %refs_4_.3) | copy-start | bytes 6291460
  57.6 27.1 %copy-start.4 = (bf16[256,2048]{1,0:T(8,128)(2,1)S(1)}, bf16[256,2048]{1,0:T(8,128)(2,1)}, u32[]{:S(2)}) copy-start(bf16[256,2048]{1,0:T(8,128)(2,1)} %refs_5_.1) | copy-start | bytes 3145732
  72.4 4.3 %collective-permute-start.7 = (bf16[128,192]{1,0:T(8,128)(2,1)S(1)}, bf16[128,192]{1,0:T(8,128)(2,1)S(1)}, u32[]{:S(2)}, u32[]{:S(2)}) collective-permute-start(bf16[128,192]{1,0:T(8,128)(2,1)S(1)} %get-tuple-element.31), channel_id=1, source_target_pairs={{0,8},{2,10},{4,12},{6,14},{8,0},{10,2},{12,4},{14,6},{16,24},{18,... | collective-permute-start | bytes 147464 | tf_op jit(solution)/shard_map/ppermute | solution.py:363
  72.4 5.2 %collective-permute-start.8 = (bf16[128,192]{1,0:T(8,128)(2,1)S(1)}, bf16[128,192]{1,0:T(8,128)(2,1)S(1)}, u32[]{:S(2)}, u32[]{:S(2)}) collective-permute-start(bf16[128,192]{1,0:T(8,128)(2,1)S(1)} %get-tuple-element.32), channel_id=1, source_target_pairs={{0,16},{2,18},{4,20},{6,22},{8,24},{10,26},{12,28},{14,30},{16,0},... | collective-permute-start | bytes 147464 | tf_op jit(solution)/shard_map/ppermute | solution.py:363
  76.6 19.6 %collective-permute-start.22 = (bf16[256,1024]{1,0:T(8,128)(2,1)S(1)}, bf16[256,1024]{1,0:T(8,128)(2,1)S(1)}, u32[]{:S(2)}, u32[]{:S(2)}) collective-permute-start(bf16[256,1024]{1,0:T(8,128)(2,1)S(1)} %collective-permute-done.20.refs_9_), channel_id=1, source_target_pairs={{0,4},{2,6},{4,0},{6,2},{8,12},{10,14},{12,8},{14,10},{16,20},{18,... | collective-permute-start | bytes 1572872 | tf_op jit(solution)/shard_map/ppermute | solution.py:370
  77.6 6.2 %collective-permute-start.9 = (bf16[128,192]{1,0:T(8,128)(2,1)S(1)}, bf16[128,192]{1,0:T(8,128)(2,1)S(1)}, u32[]{:S(2)}, u32[]{:S(2)}) collective-permute-start(bf16[128,192]{1,0:T(8,128)(2,1)S(1)} %get-tuple-element.33), channel_id=1, source_target_pairs={{0,24},{2,26},{4,28},{6,30},{8,16},{10,18},{12,20},{14,22},{16,8},... | collective-permute-start | bytes 147464 | tf_op jit(solution)/shard_map/ppermute | solution.py:363
  83.8 10.3 %collective-permute-start.31 = (bf16[128,1024]{1,0:T(8,128)(2,1)S(1)}, bf16[128,1024]{1,0:T(8,128)(2,1)S(1)}, u32[]{:S(2)}, u32[]{:S(2)}) collective-permute-start(bf16[128,1024]{1,0:T(8,128)(2,1)S(1)} %collective-permute-done.29.refs_13_), channel_id=1, source_target_pairs={{0,4},{2,6},{4,0},{6,2},{8,12},{10,14},{12,8},{14,10},{16,20},{18,... | collective-permute-start | bytes 786440 | tf_op jit(solution)/shard_map/ppermute | solution.py:370
  84.7 12.0 %copy-start.5 = (bf16[128,2048]{1,0:T(8,128)(2,1)S(1)}, bf16[128,2048]{1,0:T(8,128)(2,1)}, u32[]{:S(2)}) copy-start(bf16[128,2048]{1,0:T(8,128)(2,1)} %residual.1) | copy-start | bytes 1572868
  84.7 12.1 %copy-start.6 = (f32[2048]{0:T(1024)S(1)}, f32[2048]{0:T(1024)}, u32[]{:S(2)}) copy-start(f32[2048]{0:T(1024)} %param.29) | copy-start | bytes 24580
  86.5 45.5 %copy-start = (bf16[256,1024]{1,0:T(8,128)(2,1)S(1)}, bf16[256,1024]{1,0:T(8,128)(2,1)}, u32[]{:S(2)}) copy-start(bf16[256,1024]{1,0:T(8,128)(2,1)} %get-tuple-element.37.refs_0_) | copy-start | bytes 1572868
  86.6 8.1 %collective-permute-start.10 = (bf16[64,2048]{1,0:T(8,128)(2,1)S(1)}, bf16[64,2048]{1,0:T(8,128)(2,1)S(1)}, u32[]{:S(2)}, u32[]{:S(2)}) collective-permute-start(bf16[64,2048]{1,0:T(8,128)(2,1)S(1)} %get-tuple-element.35), channel_id=1, source_target_pairs={{0,1},{1,0},{2,3},{3,2},{4,5},{5,4},{6,7},{7,6},{8,9},{9,8},{10,11... | collective-permute-start | bytes 786440 | tf_op jit(solution)/shard_map/ppermute | solution.py:373
  94.1 26.5 %collective-permute-start.21 = (bf16[256,1024]{1,0:T(8,128)(2,1)S(1)}, bf16[256,1024]{1,0:T(8,128)(2,1)S(1)}, u32[]{:S(2)}, u32[]{:S(2)}) collective-permute-start(bf16[256,1024]{1,0:T(8,128)(2,1)S(1)} %collective-permute-done.20.refs_9_), channel_id=1, source_target_pairs={{0,2},{2,0},{4,6},{6,4},{8,10},{10,8},{12,14},{14,12},{16,18},{18,... | collective-permute-start | bytes 1572872 | tf_op jit(solution)/shard_map/ppermute | solution.py:370
  94.6 19.8 %collective-permute-start.30 = (bf16[128,1024]{1,0:T(8,128)(2,1)S(1)}, bf16[128,1024]{1,0:T(8,128)(2,1)S(1)}, u32[]{:S(2)}, u32[]{:S(2)}) collective-permute-start(bf16[128,1024]{1,0:T(8,128)(2,1)S(1)} %collective-permute-done.29.refs_13_), channel_id=1, source_target_pairs={{0,2},{2,0},{4,6},{6,4},{8,10},{10,8},{12,14},{14,12},{16,18},{18,... | collective-permute-start | bytes 786440 | tf_op jit(solution)/shard_map/ppermute | solution.py:370
  96.2 23.9 %collective-permute-start.13 = (bf16[128,1024]{1,0:T(8,128)(2,1)S(1)}, bf16[128,1024]{1,0:T(8,128)(2,1)S(1)}, u32[]{:S(2)}, u32[]{:S(2)}) collective-permute-start(bf16[128,1024]{1,0:T(8,128)(2,1)S(1)} %slice.95), channel_id=1, source_target_pairs={{0,2},{2,0},{4,6},{6,4},{8,10},{10,8},{12,14},{14,12},{16,18},{18,... | collective-permute-start | bytes 786440 | tf_op jit(solution)/shard_map/ppermute | solution.py:370
  97.6 28.1 %collective-permute-start.23 = (bf16[128,1024]{1,0:T(8,128)(2,1)S(1)}, bf16[128,1024]{1,0:T(8,128)(2,1)S(1)}, u32[]{:S(2)}, u32[]{:S(2)}) collective-permute-start(bf16[128,1024]{1,0:T(8,128)(2,1)S(1)} %slice.98), channel_id=1, source_target_pairs={{0,2},{2,0},{4,6},{6,4},{8,10},{10,8},{12,14},{14,12},{16,18},{18,... | collective-permute-start | bytes 786440 | tf_op jit(solution)/shard_map/ppermute | solution.py:370
  99.2 26.6 %collective-permute-start.24 = (bf16[64,2048]{1,0:T(8,128)(2,1)S(1)}, bf16[64,2048]{1,0:T(8,128)(2,1)S(1)}, u32[]{:S(2)}, u32[]{:S(2)}) collective-permute-start(bf16[64,2048]{1,0:T(8,128)(2,1)S(1)} %get-tuple-element.41.refs_1_), channel_id=1, source_target_pairs={{0,8},{2,10},{4,12},{6,14},{8,0},{10,2},{12,4},{14,6},{16,24},{18,... | collective-permute-start | bytes 786440 | tf_op jit(solution)/shard_map/ppermute | solution.py:363
  114.5 16.7 %collective-permute-start.18 = (bf16[192,1024]{1,0:T(8,128)(2,1)S(1)}, bf16[192,1024]{1,0:T(8,128)(2,1)S(1)}, u32[]{:S(2)}, u32[]{:S(2)}) collective-permute-start(bf16[192,1024]{1,0:T(8,128)(2,1)S(1)} %slice.96), channel_id=1, source_target_pairs={{0,2},{2,0},{4,6},{6,4},{8,10},{10,8},{12,14},{14,12},{16,18},{18,... | collective-permute-start | bytes 1179656 | tf_op jit(solution)/shard_map/ppermute | solution.py:370
  120.1 11.1 %collective-permute-start.19 = (bf16[192,1024]{1,0:T(8,128)(2,1)S(1)}, bf16[192,1024]{1,0:T(8,128)(2,1)S(1)}, u32[]{:S(2)}, u32[]{:S(2)}) collective-permute-start(bf16[192,1024]{1,0:T(8,128)(2,1)S(1)} %slice.97), channel_id=1, source_target_pairs={{0,4},{2,6},{4,0},{6,2},{8,12},{10,14},{12,8},{14,10},{16,20},{18,... | collective-permute-start | bytes 1179656 | tf_op jit(solution)/shard_map/ppermute | solution.py:370
  120.6 12.2 %collective-permute-start.36 = (bf16[64,2048]{1,0:T(8,128)(2,1)S(1)}, bf16[64,2048]{1,0:T(8,128)(2,1)S(1)}, u32[]{:S(2)}, u32[]{:S(2)}) collective-permute-start(bf16[64,2048]{1,0:T(8,128)(2,1)S(1)} %get-tuple-element.41.refs_1_), channel_id=1, source_target_pairs={{0,16},{2,18},{4,20},{6,22},{8,24},{10,26},{12,28},{14,30},{16,0},... | collective-permute-start | bytes 786440 | tf_op jit(solution)/shard_map/ppermute | solution.py:363
  125.7 9.2 %collective-permute-start.26 = (bf16[64,2048]{1,0:T(8,128)(2,1)S(1)}, bf16[64,2048]{1,0:T(8,128)(2,1)S(1)}, u32[]{:S(2)}, u32[]{:S(2)}) collective-permute-start(bf16[64,2048]{1,0:T(8,128)(2,1)S(1)} %get-tuple-element.41.refs_1_), channel_id=1, source_target_pairs={{0,1},{1,0},{2,3},{3,2},{4,5},{5,4},{6,7},{7,6},{8,9},{9,8},{10,11... | collective-permute-start | bytes 786440 | tf_op jit(solution)/shard_map/ppermute | solution.py:373
  125.7 9.3 %collective-permute-start.25 = (bf16[64,2048]{1,0:T(8,128)(2,1)S(1)}, bf16[64,2048]{1,0:T(8,128)(2,1)S(1)}, u32[]{:S(2)}, u32[]{:S(2)}) collective-permute-start(bf16[64,2048]{1,0:T(8,128)(2,1)S(1)} %collective-permute-done.24.refs_0_), channel_id=1, source_target_pairs={{0,1},{1,0},{2,3},{3,2},{4,5},{5,4},{6,7},{7,6},{8,9},{9,8},{10,11... | collective-permute-start | bytes 786440 | tf_op jit(solution)/shard_map/ppermute | solution.py:373
  131.2 10.2 %collective-permute-start.27 = (bf16[128,1024]{1,0:T(8,128)(2,1)S(1)}, bf16[128,1024]{1,0:T(8,128)(2,1)S(1)}, u32[]{:S(2)}, u32[]{:S(2)}) collective-permute-start(bf16[128,1024]{1,0:T(8,128)(2,1)S(1)} %slice.99), channel_id=1, source_target_pairs={{0,4},{2,6},{4,0},{6,2},{8,12},{10,14},{12,8},{14,10},{16,20},{18,... | collective-permute-start | bytes 786440 | tf_op jit(solution)/shard_map/ppermute | solution.py:370
  131.2 5.3 %collective-permute-start.32 = (bf16[64,1024]{1,0:T(8,128)(2,1)S(1)}, bf16[64,1024]{1,0:T(8,128)(2,1)S(1)}, u32[]{:S(2)}, u32[]{:S(2)}) collective-permute-start(bf16[64,1024]{1,0:T(8,128)(2,1)S(1)} %slice.101), channel_id=1, source_target_pairs={{0,2},{2,0},{4,6},{6,4},{8,10},{10,8},{12,14},{14,12},{16,18},{18,... | collective-permute-start | bytes 393224 | tf_op jit(solution)/shard_map/ppermute | solution.py:370
  132.8 8.6 %collective-permute-start.33 = (bf16[64,1024]{1,0:T(8,128)(2,1)S(1)}, bf16[64,1024]{1,0:T(8,128)(2,1)S(1)}, u32[]{:S(2)}, u32[]{:S(2)}) collective-permute-start(bf16[64,1024]{1,0:T(8,128)(2,1)S(1)} %slice.102), channel_id=1, source_target_pairs={{0,4},{2,6},{4,0},{6,2},{8,12},{10,14},{12,8},{14,10},{16,20},{18,... | collective-permute-start | bytes 393224 | tf_op jit(solution)/shard_map/ppermute | solution.py:370
  134.9 8.4 %collective-permute-start.28 = (bf16[128,1024]{1,0:T(8,128)(2,1)S(1)}, bf16[128,1024]{1,0:T(8,128)(2,1)S(1)}, u32[]{:S(2)}, u32[]{:S(2)}) collective-permute-start(bf16[128,1024]{1,0:T(8,128)(2,1)S(1)} %slice.100), channel_id=1, source_target_pairs={{0,4},{2,6},{4,0},{6,2},{8,12},{10,14},{12,8},{14,10},{16,20},{18,... | collective-permute-start | bytes 786440 | tf_op jit(solution)/shard_map/ppermute | solution.py:370
  135.0 6.4 %collective-permute-start.37 = (bf16[64,2048]{1,0:T(8,128)(2,1)S(1)}, bf16[64,2048]{1,0:T(8,128)(2,1)S(1)}, u32[]{:S(2)}, u32[]{:S(2)}) collective-permute-start(bf16[64,2048]{1,0:T(8,128)(2,1)S(1)} %collective-permute-done.36.refs_1_), channel_id=1, source_target_pairs={{0,8},{2,10},{4,12},{6,14},{8,0},{10,2},{12,4},{14,6},{16,24},{18,... | collective-permute-start | bytes 786440 | tf_op jit(solution)/shard_map/ppermute | solution.py:363
  136.6 8.9 %collective-permute-start.39 = (bf16[64,2048]{1,0:T(8,128)(2,1)S(1)}, bf16[64,2048]{1,0:T(8,128)(2,1)S(1)}, u32[]{:S(2)}, u32[]{:S(2)}) collective-permute-start(bf16[64,2048]{1,0:T(8,128)(2,1)S(1)} %collective-permute-done.36.refs_1_), channel_id=1, source_target_pairs={{0,1},{1,0},{2,3},{3,2},{4,5},{5,4},{6,7},{7,6},{8,9},{9,8},{10,11... | collective-permute-start | bytes 786440 | tf_op jit(solution)/shard_map/ppermute | solution.py:373
  141.4 4.1 %collective-permute-start.38 = (bf16[64,2048]{1,0:T(8,128)(2,1)S(1)}, bf16[64,2048]{1,0:T(8,128)(2,1)S(1)}, u32[]{:S(2)}, u32[]{:S(2)}) collective-permute-start(bf16[64,2048]{1,0:T(8,128)(2,1)S(1)} %collective-permute-done.37.refs_0_), channel_id=1, source_target_pairs={{0,1},{1,0},{2,3},{3,2},{4,5},{5,4},{6,7},{7,6},{8,9},{9,8},{10,11... | collective-permute-start | bytes 786440 | tf_op jit(solution)/shard_map/ppermute | solution.py:373
  145.4 3.2 %collective-permute-start.34 = (bf16[2,64,2048]{2,1,0:T(8,128)(2,1)S(1)}, bf16[2,64,2048]{2,1,0:T(8,128)(2,1)S(1)}, u32[]{:S(2)}, u32[]{:S(2)}) collective-permute-start(bf16[2,64,2048]{2,1,0:T(8,128)(2,1)S(1)} %get-tuple-element.44), channel_id=1, source_target_pairs={{0,1},{1,0},{2,3},{3,2},{4,5},{5,4},{6,7},{7,6},{8,9},{9,8},{10,11... | collective-permute-start | bytes 1572872 | tf_op jit(solution)/shard_map/ppermute | solution.py:373
  148.1 2.1 %collective-permute-start.40 = (bf16[2,64,2048]{2,1,0:T(8,128)(2,1)S(1)}, bf16[2,64,2048]{2,1,0:T(8,128)(2,1)S(1)}, u32[]{:S(2)}, u32[]{:S(2)}) collective-permute-start(bf16[2,64,2048]{2,1,0:T(8,128)(2,1)S(1)} %get-tuple-element.46), channel_id=1, source_target_pairs={{0,1},{1,0},{2,3},{3,2},{4,5},{5,4},{6,7},{7,6},{8,9},{9,8},{10,11... | collective-permute-start | bytes 1572872 | tf_op jit(solution)/shard_map/ppermute | solution.py:373
  148.8 24.7 %collective-permute-start.35 = (bf16[64,2048]{1,0:T(8,128)(2,1)S(1)}, bf16[64,2048]{1,0:T(8,128)(2,1)S(1)}, u32[]{:S(2)}, u32[]{:S(2)}) collective-permute-start(bf16[64,2048]{1,0:T(8,128)(2,1)S(1)} %fusion.5), channel_id=1, source_target_pairs={{0,8},{2,10},{4,12},{6,14},{8,0},{10,2},{12,4},{14,6},{16,24},{18,... | collective-permute-start | bytes 786440 | tf_op jit(solution)/shard_map/ppermute | solution.py:363
  150.3 13.8 %collective-permute-start.43 = (bf16[64,1536]{1,0:T(8,128)(2,1)S(1)}, bf16[64,1536]{1,0:T(8,128)(2,1)S(1)}, u32[]{:S(2)}, u32[]{:S(2)}) collective-permute-start(bf16[64,1536]{1,0:T(8,128)(2,1)S(1)} %slice.110), channel_id=1, source_target_pairs={{0,8},{2,10},{4,12},{6,14},{8,0},{10,2},{12,4},{14,6},{16,24},{18,... | collective-permute-start | bytes 589832 | tf_op jit(solution)/shard_map/ppermute | solution.py:363
  151.2 13.0 %collective-permute-start.42 = (bf16[64,512]{1,0:T(8,128)(2,1)S(1)}, bf16[64,512]{1,0:T(8,128)(2,1)S(1)}, u32[]{:S(2)}, u32[]{:S(2)}) collective-permute-start(bf16[64,512]{1,0:T(8,128)(2,1)S(1)} %slice.135), channel_id=1, source_target_pairs={{0,16},{2,18},{4,20},{6,22},{8,24},{10,26},{12,28},{14,30},{16,0},... | collective-permute-start | bytes 196616 | tf_op jit(solution)/shard_map/ppermute | solution.py:363
  151.6 12.7 %collective-permute-start.41 = (bf16[64,512]{1,0:T(8,128)(2,1)S(1)}, bf16[64,512]{1,0:T(8,128)(2,1)S(1)}, u32[]{:S(2)}, u32[]{:S(2)}) collective-permute-start(bf16[64,512]{1,0:T(8,128)(2,1)S(1)} %slice.106), channel_id=1, source_target_pairs={{0,24},{2,26},{4,28},{6,30},{8,16},{10,18},{12,20},{14,22},{16,8},... | collective-permute-start | bytes 196616 | tf_op jit(solution)/shard_map/ppermute | solution.py:363
  164.2 9.3 %collective-permute-start.44 = (bf16[64,1536]{1,0:T(8,128)(2,1)S(1)}, bf16[64,1536]{1,0:T(8,128)(2,1)S(1)}, u32[]{:S(2)}, u32[]{:S(2)}) collective-permute-start(bf16[64,1536]{1,0:T(8,128)(2,1)S(1)} %fusion.4), channel_id=1, source_target_pairs={{0,16},{2,18},{4,20},{6,22},{8,24},{10,26},{12,28},{14,30},{16,0},... | collective-permute-start | bytes 589832 | tf_op jit(solution)/shard_map/ppermute | solution.py:363
  173.6 1.6 collective-permute-start.45

commit v6 on v5

--- a/solution.py
+++ b/solution.py
@@ -130,9 +130,10 @@
     return [pl.BlockSpec(memory_space=VMEM)] * count
 
 
-def pack_kernel(slots, index, *refs):
+def pack_kernel(slots, plane, *refs):
     sources, outs, held = refs[:6], refs[6 : 6 + slots], refs[6 + slots : -2]
     packed, arrived = refs[-2:]
+    z = lax.axis_index("sp") // plane
     copies = [
         pltpu.make_async_copy(source, target, arrived.at[i])
         for i, (source, target) in enumerate(zip(sources, held))
@@ -150,17 +151,18 @@
         packed[head, :, 384:512] = query_a[:, head, :]
         packed[head, :, 512:576] = query_b[head].T
     for k in range(slots):
-        outs[k][...] = packed[index[0] ^ k]
-
-
-def cut_kernel(slots, width, index, *refs):
+        outs[k][...] = packed[z ^ k]
+
+
+def cut_kernel(slots, plane, width, *refs):
     weights, pairs, lasts = refs[:2], refs[2 : 1 + slots], refs[1 + slots : -1]
     arrived = refs[-1]
+    z = lax.axis_index("sp") // plane
     block = weights[0].shape[0]
     copies = []
     for i, (weight, last) in enumerate(zip(weights, lasts)):
         for k in range(slots):
-            place = pl.ds(pl.multiple_of((index[0] ^ k) * width, width), width)
+            place = pl.ds(pl.multiple_of((z ^ k) * width, width), width)
             target = last if k == slots - 1 else pairs[k].at[pl.ds(i * block, block), :]
             copies.append(
                 pltpu.make_async_copy(weight.at[:, place], target, arrived.at[i * slots + k])
@@ -384,26 +386,26 @@
         query_second.transpose(1, 2, 0),
     )
     packed = pl.pallas_call(
-        functools.partial(pack_kernel, slots),
+        functools.partial(pack_kernel, slots, plane),
         out_shape=(jax.ShapeDtypeStruct((tokens, 576), jnp.bfloat16),) * slots,
-        in_specs=[smem] + [pl.BlockSpec(memory_space=pltpu.HBM)] * 6,
+        in_specs=[pl.BlockSpec(memory_space=pltpu.HBM)] * 6,
         out_specs=tuple(vmem_specs(slots)),
         scratch_shapes=[VMEM(source.shape, jnp.bfloat16) for source in sources]
         + [VMEM((slots, tokens, 576), jnp.bfloat16), pltpu.SemaphoreType.DMA((6,))],
         cost_estimate=pl.CostEstimate(flops=10**8, bytes_accessed=10**6, transcendentals=0),
         name="pack",
-    )(index, *sources)
+    )(*sources)
     piece_shape = jax.ShapeDtypeStruct((block, hidden), jnp.bfloat16)
     cuts = pl.pallas_call(
-        functools.partial(cut_kernel, slots, hidden),
+        functools.partial(cut_kernel, slots, plane, hidden),
         out_shape=(jax.ShapeDtypeStruct((2 * block, hidden), jnp.bfloat16),) * (slots - 1)
         + (piece_shape,) * 2,
-        in_specs=[smem] + [pl.BlockSpec(memory_space=pltpu.HBM)] * 2,
+        in_specs=[pl.BlockSpec(memory_space=pltpu.HBM)] * 2,
         out_specs=tuple(vmem_specs(slots + 1)),
         scratch_shapes=[pltpu.SemaphoreType.DMA((2 * slots,))],
         cost_estimate=pl.CostEstimate(flops=10**8, bytes_accessed=10**6, transcendentals=0),
         name="cut",
-    )(index, up_weight, down_weight)
+    )(up_weight, down_weight)
     early, middle, distant, last_ups, last_downs = cuts
     got = [along(packed[k], k) for k in range(slots)]
     keyval = jnp.stack([piece[:, :384] for piece in got])

time: 176 us -> 175 us (level)
  no operation moved by 1% of the time
where the time goes in v6:
time: 175 us
  waiting for transfers between devices  96 us (55%)
  starting transfers between devices  53.6 us (31%)
  Pallas kernels  21.8 us (12%)
    ppermute x18, waiting for transfers between devices, along(): lax.ppermute(value, 'sp', [(i, (i // plane ^ k) * plane + i % plane) for...  51.1 us
    ppermute x20, waiting for transfers between devices, across(): return lax.ppermute(value, 'sp', [(i, i ^ k) for i in range(count)])  42.7 us
    ppermute x18, starting transfers between devices, along(): lax.ppermute(value, 'sp', [(i, (i // plane ^ k) * plane + i % plane) for...  27.7 us
    ppermute x20, starting transfers between devices, across(): return lax.ppermute(value, 'sp', [(i, i ^ k) for i in range(count)])  24.6 us
    pallas_call x1, Pallas kernels, fast_body(): pl.pallas_call(functools.partial(attend_kernel, slots, plane, tokens), ou...  6.39 us
  transfers between devices with their start and end apart: 46, of which 19 were waited for; matrix products, arithmetic and copies ran while one was open for 1% of the time, Pallas kernels for 11%

profile of v6, /device:TPU:0, one launch (start us, length us, event | category | flops | bytes accessed | tf_op | source)
XLA Modules:
  0.0 174.8 jit_solution(14862334551600224675)
XLA Ops:
  0.0 3.2 %pack.1 = (bf16[128,576]{1,0:T(8,128)(2,1)}, bf16[128,576]{1,0:T(8,128)(2,1)}, bf16[128,576]{1,0:T(8,128)(2,1)}, bf16[128,576]{1,0:T(8,128)(2,1)}) custom-call(bf16[128,4,128]{2,1,0:T(4,128)(2,1)} %refs_0_.2, bf16[4,64,128]{2,1,0:T(8,128)(2,1)} %bitcast.36, bf16[4,64,128]{2,1,0:T(8,128)(2,1)} %bitcast.37, bf16[128,4,128]{2,1,0:T(4,128)(2,1)} %refs_3_.1, ...), custom_call_target="tpu_custom_call" | custom-call | flops 100000000 | bytes 1000000 | tf_op jit(solution)/shard_map/pack/pallas_call | solution.py:388
  3.2 5.1 %collective-permute-start.2 = (bf16[128,576]{1,0:T(8,128)(2,1)}, bf16[128,576]{1,0:T(8,128)(2,1)S(1)}, u32[]{:S(2)}, u32[]{:S(2)}) collective-permute-start(bf16[128,576]{1,0:T(8,128)(2,1)} %get-tuple-element.29), channel_id=1, source_target_pairs={{0,24},{2,26},{4,28},{6,30},{8,16},{10,18},{12,20},{14,22},{16,8},... | collective-permute-start | bytes 442376 | tf_op jit(solution)/shard_map/ppermute | solution.py:365
  8.3 0.6 collective-permute-start
  9.0 2.9 %cut.1 = (bf16[256,1024]{1,0:T(8,128)(2,1)}, bf16[256,1024]{1,0:T(8,128)(2,1)}, bf16[256,1024]{1,0:T(8,128)(2,1)}, bf16[128,1024]{1,0:T(8,128)(2,1)}, bf16[128,1024]{1,0:T(8,128)(2,1)}) custom-call(bf16[128,4096]{1,0:T(8,128)(2,1)} %refs_0_.3, bf16[128,4096]{1,0:T(8,128)(2,1)} %refs_1_.1), custom_call_target="tpu_custom_call" | custom-call | flops 100000000 | bytes 1000000 | tf_op jit(solution)/shard_map/cut/pallas_call | solution.py:399
  11.9 1.5 collective-permute-start.14
  13.3 0.9 slice_bitcast_fusion.5
  14.3 8.3 %collective-permute-done.1.refs_2_ = bf16[128,576]{1,0:T(8,128)(2,1)S(1)} collective-permute-done((bf16[128,576]{1,0:T(8,128)(2,1)}, bf16[128,576]{1,0:T(8,128)(2,1)S(1)}, u32[]{:S(2)}, u32[]{:S(2)}) %collective-permute-start.1) | collective-permute-done | bytes 147488 | tf_op jit(solution)/shard_map/ppermute | solution.py:365
  22.6 1.6 collective-permute-start.4
  24.2 1.5 collective-permute-start.3
  25.7 2.5 %collective-permute-start.15 = (bf16[128,1024]{1,0:T(8,128)(2,1)}, bf16[128,1024]{1,0:T(8,128)(2,1)S(1)}, u32[]{:S(2)}, u32[]{:S(2)}) collective-permute-start(bf16[128,1024]{1,0:T(8,128)(2,1)} %get-tuple-element.39), channel_id=1, source_target_pairs={{0,24},{2,26},{4,28},{6,30},{8,16},{10,18},{12,20},{14,22},{16,8},... | collective-permute-start | bytes 786440 | tf_op jit(solution)/shard_map/ppermute | solution.py:365
  28.2 1.3 collective-permute-start.29
  29.6 3.2 %collective-permute-done.4.refs_6_ = bf16[4,128,384]{2,1,0:T(8,128)(2,1)S(1)} collective-permute-done((bf16[4,128,384]{2,1,0:T(8,128)(2,1)S(1)}, bf16[4,128,384]{2,1,0:T(8,128)(2,1)S(1)}, u32[]{:S(2)}, u32[]{:S(2)}) %collective-permute-start.4) | collective-permute-done | bytes 393248 | tf_op jit(solution)/shard_map/ppermute | solution.py:372
  32.8 1.5 collective-permute-start.12
  34.4 1.6 collective-permute-start.5
  36.0 0.6 collective-permute-start.6
  36.6 1.0 collective-permute-done.15
  37.6 1.7 collective-permute-start.11
  39.3 3.1 %collective-permute-done.29.refs_13_ = bf16[128,1024]{1,0:T(8,128)(2,1)S(1)} collective-permute-done((bf16[128,1024]{1,0:T(8,128)(2,1)}, bf16[128,1024]{1,0:T(8,128)(2,1)S(1)}, u32[]{:S(2)}, u32[]{:S(2)}) %collective-permute-start.29) | collective-permute-done | bytes 262176 | tf_op jit(solution)/shard_map/ppermute | solution.py:365
  42.4 7.2 %collective-permute-start.20 = (bf16[256,1024]{1,0:T(8,128)(2,1)}, bf16[256,1024]{1,0:T(8,128)(2,1)S(1)}, u32[]{:S(2)}, u32[]{:S(2)}) collective-permute-start(bf16[256,1024]{1,0:T(8,128)(2,1)} %get-tuple-element.40), channel_id=1, source_target_pairs={{0,16},{2,18},{4,20},{6,22},{8,24},{10,26},{12,28},{14,30},{16,0},... | collective-permute-start | bytes 1572872 | tf_op jit(solution)/shard_map/ppermute | solution.py:365
  49.6 0.5 collective-permute-start.17
  50.1 6.1 %collective-permute-start.16 = (bf16[384,1024]{1,0:T(8,128)(2,1)S(1)}, bf16[384,1024]{1,0:T(8,128)(2,1)S(1)}, u32[]{:S(2)}, u32[]{:S(2)}) collective-permute-start(bf16[384,1024]{1,0:T(8,128)(2,1)S(1)} %constant_dynamic-update-slice_fusion.refs_4_), channel_id=1, source_target_pairs={{0,2},{2,0},{4,6},{6,4},{8,10},{10,8},{12,14},{14,12},{16,18},{18,... | collective-permute-start | bytes 2359304 | tf_op jit(solution)/shard_map/ppermute | solution.py:372
  56.2 6.4 %attend.1 = (bf16[128,192]{1,0:T(8,128)(2,1)S(1)}, bf16[128,192]{1,0:T(8,128)(2,1)S(1)}, bf16[128,192]{1,0:T(8,128)(2,1)S(1)}, bf16[128,192]{1,0:T(8,128)(2,1)S(1)}) custom-call(s32[3]{0:T(128)S(1)} %pad_add_fusion.index, f32[4]{0:T(128)S(1)} %copy-done.6, f32[4]{0:T(128)S(1)} %copy-done.7, f32[1,128]{1,0:T(1,128)S(1)} %bitcast.34, f32[1,64]{1,0:T(1,128)S(1)} %bitcast.35, ...), custom_call_target="tpu_custom_call" | custom-call | flops 8000000000 | bytes 2000000 | tf_op jit(solution)/shard_map/attend/pallas_call | solution.py:475
  62.6 8.4 %collective-permute-done.20.refs_9_ = bf16[256,1024]{1,0:T(8,128)(2,1)S(1)} collective-permute-done((bf16[256,1024]{1,0:T(8,128)(2,1)}, bf16[256,1024]{1,0:T(8,128)(2,1)S(1)}, u32[]{:S(2)}, u32[]{:S(2)}) %collective-permute-start.20) | collective-permute-done | bytes 524320 | tf_op jit(solution)/shard_map/ppermute | solution.py:365
  71.0 2.1 %collective-permute-start.8 = (bf16[128,192]{1,0:T(8,128)(2,1)S(1)}, bf16[128,192]{1,0:T(8,128)(2,1)S(1)}, u32[]{:S(2)}, u32[]{:S(2)}) collective-permute-start(bf16[128,192]{1,0:T(8,128)(2,1)S(1)} %get-tuple-element.32), channel_id=1, source_target_pairs={{0,16},{2,18},{4,20},{6,22},{8,24},{10,26},{12,28},{14,30},{16,0},... | collective-permute-start | bytes 147464 | tf_op jit(solution)/shard_map/ppermute | solution.py:365
  73.1 2.2 %collective-permute-done.7.refs_1_ = bf16[128,192]{1,0:T(8,128)(2,1)S(1)} collective-permute-done((bf16[128,192]{1,0:T(8,128)(2,1)S(1)}, bf16[128,192]{1,0:T(8,128)(2,1)S(1)}, u32[]{:S(2)}, u32[]{:S(2)}) %collective-permute-start.7) | collective-permute-done | bytes 49184 | tf_op jit(solution)/shard_map/ppermute | solution.py:365
  75.3 0.5 collective-permute-start.22
  75.8 0.5 collective-permute-done.8.refs_2_
  76.3 1.5 collective-permute-start.9
  77.7 4.7 %collective-permute-done.9.refs_3_ = bf16[128,192]{1,0:T(8,128)(2,1)S(1)} collective-permute-done((bf16[128,192]{1,0:T(8,128)(2,1)S(1)}, bf16[128,192]{1,0:T(8,128)(2,1)S(1)}, u32[]{:S(2)}, u32[]{:S(2)}) %collective-permute-start.9) | collective-permute-done | bytes 49184 | tf_op jit(solution)/shard_map/ppermute | solution.py:365
  82.4 1.0 collective-permute-start.31
  83.4 1.8 %project.1 = (bf16[64,2048]{1,0:T(8,128)(2,1)S(1)}, bf16[64,2048]{1,0:T(8,128)(2,1)S(1)}) custom-call(s32[3]{0:T(128)S(1)} %pad_add_fusion.index, bf16[128,192]{1,0:T(8,128)(2,1)S(1)} %get-tuple-element.30.refs_0_, bf16[128,192]{1,0:T(8,128)(2,1)S(1)} %collective-permute-done.7.refs_1_, bf16[128,192]{1,0:T(8,128)(2,1)S(1)} %collective-permute-done.8.refs_2_, ...), custom_call_target="tpu_custom_call" | custom-call | flops 2000000000 | bytes 4000000 | tf_op jit(solution)/shard_map/project/pallas_call | solution.py:500
  85.3 7.5 %collective-permute-done.31.refs_15_ = bf16[128,1024]{1,0:T(8,128)(2,1)S(1)} collective-permute-done((bf16[128,1024]{1,0:T(8,128)(2,1)S(1)}, bf16[128,1024]{1,0:T(8,128)(2,1)S(1)}, u32[]{:S(2)}, u32[]{:S(2)}) %collective-permute-start.31) | collective-permute-done | bytes 262176 | tf_op jit(solution)/shard_map/ppermute | solution.py:372
  92.7 0.5 collective-permute-start.21
  93.3 1.6 collective-permute-start.30
  94.9 0.5 collective-permute-start.13
  95.5 0.8 norm.1
  96.3 1.6 collective-permute-start.23
  98.2 15.0 %collective-permute-done.30.refs_14_ = bf16[128,1024]{1,0:T(8,128)(2,1)S(1)} collective-permute-done((bf16[128,1024]{1,0:T(8,128)(2,1)S(1)}, bf16[128,1024]{1,0:T(8,128)(2,1)S(1)}, u32[]{:S(2)}, u32[]{:S(2)}) %collective-permute-start.30) | collective-permute-done | bytes 262176 | tf_op jit(solution)/shard_map/ppermute | solution.py:372
  113.2 0.5 collective-permute-start.18
  113.7 5.1 %collective-permute-done.13.refs_3_ = bf16[128,1024]{1,0:T(8,128)(2,1)S(1)} collective-permute-done((bf16[128,1024]{1,0:T(8,128)(2,1)S(1)}, bf16[128,1024]{1,0:T(8,128)(2,1)S(1)}, u32[]{:S(2)}, u32[]{:S(2)}) %collective-permute-start.13) | collective-permute-done | bytes 262176 | tf_op jit(solution)/shard_map/ppermute | solution.py:372
  118.8 0.5 collective-permute-start.19
  119.3 5.1 %collective-permute-done.23.refs_12_ = bf16[128,1024]{1,0:T(8,128)(2,1)S(1)} collective-permute-done((bf16[128,1024]{1,0:T(8,128)(2,1)S(1)}, bf16[128,1024]{1,0:T(8,128)(2,1)S(1)}, u32[]{:S(2)}, u32[]{:S(2)}) %collective-permute-start.23) | collective-permute-done | bytes 262176 | tf_op jit(solution)/shard_map/ppermute | solution.py:372
  124.4 0.5 collective-permute-start.25
  125.0 4.9 %collective-permute-done.18.refs_7_ = bf16[192,1024]{1,0:T(8,128)(2,1)S(1)} collective-permute-done((bf16[192,1024]{1,0:T(8,128)(2,1)S(1)}, bf16[192,1024]{1,0:T(8,128)(2,1)S(1)}, u32[]{:S(2)}, u32[]{:S(2)}) %collective-permute-start.18) | collective-permute-done | bytes 393248 | tf_op jit(solution)/shard_map/ppermute | solution.py:372
  129.9 0.8 collective-permute-start.32
  130.7 0.8 shard_map.154.up
  131.5 2.1 %collective-permute-start.33 = (bf16[64,1024]{1,0:T(8,128)(2,1)S(1)}, bf16[64,1024]{1,0:T(8,128)(2,1)S(1)}, u32[]{:S(2)}, u32[]{:S(2)}) collective-permute-start(bf16[64,1024]{1,0:T(8,128)(2,1)S(1)} %slice.102), channel_id=1, source_target_pairs={{0,4},{2,6},{4,0},{6,2},{8,12},{10,14},{12,8},{14,10},{16,20},{18,... | collective-permute-start | bytes 393224 | tf_op jit(solution)/shard_map/ppermute | solution.py:372
  134.0 1.3 shard_map.155.hidden
  135.3 4.7 %collective-permute-done.37.refs_0_ = bf16[64,2048]{1,0:T(8,128)(2,1)S(1)} collective-permute-done((bf16[64,2048]{1,0:T(8,128)(2,1)S(1)}, bf16[64,2048]{1,0:T(8,128)(2,1)S(1)}, u32[]{:S(2)}, u32[]{:S(2)}) %collective-permute-start.37) | collective-permute-done | bytes 262176 | tf_op jit(solution)/shard_map/ppermute | solution.py:365
  140.1 1.9 %collective-permute-done.28.refs_12_ = bf16[128,1024]{1,0:T(8,128)(2,1)S(1)} collective-permute-done((bf16[128,1024]{1,0:T(8,128)(2,1)S(1)}, bf16[128,1024]{1,0:T(8,128)(2,1)S(1)}, u32[]{:S(2)}, u32[]{:S(2)}) %collective-permute-start.28) | collective-permute-done | bytes 262176 | tf_op jit(solution)/shard_map/ppermute | solution.py:372
  141.9 0.8 shard_map.156.down
  142.8 1.3 shard_map.157
  144.2 1.3 shard_map.158.hidden
  145.4 1.3 shard_map.159
  146.7 0.6 collective-permute-start.40
  147.5 0.7 collective-permute-start.35
  148.1 0.7 collective-permute-done.40
  149.0 0.8 collective-permute-start.43
  149.9 0.4 collective-permute-start.42
  150.3 3.3 %collective-permute-start.41 = (bf16[64,512]{1,0:T(8,128)(2,1)S(1)}, bf16[64,512]{1,0:T(8,128)(2,1)S(1)}, u32[]{:S(2)}, u32[]{:S(2)}) collective-permute-start(bf16[64,512]{1,0:T(8,128)(2,1)S(1)} %slice.106), channel_id=1, source_target_pairs={{0,24},{2,26},{4,28},{6,30},{8,16},{10,18},{12,20},{14,22},{16,8},... | collective-permute-start | bytes 196616 | tf_op jit(solution)/shard_map/ppermute | solution.py:365
  153.6 9.2 %collective-permute-done.43 = bf16[64,1536]{1,0:T(8,128)(2,1)S(1)} collective-permute-done((bf16[64,1536]{1,0:T(8,128)(2,1)S(1)}, bf16[64,1536]{1,0:T(8,128)(2,1)S(1)}, u32[]{:S(2)}, u32[]{:S(2)}) %collective-permute-start.43) | collective-permute-done | bytes 196640 | tf_op jit(solution)/shard_map/ppermute | solution.py:365
  162.9 9.2 %collective-permute-done.44 = bf16[64,1536]{1,0:T(8,128)(2,1)S(1)} collective-permute-done((bf16[64,1536]{1,0:T(8,128)(2,1)S(1)}, bf16[64,1536]{1,0:T(8,128)(2,1)S(1)}, u32[]{:S(2)}, u32[]{:S(2)}) %collective-permute-start.44) | collective-permute-done | bytes 196640 | tf_op jit(solution)/shard_map/ppermute | solution.py:365
  172.3 1.5 collective-permute-done.45
  173.9 0.9 maximum_select_fusion
  (90 shorter events, 2.1 us)
Async XLA Ops:
  0.0 56.2 %copy-start.8 = (f32[128]{0:T(128)S(1)}, f32[128]{0:T(128)}, u32[]{:S(2)}) copy-start(f32[128]{0:T(128)} %param.25) | copy-start | bytes 1540
  0.0 56.2 %copy-start.9 = (f32[64]{0:T(128)S(1)}, f32[64]{0:T(128)}, u32[]{:S(2)}) copy-start(f32[64]{0:T(128)} %param.26) | copy-start | bytes 772
  0.0 56.2 %copy-start.6 = (f32[4]{0:T(128)S(1)}, f32[4]{0:T(128)}, u32[]{:S(2)}) copy-start(f32[4]{0:T(128)} %balance_a.1) | copy-start | bytes 52
  0.0 56.2 %copy-start.7 = (f32[4]{0:T(128)S(1)}, f32[4]{0:T(128)}, u32[]{:S(2)}) copy-start(f32[4]{0:T(128)} %balance_b.1) | copy-start | bytes 52
  3.2 53.0 %copy-start.1 = (bf16[128,576]{1,0:T(8,128)(2,1)S(1)}, bf16[128,576]{1,0:T(8,128)(2,1)}, u32[]{:S(2)}) copy-start(bf16[128,576]{1,0:T(8,128)(2,1)} %get-tuple-element.26.refs_0_) | copy-start | bytes 442372
  3.2 11.0 %collective-permute-start.2 = (bf16[128,576]{1,0:T(8,128)(2,1)}, bf16[128,576]{1,0:T(8,128)(2,1)S(1)}, u32[]{:S(2)}, u32[]{:S(2)}) collective-permute-start(bf16[128,576]{1,0:T(8,128)(2,1)} %get-tuple-element.29), channel_id=1, source_target_pairs={{0,24},{2,26},{4,28},{6,30},{8,16},{10,18},{12,20},{14,22},{16,8},... | collective-permute-start | bytes 442376 | tf_op jit(solution)/shard_map/ppermute | solution.py:365
  8.3 14.2 %collective-permute-start.1 = (bf16[128,576]{1,0:T(8,128)(2,1)}, bf16[128,576]{1,0:T(8,128)(2,1)S(1)}, u32[]{:S(2)}, u32[]{:S(2)}) collective-permute-start(bf16[128,576]{1,0:T(8,128)(2,1)} %get-tuple-element.28), channel_id=1, source_target_pairs={{0,16},{2,18},{4,20},{6,22},{8,24},{10,26},{12,28},{14,30},{16,0},... | collective-permute-start | bytes 442376 | tf_op jit(solution)/shard_map/ppermute | solution.py:365
  8.3 14.2 %collective-permute-start = (bf16[128,576]{1,0:T(8,128)(2,1)}, bf16[128,576]{1,0:T(8,128)(2,1)S(1)}, u32[]{:S(2)}, u32[]{:S(2)}) collective-permute-start(bf16[128,576]{1,0:T(8,128)(2,1)} %get-tuple-element.27), channel_id=1, source_target_pairs={{0,8},{2,10},{4,12},{6,14},{8,0},{10,2},{12,4},{14,6},{16,24},{18,... | collective-permute-start | bytes 442376 | tf_op jit(solution)/shard_map/ppermute | solution.py:365
  11.9 24.1 %collective-permute-start.14 = (bf16[256,1024]{1,0:T(8,128)(2,1)}, bf16[256,1024]{1,0:T(8,128)(2,1)S(1)}, u32[]{:S(2)}, u32[]{:S(2)}) collective-permute-start(bf16[256,1024]{1,0:T(8,128)(2,1)} %get-tuple-element.38), channel_id=1, source_target_pairs={{0,8},{2,10},{4,12},{6,14},{8,0},{10,2},{12,4},{14,6},{16,24},{18,... | collective-permute-start | bytes 1572872 | tf_op jit(solution)/shard_map/ppermute | solution.py:365
  22.6 10.2 %collective-permute-start.4 = (bf16[4,128,384]{2,1,0:T(8,128)(2,1)S(1)}, bf16[4,128,384]{2,1,0:T(8,128)(2,1)S(1)}, u32[]{:S(2)}, u32[]{:S(2)}) collective-permute-start(bf16[4,128,384]{2,1,0:T(8,128)(2,1)S(1)} %pad_maximum_fusion.refs_4_), channel_id=1, source_target_pairs={{0,4},{2,6},{4,0},{6,2},{8,12},{10,14},{12,8},{14,10},{16,20},{18,... | collective-permute-start | bytes 1179656 | tf_op jit(solution)/shard_map/ppermute | solution.py:372
  24.2 10.2 %collective-permute-start.3 = (bf16[4,128,384]{2,1,0:T(8,128)(2,1)S(1)}, bf16[4,128,384]{2,1,0:T(8,128)(2,1)S(1)}, u32[]{:S(2)}, u32[]{:S(2)}) collective-permute-start(bf16[4,128,384]{2,1,0:T(8,128)(2,1)S(1)} %pad_maximum_fusion.refs_4_), channel_id=1, source_target_pairs={{0,2},{2,0},{4,6},{6,4},{8,10},{10,8},{12,14},{14,12},{16,18},{18,... | collective-permute-start | bytes 1179656 | tf_op jit(solution)/shard_map/ppermute | solution.py:372
  25.7 11.9 %collective-permute-start.15 = (bf16[128,1024]{1,0:T(8,128)(2,1)}, bf16[128,1024]{1,0:T(8,128)(2,1)S(1)}, u32[]{:S(2)}, u32[]{:S(2)}) collective-permute-start(bf16[128,1024]{1,0:T(8,128)(2,1)} %get-tuple-element.39), channel_id=1, source_target_pairs={{0,24},{2,26},{4,28},{6,30},{8,16},{10,18},{12,20},{14,22},{16,8},... | collective-permute-start | bytes 786440 | tf_op jit(solution)/shard_map/ppermute | solution.py:365
  28.2 14.2 %collective-permute-start.29 = (bf16[128,1024]{1,0:T(8,128)(2,1)}, bf16[128,1024]{1,0:T(8,128)(2,1)S(1)}, u32[]{:S(2)}, u32[]{:S(2)}) collective-permute-start(bf16[128,1024]{1,0:T(8,128)(2,1)} %get-tuple-element.42), channel_id=1, source_target_pairs={{0,24},{2,26},{4,28},{6,30},{8,16},{10,18},{12,20},{14,22},{16,8},... | collective-permute-start | bytes 786440 | tf_op jit(solution)/shard_map/ppermute | solution.py:365
  32.8 38.2 %collective-permute-start.12 = (bf16[256,1024]{1,0:T(8,128)(2,1)}, bf16[256,1024]{1,0:T(8,128)(2,1)S(1)}, u32[]{:S(2)}, u32[]{:S(2)}) collective-permute-start(bf16[256,1024]{1,0:T(8,128)(2,1)} %get-tuple-element.37.refs_0_), channel_id=1, source_target_pairs={{0,4},{2,6},{4,0},{6,2},{8,12},{10,14},{12,8},{14,10},{16,20},{18,... | collective-permute-start | bytes 1572872 | tf_op jit(solution)/shard_map/ppermute | solution.py:372
  34.4 15.2 %collective-permute-start.5 = (bf16[2,128,384]{2,1,0:T(8,128)(2,1)S(1)}, bf16[2,128,384]{2,1,0:T(8,128)(2,1)S(1)}, u32[]{:S(2)}, u32[]{:S(2)}) collective-permute-start(bf16[2,128,384]{2,1,0:T(8,128)(2,1)S(1)} %slice.93), channel_id=1, source_target_pairs={{0,2},{2,0},{4,6},{6,4},{8,10},{10,8},{12,14},{14,12},{16,18},{18,... | collective-permute-start | bytes 589832 | tf_op jit(solution)/shard_map/ppermute | solution.py:372
  36.0 14.1 %collective-permute-start.6 = (bf16[2,128,384]{2,1,0:T(8,128)(2,1)S(1)}, bf16[2,128,384]{2,1,0:T(8,128)(2,1)S(1)}, u32[]{:S(2)}, u32[]{:S(2)}) collective-permute-start(bf16[2,128,384]{2,1,0:T(8,128)(2,1)S(1)} %slice.94), channel_id=1, source_target_pairs={{0,4},{2,6},{4,0},{6,2},{8,12},{10,14},{12,8},{14,10},{16,20},{18,... | collective-permute-start | bytes 589832 | tf_op jit(solution)/shard_map/ppermute | solution.py:372
  37.6 47.6 %collective-permute-start.11 = (bf16[256,1024]{1,0:T(8,128)(2,1)}, bf16[256,1024]{1,0:T(8,128)(2,1)S(1)}, u32[]{:S(2)}, u32[]{:S(2)}) collective-permute-start(bf16[256,1024]{1,0:T(8,128)(2,1)} %get-tuple-element.37.refs_0_), channel_id=1, source_target_pairs={{0,2},{2,0},{4,6},{6,4},{8,10},{10,8},{12,14},{14,12},{16,18},{18,... | collective-permute-start | bytes 1572872 | tf_op jit(solution)/shard_map/ppermute | solution.py:372
  42.4 28.6 %collective-permute-start.20 = (bf16[256,1024]{1,0:T(8,128)(2,1)}, bf16[256,1024]{1,0:T(8,128)(2,1)S(1)}, u32[]{:S(2)}, u32[]{:S(2)}) collective-permute-start(bf16[256,1024]{1,0:T(8,128)(2,1)} %get-tuple-element.40), channel_id=1, source_target_pairs={{0,16},{2,18},{4,20},{6,22},{8,24},{10,26},{12,28},{14,30},{16,0},... | collective-permute-start | bytes 1572872 | tf_op jit(solution)/shard_map/ppermute | solution.py:365
  49.6 46.7 %collective-permute-start.17 = (bf16[384,1024]{1,0:T(8,128)(2,1)S(1)}, bf16[384,1024]{1,0:T(8,128)(2,1)S(1)}, u32[]{:S(2)}, u32[]{:S(2)}) collective-permute-start(bf16[384,1024]{1,0:T(8,128)(2,1)S(1)} %constant_dynamic-update-slice_fusion.refs_4_), channel_id=1, source_target_pairs={{0,4},{2,6},{4,0},{6,2},{8,12},{10,14},{12,8},{14,10},{16,20},{18,... | collective-permute-start | bytes 2359304 | tf_op jit(solution)/shard_map/ppermute | solution.py:372
  50.1 47.7 %collective-permute-start.16 = (bf16[384,1024]{1,0:T(8,128)(2,1)S(1)}, bf16[384,1024]{1,0:T(8,128)(2,1)S(1)}, u32[]{:S(2)}, u32[]{:S(2)}) collective-permute-start(bf16[384,1024]{1,0:T(8,128)(2,1)S(1)} %constant_dynamic-update-slice_fusion.refs_4_), channel_id=1, source_target_pairs={{0,2},{2,0},{4,6},{6,4},{8,10},{10,8},{12,14},{14,12},{16,18},{18,... | collective-permute-start | bytes 2359304 | tf_op jit(solution)/shard_map/ppermute | solution.py:372
  56.2 27.2 %copy-start.2 = (bf16[512,2048]{1,0:T(8,128)(2,1)S(1)}, bf16[512,2048]{1,0:T(8,128)(2,1)}, u32[]{:S(2)}) copy-start(bf16[512,2048]{1,0:T(8,128)(2,1)} %refs_4_.3) | copy-start | bytes 6291460
  56.2 27.2 %copy-start.3 = (bf16[256,2048]{1,0:T(8,128)(2,1)S(1)}, bf16[256,2048]{1,0:T(8,128)(2,1)}, u32[]{:S(2)}) copy-start(bf16[256,2048]{1,0:T(8,128)(2,1)} %refs_5_.1) | copy-start | bytes 3145732
  71.0 4.3 %collective-permute-start.7 = (bf16[128,192]{1,0:T(8,128)(2,1)S(1)}, bf16[128,192]{1,0:T(8,128)(2,1)S(1)}, u32[]{:S(2)}, u32[]{:S(2)}) collective-permute-start(bf16[128,192]{1,0:T(8,128)(2,1)S(1)} %get-tuple-element.31), channel_id=1, source_target_pairs={{0,8},{2,10},{4,12},{6,14},{8,0},{10,2},{12,4},{14,6},{16,24},{18,... | collective-permute-start | bytes 147464 | tf_op jit(solution)/shard_map/ppermute | solution.py:365
  71.0 5.2 %collective-permute-start.8 = (bf16[128,192]{1,0:T(8,128)(2,1)S(1)}, bf16[128,192]{1,0:T(8,128)(2,1)S(1)}, u32[]{:S(2)}, u32[]{:S(2)}) collective-permute-start(bf16[128,192]{1,0:T(8,128)(2,1)S(1)} %get-tuple-element.32), channel_id=1, source_target_pairs={{0,16},{2,18},{4,20},{6,22},{8,24},{10,26},{12,28},{14,30},{16,0},... | collective-permute-start | bytes 147464 | tf_op jit(solution)/shard_map/ppermute | solution.py:365
  75.3 19.6 %collective-permute-start.22 = (bf16[256,1024]{1,0:T(8,128)(2,1)S(1)}, bf16[256,1024]{1,0:T(8,128)(2,1)S(1)}, u32[]{:S(2)}, u32[]{:S(2)}) collective-permute-start(bf16[256,1024]{1,0:T(8,128)(2,1)S(1)} %collective-permute-done.20.refs_9_), channel_id=1, source_target_pairs={{0,4},{2,6},{4,0},{6,2},{8,12},{10,14},{12,8},{14,10},{16,20},{18,... | collective-permute-start | bytes 1572872 | tf_op jit(solution)/shard_map/ppermute | solution.py:372
  76.3 6.2 %collective-permute-start.9 = (bf16[128,192]{1,0:T(8,128)(2,1)S(1)}, bf16[128,192]{1,0:T(8,128)(2,1)S(1)}, u32[]{:S(2)}, u32[]{:S(2)}) collective-permute-start(bf16[128,192]{1,0:T(8,128)(2,1)S(1)} %get-tuple-element.33), channel_id=1, source_target_pairs={{0,24},{2,26},{4,28},{6,30},{8,16},{10,18},{12,20},{14,22},{16,8},... | collective-permute-start | bytes 147464 | tf_op jit(solution)/shard_map/ppermute | solution.py:365
  82.4 10.3 %collective-permute-start.31 = (bf16[128,1024]{1,0:T(8,128)(2,1)S(1)}, bf16[128,1024]{1,0:T(8,128)(2,1)S(1)}, u32[]{:S(2)}, u32[]{:S(2)}) collective-permute-start(bf16[128,1024]{1,0:T(8,128)(2,1)S(1)} %collective-permute-done.29.refs_13_), channel_id=1, source_target_pairs={{0,4},{2,6},{4,0},{6,2},{8,12},{10,14},{12,8},{14,10},{16,20},{18,... | collective-permute-start | bytes 786440 | tf_op jit(solution)/shard_map/ppermute | solution.py:372
  83.4 12.0 %copy-start.4 = (bf16[128,2048]{1,0:T(8,128)(2,1)S(1)}, bf16[128,2048]{1,0:T(8,128)(2,1)}, u32[]{:S(2)}) copy-start(bf16[128,2048]{1,0:T(8,128)(2,1)} %residual.1) | copy-start | bytes 1572868
  83.4 12.1 %copy-start.5 = (f32[2048]{0:T(1024)S(1)}, f32[2048]{0:T(1024)}, u32[]{:S(2)}) copy-start(f32[2048]{0:T(1024)} %param.29) | copy-start | bytes 24580
  85.2 45.5 %copy-start = (bf16[256,1024]{1,0:T(8,128)(2,1)S(1)}, bf16[256,1024]{1,0:T(8,128)(2,1)}, u32[]{:S(2)}) copy-start(bf16[256,1024]{1,0:T(8,128)(2,1)} %get-tuple-element.37.refs_0_) | copy-start | bytes 1572868
  85.2 8.1 %collective-permute-start.10 = (bf16[64,2048]{1,0:T(8,128)(2,1)S(1)}, bf16[64,2048]{1,0:T(8,128)(2,1)S(1)}, u32[]{:S(2)}, u32[]{:S(2)}) collective-permute-start(bf16[64,2048]{1,0:T(8,128)(2,1)S(1)} %get-tuple-element.35), channel_id=1, source_target_pairs={{0,1},{1,0},{2,3},{3,2},{4,5},{5,4},{6,7},{7,6},{8,9},{9,8},{10,11... | collective-permute-start | bytes 786440 | tf_op jit(solution)/shard_map/ppermute | solution.py:375
  92.7 26.5 %collective-permute-start.21 = (bf16[256,1024]{1,0:T(8,128)(2,1)S(1)}, bf16[256,1024]{1,0:T(8,128)(2,1)S(1)}, u32[]{:S(2)}, u32[]{:S(2)}) collective-permute-start(bf16[256,1024]{1,0:T(8,128)(2,1)S(1)} %collective-permute-done.20.refs_9_), channel_id=1, source_target_pairs={{0,2},{2,0},{4,6},{6,4},{8,10},{10,8},{12,14},{14,12},{16,18},{18,... | collective-permute-start | bytes 1572872 | tf_op jit(solution)/shard_map/ppermute | solution.py:372
  93.3 19.8 %collective-permute-start.30 = (bf16[128,1024]{1,0:T(8,128)(2,1)S(1)}, bf16[128,1024]{1,0:T(8,128)(2,1)S(1)}, u32[]{:S(2)}, u32[]{:S(2)}) collective-permute-start(bf16[128,1024]{1,0:T(8,128)(2,1)S(1)} %collective-permute-done.29.refs_13_), channel_id=1, source_target_pairs={{0,2},{2,0},{4,6},{6,4},{8,10},{10,8},{12,14},{14,12},{16,18},{18,... | collective-permute-start | bytes 786440 | tf_op jit(solution)/shard_map/ppermute | solution.py:372
  94.9 23.9 %collective-permute-start.13 = (bf16[128,1024]{1,0:T(8,128)(2,1)S(1)}, bf16[128,1024]{1,0:T(8,128)(2,1)S(1)}, u32[]{:S(2)}, u32[]{:S(2)}) collective-permute-start(bf16[128,1024]{1,0:T(8,128)(2,1)S(1)} %slice.95), channel_id=1, source_target_pairs={{0,2},{2,0},{4,6},{6,4},{8,10},{10,8},{12,14},{14,12},{16,18},{18,... | collective-permute-start | bytes 786440 | tf_op jit(solution)/shard_map/ppermute | solution.py:372
  96.3 28.1 %collective-permute-start.23 = (bf16[128,1024]{1,0:T(8,128)(2,1)S(1)}, bf16[128,1024]{1,0:T(8,128)(2,1)S(1)}, u32[]{:S(2)}, u32[]{:S(2)}) collective-permute-start(bf16[128,1024]{1,0:T(8,128)(2,1)S(1)} %slice.98), channel_id=1, source_target_pairs={{0,2},{2,0},{4,6},{6,4},{8,10},{10,8},{12,14},{14,12},{16,18},{18,... | collective-permute-start | bytes 786440 | tf_op jit(solution)/shard_map/ppermute | solution.py:372
  97.8 26.6 %collective-permute-start.24 = (bf16[64,2048]{1,0:T(8,128)(2,1)S(1)}, bf16[64,2048]{1,0:T(8,128)(2,1)S(1)}, u32[]{:S(2)}, u32[]{:S(2)}) collective-permute-start(bf16[64,2048]{1,0:T(8,128)(2,1)S(1)} %get-tuple-element.41.refs_1_), channel_id=1, source_target_pairs={{0,8},{2,10},{4,12},{6,14},{8,0},{10,2},{12,4},{14,6},{16,24},{18,... | collective-permute-start | bytes 786440 | tf_op jit(solution)/shard_map/ppermute | solution.py:365
  113.2 16.7 %collective-permute-start.18 = (bf16[192,1024]{1,0:T(8,128)(2,1)S(1)}, bf16[192,1024]{1,0:T(8,128)(2,1)S(1)}, u32[]{:S(2)}, u32[]{:S(2)}) collective-permute-start(bf16[192,1024]{1,0:T(8,128)(2,1)S(1)} %slice.96), channel_id=1, source_target_pairs={{0,2},{2,0},{4,6},{6,4},{8,10},{10,8},{12,14},{14,12},{16,18},{18,... | collective-permute-start | bytes 1179656 | tf_op jit(solution)/shard_map/ppermute | solution.py:372
  118.8 11.1 %collective-permute-start.19 = (bf16[192,1024]{1,0:T(8,128)(2,1)S(1)}, bf16[192,1024]{1,0:T(8,128)(2,1)S(1)}, u32[]{:S(2)}, u32[]{:S(2)}) collective-permute-start(bf16[192,1024]{1,0:T(8,128)(2,1)S(1)} %slice.97), channel_id=1, source_target_pairs={{0,4},{2,6},{4,0},{6,2},{8,12},{10,14},{12,8},{14,10},{16,20},{18,... | collective-permute-start | bytes 1179656 | tf_op jit(solution)/shard_map/ppermute | solution.py:372
  119.3 12.2 %collective-permute-start.36 = (bf16[64,2048]{1,0:T(8,128)(2,1)S(1)}, bf16[64,2048]{1,0:T(8,128)(2,1)S(1)}, u32[]{:S(2)}, u32[]{:S(2)}) collective-permute-start(bf16[64,2048]{1,0:T(8,128)(2,1)S(1)} %get-tuple-element.41.refs_1_), channel_id=1, source_target_pairs={{0,16},{2,18},{4,20},{6,22},{8,24},{10,26},{12,28},{14,30},{16,0},... | collective-permute-start | bytes 786440 | tf_op jit(solution)/shard_map/ppermute | solution.py:365
  124.4 9.2 %collective-permute-start.26 = (bf16[64,2048]{1,0:T(8,128)(2,1)S(1)}, bf16[64,2048]{1,0:T(8,128)(2,1)S(1)}, u32[]{:S(2)}, u32[]{:S(2)}) collective-permute-start(bf16[64,2048]{1,0:T(8,128)(2,1)S(1)} %get-tuple-element.41.refs_1_), channel_id=1, source_target_pairs={{0,1},{1,0},{2,3},{3,2},{4,5},{5,4},{6,7},{7,6},{8,9},{9,8},{10,11... | collective-permute-start | bytes 786440 | tf_op jit(solution)/shard_map/ppermute | solution.py:375
  124.4 9.3 %collective-permute-start.25 = (bf16[64,2048]{1,0:T(8,128)(2,1)S(1)}, bf16[64,2048]{1,0:T(8,128)(2,1)S(1)}, u32[]{:S(2)}, u32[]{:S(2)}) collective-permute-start(bf16[64,2048]{1,0:T(8,128)(2,1)S(1)} %collective-permute-done.24.refs_0_), channel_id=1, source_target_pairs={{0,1},{1,0},{2,3},{3,2},{4,5},{5,4},{6,7},{7,6},{8,9},{9,8},{10,11... | collective-permute-start | bytes 786440 | tf_op jit(solution)/shard_map/ppermute | solution.py:375
  129.9 10.2 %collective-permute-start.27 = (bf16[128,1024]{1,0:T(8,128)(2,1)S(1)}, bf16[128,1024]{1,0:T(8,128)(2,1)S(1)}, u32[]{:S(2)}, u32[]{:S(2)}) collective-permute-start(bf16[128,1024]{1,0:T(8,128)(2,1)S(1)} %slice.99), channel_id=1, source_target_pairs={{0,4},{2,6},{4,0},{6,2},{8,12},{10,14},{12,8},{14,10},{16,20},{18,... | collective-permute-start | bytes 786440 | tf_op jit(solution)/shard_map/ppermute | solution.py:372
  129.9 5.3 %collective-permute-start.32 = (bf16[64,1024]{1,0:T(8,128)(2,1)S(1)}, bf16[64,1024]{1,0:T(8,128)(2,1)S(1)}, u32[]{:S(2)}, u32[]{:S(2)}) collective-permute-start(bf16[64,1024]{1,0:T(8,128)(2,1)S(1)} %slice.101), channel_id=1, source_target_pairs={{0,2},{2,0},{4,6},{6,4},{8,10},{10,8},{12,14},{14,12},{16,18},{18,... | collective-permute-start | bytes 393224 | tf_op jit(solution)/shard_map/ppermute | solution.py:372
  131.5 8.6 %collective-permute-start.33 = (bf16[64,1024]{1,0:T(8,128)(2,1)S(1)}, bf16[64,1024]{1,0:T(8,128)(2,1)S(1)}, u32[]{:S(2)}, u32[]{:S(2)}) collective-permute-start(bf16[64,1024]{1,0:T(8,128)(2,1)S(1)} %slice.102), channel_id=1, source_target_pairs={{0,4},{2,6},{4,0},{6,2},{8,12},{10,14},{12,8},{14,10},{16,20},{18,... | collective-permute-start | bytes 393224 | tf_op jit(solution)/shard_map/ppermute | solution.py:372
  133.6 8.4 %collective-permute-start.28 = (bf16[128,1024]{1,0:T(8,128)(2,1)S(1)}, bf16[128,1024]{1,0:T(8,128)(2,1)S(1)}, u32[]{:S(2)}, u32[]{:S(2)}) collective-permute-start(bf16[128,1024]{1,0:T(8,128)(2,1)S(1)} %slice.100), channel_id=1, source_target_pairs={{0,4},{2,6},{4,0},{6,2},{8,12},{10,14},{12,8},{14,10},{16,20},{18,... | collective-permute-start | bytes 786440 | tf_op jit(solution)/shard_map/ppermute | solution.py:372
  133.7 6.4 %collective-permute-start.37 = (bf16[64,2048]{1,0:T(8,128)(2,1)S(1)}, bf16[64,2048]{1,0:T(8,128)(2,1)S(1)}, u32[]{:S(2)}, u32[]{:S(2)}) collective-permute-start(bf16[64,2048]{1,0:T(8,128)(2,1)S(1)} %collective-permute-done.36.refs_1_), channel_id=1, source_target_pairs={{0,8},{2,10},{4,12},{6,14},{8,0},{10,2},{12,4},{14,6},{16,24},{18,... | collective-permute-start | bytes 786440 | tf_op jit(solution)/shard_map/ppermute | solution.py:365
  135.2 8.9 %collective-permute-start.39 = (bf16[64,2048]{1,0:T(8,128)(2,1)S(1)}, bf16[64,2048]{1,0:T(8,128)(2,1)S(1)}, u32[]{:S(2)}, u32[]{:S(2)}) collective-permute-start(bf16[64,2048]{1,0:T(8,128)(2,1)S(1)} %collective-permute-done.36.refs_1_), channel_id=1, source_target_pairs={{0,1},{1,0},{2,3},{3,2},{4,5},{5,4},{6,7},{7,6},{8,9},{9,8},{10,11... | collective-permute-start | bytes 786440 | tf_op jit(solution)/shard_map/ppermute | solution.py:375
  140.0 4.1 %collective-permute-start.38 = (bf16[64,2048]{1,0:T(8,128)(2,1)S(1)}, bf16[64,2048]{1,0:T(8,128)(2,1)S(1)}, u32[]{:S(2)}, u32[]{:S(2)}) collective-permute-start(bf16[64,2048]{1,0:T(8,128)(2,1)S(1)} %collective-permute-done.37.refs_0_), channel_id=1, source_target_pairs={{0,1},{1,0},{2,3},{3,2},{4,5},{5,4},{6,7},{7,6},{8,9},{9,8},{10,11... | collective-permute-start | bytes 786440 | tf_op jit(solution)/shard_map/ppermute | solution.py:375
  144.1 3.2 %collective-permute-start.34 = (bf16[2,64,2048]{2,1,0:T(8,128)(2,1)S(1)}, bf16[2,64,2048]{2,1,0:T(8,128)(2,1)S(1)}, u32[]{:S(2)}, u32[]{:S(2)}) collective-permute-start(bf16[2,64,2048]{2,1,0:T(8,128)(2,1)S(1)} %get-tuple-element.44), channel_id=1, source_target_pairs={{0,1},{1,0},{2,3},{3,2},{4,5},{5,4},{6,7},{7,6},{8,9},{9,8},{10,11... | collective-permute-start | bytes 1572872 | tf_op jit(solution)/shard_map/ppermute | solution.py:375
  146.7 2.1 %collective-permute-start.40 = (bf16[2,64,2048]{2,1,0:T(8,128)(2,1)S(1)}, bf16[2,64,2048]{2,1,0:T(8,128)(2,1)S(1)}, u32[]{:S(2)}, u32[]{:S(2)}) collective-permute-start(bf16[2,64,2048]{2,1,0:T(8,128)(2,1)S(1)} %get-tuple-element.46), channel_id=1, source_target_pairs={{0,1},{1,0},{2,3},{3,2},{4,5},{5,4},{6,7},{7,6},{8,9},{9,8},{10,11... | collective-permute-start | bytes 1572872 | tf_op jit(solution)/shard_map/ppermute | solution.py:375
  147.5 24.7 %collective-permute-start.35 = (bf16[64,2048]{1,0:T(8,128)(2,1)S(1)}, bf16[64,2048]{1,0:T(8,128)(2,1)S(1)}, u32[]{:S(2)}, u32[]{:S(2)}) collective-permute-start(bf16[64,2048]{1,0:T(8,128)(2,1)S(1)} %fusion.5), channel_id=1, source_target_pairs={{0,8},{2,10},{4,12},{6,14},{8,0},{10,2},{12,4},{14,6},{16,24},{18,... | collective-permute-start | bytes 786440 | tf_op jit(solution)/shard_map/ppermute | solution.py:365
  149.0 13.8 %collective-permute-start.43 = (bf16[64,1536]{1,0:T(8,128)(2,1)S(1)}, bf16[64,1536]{1,0:T(8,128)(2,1)S(1)}, u32[]{:S(2)}, u32[]{:S(2)}) collective-permute-start(bf16[64,1536]{1,0:T(8,128)(2,1)S(1)} %slice.110), channel_id=1, source_target_pairs={{0,8},{2,10},{4,12},{6,14},{8,0},{10,2},{12,4},{14,6},{16,24},{18,... | collective-permute-start | bytes 589832 | tf_op jit(solution)/shard_map/ppermute | solution.py:365
  149.9 13.0 %collective-permute-start.42 = (bf16[64,512]{1,0:T(8,128)(2,1)S(1)}, bf16[64,512]{1,0:T(8,128)(2,1)S(1)}, u32[]{:S(2)}, u32[]{:S(2)}) collective-permute-start(bf16[64,512]{1,0:T(8,128)(2,1)S(1)} %slice.135), channel_id=1, source_target_pairs={{0,16},{2,18},{4,20},{6,22},{8,24},{10,26},{12,28},{14,30},{16,0},... | collective-permute-start | bytes 196616 | tf_op jit(solution)/shard_map/ppermute | solution.py:365
  150.3 12.6 %collective-permute-start.41 = (bf16[64,512]{1,0:T(8,128)(2,1)S(1)}, bf16[64,512]{1,0:T(8,128)(2,1)S(1)}, u32[]{:S(2)}, u32[]{:S(2)}) collective-permute-start(bf16[64,512]{1,0:T(8,128)(2,1)S(1)} %slice.106), channel_id=1, source_target_pairs={{0,24},{2,26},{4,28},{6,30},{8,16},{10,18},{12,20},{14,22},{16,8},... | collective-permute-start | bytes 196616 | tf_op jit(solution)/shard_map/ppermute | solution.py:365
  162.8 9.3 %collective-permute-start.44 = (bf16[64,1536]{1,0:T(8,128)(2,1)S(1)}, bf16[64,1536]{1,0:T(8,128)(2,1)S(1)}, u32[]{:S(2)}, u32[]{:S(2)}) collective-permute-start(bf16[64,1536]{1,0:T(8,128)(2,1)S(1)} %fusion.4), channel_id=1, source_target_pairs={{0,16},{2,18},{4,20},{6,22},{8,24},{10,26},{12,28},{14,30},{16,0},... | collective-permute-start | bytes 589832 | tf_op jit(solution)/shard_map/ppermute | solution.py:365
  172.3 1.6 collective-permute-start.45

commit v7 on v6

--- a/solution.py
+++ b/solution.py
@@ -333,6 +333,12 @@
             other[r, :, span] = part[rest : rest + half]
 
 
+def join_kernel(half, mine, theirs, out):
+    core = lax.axis_index("tp")
+    out[pl.ds(pl.multiple_of(core * half, half), half), :] = mine[...]
+    out[pl.ds(pl.multiple_of((1 - core) * half, half), half), :] = theirs[...]
+
+
 def fast_body(slots, plane, *arguments):
     (
         residual,
@@ -563,9 +569,15 @@
     total = total + jnp.concatenate([straight, relayed], axis=1)
     mine = (mixed.astype(jnp.float32) + total).astype(jnp.bfloat16)
     theirs = swap(mine)
-    return jnp.where(
-        core == 0, jnp.concatenate([mine, theirs]), jnp.concatenate([theirs, mine])
-    )
+    return pl.pallas_call(
+        functools.partial(join_kernel, half),
+        out_shape=jax.ShapeDtypeStruct((tokens, width), jnp.bfloat16),
+        in_specs=vmem_specs(2),
+        out_specs=pl.BlockSpec(memory_space=VMEM),
+        compiler_params=pltpu.CompilerParams(vmem_limit_bytes=8 * 2**20),
+        cost_estimate=pl.CostEstimate(flops=10**6, bytes_accessed=10**6, transcendentals=0),
+        name="join",
+    )(mine, theirs)
 
 
 def dispatch(count, cores, *arguments):

time: 175 us -> 175 us (level)
  no operation moved by 1% of the time
where the time goes in v7:
time: 175 us
  waiting for transfers between devices  96 us (55%)
  starting transfers between devices  53.6 us (31%)
  Pallas kernels  22.6 us (13%)
    ppermute x18, waiting for transfers between devices, along(): lax.ppermute(value, 'sp', [(i, (i // plane ^ k) * plane + i % plane) for...  51.1 us
    ppermute x20, waiting for transfers between devices, across(): return lax.ppermute(value, 'sp', [(i, i ^ k) for i in range(count)])  42.7 us
    ppermute x18, starting transfers between devices, along(): lax.ppermute(value, 'sp', [(i, (i // plane ^ k) * plane + i % plane) for...  27.7 us
    ppermute x20, starting transfers between devices, across(): return lax.ppermute(value, 'sp', [(i, i ^ k) for i in range(count)])  24.6 us
    pallas_call x1, Pallas kernels, fast_body(): pl.pallas_call(functools.partial(attend_kernel, slots, plane, tokens), ou...  6.39 us
  transfers between devices with their start and end apart: 46, of which 19 were waited for; matrix products, arithmetic and copies ran while one was open for 1% of the time, Pallas kernels for 11%

profile of v7, /device:TPU:0, one launch (start us, length us, event | category | flops | bytes accessed | tf_op | source)
XLA Modules:
  0.0 174.7 jit_solution(1548912603856166584)
XLA Ops:
  0.0 3.2 %pack.1 = (bf16[128,576]{1,0:T(8,128)(2,1)}, bf16[128,576]{1,0:T(8,128)(2,1)}, bf16[128,576]{1,0:T(8,128)(2,1)}, bf16[128,576]{1,0:T(8,128)(2,1)}) custom-call(bf16[128,4,128]{2,1,0:T(4,128)(2,1)} %refs_0_.2, bf16[4,64,128]{2,1,0:T(8,128)(2,1)} %bitcast.36, bf16[4,64,128]{2,1,0:T(8,128)(2,1)} %bitcast.37, bf16[128,4,128]{2,1,0:T(4,128)(2,1)} %refs_3_.1, ...), custom_call_target="tpu_custom_call" | custom-call | flops 100000000 | bytes 1000000 | tf_op jit(solution)/shard_map/pack/pallas_call | solution.py:394
  3.2 5.1 %collective-permute-start.2 = (bf16[128,576]{1,0:T(8,128)(2,1)}, bf16[128,576]{1,0:T(8,128)(2,1)S(1)}, u32[]{:S(2)}, u32[]{:S(2)}) collective-permute-start(bf16[128,576]{1,0:T(8,128)(2,1)} %get-tuple-element.29), channel_id=1, source_target_pairs={{0,24},{2,26},{4,28},{6,30},{8,16},{10,18},{12,20},{14,22},{16,8},... | collective-permute-start | bytes 442376 | tf_op jit(solution)/shard_map/ppermute | solution.py:371
  8.3 0.6 collective-permute-start
  9.0 2.9 %cut.1 = (bf16[256,1024]{1,0:T(8,128)(2,1)}, bf16[256,1024]{1,0:T(8,128)(2,1)}, bf16[256,1024]{1,0:T(8,128)(2,1)}, bf16[128,1024]{1,0:T(8,128)(2,1)}, bf16[128,1024]{1,0:T(8,128)(2,1)}) custom-call(bf16[128,4096]{1,0:T(8,128)(2,1)} %refs_0_.3, bf16[128,4096]{1,0:T(8,128)(2,1)} %refs_1_.1), custom_call_target="tpu_custom_call" | custom-call | flops 100000000 | bytes 1000000 | tf_op jit(solution)/shard_map/cut/pallas_call | solution.py:405
  11.9 1.5 collective-permute-start.14
  13.3 0.9 slice_bitcast_fusion.5
  14.3 8.3 %collective-permute-done.1.refs_2_ = bf16[128,576]{1,0:T(8,128)(2,1)S(1)} collective-permute-done((bf16[128,576]{1,0:T(8,128)(2,1)}, bf16[128,576]{1,0:T(8,128)(2,1)S(1)}, u32[]{:S(2)}, u32[]{:S(2)}) %collective-permute-start.1) | collective-permute-done | bytes 147488 | tf_op jit(solution)/shard_map/ppermute | solution.py:371
  22.6 1.6 collective-permute-start.4
  24.2 1.5 collective-permute-start.3
  25.7 2.5 %collective-permute-start.15 = (bf16[128,1024]{1,0:T(8,128)(2,1)}, bf16[128,1024]{1,0:T(8,128)(2,1)S(1)}, u32[]{:S(2)}, u32[]{:S(2)}) collective-permute-start(bf16[128,1024]{1,0:T(8,128)(2,1)} %get-tuple-element.39), channel_id=1, source_target_pairs={{0,24},{2,26},{4,28},{6,30},{8,16},{10,18},{12,20},{14,22},{16,8},... | collective-permute-start | bytes 786440 | tf_op jit(solution)/shard_map/ppermute | solution.py:371
  28.2 1.3 collective-permute-start.29
  29.6 3.2 %collective-permute-done.4.refs_6_ = bf16[4,128,384]{2,1,0:T(8,128)(2,1)S(1)} collective-permute-done((bf16[4,128,384]{2,1,0:T(8,128)(2,1)S(1)}, bf16[4,128,384]{2,1,0:T(8,128)(2,1)S(1)}, u32[]{:S(2)}, u32[]{:S(2)}) %collective-permute-start.4) | collective-permute-done | bytes 393248 | tf_op jit(solution)/shard_map/ppermute | solution.py:378
  32.8 1.5 collective-permute-start.12
  34.4 1.6 collective-permute-start.5
  36.0 0.6 collective-permute-start.6
  36.6 1.0 collective-permute-done.15
  37.6 1.7 collective-permute-start.11
  39.3 3.1 %collective-permute-done.29.refs_13_ = bf16[128,1024]{1,0:T(8,128)(2,1)S(1)} collective-permute-done((bf16[128,1024]{1,0:T(8,128)(2,1)}, bf16[128,1024]{1,0:T(8,128)(2,1)S(1)}, u32[]{:S(2)}, u32[]{:S(2)}) %collective-permute-start.29) | collective-permute-done | bytes 262176 | tf_op jit(solution)/shard_map/ppermute | solution.py:371
  42.4 7.2 %collective-permute-start.20 = (bf16[256,1024]{1,0:T(8,128)(2,1)}, bf16[256,1024]{1,0:T(8,128)(2,1)S(1)}, u32[]{:S(2)}, u32[]{:S(2)}) collective-permute-start(bf16[256,1024]{1,0:T(8,128)(2,1)} %get-tuple-element.40), channel_id=1, source_target_pairs={{0,16},{2,18},{4,20},{6,22},{8,24},{10,26},{12,28},{14,30},{16,0},... | collective-permute-start | bytes 1572872 | tf_op jit(solution)/shard_map/ppermute | solution.py:371
  49.6 0.5 collective-permute-start.17
  50.1 6.1 %collective-permute-start.16 = (bf16[384,1024]{1,0:T(8,128)(2,1)S(1)}, bf16[384,1024]{1,0:T(8,128)(2,1)S(1)}, u32[]{:S(2)}, u32[]{:S(2)}) collective-permute-start(bf16[384,1024]{1,0:T(8,128)(2,1)S(1)} %constant_dynamic-update-slice_fusion.refs_4_), channel_id=1, source_target_pairs={{0,2},{2,0},{4,6},{6,4},{8,10},{10,8},{12,14},{14,12},{16,18},{18,... | collective-permute-start | bytes 2359304 | tf_op jit(solution)/shard_map/ppermute | solution.py:378
  56.2 6.4 %attend.1 = (bf16[128,192]{1,0:T(8,128)(2,1)S(1)}, bf16[128,192]{1,0:T(8,128)(2,1)S(1)}, bf16[128,192]{1,0:T(8,128)(2,1)S(1)}, bf16[128,192]{1,0:T(8,128)(2,1)S(1)}) custom-call(s32[3]{0:T(128)S(1)} %pad_add_fusion.index, f32[4]{0:T(128)S(1)} %copy-done.6, f32[4]{0:T(128)S(1)} %copy-done.7, f32[1,128]{1,0:T(1,128)S(1)} %bitcast.34, f32[1,64]{1,0:T(1,128)S(1)} %bitcast.35, ...), custom_call_target="tpu_custom_call" | custom-call | flops 8000000000 | bytes 2000000 | tf_op jit(solution)/shard_map/attend/pallas_call | solution.py:481
  62.6 8.4 %collective-permute-done.20.refs_9_ = bf16[256,1024]{1,0:T(8,128)(2,1)S(1)} collective-permute-done((bf16[256,1024]{1,0:T(8,128)(2,1)}, bf16[256,1024]{1,0:T(8,128)(2,1)S(1)}, u32[]{:S(2)}, u32[]{:S(2)}) %collective-permute-start.20) | collective-permute-done | bytes 524320 | tf_op jit(solution)/shard_map/ppermute | solution.py:371
  71.0 2.1 %collective-permute-start.8 = (bf16[128,192]{1,0:T(8,128)(2,1)S(1)}, bf16[128,192]{1,0:T(8,128)(2,1)S(1)}, u32[]{:S(2)}, u32[]{:S(2)}) collective-permute-start(bf16[128,192]{1,0:T(8,128)(2,1)S(1)} %get-tuple-element.32), channel_id=1, source_target_pairs={{0,16},{2,18},{4,20},{6,22},{8,24},{10,26},{12,28},{14,30},{16,0},... | collective-permute-start | bytes 147464 | tf_op jit(solution)/shard_map/ppermute | solution.py:371
  73.1 2.2 %collective-permute-done.7.refs_1_ = bf16[128,192]{1,0:T(8,128)(2,1)S(1)} collective-permute-done((bf16[128,192]{1,0:T(8,128)(2,1)S(1)}, bf16[128,192]{1,0:T(8,128)(2,1)S(1)}, u32[]{:S(2)}, u32[]{:S(2)}) %collective-permute-start.7) | collective-permute-done | bytes 49184 | tf_op jit(solution)/shard_map/ppermute | solution.py:371
  75.3 0.5 collective-permute-start.22
  75.8 0.5 collective-permute-done.8.refs_2_
  76.3 1.5 collective-permute-start.9
  77.7 4.7 %collective-permute-done.9.refs_3_ = bf16[128,192]{1,0:T(8,128)(2,1)S(1)} collective-permute-done((bf16[128,192]{1,0:T(8,128)(2,1)S(1)}, bf16[128,192]{1,0:T(8,128)(2,1)S(1)}, u32[]{:S(2)}, u32[]{:S(2)}) %collective-permute-start.9) | collective-permute-done | bytes 49184 | tf_op jit(solution)/shard_map/ppermute | solution.py:371
  82.4 1.0 collective-permute-start.31
  83.4 1.8 %project.1 = (bf16[64,2048]{1,0:T(8,128)(2,1)S(1)}, bf16[64,2048]{1,0:T(8,128)(2,1)S(1)}) custom-call(s32[3]{0:T(128)S(1)} %pad_add_fusion.index, bf16[128,192]{1,0:T(8,128)(2,1)S(1)} %get-tuple-element.30.refs_0_, bf16[128,192]{1,0:T(8,128)(2,1)S(1)} %collective-permute-done.7.refs_1_, bf16[128,192]{1,0:T(8,128)(2,1)S(1)} %collective-permute-done.8.refs_2_, ...), custom_call_target="tpu_custom_call" | custom-call | flops 2000000000 | bytes 4000000 | tf_op jit(solution)/shard_map/project/pallas_call | solution.py:506
  85.3 7.5 %collective-permute-done.31.refs_15_ = bf16[128,1024]{1,0:T(8,128)(2,1)S(1)} collective-permute-done((bf16[128,1024]{1,0:T(8,128)(2,1)S(1)}, bf16[128,1024]{1,0:T(8,128)(2,1)S(1)}, u32[]{:S(2)}, u32[]{:S(2)}) %collective-permute-start.31) | collective-permute-done | bytes 262176 | tf_op jit(solution)/shard_map/ppermute | solution.py:378
  92.7 0.5 collective-permute-start.21
  93.3 1.6 collective-permute-start.30
  94.9 0.5 collective-permute-start.13
  95.5 0.8 norm.1
  96.3 1.6 collective-permute-start.23
  98.2 15.0 %collective-permute-done.30.refs_14_ = bf16[128,1024]{1,0:T(8,128)(2,1)S(1)} collective-permute-done((bf16[128,1024]{1,0:T(8,128)(2,1)S(1)}, bf16[128,1024]{1,0:T(8,128)(2,1)S(1)}, u32[]{:S(2)}, u32[]{:S(2)}) %collective-permute-start.30) | collective-permute-done | bytes 262176 | tf_op jit(solution)/shard_map/ppermute | solution.py:378
  113.2 0.5 collective-permute-start.18
  113.7 5.1 %collective-permute-done.13.refs_3_ = bf16[128,1024]{1,0:T(8,128)(2,1)S(1)} collective-permute-done((bf16[128,1024]{1,0:T(8,128)(2,1)S(1)}, bf16[128,1024]{1,0:T(8,128)(2,1)S(1)}, u32[]{:S(2)}, u32[]{:S(2)}) %collective-permute-start.13) | collective-permute-done | bytes 262176 | tf_op jit(solution)/shard_map/ppermute | solution.py:378
  118.8 0.5 collective-permute-start.19
  119.3 5.1 %collective-permute-done.23.refs_12_ = bf16[128,1024]{1,0:T(8,128)(2,1)S(1)} collective-permute-done((bf16[128,1024]{1,0:T(8,128)(2,1)S(1)}, bf16[128,1024]{1,0:T(8,128)(2,1)S(1)}, u32[]{:S(2)}, u32[]{:S(2)}) %collective-permute-start.23) | collective-permute-done | bytes 262176 | tf_op jit(solution)/shard_map/ppermute | solution.py:378
  124.4 0.5 collective-permute-start.25
  125.0 4.9 %collective-permute-done.18.refs_7_ = bf16[192,1024]{1,0:T(8,128)(2,1)S(1)} collective-permute-done((bf16[192,1024]{1,0:T(8,128)(2,1)S(1)}, bf16[192,1024]{1,0:T(8,128)(2,1)S(1)}, u32[]{:S(2)}, u32[]{:S(2)}) %collective-permute-start.18) | collective-permute-done | bytes 393248 | tf_op jit(solution)/shard_map/ppermute | solution.py:378
  129.9 0.8 collective-permute-start.32
  130.7 0.8 shard_map.154.up
  131.5 2.1 %collective-permute-start.33 = (bf16[64,1024]{1,0:T(8,128)(2,1)S(1)}, bf16[64,1024]{1,0:T(8,128)(2,1)S(1)}, u32[]{:S(2)}, u32[]{:S(2)}) collective-permute-start(bf16[64,1024]{1,0:T(8,128)(2,1)S(1)} %slice.102), channel_id=1, source_target_pairs={{0,4},{2,6},{4,0},{6,2},{8,12},{10,14},{12,8},{14,10},{16,20},{18,... | collective-permute-start | bytes 393224 | tf_op jit(solution)/shard_map/ppermute | solution.py:378
  134.0 1.3 shard_map.155.hidden
  135.3 4.7 %collective-permute-done.37.refs_0_ = bf16[64,2048]{1,0:T(8,128)(2,1)S(1)} collective-permute-done((bf16[64,2048]{1,0:T(8,128)(2,1)S(1)}, bf16[64,2048]{1,0:T(8,128)(2,1)S(1)}, u32[]{:S(2)}, u32[]{:S(2)}) %collective-permute-start.37) | collective-permute-done | bytes 262176 | tf_op jit(solution)/shard_map/ppermute | solution.py:371
  140.1 1.9 %collective-permute-done.28.refs_12_ = bf16[128,1024]{1,0:T(8,128)(2,1)S(1)} collective-permute-done((bf16[128,1024]{1,0:T(8,128)(2,1)S(1)}, bf16[128,1024]{1,0:T(8,128)(2,1)S(1)}, u32[]{:S(2)}, u32[]{:S(2)}) %collective-permute-start.28) | collective-permute-done | bytes 262176 | tf_op jit(solution)/shard_map/ppermute | solution.py:378
  141.9 0.8 shard_map.156.down
  142.8 1.3 shard_map.157
  144.2 1.3 shard_map.158.hidden
  145.4 1.3 shard_map.159
  146.7 0.6 collective-permute-start.40
  147.5 0.7 collective-permute-start.35
  148.1 0.7 collective-permute-done.40
  149.0 0.8 collective-permute-start.43
  149.9 0.4 collective-permute-start.42
  150.3 3.3 %collective-permute-start.41 = (bf16[64,512]{1,0:T(8,128)(2,1)S(1)}, bf16[64,512]{1,0:T(8,128)(2,1)S(1)}, u32[]{:S(2)}, u32[]{:S(2)}) collective-permute-start(bf16[64,512]{1,0:T(8,128)(2,1)S(1)} %slice.106), channel_id=1, source_target_pairs={{0,24},{2,26},{4,28},{6,30},{8,16},{10,18},{12,20},{14,22},{16,8},... | collective-permute-start | bytes 196616 | tf_op jit(solution)/shard_map/ppermute | solution.py:371
  153.6 9.2 %collective-permute-done.43 = bf16[64,1536]{1,0:T(8,128)(2,1)S(1)} collective-permute-done((bf16[64,1536]{1,0:T(8,128)(2,1)S(1)}, bf16[64,1536]{1,0:T(8,128)(2,1)S(1)}, u32[]{:S(2)}, u32[]{:S(2)}) %collective-permute-start.43) | collective-permute-done | bytes 196640 | tf_op jit(solution)/shard_map/ppermute | solution.py:371
  162.9 9.2 %collective-permute-done.44 = bf16[64,1536]{1,0:T(8,128)(2,1)S(1)} collective-permute-done((bf16[64,1536]{1,0:T(8,128)(2,1)S(1)}, bf16[64,1536]{1,0:T(8,128)(2,1)S(1)}, u32[]{:S(2)}, u32[]{:S(2)}) %collective-permute-start.44) | collective-permute-done | bytes 196640 | tf_op jit(solution)/shard_map/ppermute | solution.py:371
  172.3 1.5 collective-permute-done.45.theirs
  173.9 0.8 join.1
  (90 shorter events, 2.1 us)
Async XLA Ops:
  0.0 56.2 %copy-start.8 = (f32[128]{0:T(128)S(1)}, f32[128]{0:T(128)}, u32[]{:S(2)}) copy-start(f32[128]{0:T(128)} %param.25) | copy-start | bytes 1540
  0.0 56.2 %copy-start.9 = (f32[64]{0:T(128)S(1)}, f32[64]{0:T(128)}, u32[]{:S(2)}) copy-start(f32[64]{0:T(128)} %param.26) | copy-start | bytes 772
  0.0 56.2 %copy-start.6 = (f32[4]{0:T(128)S(1)}, f32[4]{0:T(128)}, u32[]{:S(2)}) copy-start(f32[4]{0:T(128)} %balance_a.1) | copy-start | bytes 52
  0.0 56.2 %copy-start.7 = (f32[4]{0:T(128)S(1)}, f32[4]{0:T(128)}, u32[]{:S(2)}) copy-start(f32[4]{0:T(128)} %balance_b.1) | copy-start | bytes 52
  3.2 53.0 %copy-start.1 = (bf16[128,576]{1,0:T(8,128)(2,1)S(1)}, bf16[128,576]{1,0:T(8,128)(2,1)}, u32[]{:S(2)}) copy-start(bf16[128,576]{1,0:T(8,128)(2,1)} %get-tuple-element.26.refs_0_) | copy-start | bytes 442372
  3.2 11.0 %collective-permute-start.2 = (bf16[128,576]{1,0:T(8,128)(2,1)}, bf16[128,576]{1,0:T(8,128)(2,1)S(1)}, u32[]{:S(2)}, u32[]{:S(2)}) collective-permute-start(bf16[128,576]{1,0:T(8,128)(2,1)} %get-tuple-element.29), channel_id=1, source_target_pairs={{0,24},{2,26},{4,28},{6,30},{8,16},{10,18},{12,20},{14,22},{16,8},... | collective-permute-start | bytes 442376 | tf_op jit(solution)/shard_map/ppermute | solution.py:371
  8.3 14.2 %collective-permute-start.1 = (bf16[128,576]{1,0:T(8,128)(2,1)}, bf16[128,576]{1,0:T(8,128)(2,1)S(1)}, u32[]{:S(2)}, u32[]{:S(2)}) collective-permute-start(bf16[128,576]{1,0:T(8,128)(2,1)} %get-tuple-element.28), channel_id=1, source_target_pairs={{0,16},{2,18},{4,20},{6,22},{8,24},{10,26},{12,28},{14,30},{16,0},... | collective-permute-start | bytes 442376 | tf_op jit(solution)/shard_map/ppermute | solution.py:371
  8.3 14.2 %collective-permute-start = (bf16[128,576]{1,0:T(8,128)(2,1)}, bf16[128,576]{1,0:T(8,128)(2,1)S(1)}, u32[]{:S(2)}, u32[]{:S(2)}) collective-permute-start(bf16[128,576]{1,0:T(8,128)(2,1)} %get-tuple-element.27), channel_id=1, source_target_pairs={{0,8},{2,10},{4,12},{6,14},{8,0},{10,2},{12,4},{14,6},{16,24},{18,... | collective-permute-start | bytes 442376 | tf_op jit(solution)/shard_map/ppermute | solution.py:371
  11.9 24.1 %collective-permute-start.14 = (bf16[256,1024]{1,0:T(8,128)(2,1)}, bf16[256,1024]{1,0:T(8,128)(2,1)S(1)}, u32[]{:S(2)}, u32[]{:S(2)}) collective-permute-start(bf16[256,1024]{1,0:T(8,128)(2,1)} %get-tuple-element.38), channel_id=1, source_target_pairs={{0,8},{2,10},{4,12},{6,14},{8,0},{10,2},{12,4},{14,6},{16,24},{18,... | collective-permute-start | bytes 1572872 | tf_op jit(solution)/shard_map/ppermute | solution.py:371
  22.6 10.2 %collective-permute-start.4 = (bf16[4,128,384]{2,1,0:T(8,128)(2,1)S(1)}, bf16[4,128,384]{2,1,0:T(8,128)(2,1)S(1)}, u32[]{:S(2)}, u32[]{:S(2)}) collective-permute-start(bf16[4,128,384]{2,1,0:T(8,128)(2,1)S(1)} %pad_maximum_fusion.refs_4_), channel_id=1, source_target_pairs={{0,4},{2,6},{4,0},{6,2},{8,12},{10,14},{12,8},{14,10},{16,20},{18,... | collective-permute-start | bytes 1179656 | tf_op jit(solution)/shard_map/ppermute | solution.py:378
  24.2 10.2 %collective-permute-start.3 = (bf16[4,128,384]{2,1,0:T(8,128)(2,1)S(1)}, bf16[4,128,384]{2,1,0:T(8,128)(2,1)S(1)}, u32[]{:S(2)}, u32[]{:S(2)}) collective-permute-start(bf16[4,128,384]{2,1,0:T(8,128)(2,1)S(1)} %pad_maximum_fusion.refs_4_), channel_id=1, source_target_pairs={{0,2},{2,0},{4,6},{6,4},{8,10},{10,8},{12,14},{14,12},{16,18},{18,... | collective-permute-start | bytes 1179656 | tf_op jit(solution)/shard_map/ppermute | solution.py:378
  25.7 11.9 %collective-permute-start.15 = (bf16[128,1024]{1,0:T(8,128)(2,1)}, bf16[128,1024]{1,0:T(8,128)(2,1)S(1)}, u32[]{:S(2)}, u32[]{:S(2)}) collective-permute-start(bf16[128,1024]{1,0:T(8,128)(2,1)} %get-tuple-element.39), channel_id=1, source_target_pairs={{0,24},{2,26},{4,28},{6,30},{8,16},{10,18},{12,20},{14,22},{16,8},... | collective-permute-start | bytes 786440 | tf_op jit(solution)/shard_map/ppermute | solution.py:371
  28.2 14.2 %collective-permute-start.29 = (bf16[128,1024]{1,0:T(8,128)(2,1)}, bf16[128,1024]{1,0:T(8,128)(2,1)S(1)}, u32[]{:S(2)}, u32[]{:S(2)}) collective-permute-start(bf16[128,1024]{1,0:T(8,128)(2,1)} %get-tuple-element.42), channel_id=1, source_target_pairs={{0,24},{2,26},{4,28},{6,30},{8,16},{10,18},{12,20},{14,22},{16,8},... | collective-permute-start | bytes 786440 | tf_op jit(solution)/shard_map/ppermute | solution.py:371
  32.8 38.2 %collective-permute-start.12 = (bf16[256,1024]{1,0:T(8,128)(2,1)}, bf16[256,1024]{1,0:T(8,128)(2,1)S(1)}, u32[]{:S(2)}, u32[]{:S(2)}) collective-permute-start(bf16[256,1024]{1,0:T(8,128)(2,1)} %get-tuple-element.37.refs_0_), channel_id=1, source_target_pairs={{0,4},{2,6},{4,0},{6,2},{8,12},{10,14},{12,8},{14,10},{16,20},{18,... | collective-permute-start | bytes 1572872 | tf_op jit(solution)/shard_map/ppermute | solution.py:378
  34.4 15.2 %collective-permute-start.5 = (bf16[2,128,384]{2,1,0:T(8,128)(2,1)S(1)}, bf16[2,128,384]{2,1,0:T(8,128)(2,1)S(1)}, u32[]{:S(2)}, u32[]{:S(2)}) collective-permute-start(bf16[2,128,384]{2,1,0:T(8,128)(2,1)S(1)} %slice.93), channel_id=1, source_target_pairs={{0,2},{2,0},{4,6},{6,4},{8,10},{10,8},{12,14},{14,12},{16,18},{18,... | collective-permute-start | bytes 589832 | tf_op jit(solution)/shard_map/ppermute | solution.py:378
  36.0 14.1 %collective-permute-start.6 = (bf16[2,128,384]{2,1,0:T(8,128)(2,1)S(1)}, bf16[2,128,384]{2,1,0:T(8,128)(2,1)S(1)}, u32[]{:S(2)}, u32[]{:S(2)}) collective-permute-start(bf16[2,128,384]{2,1,0:T(8,128)(2,1)S(1)} %slice.94), channel_id=1, source_target_pairs={{0,4},{2,6},{4,0},{6,2},{8,12},{10,14},{12,8},{14,10},{16,20},{18,... | collective-permute-start | bytes 589832 | tf_op jit(solution)/shard_map/ppermute | solution.py:378
  37.6 47.6 %collective-permute-start.11 = (bf16[256,1024]{1,0:T(8,128)(2,1)}, bf16[256,1024]{1,0:T(8,128)(2,1)S(1)}, u32[]{:S(2)}, u32[]{:S(2)}) collective-permute-start(bf16[256,1024]{1,0:T(8,128)(2,1)} %get-tuple-element.37.refs_0_), channel_id=1, source_target_pairs={{0,2},{2,0},{4,6},{6,4},{8,10},{10,8},{12,14},{14,12},{16,18},{18,... | collective-permute-start | bytes 1572872 | tf_op jit(solution)/shard_map/ppermute | solution.py:378
  42.4 28.6 %collective-permute-start.20 = (bf16[256,1024]{1,0:T(8,128)(2,1)}, bf16[256,1024]{1,0:T(8,128)(2,1)S(1)}, u32[]{:S(2)}, u32[]{:S(2)}) collective-permute-start(bf16[256,1024]{1,0:T(8,128)(2,1)} %get-tuple-element.40), channel_id=1, source_target_pairs={{0,16},{2,18},{4,20},{6,22},{8,24},{10,26},{12,28},{14,30},{16,0},... | collective-permute-start | bytes 1572872 | tf_op jit(solution)/shard_map/ppermute | solution.py:371
  49.6 46.7 %collective-permute-start.17 = (bf16[384,1024]{1,0:T(8,128)(2,1)S(1)}, bf16[384,1024]{1,0:T(8,128)(2,1)S(1)}, u32[]{:S(2)}, u32[]{:S(2)}) collective-permute-start(bf16[384,1024]{1,0:T(8,128)(2,1)S(1)} %constant_dynamic-update-slice_fusion.refs_4_), channel_id=1, source_target_pairs={{0,4},{2,6},{4,0},{6,2},{8,12},{10,14},{12,8},{14,10},{16,20},{18,... | collective-permute-start | bytes 2359304 | tf_op jit(solution)/shard_map/ppermute | solution.py:378
  50.1 47.7 %collective-permute-start.16 = (bf16[384,1024]{1,0:T(8,128)(2,1)S(1)}, bf16[384,1024]{1,0:T(8,128)(2,1)S(1)}, u32[]{:S(2)}, u32[]{:S(2)}) collective-permute-start(bf16[384,1024]{1,0:T(8,128)(2,1)S(1)} %constant_dynamic-update-slice_fusion.refs_4_), channel_id=1, source_target_pairs={{0,2},{2,0},{4,6},{6,4},{8,10},{10,8},{12,14},{14,12},{16,18},{18,... | collective-permute-start | bytes 2359304 | tf_op jit(solution)/shard_map/ppermute | solution.py:378
  56.2 27.2 %copy-start.2 = (bf16[512,2048]{1,0:T(8,128)(2,1)S(1)}, bf16[512,2048]{1,0:T(8,128)(2,1)}, u32[]{:S(2)}) copy-start(bf16[512,2048]{1,0:T(8,128)(2,1)} %refs_4_.3) | copy-start | bytes 6291460
  56.2 27.2 %copy-start.3 = (bf16[256,2048]{1,0:T(8,128)(2,1)S(1)}, bf16[256,2048]{1,0:T(8,128)(2,1)}, u32[]{:S(2)}) copy-start(bf16[256,2048]{1,0:T(8,128)(2,1)} %refs_5_.1) | copy-start | bytes 3145732
  71.0 4.3 %collective-permute-start.7 = (bf16[128,192]{1,0:T(8,128)(2,1)S(1)}, bf16[128,192]{1,0:T(8,128)(2,1)S(1)}, u32[]{:S(2)}, u32[]{:S(2)}) collective-permute-start(bf16[128,192]{1,0:T(8,128)(2,1)S(1)} %get-tuple-element.31), channel_id=1, source_target_pairs={{0,8},{2,10},{4,12},{6,14},{8,0},{10,2},{12,4},{14,6},{16,24},{18,... | collective-permute-start | bytes 147464 | tf_op jit(solution)/shard_map/ppermute | solution.py:371
  71.0 5.2 %collective-permute-start.8 = (bf16[128,192]{1,0:T(8,128)(2,1)S(1)}, bf16[128,192]{1,0:T(8,128)(2,1)S(1)}, u32[]{:S(2)}, u32[]{:S(2)}) collective-permute-start(bf16[128,192]{1,0:T(8,128)(2,1)S(1)} %get-tuple-element.32), channel_id=1, source_target_pairs={{0,16},{2,18},{4,20},{6,22},{8,24},{10,26},{12,28},{14,30},{16,0},... | collective-permute-start | bytes 147464 | tf_op jit(solution)/shard_map/ppermute | solution.py:371
  75.3 19.6 %collective-permute-start.22 = (bf16[256,1024]{1,0:T(8,128)(2,1)S(1)}, bf16[256,1024]{1,0:T(8,128)(2,1)S(1)}, u32[]{:S(2)}, u32[]{:S(2)}) collective-permute-start(bf16[256,1024]{1,0:T(8,128)(2,1)S(1)} %collective-permute-done.20.refs_9_), channel_id=1, source_target_pairs={{0,4},{2,6},{4,0},{6,2},{8,12},{10,14},{12,8},{14,10},{16,20},{18,... | collective-permute-start | bytes 1572872 | tf_op jit(solution)/shard_map/ppermute | solution.py:378
  76.3 6.2 %collective-permute-start.9 = (bf16[128,192]{1,0:T(8,128)(2,1)S(1)}, bf16[128,192]{1,0:T(8,128)(2,1)S(1)}, u32[]{:S(2)}, u32[]{:S(2)}) collective-permute-start(bf16[128,192]{1,0:T(8,128)(2,1)S(1)} %get-tuple-element.33), channel_id=1, source_target_pairs={{0,24},{2,26},{4,28},{6,30},{8,16},{10,18},{12,20},{14,22},{16,8},... | collective-permute-start | bytes 147464 | tf_op jit(solution)/shard_map/ppermute | solution.py:371
  82.4 10.3 %collective-permute-start.31 = (bf16[128,1024]{1,0:T(8,128)(2,1)S(1)}, bf16[128,1024]{1,0:T(8,128)(2,1)S(1)}, u32[]{:S(2)}, u32[]{:S(2)}) collective-permute-start(bf16[128,1024]{1,0:T(8,128)(2,1)S(1)} %collective-permute-done.29.refs_13_), channel_id=1, source_target_pairs={{0,4},{2,6},{4,0},{6,2},{8,12},{10,14},{12,8},{14,10},{16,20},{18,... | collective-permute-start | bytes 786440 | tf_op jit(solution)/shard_map/ppermute | solution.py:378
  83.4 12.0 %copy-start.4 = (bf16[128,2048]{1,0:T(8,128)(2,1)S(1)}, bf16[128,2048]{1,0:T(8,128)(2,1)}, u32[]{:S(2)}) copy-start(bf16[128,2048]{1,0:T(8,128)(2,1)} %residual.1) | copy-start | bytes 1572868
  83.4 12.1 %copy-start.5 = (f32[2048]{0:T(1024)S(1)}, f32[2048]{0:T(1024)}, u32[]{:S(2)}) copy-start(f32[2048]{0:T(1024)} %param.29) | copy-start | bytes 24580
  85.2 45.5 %copy-start = (bf16[256,1024]{1,0:T(8,128)(2,1)S(1)}, bf16[256,1024]{1,0:T(8,128)(2,1)}, u32[]{:S(2)}) copy-start(bf16[256,1024]{1,0:T(8,128)(2,1)} %get-tuple-element.37.refs_0_) | copy-start | bytes 1572868
  85.2 8.1 %collective-permute-start.10 = (bf16[64,2048]{1,0:T(8,128)(2,1)S(1)}, bf16[64,2048]{1,0:T(8,128)(2,1)S(1)}, u32[]{:S(2)}, u32[]{:S(2)}) collective-permute-start(bf16[64,2048]{1,0:T(8,128)(2,1)S(1)} %get-tuple-element.35), channel_id=1, source_target_pairs={{0,1},{1,0},{2,3},{3,2},{4,5},{5,4},{6,7},{7,6},{8,9},{9,8},{10,11... | collective-permute-start | bytes 786440 | tf_op jit(solution)/shard_map/ppermute | solution.py:381
  92.7 26.5 %collective-permute-start.21 = (bf16[256,1024]{1,0:T(8,128)(2,1)S(1)}, bf16[256,1024]{1,0:T(8,128)(2,1)S(1)}, u32[]{:S(2)}, u32[]{:S(2)}) collective-permute-start(bf16[256,1024]{1,0:T(8,128)(2,1)S(1)} %collective-permute-done.20.refs_9_), channel_id=1, source_target_pairs={{0,2},{2,0},{4,6},{6,4},{8,10},{10,8},{12,14},{14,12},{16,18},{18,... | collective-permute-start | bytes 1572872 | tf_op jit(solution)/shard_map/ppermute | solution.py:378
  93.3 19.8 %collective-permute-start.30 = (bf16[128,1024]{1,0:T(8,128)(2,1)S(1)}, bf16[128,1024]{1,0:T(8,128)(2,1)S(1)}, u32[]{:S(2)}, u32[]{:S(2)}) collective-permute-start(bf16[128,1024]{1,0:T(8,128)(2,1)S(1)} %collective-permute-done.29.refs_13_), channel_id=1, source_target_pairs={{0,2},{2,0},{4,6},{6,4},{8,10},{10,8},{12,14},{14,12},{16,18},{18,... | collective-permute-start | bytes 786440 | tf_op jit(solution)/shard_map/ppermute | solution.py:378
  94.9 23.9 %collective-permute-start.13 = (bf16[128,1024]{1,0:T(8,128)(2,1)S(1)}, bf16[128,1024]{1,0:T(8,128)(2,1)S(1)}, u32[]{:S(2)}, u32[]{:S(2)}) collective-permute-start(bf16[128,1024]{1,0:T(8,128)(2,1)S(1)} %slice.95), channel_id=1, source_target_pairs={{0,2},{2,0},{4,6},{6,4},{8,10},{10,8},{12,14},{14,12},{16,18},{18,... | collective-permute-start | bytes 786440 | tf_op jit(solution)/shard_map/ppermute | solution.py:378
  96.3 28.1 %collective-permute-start.23 = (bf16[128,1024]{1,0:T(8,128)(2,1)S(1)}, bf16[128,1024]{1,0:T(8,128)(2,1)S(1)}, u32[]{:S(2)}, u32[]{:S(2)}) collective-permute-start(bf16[128,1024]{1,0:T(8,128)(2,1)S(1)} %slice.98), channel_id=1, source_target_pairs={{0,2},{2,0},{4,6},{6,4},{8,10},{10,8},{12,14},{14,12},{16,18},{18,... | collective-permute-start | bytes 786440 | tf_op jit(solution)/shard_map/ppermute | solution.py:378
  97.8 26.6 %collective-permute-start.24 = (bf16[64,2048]{1,0:T(8,128)(2,1)S(1)}, bf16[64,2048]{1,0:T(8,128)(2,1)S(1)}, u32[]{:S(2)}, u32[]{:S(2)}) collective-permute-start(bf16[64,2048]{1,0:T(8,128)(2,1)S(1)} %get-tuple-element.41.refs_1_), channel_id=1, source_target_pairs={{0,8},{2,10},{4,12},{6,14},{8,0},{10,2},{12,4},{14,6},{16,24},{18,... | collective-permute-start | bytes 786440 | tf_op jit(solution)/shard_map/ppermute | solution.py:371
  113.2 16.7 %collective-permute-start.18 = (bf16[192,1024]{1,0:T(8,128)(2,1)S(1)}, bf16[192,1024]{1,0:T(8,128)(2,1)S(1)}, u32[]{:S(2)}, u32[]{:S(2)}) collective-permute-start(bf16[192,1024]{1,0:T(8,128)(2,1)S(1)} %slice.96), channel_id=1, source_target_pairs={{0,2},{2,0},{4,6},{6,4},{8,10},{10,8},{12,14},{14,12},{16,18},{18,... | collective-permute-start | bytes 1179656 | tf_op jit(solution)/shard_map/ppermute | solution.py:378
  118.8 11.1 %collective-permute-start.19 = (bf16[192,1024]{1,0:T(8,128)(2,1)S(1)}, bf16[192,1024]{1,0:T(8,128)(2,1)S(1)}, u32[]{:S(2)}, u32[]{:S(2)}) collective-permute-start(bf16[192,1024]{1,0:T(8,128)(2,1)S(1)} %slice.97), channel_id=1, source_target_pairs={{0,4},{2,6},{4,0},{6,2},{8,12},{10,14},{12,8},{14,10},{16,20},{18,... | collective-permute-start | bytes 1179656 | tf_op jit(solution)/shard_map/ppermute | solution.py:378
  119.3 12.2 %collective-permute-start.36 = (bf16[64,2048]{1,0:T(8,128)(2,1)S(1)}, bf16[64,2048]{1,0:T(8,128)(2,1)S(1)}, u32[]{:S(2)}, u32[]{:S(2)}) collective-permute-start(bf16[64,2048]{1,0:T(8,128)(2,1)S(1)} %get-tuple-element.41.refs_1_), channel_id=1, source_target_pairs={{0,16},{2,18},{4,20},{6,22},{8,24},{10,26},{12,28},{14,30},{16,0},... | collective-permute-start | bytes 786440 | tf_op jit(solution)/shard_map/ppermute | solution.py:371
  124.4 9.2 %collective-permute-start.26 = (bf16[64,2048]{1,0:T(8,128)(2,1)S(1)}, bf16[64,2048]{1,0:T(8,128)(2,1)S(1)}, u32[]{:S(2)}, u32[]{:S(2)}) collective-permute-start(bf16[64,2048]{1,0:T(8,128)(2,1)S(1)} %get-tuple-element.41.refs_1_), channel_id=1, source_target_pairs={{0,1},{1,0},{2,3},{3,2},{4,5},{5,4},{6,7},{7,6},{8,9},{9,8},{10,11... | collective-permute-start | bytes 786440 | tf_op jit(solution)/shard_map/ppermute | solution.py:381
  124.4 9.3 %collective-permute-start.25 = (bf16[64,2048]{1,0:T(8,128)(2,1)S(1)}, bf16[64,2048]{1,0:T(8,128)(2,1)S(1)}, u32[]{:S(2)}, u32[]{:S(2)}) collective-permute-start(bf16[64,2048]{1,0:T(8,128)(2,1)S(1)} %collective-permute-done.24.refs_0_), channel_id=1, source_target_pairs={{0,1},{1,0},{2,3},{3,2},{4,5},{5,4},{6,7},{7,6},{8,9},{9,8},{10,11... | collective-permute-start | bytes 786440 | tf_op jit(solution)/shard_map/ppermute | solution.py:381
  129.9 10.2 %collective-permute-start.27 = (bf16[128,1024]{1,0:T(8,128)(2,1)S(1)}, bf16[128,1024]{1,0:T(8,128)(2,1)S(1)}, u32[]{:S(2)}, u32[]{:S(2)}) collective-permute-start(bf16[128,1024]{1,0:T(8,128)(2,1)S(1)} %slice.99), channel_id=1, source_target_pairs={{0,4},{2,6},{4,0},{6,2},{8,12},{10,14},{12,8},{14,10},{16,20},{18,... | collective-permute-start | bytes 786440 | tf_op jit(solution)/shard_map/ppermute | solution.py:378
  129.9 5.3 %collective-permute-start.32 = (bf16[64,1024]{1,0:T(8,128)(2,1)S(1)}, bf16[64,1024]{1,0:T(8,128)(2,1)S(1)}, u32[]{:S(2)}, u32[]{:S(2)}) collective-permute-start(bf16[64,1024]{1,0:T(8,128)(2,1)S(1)} %slice.101), channel_id=1, source_target_pairs={{0,2},{2,0},{4,6},{6,4},{8,10},{10,8},{12,14},{14,12},{16,18},{18,... | collective-permute-start | bytes 393224 | tf_op jit(solution)/shard_map/ppermute | solution.py:378
  131.5 8.6 %collective-permute-start.33 = (bf16[64,1024]{1,0:T(8,128)(2,1)S(1)}, bf16[64,1024]{1,0:T(8,128)(2,1)S(1)}, u32[]{:S(2)}, u32[]{:S(2)}) collective-permute-start(bf16[64,1024]{1,0:T(8,128)(2,1)S(1)} %slice.102), channel_id=1, source_target_pairs={{0,4},{2,6},{4,0},{6,2},{8,12},{10,14},{12,8},{14,10},{16,20},{18,... | collective-permute-start | bytes 393224 | tf_op jit(solution)/shard_map/ppermute | solution.py:378
  133.6 8.4 %collective-permute-start.28 = (bf16[128,1024]{1,0:T(8,128)(2,1)S(1)}, bf16[128,1024]{1,0:T(8,128)(2,1)S(1)}, u32[]{:S(2)}, u32[]{:S(2)}) collective-permute-start(bf16[128,1024]{1,0:T(8,128)(2,1)S(1)} %slice.100), channel_id=1, source_target_pairs={{0,4},{2,6},{4,0},{6,2},{8,12},{10,14},{12,8},{14,10},{16,20},{18,... | collective-permute-start | bytes 786440 | tf_op jit(solution)/shard_map/ppermute | solution.py:378
  133.7 6.4 %collective-permute-start.37 = (bf16[64,2048]{1,0:T(8,128)(2,1)S(1)}, bf16[64,2048]{1,0:T(8,128)(2,1)S(1)}, u32[]{:S(2)}, u32[]{:S(2)}) collective-permute-start(bf16[64,2048]{1,0:T(8,128)(2,1)S(1)} %collective-permute-done.36.refs_1_), channel_id=1, source_target_pairs={{0,8},{2,10},{4,12},{6,14},{8,0},{10,2},{12,4},{14,6},{16,24},{18,... | collective-permute-start | bytes 786440 | tf_op jit(solution)/shard_map/ppermute | solution.py:371
  135.2 8.9 %collective-permute-start.39 = (bf16[64,2048]{1,0:T(8,128)(2,1)S(1)}, bf16[64,2048]{1,0:T(8,128)(2,1)S(1)}, u32[]{:S(2)}, u32[]{:S(2)}) collective-permute-start(bf16[64,2048]{1,0:T(8,128)(2,1)S(1)} %collective-permute-done.36.refs_1_), channel_id=1, source_target_pairs={{0,1},{1,0},{2,3},{3,2},{4,5},{5,4},{6,7},{7,6},{8,9},{9,8},{10,11... | collective-permute-start | bytes 786440 | tf_op jit(solution)/shard_map/ppermute | solution.py:381
  140.0 4.1 %collective-permute-start.38 = (bf16[64,2048]{1,0:T(8,128)(2,1)S(1)}, bf16[64,2048]{1,0:T(8,128)(2,1)S(1)}, u32[]{:S(2)}, u32[]{:S(2)}) collective-permute-start(bf16[64,2048]{1,0:T(8,128)(2,1)S(1)} %collective-permute-done.37.refs_0_), channel_id=1, source_target_pairs={{0,1},{1,0},{2,3},{3,2},{4,5},{5,4},{6,7},{7,6},{8,9},{9,8},{10,11... | collective-permute-start | bytes 786440 | tf_op jit(solution)/shard_map/ppermute | solution.py:381
  144.1 3.2 %collective-permute-start.34 = (bf16[2,64,2048]{2,1,0:T(8,128)(2,1)S(1)}, bf16[2,64,2048]{2,1,0:T(8,128)(2,1)S(1)}, u32[]{:S(2)}, u32[]{:S(2)}) collective-permute-start(bf16[2,64,2048]{2,1,0:T(8,128)(2,1)S(1)} %get-tuple-element.44), channel_id=1, source_target_pairs={{0,1},{1,0},{2,3},{3,2},{4,5},{5,4},{6,7},{7,6},{8,9},{9,8},{10,11... | collective-permute-start | bytes 1572872 | tf_op jit(solution)/shard_map/ppermute | solution.py:381
  146.7 2.1 %collective-permute-start.40 = (bf16[2,64,2048]{2,1,0:T(8,128)(2,1)S(1)}, bf16[2,64,2048]{2,1,0:T(8,128)(2,1)S(1)}, u32[]{:S(2)}, u32[]{:S(2)}) collective-permute-start(bf16[2,64,2048]{2,1,0:T(8,128)(2,1)S(1)} %get-tuple-element.46), channel_id=1, source_target_pairs={{0,1},{1,0},{2,3},{3,2},{4,5},{5,4},{6,7},{7,6},{8,9},{9,8},{10,11... | collective-permute-start | bytes 1572872 | tf_op jit(solution)/shard_map/ppermute | solution.py:381
  147.5 24.7 %collective-permute-start.35 = (bf16[64,2048]{1,0:T(8,128)(2,1)S(1)}, bf16[64,2048]{1,0:T(8,128)(2,1)S(1)}, u32[]{:S(2)}, u32[]{:S(2)}) collective-permute-start(bf16[64,2048]{1,0:T(8,128)(2,1)S(1)} %fusion.5), channel_id=1, source_target_pairs={{0,8},{2,10},{4,12},{6,14},{8,0},{10,2},{12,4},{14,6},{16,24},{18,... | collective-permute-start | bytes 786440 | tf_op jit(solution)/shard_map/ppermute | solution.py:371
  149.0 13.8 %collective-permute-start.43 = (bf16[64,1536]{1,0:T(8,128)(2,1)S(1)}, bf16[64,1536]{1,0:T(8,128)(2,1)S(1)}, u32[]{:S(2)}, u32[]{:S(2)}) collective-permute-start(bf16[64,1536]{1,0:T(8,128)(2,1)S(1)} %slice.110), channel_id=1, source_target_pairs={{0,8},{2,10},{4,12},{6,14},{8,0},{10,2},{12,4},{14,6},{16,24},{18,... | collective-permute-start | bytes 589832 | tf_op jit(solution)/shard_map/ppermute | solution.py:371
  149.9 13.0 %collective-permute-start.42 = (bf16[64,512]{1,0:T(8,128)(2,1)S(1)}, bf16[64,512]{1,0:T(8,128)(2,1)S(1)}, u32[]{:S(2)}, u32[]{:S(2)}) collective-permute-start(bf16[64,512]{1,0:T(8,128)(2,1)S(1)} %slice.135), channel_id=1, source_target_pairs={{0,16},{2,18},{4,20},{6,22},{8,24},{10,26},{12,28},{14,30},{16,0},... | collective-permute-start | bytes 196616 | tf_op jit(solution)/shard_map/ppermute | solution.py:371
  150.3 12.6 %collective-permute-start.41 = (bf16[64,512]{1,0:T(8,128)(2,1)S(1)}, bf16[64,512]{1,0:T(8,128)(2,1)S(1)}, u32[]{:S(2)}, u32[]{:S(2)}) collective-permute-start(bf16[64,512]{1,0:T(8,128)(2,1)S(1)} %slice.106), channel_id=1, source_target_pairs={{0,24},{2,26},{4,28},{6,30},{8,16},{10,18},{12,20},{14,22},{16,8},... | collective-permute-start | bytes 196616 | tf_op jit(solution)/shard_map/ppermute | solution.py:371
  162.8 9.3 %collective-permute-start.44 = (bf16[64,1536]{1,0:T(8,128)(2,1)S(1)}, bf16[64,1536]{1,0:T(8,128)(2,1)S(1)}, u32[]{:S(2)}, u32[]{:S(2)}) collective-permute-start(bf16[64,1536]{1,0:T(8,128)(2,1)S(1)} %fusion.4), channel_id=1, source_target_pairs={{0,16},{2,18},{4,20},{6,22},{8,24},{10,26},{12,28},{14,30},{16,0},... | collective-permute-start | bytes 589832 | tf_op jit(solution)/shard_map/ppermute | solution.py:371
  172.3 1.6 collective-permute-start.45
